TPU v7x, 512 devices: a whole 4x8x8 slice. The times are simulated.
512 devices in a mesh: sp: 64 (over z, y), dp: 8 (over x, core).
Axes of the slice: x: 4, y: 8, z: 8, core: 2. Of those that a mesh axis runs over, the one named last changes fastest.
Arguments:
- gated: bfloat16 [8, 8192, 3072], P('dp', 'sp'), may hold values from -6 to 6
- values_in: bfloat16 [8, 8192, 3072], P('dp', 'sp'), may hold values from -6 to 6
- upstream: bfloat16 [8, 8192, 3072], P('dp', 'sp'), may hold values from -6 to 6
- gain: float32 [3072], replicated, may hold values from 0.1 to 1.9
- shift: float32 [3072], replicated, may hold values from -3 to 3
- mix_w: bfloat16 [512, 4, 512], P('dp'), may hold values from -0.375 to 0.375
- mix_bias: float32 [4, 512], replicated, may hold values from 0.1 to 1.9
Outputs:
- grad_u: bfloat16 [8, 8192, 3072], P('dp', 'sp')
- grad_v: bfloat16 [8, 8192, 3072], P('dp', 'sp')
- grad_mix: float32 [512, 4, 512], P('dp')
- grad_bias: float32 [4, 512], replicated
- grad_gain: float32 [3072], replicated
- grad_shift: float32 [3072], replicated
All inputs are finite; a program needn't handle non-finite values.
Results may differ from a plain program's by a relative error of at most 0.014.
Values may be sent and summed in bfloat16 or wider, within the bound.
No kernel may reach another device: no remote copies, remote signals or barrier semaphores. Data moves between devices by JAX's collectives and lax.ppermute only.
A program may use at most 64 MiB of HBM per device.

v0:
```python
import functools

import jax
import jax.numpy as jnp
from jax import lax
from jax.experimental import pallas as pl
from jax.experimental.pallas import tpu as pltpu
from jax.sharding import Mesh
from jax.sharding import PartitionSpec as P


SEG = 64
ROWS = 128
GROUPS = 4
WIDTH = 768
HALF = GROUPS * WIDTH
QUAD = 4
DP = ("dp_0", "dp_1")
SP = ("sp_0", "sp_1")
Y = "sp_1"
Z = "sp_0"
X = "dp_0"
CORE = "dp_1"
EPS = 1e-05

NEAR = [(0, 1), (3, 2), (4, 5), (7, 6)]
FAR = [(0, 2), (3, 1), (4, 6), (7, 5)]
SWAP = [(1, 2), (2, 1), (5, 6), (6, 5)]
OUT = [(1, 0), (2, 3), (5, 4), (6, 7)]
PARTNER = [(0, 1), (1, 0)]
CHIPS = [[(i, (i + k) % 4) for i in range(4)] for k in range(4)]
SETS = ((0, 1, 2), (3,))


VMEM = pl.BlockSpec(memory_space=pltpu.VMEM)
SMEM = pl.BlockSpec(memory_space=pltpu.SMEM)
F32 = jnp.float32
BF16 = jnp.bfloat16


def call(kernel, out_shape, inputs, scalars=1, scratch=(), vmem=16):
    return pl.pallas_call(
        kernel,
        out_shape=out_shape,
        in_specs=[SMEM] * scalars + [VMEM] * (len(inputs) - scalars),
        out_specs=jax.tree.map(lambda _: VMEM, out_shape),
        scratch_shapes=list(scratch),
        compiler_params=pltpu.CompilerParams(vmem_limit_bytes=vmem << 20),
    )(*inputs)


def shape(dims, dtype):
    return jax.ShapeDtypeStruct(dims, dtype)


def nt(a, b):
    return lax.dot_general(a, b, (((1,), (1,)), ((), ())), preferred_element_type=F32)


def tn(a, b):
    return lax.dot_general(a, b, (((0,), (0,)), ((), ())), preferred_element_type=F32)


def nn(a, b):
    return jnp.dot(a, b, preferred_element_type=F32)


def pre_kernel(place, values, gated, upstream, gain, shift, *outs):
    us, vs, stats, bias = outs[:4], outs[4:8], outs[8], outs[9]
    low = place[0] < 2
    step = 16

    def block(i, carry):
        rows = pl.ds(pl.multiple_of(i * step, step), step)
        raw = values[0, rows, :].astype(F32)
        mean = jnp.sum(raw, axis=1, keepdims=True) * (1.0 / HALF)
        centred = raw - mean
        var = jnp.sum(centred * centred, axis=1, keepdims=True) * (1.0 / HALF)
        inv = lax.rsqrt(var + EPS)
        stats[0, rows, :] = jnp.broadcast_to(mean, (step, 128))
        stats[1, rows, :] = jnp.broadcast_to(inv, (step, 128))
        for g in range(GROUPS):
            cols = slice(g * WIDTH, (g + 1) * WIDTH)
            unit = (values[0, rows, cols].astype(F32) - mean) * inv
            normed = (unit * gain[:, cols] + shift[:, cols]).astype(BF16)
            grad = (upstream[0, rows, cols].astype(F32) * gated[0, rows, cols].astype(F32)).astype(BF16)
            us[g][rows, :] = jnp.where(low, grad, normed)
            vs[g][rows, :] = jnp.where(low, normed, grad)
        return carry

    lax.fori_loop(0, ROWS // step, block, 0)
    bias[...] = jnp.zeros_like(bias)
    ones = jnp.ones((8, WIDTH), BF16)
    for g in range(GROUPS):
        grad = jnp.where(low, us[g][...], vs[g][...])
        bias[pl.ds(g * QUAD + place[0], 1), :] = nt(ones, grad)[:1]


def weight_kernel(place, *refs):
    mine, theirs, out, held = refs[:4], refs[4:8], refs[8], refs[9]
    p, x, core = place[0], place[1], place[2]
    low = p < 2
    for k in range(4):
        b = (x + 4 - k) % 4
        held[b, core] = mine[k][...]
        held[b, 1 - core] = theirs[k][...]
    start = jnp.where(p == 3, 1, 0)
    r = lax.broadcasted_iota(jnp.int32, (ROWS, ROWS), 0) // SEG
    c = lax.broadcasted_iota(jnp.int32, (ROWS, ROWS), 1) // SEG

    def piece(t, g, s):
        cols = pl.ds(pl.multiple_of((s - start) * ROWS, ROWS), ROWS)
        return jnp.concatenate([held[t, 0, g, :, cols], held[t, 1, g, :, cols]], axis=0)

    @pl.when(low)
    def _():
        for g in range(GROUPS):
            for i in range(2):
                for j in range(3):
                    got = piece(p + j, g, jnp.maximum(p - i, 0)).astype(F32)
                    if i == 0 and j == 0:
                        got = jnp.where(r >= c, got, 0.0)
                    out[g, i * ROWS : (i + 1) * ROWS, j * ROWS : (j + 1) * ROWS] = got.T.astype(BF16)

    @pl.when(jnp.logical_not(low))
    def _():
        for g in range(GROUPS):
            for i in range(2):
                for j in range(3):
                    got = piece(jnp.minimum(p + i, 3), g, p - j)
                    if i == 0 and j == 0:
                        got = jnp.where(r >= c, got.astype(F32), 0.0).astype(BF16)
                    out[g, i * ROWS : (i + 1) * ROWS, j * ROWS : (j + 1) * ROWS] = got


def product_kernel(g, u, v, near, far, swap, weights, part, out_u, out_v):
    own, other = weights[g, :ROWS, :], weights[g, ROWS:, :]
    long_side = jnp.concatenate([u[...], swap[...], far[...]], axis=0)
    part[...] = nn(other, long_side).astype(BF16)
    out_u[...] = nn(own, long_side)
    short_side = jnp.concatenate([v[...], near[...]], axis=0)
    both = jnp.concatenate([own[:, :ROWS], other[:, :ROWS]], axis=0)
    out_v[...] = tn(both, short_side)


def mix_grad_kernel(n, place, *refs):
    ins, keep, send = refs[: 5 * n], refs[5 * n], refs[5 * n + 1]
    p, core = place[0], place[2]
    first = core == 0
    r = lax.broadcasted_iota(jnp.int32, (ROWS, ROWS), 0) // SEG
    c = lax.broadcasted_iota(jnp.int32, (ROWS, ROWS), 1) // SEG
    keep[...] = jnp.zeros_like(keep)
    send[...] = jnp.zeros_like(send)

    def put(target, slot, k, got):
        lanes = slice(k * ROWS, (k + 1) * ROWS)
        keep[target, slot, :, lanes] = jnp.where(first, got[:SEG], got[SEG:])
        send[target, slot, :, lanes] = jnp.where(first, got[SEG:], got[:SEG]).astype(BF16)

    for k in range(n):
        u, v, near, far, swap = ins[5 * k : 5 * k + 5]

        @pl.when(p == 0)
        def _():
            put(0, 0, k, jnp.where(r >= c, nt(u[...], v[...]), 0.0))

        @pl.when(p == 1)
        def _():
            put(1, 0, k, nt(u[...], near[...]))
            put(1, 1, k, jnp.where(r >= c, nt(u[...], v[...]), 0.0))
            put(2, 0, k, nt(swap[...], near[...]))
            put(3, 0, k, nt(far[...], near[...]))

        @pl.when(p == 2)
        def _():
            put(2, 0, k, jnp.where(r >= c, nt(v[...], u[...]), 0.0))
            put(2, 1, k, nt(v[...], swap[...]))
            put(3, 0, k, nt(near[...], u[...]))
            put(3, 1, k, nt(near[...], swap[...]))

        @pl.when(p == 3)
        def _():
            put(3, 0, k, jnp.where(r >= c, nt(v[...], u[...]), 0.0))


def core_sum_kernel(place, keep, got, mine, *sends):
    x = place[1]
    mine[...] = keep[x] + got[x].astype(F32)
    for k in range(1, 4):
        b = (x + k) % 4
        sends[k - 1][...] = (keep[b] + got[b].astype(F32)).astype(BF16)


def split(x):
    high = x.astype(BF16)
    return high, (x - high.astype(F32)).astype(BF16)


def deal_kernel(*refs):
    small, out = refs[8:12], refs[12]
    extra = small[0][...] + small[1][...] + small[2][...] + small[3][...]
    high, low = split(extra)
    for z in range(8):
        out[z, :, 1024:1152] = high[z * 8 : (z + 1) * 8]
        out[z, :, 1152:1280] = low[z * 8 : (z + 1) * 8]
    lane = 0
    for i, groups in enumerate(SETS):
        parts = refs[4 * i : 4 * i + 4]
        width = len(groups) * ROWS
        for slot in range(2):
            total = parts[0][slot]
            for k in range(1, 4):
                total = total + parts[k][slot].astype(F32)
            total = total.astype(BF16)
            for z in range(8):
                out[z, :, slot * 512 + lane : slot * 512 + lane + width] = total[z * 8 : (z + 1) * 8]
        lane += width


def add_kernel(got, out):
    total = got[0].astype(F32)
    for z in range(1, 8):
        total = total + got[z].astype(F32)
    extra = total[:, 1024:1152] + total[:, 1152:1280]
    high, low = split(extra)
    total = total[:, :1024].astype(BF16)
    for y in range(8):
        out[y, :, :1024] = total
        out[y, :, 1024:1152] = high
        out[y, :, 1152:1280] = low


def place_kernel(got, out):
    def at(place, slot):
        lanes = slice(slot * 512, (slot + 1) * 512)
        return got[place, :, lanes].astype(F32) + got[place + QUAD, :, lanes].astype(F32)

    columns = (at(0, 0) + at(1, 0), at(1, 1) + at(2, 1), at(2, 0), at(3, 0))
    columns = [c.astype(BF16) for c in columns]
    extra = jnp.zeros((8, 128), F32)
    for y in range(8):
        extra = extra + got[y, :, 1024:1152].astype(F32) + got[y, :, 1152:1280].astype(F32)
    high, low = split(extra)
    for z in range(8):
        for s in range(4):
            for g in range(GROUPS):
                out[z, :, g * 512 + s * ROWS : g * 512 + (s + 1) * ROWS] = columns[s][
                    :, g * ROWS : (g + 1) * ROWS
                ]
        out[z, :, 2048:2176] = high
        out[z, :, 2176:2304] = low


def final_kernel(got, grad_mix, small):
    for z in range(8):
        rows = slice(z * 8, (z + 1) * 8)
        for g in range(GROUPS):
            grad_mix[rows, g, :] = got[z, :, g * 512 : (g + 1) * 512].astype(F32)
        small[rows, :] = got[z, :, 2048:2176].astype(F32) + got[z, :, 2176:2304].astype(F32)


def sums_kernel(place, values, stats, bias, *refs):
    outs_u, outs_v, got, out = refs[:4], refs[4:8], refs[8:12], refs[12]
    low = place[0] < 2
    out[:16] = bias[...]
    mean = stats[0, :, :1]
    inv = stats[1, :, :1]
    for g in range(GROUPS):
        for i in range(WIDTH // 128):
            own = slice(i * 128, (i + 1) * 128)
            cols = slice(g * WIDTH + i * 128, g * WIDTH + (i + 1) * 128)
            back = jnp.where(low, outs_u[g][:, own] + got[g][:, own].astype(F32), outs_v[g][:, own])
            back = back.astype(BF16).astype(F32)
            unit = (values[0, :, cols].astype(F32) - mean) * inv
            row = 16 + g * 6 + i
            out[row : row + 1] = jnp.sum(back * unit, axis=0, keepdims=True)
            out[row + 24 : row + 25] = jnp.sum(back, axis=0, keepdims=True)


def post_kernel(place, values, upstream, stats, gain, bias_row, *refs):
    outs_u, outs_v, got, grad_u, grad_v = refs[:4], refs[4:8], refs[8:12], refs[12], refs[13]
    low = place[0] < 2
    step = 16

    def block(i, carry):
        rows = pl.ds(pl.multiple_of(i * step, step), step)
        mean = stats[0, rows, :1]
        inv = stats[1, rows, :1]
        first = jnp.zeros((step, 1), F32)
        second = jnp.zeros((step, 1), F32)
        for g in range(GROUPS):
            cols = slice(g * WIDTH, (g + 1) * WIDTH)
            long_side = outs_u[g][rows, :] + got[g][rows, :].astype(F32)
            short_side = outs_v[g][rows, :]
            mixed = jnp.where(low, short_side, long_side) + bias_row[rows, g : g + 1]
            mixed = mixed.astype(BF16).astype(F32)
            grad_u[0, rows, cols] = (upstream[0, rows, cols].astype(F32) * mixed).astype(BF16)
            back = jnp.where(low, long_side, short_side).astype(BF16).astype(F32)
            scaled = back * gain[:, cols]
            unit = (values[0, rows, cols].astype(F32) - mean) * inv
            first = first + jnp.sum(scaled, axis=1, keepdims=True)
            second = second + jnp.sum(scaled * unit, axis=1, keepdims=True)
        first = first * (1.0 / HALF)
        second = second * (1.0 / HALF)
        for g in range(GROUPS):
            cols = slice(g * WIDTH, (g + 1) * WIDTH)
            long_side = outs_u[g][rows, :] + got[g][rows, :].astype(F32)
            back = jnp.where(low, long_side, outs_v[g][rows, :]).astype(BF16).astype(F32)
            scaled = back * gain[:, cols]
            unit = (values[0, rows, cols].astype(F32) - mean) * inv
            grad_v[0, rows, cols] = (inv * (scaled - first - unit * second)).astype(BF16)
        return carry

    lax.fori_loop(0, ROWS // step, block, 0)


def exchanged(x, axis):
    return lax.all_to_all(x, axis, split_axis=0, concat_axis=0, tiled=True)


def compute(gated, values_in, upstream, gain, shift, mix_w, mix_bias):
    spot = lax.axis_index(Y) % QUAD
    place = jnp.stack([spot, lax.axis_index(X), lax.axis_index(CORE)]).astype(jnp.int32)
    gain_row, shift_row = gain.reshape(1, HALF), shift.reshape(1, HALF)

    half = shape((ROWS, WIDTH), BF16)
    full = shape((ROWS, WIDTH), F32)

    first = jnp.where(spot == 3, ROWS, 0)
    own_rows = lax.dynamic_slice_in_dim(jnp.swapaxes(mix_w, 0, 1), first, 3 * ROWS, 2)
    mine = [own_rows] + [lax.ppermute(own_rows, X, CHIPS[k]) for k in range(1, 4)]
    theirs = [lax.ppermute(rows, CORE, PARTNER) for rows in mine]

    pre = call(
        pre_kernel,
        [half] * 8 + [shape((2, ROWS, 128), F32), shape((16, 128), F32)],
        (place, values_in, gated, upstream, gain_row, shift_row),
    )
    us, vs, stats, bias_term = pre[:4], pre[4:8], pre[8], pre[9]

    near, far, swap = [], [], []
    for g in range(GROUPS):
        near.append(lax.ppermute(vs[g], Y, NEAR))
        far.append(lax.ppermute(vs[g], Y, FAR))
        swap.append(lax.ppermute(vs[g], Y, SWAP))

    weights = call(
        weight_kernel,
        shape((GROUPS, 2 * ROWS, 3 * ROWS), BF16),
        (place, *mine, *theirs),
        scratch=[pltpu.VMEM((4, 2, GROUPS, SEG, 3 * ROWS), BF16)],
    )

    outs_u, outs_v, got = [], [], []
    for g in range(GROUPS):
        part, out_u, out_v = call(
            functools.partial(product_kernel, g),
            [half, full, full],
            (us[g], vs[g], near[g], far[g], swap[g], weights),
            0,
        )
        got.append(lax.ppermute(part, Y, OUT))
        outs_u.append(out_u)
        outs_v.append(out_v)

    terms = []
    for groups in SETS:
        operands = []
        for g in groups:
            operands += [us[g], vs[g], near[g], far[g], swap[g]]
        width = len(groups) * ROWS
        keep, send = call(
            functools.partial(mix_grad_kernel, len(groups)),
            [shape((4, 2, SEG, width), F32), shape((4, 2, SEG, width), BF16)],
            (place, *operands),
        )
        sums = call(
            core_sum_kernel,
            [shape((2, SEG, width), F32)] + [shape((2, SEG, width), BF16)] * 3,
            (place, keep, lax.ppermute(send, CORE, PARTNER)),
        )
        terms += [sums[0]] + [lax.ppermute(sums[k], X, CHIPS[k]) for k in range(1, 4)]

    small = call(
        sums_kernel,
        shape((64, 128), F32),
        (place, values_in, stats, bias_term, *outs_u, *outs_v, *got),
    )
    small = small + lax.ppermute(small, CORE, PARTNER)
    smalls = [small] + [lax.ppermute(small, X, CHIPS[k]) for k in range(1, 4)]

    dealt = call(deal_kernel, shape((8, 8, 1280), BF16), (*terms, *smalls), 0)
    added = call(add_kernel, shape((8, 8, 1280), BF16), (exchanged(dealt, Z),), 0)
    placed = call(place_kernel, shape((8, 8, 2304), BF16), (exchanged(added, Y),), 0)
    grad_mix, small = call(
        final_kernel,
        [shape((SEG, GROUPS, 512), F32), shape((64, 128), F32)],
        (exchanged(placed, Z),),
        0,
    )

    bias_row = lax.dynamic_slice_in_dim(mix_bias, spot * ROWS, ROWS, 1).T
    grad_u, grad_v = call(
        post_kernel,
        [shape((1, ROWS, HALF), BF16)] * 2,
        (place, values_in, upstream, stats, gain_row, bias_row, *outs_u, *outs_v, *got),
    )
    return (
        grad_u,
        grad_v,
        grad_mix,
        small[:16].reshape(GROUPS, 512),
        small[16:40].reshape(HALF),
        small[40:].reshape(HALF),
    )


def solution(mesh):
    torus = Mesh(mesh.devices.reshape(8, 8, 4, 2), ("sp_0", "sp_1", "dp_0", "dp_1"))
    return jax.shard_map(
        compute,
        mesh=torus,
        in_specs=(
            P(DP, SP, None),
            P(DP, SP, None),
            P(DP, SP, None),
            P(),
            P(),
            P(DP, None, None),
            P(),
        ),
        out_specs=(P(DP, SP, None), P(DP, SP, None), P(DP, None, None), P(), P(), P()),
        check_vma=False,
    )
```

profile of v0, /device:TPU:64, one launch (start us, length us, event | category | flops | bytes accessed | tf_op | source)
XLA Modules:
  0.0 183.4 jit_solution(17825048733315946918)
XLA Ops:
  0.7 0.9 copy-done
  1.7 1.9 %collective-permute-start.6 = (bf16[4,64,384]{2,1,0:T(8,128)(2,1)S(1)}, bf16[4,64,384]{2,1,0:T(8,128)(2,1)S(1)}, u32[]{:S(2)}, u32[]{:S(2)}) collective-permute-start(bf16[4,64,384]{2,1,0:T(8,128)(2,1)S(1)} %bitcast.13), channel_id=1, source_target_pairs={{0,1},{1,0},{2,3},{3,2},{4,5},{5,4},{6,7},{7,6},{8,9},{9,8},{10,11... | collective-permute-start | bytes 589832 | tf_op jit(solution)/shard_map/ppermute | solution.py:332
  3.6 4.7 %collective-permute-start.5 = (bf16[4,64,384]{2,1,0:T(8,128)(2,1)S(1)}, bf16[4,64,384]{2,1,0:T(8,128)(2,1)S(1)}, u32[]{:S(2)}, u32[]{:S(2)}) collective-permute-start(bf16[4,64,384]{2,1,0:T(8,128)(2,1)S(1)} %bitcast.14), channel_id=1, source_target_pairs={{0,6},{2,0},{4,2},{6,4},{1,7},{3,1},{5,3},{7,5},{8,14},{10,8},{12,... | collective-permute-start | bytes 589832 | tf_op jit(solution)/shard_map/ppermute | solution.py:331
  8.3 2.7 %collective-permute-start.4 = (bf16[4,64,384]{2,1,0:T(8,128)(2,1)S(1)}, bf16[4,64,384]{2,1,0:T(8,128)(2,1)S(1)}, u32[]{:S(2)}, u32[]{:S(2)}) collective-permute-start(bf16[4,64,384]{2,1,0:T(8,128)(2,1)S(1)} %bitcast.15), channel_id=1, source_target_pairs={{0,4},{2,6},{4,0},{6,2},{1,5},{3,7},{5,1},{7,3},{8,12},{10,14},{12... | collective-permute-start | bytes 589832 | tf_op jit(solution)/shard_map/ppermute | solution.py:331
  11.0 2.8 %collective-permute-start.3 = (bf16[4,64,384]{2,1,0:T(8,128)(2,1)S(1)}, bf16[4,64,384]{2,1,0:T(8,128)(2,1)S(1)}, u32[]{:S(2)}, u32[]{:S(2)}) collective-permute-start(bf16[4,64,384]{2,1,0:T(8,128)(2,1)S(1)} %bitcast.16), channel_id=1, source_target_pairs={{0,2},{2,4},{4,6},{6,0},{1,3},{3,5},{5,7},{7,1},{8,10},{10,12},{12... | collective-permute-start | bytes 589832 | tf_op jit(solution)/shard_map/ppermute | solution.py:331
  13.9 1.1 copy-done.2
  15.1 1.1 copy-done.21
  16.2 2.8 %shard_map.118 = (bf16[128,768]{1,0:T(8,128)(2,1)S(1)}, bf16[128,768]{1,0:T(8,128)(2,1)S(1)}, bf16[128,768]{1,0:T(8,128)(2,1)S(1)}, bf16[128,768]{1,0:T(8,128)(2...) custom-call(s32[3]{0:T(128)S(1)} %pad_add_fusion.place, ...), custom_call_target="tpu_custom_call" | custom-call | tf_op jit(solution)/shard_map/pallas_call | solution.py:42
  19.1 0.7 collective-permute-start.2
  19.8 6.2 %collective-permute-start.1 = (bf16[128,768]{1,0:T(8,128)(2,1)S(1)}, bf16[128,768]{1,0:T(8,128)(2,1)S(1)}, u32[]{:S(2)}, u32[]{:S(2)}) collective-permute-start(bf16[128,768]{1,0:T(8,128)(2,1)S(1)} %get-tuple-element.46.v.refs_1_), channel_id=1, source_target_pairs={{0,16},{24,8},{32,48},{56,40},{1,17},{25,9},{33,49},{57,41},{2,18}... | collective-permute-start | bytes 589832 | tf_op jit(solution)/shard_map/ppermute | solution.py:344
  26.0 1.4 collective-permute-start
  28.1 4.0 %collective-permute-start.11 = (bf16[128,768]{1,0:T(8,128)(2,1)S(1)}, bf16[128,768]{1,0:T(8,128)(2,1)S(1)}, u32[]{:S(2)}, u32[]{:S(2)}) collective-permute-start(bf16[128,768]{1,0:T(8,128)(2,1)S(1)} %get-tuple-element.49.v.refs_6_), channel_id=1, source_target_pairs={{0,16},{24,8},{32,48},{56,40},{1,17},{25,9},{33,49},{57,41},{2,18}... | collective-permute-start | bytes 589832 | tf_op jit(solution)/shard_map/ppermute | solution.py:344
  32.1 3.1 %collective-permute-start.10 = (bf16[128,768]{1,0:T(8,128)(2,1)S(1)}, bf16[128,768]{1,0:T(8,128)(2,1)S(1)}, u32[]{:S(2)}, u32[]{:S(2)}) collective-permute-start(bf16[128,768]{1,0:T(8,128)(2,1)S(1)} %get-tuple-element.49.v.refs_6_), channel_id=1, source_target_pairs={{0,8},{24,16},{32,40},{56,48},{1,9},{25,17},{33,41},{57,49},{2,10}... | collective-permute-start | bytes 589832 | tf_op jit(solution)/shard_map/ppermute | solution.py:343
  35.9 4.9 %collective-permute-start.14 = (bf16[128,768]{1,0:T(8,128)(2,1)S(1)}, bf16[128,768]{1,0:T(8,128)(2,1)S(1)}, u32[]{:S(2)}, u32[]{:S(2)}) collective-permute-start(bf16[128,768]{1,0:T(8,128)(2,1)S(1)} %get-tuple-element.52.v.refs_11_), channel_id=1, source_target_pairs={{0,16},{24,8},{32,48},{56,40},{1,17},{25,9},{33,49},{57,41},{2,18}... | collective-permute-start | bytes 589832 | tf_op jit(solution)/shard_map/ppermute | solution.py:344
  40.9 2.8 %collective-permute-start.13 = (bf16[128,768]{1,0:T(8,128)(2,1)S(1)}, bf16[128,768]{1,0:T(8,128)(2,1)S(1)}, u32[]{:S(2)}, u32[]{:S(2)}) collective-permute-start(bf16[128,768]{1,0:T(8,128)(2,1)S(1)} %get-tuple-element.52.v.refs_11_), channel_id=1, source_target_pairs={{0,8},{24,16},{32,40},{56,48},{1,9},{25,17},{33,41},{57,49},{2,10}... | collective-permute-start | bytes 589832 | tf_op jit(solution)/shard_map/ppermute | solution.py:343
  43.6 1.9 %collective-permute-start.9 = (bf16[4,64,384]{2,1,0:T(8,128)(2,1)S(1)}, bf16[4,64,384]{2,1,0:T(8,128)(2,1)S(1)}, u32[]{:S(2)}, u32[]{:S(2)}) collective-permute-start(bf16[4,64,384]{2,1,0:T(8,128)(2,1)S(1)} %collective-permute-done.5.refs_3_), channel_id=1, source_target_pairs={{0,1},{1,0},{2,3},{3,2},{4,5},{5,4},{6,7},{7,6},{8,9},{9,8},{10,11... | collective-permute-start | bytes 589832 | tf_op jit(solution)/shard_map/ppermute | solution.py:332
  45.6 2.4 %collective-permute-start.8 = (bf16[4,64,384]{2,1,0:T(8,128)(2,1)S(1)}, bf16[4,64,384]{2,1,0:T(8,128)(2,1)S(1)}, u32[]{:S(2)}, u32[]{:S(2)}) collective-permute-start(bf16[4,64,384]{2,1,0:T(8,128)(2,1)S(1)} %collective-permute-done.4.refs_2_), channel_id=1, source_target_pairs={{0,1},{1,0},{2,3},{3,2},{4,5},{5,4},{6,7},{7,6},{8,9},{9,8},{10,11... | collective-permute-start | bytes 589832 | tf_op jit(solution)/shard_map/ppermute | solution.py:332
  48.7 1.9 %collective-permute-start.7 = (bf16[4,64,384]{2,1,0:T(8,128)(2,1)S(1)}, bf16[4,64,384]{2,1,0:T(8,128)(2,1)S(1)}, u32[]{:S(2)}, u32[]{:S(2)}) collective-permute-start(bf16[4,64,384]{2,1,0:T(8,128)(2,1)S(1)} %collective-permute-done.3.refs_1_), channel_id=1, source_target_pairs={{0,1},{1,0},{2,3},{3,2},{4,5},{5,4},{6,7},{7,6},{8,9},{9,8},{10,11... | collective-permute-start | bytes 589832 | tf_op jit(solution)/shard_map/ppermute | solution.py:332
  50.8 5.6 %collective-permute-start.17 = (bf16[128,768]{1,0:T(8,128)(2,1)S(1)}, bf16[128,768]{1,0:T(8,128)(2,1)S(1)}, u32[]{:S(2)}, u32[]{:S(2)}) collective-permute-start(bf16[128,768]{1,0:T(8,128)(2,1)S(1)} %get-tuple-element.55.v.refs_1_), channel_id=1, source_target_pairs={{0,16},{24,8},{32,48},{56,40},{1,17},{25,9},{33,49},{57,41},{2,18}... | collective-permute-start | bytes 589832 | tf_op jit(solution)/shard_map/ppermute | solution.py:344
  56.4 1.8 %collective-permute-start.16 = (bf16[128,768]{1,0:T(8,128)(2,1)S(1)}, bf16[128,768]{1,0:T(8,128)(2,1)S(1)}, u32[]{:S(2)}, u32[]{:S(2)}) collective-permute-start(bf16[128,768]{1,0:T(8,128)(2,1)S(1)} %get-tuple-element.55.v.refs_1_), channel_id=1, source_target_pairs={{0,8},{24,16},{32,40},{56,48},{1,9},{25,17},{33,41},{57,49},{2,10}... | collective-permute-start | bytes 589832 | tf_op jit(solution)/shard_map/ppermute | solution.py:343
  58.3 1.3 shard_map.125
  59.5 2.1 %collective-permute-start.23 = (bf16[4,2,64,384]{3,2,1,0:T(8,128)(2,1)S(1)}, bf16[4,2,64,384]{3,2,1,0:T(8,128)(2,1)S(1)}, u32[]{:S(2)}, u32[]{:S(2)}) collective-permute-start(bf16[4,2,64,384]{3,2,1,0:T(8,128)(2,1)S(1)} %get-tuple-element.68), channel_id=1, source_target_pairs={{0,1},{1,0},{2,3},{3,2},{4,5},{5,4},{6,7},{7,6},{8,9},{9,8},{10,11... | collective-permute-start | bytes 1179656 | tf_op jit(solution)/shard_map/ppermute | solution.py:380
  61.7 1.0 shard_map.119.weights
  62.7 2.7 %collective-permute-done.16.near.refs_2_ = bf16[128,768]{1,0:T(8,128)(2,1)S(1)} collective-permute-done((bf16[128,768]{1,0:T(8,128)(2,1)S(1)}, bf16[128,768]{1,0:T(8,128)(2,1)S(1)}, u32[]{:S(2)}, u32[]{:S(2)}) %collective-permute-start.16) | collective-permute-done | bytes 196640 | tf_op jit(solution)/shard_map/ppermute | solution.py:343
  65.8 1.3 collective-permute-start.22
  67.5 1.3 collective-permute-start.20
  69.3 1.3 collective-permute-start.19
  71.0 1.3 collective-permute-start.21
  72.3 0.8 shard_map.127
  73.1 2.4 %collective-permute-done.22.refs_11_ = bf16[128,768]{1,0:T(8,128)(2,1)S(1)} collective-permute-done((bf16[128,768]{1,0:T(8,128)(2,1)S(1)}, bf16[128,768]{1,0:T(8,128)(2,1)S(1)}, u32[]{:S(2)}, u32[]{:S(2)}) %collective-permute-start.22) | collective-permute-done | bytes 196640 | tf_op jit(solution)/shard_map/ppermute | solution.py:362
  75.5 1.9 %collective-permute-start.27 = (bf16[4,2,64,128]{3,2,1,0:T(8,128)(2,1)S(1)}, bf16[4,2,64,128]{3,2,1,0:T(8,128)(2,1)S(1)}, u32[]{:S(2)}, u32[]{:S(2)}) collective-permute-start(bf16[4,2,64,128]{3,2,1,0:T(8,128)(2,1)S(1)} %get-tuple-element.74), channel_id=1, source_target_pairs={{0,1},{1,0},{2,3},{3,2},{4,5},{5,4},{6,7},{7,6},{8,9},{9,8},{10,11... | collective-permute-start | bytes 393224 | tf_op jit(solution)/shard_map/ppermute | solution.py:380
  77.4 2.3 %collective-permute-done.20.refs_9_ = bf16[128,768]{1,0:T(8,128)(2,1)S(1)} collective-permute-done((bf16[128,768]{1,0:T(8,128)(2,1)S(1)}, bf16[128,768]{1,0:T(8,128)(2,1)S(1)}, u32[]{:S(2)}, u32[]{:S(2)}) %collective-permute-start.20) | collective-permute-done | bytes 196640 | tf_op jit(solution)/shard_map/ppermute | solution.py:362
  79.7 4.2 %collective-permute-done.19.refs_8_ = bf16[128,768]{1,0:T(8,128)(2,1)S(1)} collective-permute-done((bf16[128,768]{1,0:T(8,128)(2,1)S(1)}, bf16[128,768]{1,0:T(8,128)(2,1)S(1)}, u32[]{:S(2)}, u32[]{:S(2)}) %collective-permute-start.19) | collective-permute-done | bytes 196640 | tf_op jit(solution)/shard_map/ppermute | solution.py:362
  83.9 3.0 %collective-permute-done.21.refs_10_ = bf16[128,768]{1,0:T(8,128)(2,1)S(1)} collective-permute-done((bf16[128,768]{1,0:T(8,128)(2,1)S(1)}, bf16[128,768]{1,0:T(8,128)(2,1)S(1)}, u32[]{:S(2)}, u32[]{:S(2)}) %collective-permute-start.21) | collective-permute-done | bytes 196640 | tf_op jit(solution)/shard_map/ppermute | solution.py:362
  86.9 1.2 shard_map.129
  88.2 1.9 %collective-permute-start.31 = (f32[64,128]{1,0:T(8,128)S(1)}, f32[64,128]{1,0:T(8,128)S(1)}, u32[]{:S(2)}, u32[]{:S(2)}) collective-permute-start(f32[64,128]{1,0:T(8,128)S(1)} %shard_map.129), channel_id=1, source_target_pairs={{0,1},{1,0},{2,3},{3,2},{4,5},{5,4},{6,7},{7,6},{8,9},{9,8},{10,11... | collective-permute-start | bytes 98312 | tf_op jit(solution)/shard_map/ppermute | solution.py:389
  90.7 3.7 %collective-permute-start.28 = (bf16[2,64,128]{2,1,0:T(8,128)(2,1)S(1)}, bf16[2,64,128]{2,1,0:T(8,128)(2,1)S(1)}, u32[]{:S(2)}, u32[]{:S(2)}) collective-permute-start(bf16[2,64,128]{2,1,0:T(8,128)(2,1)S(1)} %get-tuple-element.76), channel_id=1, source_target_pairs={{0,2},{2,4},{4,6},{6,0},{1,3},{3,5},{5,7},{7,1},{8,10},{10,12},{12... | collective-permute-start | bytes 98312 | tf_op jit(solution)/shard_map/ppermute | solution.py:382
  94.4 3.9 %collective-permute-start.29 = (bf16[2,64,128]{2,1,0:T(8,128)(2,1)S(1)}, bf16[2,64,128]{2,1,0:T(8,128)(2,1)S(1)}, u32[]{:S(2)}, u32[]{:S(2)}) collective-permute-start(bf16[2,64,128]{2,1,0:T(8,128)(2,1)S(1)} %get-tuple-element.77), channel_id=1, source_target_pairs={{0,4},{2,6},{4,0},{6,2},{1,5},{3,7},{5,1},{7,3},{8,12},{10,14},{12... | collective-permute-start | bytes 98312 | tf_op jit(solution)/shard_map/ppermute | solution.py:382
  99.0 2.2 %collective-permute-start.24 = (bf16[2,64,384]{2,1,0:T(8,128)(2,1)S(1)}, bf16[2,64,384]{2,1,0:T(8,128)(2,1)S(1)}, u32[]{:S(2)}, u32[]{:S(2)}) collective-permute-start(bf16[2,64,384]{2,1,0:T(8,128)(2,1)S(1)} %get-tuple-element.70), channel_id=1, source_target_pairs={{0,2},{2,4},{4,6},{6,0},{1,3},{3,5},{5,7},{7,1},{8,10},{10,12},{12... | collective-permute-start | bytes 294920 | tf_op jit(solution)/shard_map/ppermute | solution.py:382
  101.2 4.3 %collective-permute-start.25 = (bf16[2,64,384]{2,1,0:T(8,128)(2,1)S(1)}, bf16[2,64,384]{2,1,0:T(8,128)(2,1)S(1)}, u32[]{:S(2)}, u32[]{:S(2)}) collective-permute-start(bf16[2,64,384]{2,1,0:T(8,128)(2,1)S(1)} %get-tuple-element.71), channel_id=1, source_target_pairs={{0,4},{2,6},{4,0},{6,2},{1,5},{3,7},{5,1},{7,3},{8,12},{10,14},{12... | collective-permute-start | bytes 294920 | tf_op jit(solution)/shard_map/ppermute | solution.py:382
  105.5 3.4 %collective-permute-start.26 = (bf16[2,64,384]{2,1,0:T(8,128)(2,1)S(1)}, bf16[2,64,384]{2,1,0:T(8,128)(2,1)S(1)}, u32[]{:S(2)}, u32[]{:S(2)}) collective-permute-start(bf16[2,64,384]{2,1,0:T(8,128)(2,1)S(1)} %get-tuple-element.72), channel_id=1, source_target_pairs={{0,6},{2,0},{4,2},{6,4},{1,7},{3,1},{5,3},{7,5},{8,14},{10,8},{12,... | collective-permute-start | bytes 294920 | tf_op jit(solution)/shard_map/ppermute | solution.py:382
  108.9 2.1 %collective-permute-start.30 = (bf16[2,64,128]{2,1,0:T(8,128)(2,1)S(1)}, bf16[2,64,128]{2,1,0:T(8,128)(2,1)S(1)}, u32[]{:S(2)}, u32[]{:S(2)}) collective-permute-start(bf16[2,64,128]{2,1,0:T(8,128)(2,1)S(1)} %get-tuple-element.78), channel_id=1, source_target_pairs={{0,6},{2,0},{4,2},{6,4},{1,7},{3,1},{5,3},{7,5},{8,14},{10,8},{12,... | collective-permute-start | bytes 98312 | tf_op jit(solution)/shard_map/ppermute | solution.py:382
  111.1 4.3 %collective-permute-start.34 = (f32[64,128]{1,0:T(8,128)S(1)}, f32[64,128]{1,0:T(8,128)S(1)}, u32[]{:S(2)}, u32[]{:S(2)}) collective-permute-start(f32[64,128]{1,0:T(8,128)S(1)} %add.13.refs_8_), channel_id=1, source_target_pairs={{0,6},{2,0},{4,2},{6,4},{1,7},{3,1},{5,3},{7,5},{8,14},{10,8},{12,... | collective-permute-start | bytes 98312 | tf_op jit(solution)/shard_map/ppermute | solution.py:390
  115.4 3.4 %collective-permute-start.33 = (f32[64,128]{1,0:T(8,128)S(1)}, f32[64,128]{1,0:T(8,128)S(1)}, u32[]{:S(2)}, u32[]{:S(2)}) collective-permute-start(f32[64,128]{1,0:T(8,128)S(1)} %add.13.refs_8_), channel_id=1, source_target_pairs={{0,4},{2,6},{4,0},{6,2},{1,5},{3,7},{5,1},{7,3},{8,12},{10,14},{12... | collective-permute-start | bytes 98312 | tf_op jit(solution)/shard_map/ppermute | solution.py:390
  118.8 2.0 %collective-permute-start.32 = (f32[64,128]{1,0:T(8,128)S(1)}, f32[64,128]{1,0:T(8,128)S(1)}, u32[]{:S(2)}, u32[]{:S(2)}) collective-permute-start(f32[64,128]{1,0:T(8,128)S(1)} %add.13.refs_8_), channel_id=1, source_target_pairs={{0,2},{2,4},{4,6},{6,0},{1,3},{3,5},{5,7},{7,1},{8,10},{10,12},{12... | collective-permute-start | bytes 98312 | tf_op jit(solution)/shard_map/ppermute | solution.py:390
  120.9 2.0 %collective-permute-done.33.refs_10_ = f32[64,128]{1,0:T(8,128)S(1)} collective-permute-done((f32[64,128]{1,0:T(8,128)S(1)}, f32[64,128]{1,0:T(8,128)S(1)}, u32[]{:S(2)}, u32[]{:S(2)}) %collective-permute-start.33) | collective-permute-done | bytes 32800 | tf_op jit(solution)/shard_map/ppermute | solution.py:390
  122.9 3.0 %collective-permute-done.32.refs_9_ = f32[64,128]{1,0:T(8,128)S(1)} collective-permute-done((f32[64,128]{1,0:T(8,128)S(1)}, f32[64,128]{1,0:T(8,128)S(1)}, u32[]{:S(2)}, u32[]{:S(2)}) %collective-permute-start.32) | collective-permute-done | bytes 32800 | tf_op jit(solution)/shard_map/ppermute | solution.py:390
  125.9 17.7 %all_to_all.15.got = bf16[8,8,1280]{2,1,0:T(8,128)(2,1)S(1)} all-to-all(bf16[8,8,1280]{2,1,0:T(8,128)(2,1)S(1)} %shard_map.130), channel_id=1, replica_groups=mesh['sp_0'=8,'sp_1'=8,'dp_0'=4,'dp_1'=2] {'sp_0'}, dimensions={0} | all-to-all | bytes 327680 | tf_op jit(solution)/shard_map/all_to_all | solution.py:318
  143.7 15.8 %all_to_all.16.got = bf16[8,8,1280]{2,1,0:T(8,128)(2,1)S(1)} all-to-all(bf16[8,8,1280]{2,1,0:T(8,128)(2,1)S(1)} %shard_map.131), channel_id=1, replica_groups=mesh['sp_0'=8,'sp_1'=8,'dp_0'=4,'dp_1'=2] {'sp_1'}, dimensions={0} | all-to-all | bytes 327680 | tf_op jit(solution)/shard_map/all_to_all | solution.py:318
  159.5 0.7 copy-done.12
  160.2 5.4 %all-to-all-start.2 = ((bf16[8,8,2304]{2,1,0:T(8,128)(2,1)}), bf16[8,8,2304]{2,1,0:T(8,128)(2,1)}, u32[]{:S(2)}, u32[]{:S(2)}) async-start(bf16[8,8,2304]{2,1,0:T(8,128)(2,1)} %copy-done.12), calls=%async_computation.2 | async-start | bytes 589824 | tf_op jit(solution)/shard_map/all_to_all | solution.py:318
  165.6 1.3 constant_dynamic-slice_fusion.1
  166.9 1.4 copy.15
  168.3 1.0 copy-done.5
  169.3 1.0 copy-done.7
  170.3 1.0 copy-done.9
  171.3 1.0 copy-done.11
  172.3 0.9 copy-done.14
  173.2 0.9 copy-done.16
  174.1 0.9 copy-done.18
  175.1 0.9 copy-done.20
  176.0 0.8 copy-done.22
  176.8 3.5 %shard_map.124 = (bf16[1,128,3072]{2,1,0:T(8,128)(2,1)}, bf16[1,128,3072]{2,1,0:T(8,128)(2,1)}) custom-call(s32[3]{0:T(128)S(1)} %pad_add_fusion.place, bf16[1,128,3072]{2,1,0:T(8,128)(2,1)S(1)} %copy-done.1, bf16[1,128,3072]{2,1,0:T(8,128)(2,1)S(1)} %copy-done.3, f32[2,128,128]{2,1,0:T(8,128)S(1)} %get-tuple-element.44.stats, f32[1,3072]{1,0:T(1,128)S(1)} %bitcast.20, ...), custom_call_target="tpu_custom_call" | custom-call | tf_op jit(solution)/shard_map/pallas_call | solution.py:42
  180.3 1.9 %shard_map.133 = (f32[64,4,512]{2,1,0:T(4,128)}, f32[64,128]{1,0:T(8,128)S(1)}) custom-call(bf16[8,8,2304]{2,1,0:T(8,128)(2,1)} %all-to-all-done.2.got), custom_call_target="tpu_custom_call" | custom-call | tf_op jit(solution)/shard_map/pallas_call | solution.py:42
  (85 shorter events, 6.8 us)
Async XLA Ops:
  0.6 1.0 copy-start
  0.6 13.3 %copy-start.1 = (bf16[1,128,3072]{2,1,0:T(8,128)(2,1)S(1)}, bf16[1,128,3072]{2,1,0:T(8,128)(2,1)}, u32[]{:S(2)}) copy-start(bf16[1,128,3072]{2,1,0:T(8,128)(2,1)} %values.5) | copy-start | bytes 2359300
  1.7 12.3 %copy-start.24 = (f32[3072]{0:T(1024)S(1)}, f32[3072]{0:T(1024)}, u32[]{:S(2)}) copy-start(f32[3072]{0:T(1024)} %param.11) | copy-start | bytes 36868
  1.7 12.2 %copy-start.23 = (f32[3072]{0:T(1024)S(1)}, f32[3072]{0:T(1024)}, u32[]{:S(2)}) copy-start(f32[3072]{0:T(1024)} %param.10) | copy-start | bytes 36868
  1.7 18.0 %collective-permute-start.6 = (bf16[4,64,384]{2,1,0:T(8,128)(2,1)S(1)}, bf16[4,64,384]{2,1,0:T(8,128)(2,1)S(1)}, u32[]{:S(2)}, u32[]{:S(2)}) collective-permute-start(bf16[4,64,384]{2,1,0:T(8,128)(2,1)S(1)} %bitcast.13), channel_id=1, source_target_pairs={{0,1},{1,0},{2,3},{3,2},{4,5},{5,4},{6,7},{7,6},{8,9},{9,8},{10,11... | collective-permute-start | bytes 589832 | tf_op jit(solution)/shard_map/ppermute | solution.py:332
  3.6 22.3 %collective-permute-start.5 = (bf16[4,64,384]{2,1,0:T(8,128)(2,1)S(1)}, bf16[4,64,384]{2,1,0:T(8,128)(2,1)S(1)}, u32[]{:S(2)}, u32[]{:S(2)}) collective-permute-start(bf16[4,64,384]{2,1,0:T(8,128)(2,1)S(1)} %bitcast.14), channel_id=1, source_target_pairs={{0,6},{2,0},{4,2},{6,4},{1,7},{3,1},{5,3},{7,5},{8,14},{10,8},{12,... | collective-permute-start | bytes 589832 | tf_op jit(solution)/shard_map/ppermute | solution.py:331
  8.3 19.1 %collective-permute-start.4 = (bf16[4,64,384]{2,1,0:T(8,128)(2,1)S(1)}, bf16[4,64,384]{2,1,0:T(8,128)(2,1)S(1)}, u32[]{:S(2)}, u32[]{:S(2)}) collective-permute-start(bf16[4,64,384]{2,1,0:T(8,128)(2,1)S(1)} %bitcast.15), channel_id=1, source_target_pairs={{0,4},{2,6},{4,0},{6,2},{1,5},{3,7},{5,1},{7,3},{8,12},{10,14},{12... | collective-permute-start | bytes 589832 | tf_op jit(solution)/shard_map/ppermute | solution.py:331
  11.0 17.0 %collective-permute-start.3 = (bf16[4,64,384]{2,1,0:T(8,128)(2,1)S(1)}, bf16[4,64,384]{2,1,0:T(8,128)(2,1)S(1)}, u32[]{:S(2)}, u32[]{:S(2)}) collective-permute-start(bf16[4,64,384]{2,1,0:T(8,128)(2,1)S(1)} %bitcast.16), channel_id=1, source_target_pairs={{0,2},{2,4},{4,6},{6,0},{1,3},{3,5},{5,7},{7,1},{8,10},{10,12},{12... | collective-permute-start | bytes 589832 | tf_op jit(solution)/shard_map/ppermute | solution.py:331
  13.9 1.1 copy-start.2
  15.1 1.1 copy-start.21
  19.1 13.0 %collective-permute-start.2 = (bf16[128,768]{1,0:T(8,128)(2,1)S(1)}, bf16[128,768]{1,0:T(8,128)(2,1)S(1)}, u32[]{:S(2)}, u32[]{:S(2)}) collective-permute-start(bf16[128,768]{1,0:T(8,128)(2,1)S(1)} %get-tuple-element.46.v.refs_1_), channel_id=1, source_target_pairs={{8,16},{16,8},{40,48},{48,40},{9,17},{17,9},{41,49},{49,41},{10,18... | collective-permute-start | bytes 589832 | tf_op jit(solution)/shard_map/ppermute | solution.py:345
  19.8 15.4 %collective-permute-start.1 = (bf16[128,768]{1,0:T(8,128)(2,1)S(1)}, bf16[128,768]{1,0:T(8,128)(2,1)S(1)}, u32[]{:S(2)}, u32[]{:S(2)}) collective-permute-start(bf16[128,768]{1,0:T(8,128)(2,1)S(1)} %get-tuple-element.46.v.refs_1_), channel_id=1, source_target_pairs={{0,16},{24,8},{32,48},{56,40},{1,17},{25,9},{33,49},{57,41},{2,18}... | collective-permute-start | bytes 589832 | tf_op jit(solution)/shard_map/ppermute | solution.py:344
  26.0 9.9 %collective-permute-start = (bf16[128,768]{1,0:T(8,128)(2,1)S(1)}, bf16[128,768]{1,0:T(8,128)(2,1)S(1)}, u32[]{:S(2)}, u32[]{:S(2)}) collective-permute-start(bf16[128,768]{1,0:T(8,128)(2,1)S(1)} %get-tuple-element.46.v.refs_1_), channel_id=1, source_target_pairs={{0,8},{24,16},{32,40},{56,48},{1,9},{25,17},{33,41},{57,49},{2,10}... | collective-permute-start | bytes 589832 | tf_op jit(solution)/shard_map/ppermute | solution.py:343
  27.4 13.5 %collective-permute-start.12 = (bf16[128,768]{1,0:T(8,128)(2,1)S(1)}, bf16[128,768]{1,0:T(8,128)(2,1)S(1)}, u32[]{:S(2)}, u32[]{:S(2)}) collective-permute-start(bf16[128,768]{1,0:T(8,128)(2,1)S(1)} %get-tuple-element.49.v.refs_6_), channel_id=1, source_target_pairs={{8,16},{16,8},{40,48},{48,40},{9,17},{17,9},{41,49},{49,41},{10,18... | collective-permute-start | bytes 589832 | tf_op jit(solution)/shard_map/ppermute | solution.py:345
  28.1 15.5 %collective-permute-start.11 = (bf16[128,768]{1,0:T(8,128)(2,1)S(1)}, bf16[128,768]{1,0:T(8,128)(2,1)S(1)}, u32[]{:S(2)}, u32[]{:S(2)}) collective-permute-start(bf16[128,768]{1,0:T(8,128)(2,1)S(1)} %get-tuple-element.49.v.refs_6_), channel_id=1, source_target_pairs={{0,16},{24,8},{32,48},{56,40},{1,17},{25,9},{33,49},{57,41},{2,18}... | collective-permute-start | bytes 589832 | tf_op jit(solution)/shard_map/ppermute | solution.py:344
  32.1 13.5 %collective-permute-start.10 = (bf16[128,768]{1,0:T(8,128)(2,1)S(1)}, bf16[128,768]{1,0:T(8,128)(2,1)S(1)}, u32[]{:S(2)}, u32[]{:S(2)}) collective-permute-start(bf16[128,768]{1,0:T(8,128)(2,1)S(1)} %get-tuple-element.49.v.refs_6_), channel_id=1, source_target_pairs={{0,8},{24,16},{32,40},{56,48},{1,9},{25,17},{33,41},{57,49},{2,10}... | collective-permute-start | bytes 589832 | tf_op jit(solution)/shard_map/ppermute | solution.py:343
  35.2 12.8 %collective-permute-start.15 = (bf16[128,768]{1,0:T(8,128)(2,1)S(1)}, bf16[128,768]{1,0:T(8,128)(2,1)S(1)}, u32[]{:S(2)}, u32[]{:S(2)}) collective-permute-start(bf16[128,768]{1,0:T(8,128)(2,1)S(1)} %get-tuple-element.52.v.refs_11_), channel_id=1, source_target_pairs={{8,16},{16,8},{40,48},{48,40},{9,17},{17,9},{41,49},{49,41},{10,18... | collective-permute-start | bytes 589832 | tf_op jit(solution)/shard_map/ppermute | solution.py:345
  35.9 12.8 %collective-permute-start.14 = (bf16[128,768]{1,0:T(8,128)(2,1)S(1)}, bf16[128,768]{1,0:T(8,128)(2,1)S(1)}, u32[]{:S(2)}, u32[]{:S(2)}) collective-permute-start(bf16[128,768]{1,0:T(8,128)(2,1)S(1)} %get-tuple-element.52.v.refs_11_), channel_id=1, source_target_pairs={{0,16},{24,8},{32,48},{56,40},{1,17},{25,9},{33,49},{57,41},{2,18}... | collective-permute-start | bytes 589832 | tf_op jit(solution)/shard_map/ppermute | solution.py:344
  40.9 10.0 %collective-permute-start.13 = (bf16[128,768]{1,0:T(8,128)(2,1)S(1)}, bf16[128,768]{1,0:T(8,128)(2,1)S(1)}, u32[]{:S(2)}, u32[]{:S(2)}) collective-permute-start(bf16[128,768]{1,0:T(8,128)(2,1)S(1)} %get-tuple-element.52.v.refs_11_), channel_id=1, source_target_pairs={{0,8},{24,16},{32,40},{56,48},{1,9},{25,17},{33,41},{57,49},{2,10}... | collective-permute-start | bytes 589832 | tf_op jit(solution)/shard_map/ppermute | solution.py:343
  43.6 12.8 %collective-permute-start.9 = (bf16[4,64,384]{2,1,0:T(8,128)(2,1)S(1)}, bf16[4,64,384]{2,1,0:T(8,128)(2,1)S(1)}, u32[]{:S(2)}, u32[]{:S(2)}) collective-permute-start(bf16[4,64,384]{2,1,0:T(8,128)(2,1)S(1)} %collective-permute-done.5.refs_3_), channel_id=1, source_target_pairs={{0,1},{1,0},{2,3},{3,2},{4,5},{5,4},{6,7},{7,6},{8,9},{9,8},{10,11... | collective-permute-start | bytes 589832 | tf_op jit(solution)/shard_map/ppermute | solution.py:332
  45.6 14.0 %collective-permute-start.8 = (bf16[4,64,384]{2,1,0:T(8,128)(2,1)S(1)}, bf16[4,64,384]{2,1,0:T(8,128)(2,1)S(1)}, u32[]{:S(2)}, u32[]{:S(2)}) collective-permute-start(bf16[4,64,384]{2,1,0:T(8,128)(2,1)S(1)} %collective-permute-done.4.refs_2_), channel_id=1, source_target_pairs={{0,1},{1,0},{2,3},{3,2},{4,5},{5,4},{6,7},{7,6},{8,9},{9,8},{10,11... | collective-permute-start | bytes 589832 | tf_op jit(solution)/shard_map/ppermute | solution.py:332
  48.0 14.7 %collective-permute-start.18 = (bf16[128,768]{1,0:T(8,128)(2,1)S(1)}, bf16[128,768]{1,0:T(8,128)(2,1)S(1)}, u32[]{:S(2)}, u32[]{:S(2)}) collective-permute-start(bf16[128,768]{1,0:T(8,128)(2,1)S(1)} %get-tuple-element.55.v.refs_1_), channel_id=1, source_target_pairs={{8,16},{16,8},{40,48},{48,40},{9,17},{17,9},{41,49},{49,41},{10,18... | collective-permute-start | bytes 589832 | tf_op jit(solution)/shard_map/ppermute | solution.py:345
  48.7 13.0 %collective-permute-start.7 = (bf16[4,64,384]{2,1,0:T(8,128)(2,1)S(1)}, bf16[4,64,384]{2,1,0:T(8,128)(2,1)S(1)}, u32[]{:S(2)}, u32[]{:S(2)}) collective-permute-start(bf16[4,64,384]{2,1,0:T(8,128)(2,1)S(1)} %collective-permute-done.3.refs_1_), channel_id=1, source_target_pairs={{0,1},{1,0},{2,3},{3,2},{4,5},{5,4},{6,7},{7,6},{8,9},{9,8},{10,11... | collective-permute-start | bytes 589832 | tf_op jit(solution)/shard_map/ppermute | solution.py:332
  50.8 11.9 %collective-permute-start.17 = (bf16[128,768]{1,0:T(8,128)(2,1)S(1)}, bf16[128,768]{1,0:T(8,128)(2,1)S(1)}, u32[]{:S(2)}, u32[]{:S(2)}) collective-permute-start(bf16[128,768]{1,0:T(8,128)(2,1)S(1)} %get-tuple-element.55.v.refs_1_), channel_id=1, source_target_pairs={{0,16},{24,8},{32,48},{56,40},{1,17},{25,9},{33,49},{57,41},{2,18}... | collective-permute-start | bytes 589832 | tf_op jit(solution)/shard_map/ppermute | solution.py:344
  56.4 9.0 %collective-permute-start.16 = (bf16[128,768]{1,0:T(8,128)(2,1)S(1)}, bf16[128,768]{1,0:T(8,128)(2,1)S(1)}, u32[]{:S(2)}, u32[]{:S(2)}) collective-permute-start(bf16[128,768]{1,0:T(8,128)(2,1)S(1)} %get-tuple-element.55.v.refs_1_), channel_id=1, source_target_pairs={{0,8},{24,16},{32,40},{56,48},{1,9},{25,17},{33,41},{57,49},{2,10}... | collective-permute-start | bytes 589832 | tf_op jit(solution)/shard_map/ppermute | solution.py:343
  59.5 38.8 %collective-permute-start.23 = (bf16[4,2,64,384]{3,2,1,0:T(8,128)(2,1)S(1)}, bf16[4,2,64,384]{3,2,1,0:T(8,128)(2,1)S(1)}, u32[]{:S(2)}, u32[]{:S(2)}) collective-permute-start(bf16[4,2,64,384]{3,2,1,0:T(8,128)(2,1)S(1)} %get-tuple-element.68), channel_id=1, source_target_pairs={{0,1},{1,0},{2,3},{3,2},{4,5},{5,4},{6,7},{7,6},{8,9},{9,8},{10,11... | collective-permute-start | bytes 1179656 | tf_op jit(solution)/shard_map/ppermute | solution.py:380
  65.8 9.7 %collective-permute-start.22 = (bf16[128,768]{1,0:T(8,128)(2,1)S(1)}, bf16[128,768]{1,0:T(8,128)(2,1)S(1)}, u32[]{:S(2)}, u32[]{:S(2)}) collective-permute-start(bf16[128,768]{1,0:T(8,128)(2,1)S(1)} %get-tuple-element.64), channel_id=1, source_target_pairs={{8,0},{16,24},{40,32},{48,56},{9,1},{17,25},{41,33},{49,57},{10,2}... | collective-permute-start | bytes 589832 | tf_op jit(solution)/shard_map/ppermute | solution.py:362
  67.5 12.2 %collective-permute-start.20 = (bf16[128,768]{1,0:T(8,128)(2,1)S(1)}, bf16[128,768]{1,0:T(8,128)(2,1)S(1)}, u32[]{:S(2)}, u32[]{:S(2)}) collective-permute-start(bf16[128,768]{1,0:T(8,128)(2,1)S(1)} %get-tuple-element.62), channel_id=1, source_target_pairs={{8,0},{16,24},{40,32},{48,56},{9,1},{17,25},{41,33},{49,57},{10,2}... | collective-permute-start | bytes 589832 | tf_op jit(solution)/shard_map/ppermute | solution.py:362
  69.3 17.7 %copy-start.4 = (f32[128,768]{1,0:T(8,128)}, f32[128,768]{1,0:T(8,128)S(1)}, u32[]{:S(2)}) copy-start(f32[128,768]{1,0:T(8,128)S(1)} %get-tuple-element.47.refs_0_) | copy-start | bytes 1179652
  69.3 17.7 %copy-start.6 = (f32[128,768]{1,0:T(8,128)}, f32[128,768]{1,0:T(8,128)S(1)}, u32[]{:S(2)}) copy-start(f32[128,768]{1,0:T(8,128)S(1)} %get-tuple-element.57.refs_4_) | copy-start | bytes 1179652
  69.3 14.6 %collective-permute-start.19 = (bf16[128,768]{1,0:T(8,128)(2,1)S(1)}, bf16[128,768]{1,0:T(8,128)(2,1)S(1)}, u32[]{:S(2)}, u32[]{:S(2)}) collective-permute-start(bf16[128,768]{1,0:T(8,128)(2,1)S(1)} %get-tuple-element.61), channel_id=1, source_target_pairs={{8,0},{16,24},{40,32},{48,56},{9,1},{17,25},{41,33},{49,57},{10,2}... | collective-permute-start | bytes 589832 | tf_op jit(solution)/shard_map/ppermute | solution.py:362
  71.0 15.9 %copy-start.8 = (f32[128,768]{1,0:T(8,128)}, f32[128,768]{1,0:T(8,128)S(1)}, u32[]{:S(2)}) copy-start(f32[128,768]{1,0:T(8,128)S(1)} %get-tuple-element.53.refs_2_) | copy-start | bytes 1179652
  71.0 15.9 %copy-start.10 = (f32[128,768]{1,0:T(8,128)}, f32[128,768]{1,0:T(8,128)S(1)}, u32[]{:S(2)}) copy-start(f32[128,768]{1,0:T(8,128)S(1)} %get-tuple-element.59.refs_6_) | copy-start | bytes 1179652
  71.0 15.9 %collective-permute-start.21 = (bf16[128,768]{1,0:T(8,128)(2,1)S(1)}, bf16[128,768]{1,0:T(8,128)(2,1)S(1)}, u32[]{:S(2)}, u32[]{:S(2)}) collective-permute-start(bf16[128,768]{1,0:T(8,128)(2,1)S(1)} %get-tuple-element.63), channel_id=1, source_target_pairs={{8,0},{16,24},{40,32},{48,56},{9,1},{17,25},{41,33},{49,57},{10,2}... | collective-permute-start | bytes 589832 | tf_op jit(solution)/shard_map/ppermute | solution.py:362
  75.5 12.7 %copy-start.13 = (bf16[128,768]{1,0:T(8,128)(2,1)}, bf16[128,768]{1,0:T(8,128)(2,1)S(1)}, u32[]{:S(2)}) copy-start(bf16[128,768]{1,0:T(8,128)(2,1)S(1)} %collective-permute-done.22.refs_11_) | copy-start | bytes 589828
  75.5 14.6 %collective-permute-start.27 = (bf16[4,2,64,128]{3,2,1,0:T(8,128)(2,1)S(1)}, bf16[4,2,64,128]{3,2,1,0:T(8,128)(2,1)S(1)}, u32[]{:S(2)}, u32[]{:S(2)}) collective-permute-start(bf16[4,2,64,128]{3,2,1,0:T(8,128)(2,1)S(1)} %get-tuple-element.74), channel_id=1, source_target_pairs={{0,1},{1,0},{2,3},{3,2},{4,5},{5,4},{6,7},{7,6},{8,9},{9,8},{10,11... | collective-permute-start | bytes 393224 | tf_op jit(solution)/shard_map/ppermute | solution.py:380
  79.7 8.5 %copy-start.15 = (bf16[128,768]{1,0:T(8,128)(2,1)}, bf16[128,768]{1,0:T(8,128)(2,1)S(1)}, u32[]{:S(2)}) copy-start(bf16[128,768]{1,0:T(8,128)(2,1)S(1)} %collective-permute-done.20.refs_9_) | copy-start | bytes 589828
  83.9 4.3 %copy-start.17 = (bf16[128,768]{1,0:T(8,128)(2,1)}, bf16[128,768]{1,0:T(8,128)(2,1)S(1)}, u32[]{:S(2)}) copy-start(bf16[128,768]{1,0:T(8,128)(2,1)S(1)} %collective-permute-done.19.refs_8_) | copy-start | bytes 589828
  86.9 1.3 copy-start.19
  88.2 17.3 %collective-permute-start.31 = (f32[64,128]{1,0:T(8,128)S(1)}, f32[64,128]{1,0:T(8,128)S(1)}, u32[]{:S(2)}, u32[]{:S(2)}) collective-permute-start(f32[64,128]{1,0:T(8,128)S(1)} %shard_map.129), channel_id=1, source_target_pairs={{0,1},{1,0},{2,3},{3,2},{4,5},{5,4},{6,7},{7,6},{8,9},{9,8},{10,11... | collective-permute-start | bytes 98312 | tf_op jit(solution)/shard_map/ppermute | solution.py:389
  90.7 18.2 %collective-permute-start.28 = (bf16[2,64,128]{2,1,0:T(8,128)(2,1)S(1)}, bf16[2,64,128]{2,1,0:T(8,128)(2,1)S(1)}, u32[]{:S(2)}, u32[]{:S(2)}) collective-permute-start(bf16[2,64,128]{2,1,0:T(8,128)(2,1)S(1)} %get-tuple-element.76), channel_id=1, source_target_pairs={{0,2},{2,4},{4,6},{6,0},{1,3},{3,5},{5,7},{7,1},{8,10},{10,12},{12... | collective-permute-start | bytes 98312 | tf_op jit(solution)/shard_map/ppermute | solution.py:382
  94.4 16.6 %collective-permute-start.29 = (bf16[2,64,128]{2,1,0:T(8,128)(2,1)S(1)}, bf16[2,64,128]{2,1,0:T(8,128)(2,1)S(1)}, u32[]{:S(2)}, u32[]{:S(2)}) collective-permute-start(bf16[2,64,128]{2,1,0:T(8,128)(2,1)S(1)} %get-tuple-element.77), channel_id=1, source_target_pairs={{0,4},{2,6},{4,0},{6,2},{1,5},{3,7},{5,1},{7,3},{8,12},{10,14},{12... | collective-permute-start | bytes 98312 | tf_op jit(solution)/shard_map/ppermute | solution.py:382
  99.0 26.8 %collective-permute-start.24 = (bf16[2,64,384]{2,1,0:T(8,128)(2,1)S(1)}, bf16[2,64,384]{2,1,0:T(8,128)(2,1)S(1)}, u32[]{:S(2)}, u32[]{:S(2)}) collective-permute-start(bf16[2,64,384]{2,1,0:T(8,128)(2,1)S(1)} %get-tuple-element.70), channel_id=1, source_target_pairs={{0,2},{2,4},{4,6},{6,0},{1,3},{3,5},{5,7},{7,1},{8,10},{10,12},{12... | collective-permute-start | bytes 294920 | tf_op jit(solution)/shard_map/ppermute | solution.py:382
  101.2 24.6 %collective-permute-start.25 = (bf16[2,64,384]{2,1,0:T(8,128)(2,1)S(1)}, bf16[2,64,384]{2,1,0:T(8,128)(2,1)S(1)}, u32[]{:S(2)}, u32[]{:S(2)}) collective-permute-start(bf16[2,64,384]{2,1,0:T(8,128)(2,1)S(1)} %get-tuple-element.71), channel_id=1, source_target_pairs={{0,4},{2,6},{4,0},{6,2},{1,5},{3,7},{5,1},{7,3},{8,12},{10,14},{12... | collective-permute-start | bytes 294920 | tf_op jit(solution)/shard_map/ppermute | solution.py:382
  105.5 20.3 %collective-permute-start.26 = (bf16[2,64,384]{2,1,0:T(8,128)(2,1)S(1)}, bf16[2,64,384]{2,1,0:T(8,128)(2,1)S(1)}, u32[]{:S(2)}, u32[]{:S(2)}) collective-permute-start(bf16[2,64,384]{2,1,0:T(8,128)(2,1)S(1)} %get-tuple-element.72), channel_id=1, source_target_pairs={{0,6},{2,0},{4,2},{6,4},{1,7},{3,1},{5,3},{7,5},{8,14},{10,8},{12,... | collective-permute-start | bytes 294920 | tf_op jit(solution)/shard_map/ppermute | solution.py:382
  108.9 6.4 %collective-permute-start.30 = (bf16[2,64,128]{2,1,0:T(8,128)(2,1)S(1)}, bf16[2,64,128]{2,1,0:T(8,128)(2,1)S(1)}, u32[]{:S(2)}, u32[]{:S(2)}) collective-permute-start(bf16[2,64,128]{2,1,0:T(8,128)(2,1)S(1)} %get-tuple-element.78), channel_id=1, source_target_pairs={{0,6},{2,0},{4,2},{6,4},{1,7},{3,1},{5,3},{7,5},{8,14},{10,8},{12,... | collective-permute-start | bytes 98312 | tf_op jit(solution)/shard_map/ppermute | solution.py:382
  111.1 7.7 %collective-permute-start.34 = (f32[64,128]{1,0:T(8,128)S(1)}, f32[64,128]{1,0:T(8,128)S(1)}, u32[]{:S(2)}, u32[]{:S(2)}) collective-permute-start(f32[64,128]{1,0:T(8,128)S(1)} %add.13.refs_8_), channel_id=1, source_target_pairs={{0,6},{2,0},{4,2},{6,4},{1,7},{3,1},{5,3},{7,5},{8,14},{10,8},{12,... | collective-permute-start | bytes 98312 | tf_op jit(solution)/shard_map/ppermute | solution.py:390
  115.4 7.5 %collective-permute-start.33 = (f32[64,128]{1,0:T(8,128)S(1)}, f32[64,128]{1,0:T(8,128)S(1)}, u32[]{:S(2)}, u32[]{:S(2)}) collective-permute-start(f32[64,128]{1,0:T(8,128)S(1)} %add.13.refs_8_), channel_id=1, source_target_pairs={{0,4},{2,6},{4,0},{6,2},{1,5},{3,7},{5,1},{7,3},{8,12},{10,14},{12... | collective-permute-start | bytes 98312 | tf_op jit(solution)/shard_map/ppermute | solution.py:390
  118.8 7.0 %collective-permute-start.32 = (f32[64,128]{1,0:T(8,128)S(1)}, f32[64,128]{1,0:T(8,128)S(1)}, u32[]{:S(2)}, u32[]{:S(2)}) collective-permute-start(f32[64,128]{1,0:T(8,128)S(1)} %add.13.refs_8_), channel_id=1, source_target_pairs={{0,2},{2,4},{4,6},{6,0},{1,3},{3,5},{5,7},{7,1},{8,10},{10,12},{12... | collective-permute-start | bytes 98312 | tf_op jit(solution)/shard_map/ppermute | solution.py:390
  143.7 24.6 %copy-start.3 = (bf16[1,128,3072]{2,1,0:T(8,128)(2,1)S(1)}, bf16[1,128,3072]{2,1,0:T(8,128)(2,1)}, u32[]{:S(2)}) copy-start(bf16[1,128,3072]{2,1,0:T(8,128)(2,1)} %upstream.3) | copy-start | bytes 2359300
  159.5 0.7 copy-start.12
  160.2 20.1 %all-to-all-start.2 = ((bf16[8,8,2304]{2,1,0:T(8,128)(2,1)}), bf16[8,8,2304]{2,1,0:T(8,128)(2,1)}, u32[]{:S(2)}, u32[]{:S(2)}) async-start(bf16[8,8,2304]{2,1,0:T(8,128)(2,1)} %copy-done.12), calls=%async_computation.2 | async-start | bytes 589824 | tf_op jit(solution)/shard_map/all_to_all | solution.py:318
  168.3 1.0 copy-start.5
  169.3 1.0 copy-start.7
  170.3 1.0 copy-start.9
  171.3 1.0 copy-start.11
  172.3 0.9 copy-start.14
  173.2 0.9 copy-start.16
  174.1 0.9 copy-start.18
  175.1 0.9 copy-start.20
  176.0 0.8 copy-start.22
where the time goes:
time: 185 us; the launch traced here: 183 us
  starting transfers between devices  96.7 us (52%)
  blocking collectives  33.5 us (18%)
  waiting for transfers between devices  19.8 us (11%)
  local copies, waits for them, and re-layouts  16.4 us (9%)
  Pallas kernels  15.5 us (8%)
    all_to_all x2, blocking collectives, exchanged(): return lax.all_to_all(x, axis, split_axis=0, concat_axis=0, tiled=True)  33.5 us
    ppermute x4, starting transfers between devices, compute(): far.append(lax.ppermute(vs[g], Y, FAR))  20.7 us
    ppermute x6, starting transfers between devices, compute(): lax.ppermute(sums[k], X, CHIPS[k])  19.6 us
    pallas_call x16, Pallas kernels, call(): pl.pallas_call(kernel, out_shape=out_shape, in_specs=[SMEM] * scalars + [...  15.5 us
    unnamed x52, local copies, waits for them, and re-layouts  13.9 us
    ppermute x4, waiting for transfers between devices, compute(): got.append(lax.ppermute(part, Y, OUT))  11.9 us
    ppermute x3, starting transfers between devices, compute(): lax.ppermute(own_rows, X, CHIPS[k])  10.2 us
    ppermute x3, starting transfers between devices, compute(): smalls = [small] + [lax.ppermute(small, X, CHIPS[k]) for k in range(1, 4)]  9.74 us
  transfers between devices with their start and end apart: 36, of which 8 were waited for; matrix products, arithmetic and copies ran while one was open for 1% of the time, Pallas kernels for 7%

commit v1 on v0

v1 whole, which is shorter than its diff:
```python
import functools

import jax
import jax.numpy as jnp
from jax import lax
from jax.experimental import pallas as pl
from jax.experimental.pallas import tpu as pltpu
from jax.sharding import Mesh
from jax.sharding import PartitionSpec as P


SEG = 64
ROWS = 128
GROUPS = 4
WIDTH = 768
HALF = GROUPS * WIDTH
QUAD = 4
DP = ("dp_0", "dp_1")
SP = ("sp_0", "sp_1")
Y = "sp_1"
Z = "sp_0"
X = "dp_0"
CORE = "dp_1"
EPS = 1e-05

NEAR = [(0, 1), (3, 2), (4, 5), (7, 6)]
FAR = [(0, 2), (3, 1), (4, 6), (7, 5)]
SWAP = [(1, 2), (2, 1), (5, 6), (6, 5)]
OUT = [(1, 0), (2, 3), (5, 4), (6, 7)]
PARTNER = [(0, 1), (1, 0)]

CHUNKS = (3, 1)
PLACES = [(i, k * WIDTH) for i, n in enumerate(CHUNKS) for k in range(n)]


VMEM = pl.BlockSpec(memory_space=pltpu.VMEM)
SMEM = pl.BlockSpec(memory_space=pltpu.SMEM)
F32 = jnp.float32
BF16 = jnp.bfloat16


def call(kernel, out_shape, inputs, scalars=1, scratch=(), vmem=16):
    return pl.pallas_call(
        kernel,
        out_shape=out_shape,
        in_specs=[SMEM] * scalars + [VMEM] * (len(inputs) - scalars),
        out_specs=jax.tree.map(lambda _: VMEM, out_shape),
        scratch_shapes=list(scratch),
        compiler_params=pltpu.CompilerParams(vmem_limit_bytes=vmem << 20),
    )(*inputs)


def shape(dims, dtype):
    return jax.ShapeDtypeStruct(dims, dtype)


def nt(a, b):
    return lax.dot_general(a, b, (((1,), (1,)), ((), ())), preferred_element_type=F32)


def tn(a, b):
    return lax.dot_general(a, b, (((0,), (0,)), ((), ())), preferred_element_type=F32)


def nn(a, b):
    return jnp.dot(a, b, preferred_element_type=F32)


def lanes_of(g, width=WIDTH):
    chunk, start = PLACES[g]
    start = start // WIDTH * width
    return chunk, slice(start, start + width)


def pre_kernel(place, values, gated, upstream, gain, shift, mix_bias, *outs):
    n = len(CHUNKS)
    us, vs, stats, bias = outs[:n], outs[n : 2 * n], outs[2 * n], outs[2 * n + 1]
    p = place[0]
    low = p < 2
    step = 16

    def block(i, carry):
        rows = pl.ds(pl.multiple_of(i * step, step), step)
        raw = values[0, rows, :].astype(F32)
        mean = jnp.sum(raw, axis=1, keepdims=True) * (1.0 / HALF)
        centred = raw - mean
        var = jnp.sum(centred * centred, axis=1, keepdims=True) * (1.0 / HALF)
        inv = lax.rsqrt(var + EPS)
        stats[0, rows, :] = jnp.broadcast_to(mean, (step, 128))
        stats[1, rows, :] = jnp.broadcast_to(inv, (step, 128))
        for g in range(GROUPS):
            cols = slice(g * WIDTH, (g + 1) * WIDTH)
            unit = (values[0, rows, cols].astype(F32) - mean) * inv
            normed = (unit * gain[:, cols] + shift[:, cols]).astype(BF16)
            grad = (upstream[0, rows, cols].astype(F32) * gated[0, rows, cols].astype(F32)).astype(BF16)
            i, lanes = lanes_of(g)
            us[i][rows, lanes] = jnp.where(low, grad, normed)
            vs[i][rows, lanes] = jnp.where(low, normed, grad)
        return carry

    lax.fori_loop(0, ROWS // step, block, 0)
    own_bias = mix_bias[:, pl.ds(pl.multiple_of(p * ROWS, ROWS), ROWS)]
    stats[2] = jnp.concatenate([own_bias, jnp.zeros((ROWS - GROUPS, ROWS), F32)], axis=0).T
    bias[...] = jnp.zeros_like(bias)
    ones = jnp.ones((8, WIDTH), BF16)
    for g in range(GROUPS):
        i, lanes = lanes_of(g)
        grad = jnp.where(low, us[i][:, lanes], vs[i][:, lanes])
        bias[pl.ds(g * QUAD + p, 1), :] = nt(ones, grad)[:1]


def weight_kernel(place, held, out):
    p = place[0]
    low = p < 2
    start = jnp.where(p == 3, 1, 0)
    r = lax.broadcasted_iota(jnp.int32, (ROWS, ROWS), 0) // SEG
    c = lax.broadcasted_iota(jnp.int32, (ROWS, ROWS), 1) // SEG

    def piece(t, g, s):
        cols = pl.ds(pl.multiple_of((s - start) * ROWS, ROWS), ROWS)
        return jnp.concatenate([held[2 * t, g, :, cols], held[2 * t + 1, g, :, cols]], axis=0)

    @pl.when(low)
    def _():
        for g in range(GROUPS):
            for i in range(2):
                for j in range(3):
                    got = piece(p + j, g, jnp.maximum(p - i, 0)).astype(F32)
                    if i == 0 and j == 0:
                        got = jnp.where(r >= c, got, 0.0)
                    out[g, i * ROWS : (i + 1) * ROWS, j * ROWS : (j + 1) * ROWS] = got.T.astype(BF16)

    @pl.when(jnp.logical_not(low))
    def _():
        for g in range(GROUPS):
            for i in range(2):
                for j in range(3):
                    got = piece(jnp.minimum(p + i, 3), g, p - j)
                    if i == 0 and j == 0:
                        got = jnp.where(r >= c, got.astype(F32), 0.0).astype(BF16)
                    out[g, i * ROWS : (i + 1) * ROWS, j * ROWS : (j + 1) * ROWS] = got


def product_kernel(chunk, u, v, near, far, swap, weights, part, out_u, out_v):
    for g in range(GROUPS):
        i, lanes = lanes_of(g)
        if i != chunk:
            continue
        own, other = weights[g, :ROWS, :], weights[g, ROWS:, :]
        long_side = jnp.concatenate([u[:, lanes], swap[:, lanes], far[:, lanes]], axis=0)
        part[:, lanes] = nn(other, long_side).astype(BF16)
        out_u[:, lanes] = nn(own, long_side)
        short_side = jnp.concatenate([v[:, lanes], near[:, lanes]], axis=0)
        both = jnp.concatenate([own[:, :ROWS], other[:, :ROWS]], axis=0)
        out_v[:, lanes] = tn(both, short_side)


def mix_grad_kernel(n, place, u, v, near, far, swap, keep, send):
    p, core = place[0], place[2]
    first = core == 0
    r = lax.broadcasted_iota(jnp.int32, (ROWS, ROWS), 0) // SEG
    c = lax.broadcasted_iota(jnp.int32, (ROWS, ROWS), 1) // SEG
    keep[...] = jnp.zeros_like(keep)
    send[...] = jnp.zeros_like(send)

    def put(target, slot, k, got):
        lanes = slice((slot * n + k) * ROWS, (slot * n + k + 1) * ROWS)
        keep[target, :, lanes] = jnp.where(first, got[:SEG], got[SEG:])
        send[target, :, lanes] = jnp.where(first, got[SEG:], got[:SEG]).astype(BF16)

    for k in range(n):
        at = slice(k * WIDTH, (k + 1) * WIDTH)

        @pl.when(p == 0)
        def _():
            put(0, 0, k, jnp.where(r >= c, nt(u[:, at], v[:, at]), 0.0))

        @pl.when(p == 1)
        def _():
            put(1, 0, k, nt(u[:, at], near[:, at]))
            put(1, 1, k, jnp.where(r >= c, nt(u[:, at], v[:, at]), 0.0))
            put(2, 0, k, nt(swap[:, at], near[:, at]))
            put(3, 0, k, nt(far[:, at], near[:, at]))

        @pl.when(p == 2)
        def _():
            put(2, 0, k, jnp.where(r >= c, nt(v[:, at], u[:, at]), 0.0))
            put(2, 1, k, nt(v[:, at], swap[:, at]))
            put(3, 0, k, nt(near[:, at], u[:, at]))
            put(3, 1, k, nt(near[:, at], swap[:, at]))

        @pl.when(p == 3)
        def _():
            put(3, 0, k, jnp.where(r >= c, nt(v[:, at], u[:, at]), 0.0))


def split(x):
    high = x.astype(BF16)
    return high, (x - high.astype(F32)).astype(BF16)


def sums_kernel(place, values, stats, bias, last, *refs):
    n = len(CHUNKS)
    outs_u, outs_v, got, small, send = refs[:n], refs[n : 2 * n], refs[2 * n : 3 * n], refs[3 * n], refs[3 * n + 1]
    low = place[0] < 2
    small[:16] = bias[...]
    mean = stats[0, :, :1]
    inv = stats[1, :, :1]
    for g in range(GROUPS):
        i, lanes = lanes_of(g)
        for k in range(WIDTH // 128):
            own = slice(lanes.start + k * 128, lanes.start + (k + 1) * 128)
            cols = slice(g * WIDTH + k * 128, g * WIDTH + (k + 1) * 128)
            back = jnp.where(low, outs_u[i][:, own] + got[i][:, own].astype(F32), outs_v[i][:, own])
            back = back.astype(BF16).astype(F32)
            unit = (values[0, :, cols].astype(F32) - mean) * inv
            row = 16 + g * 6 + k
            small[row : row + 1] = jnp.sum(back * unit, axis=0, keepdims=True)
            small[row + 24 : row + 25] = jnp.sum(back, axis=0, keepdims=True)
    send[:4] = last[...]
    high, low_part = split(small[...])
    send[4, :, :128] = high
    send[4, :, 128:] = low_part


def chip_kernel(keep0, keep1, small, got0, got1, out):
    extra = small[...] + (got1[4, :, :128].astype(F32) + got1[4, :, 128:].astype(F32))
    high, low = split(extra)
    for b in range(4):
        for i, (keep, got) in enumerate(((keep0, got0), (keep1, got1))):
            total = (keep[b] + got[b].astype(F32)).astype(BF16)
            width = CHUNKS[i] * ROWS
            lane = sum(CHUNKS[:i]) * ROWS
            for slot in range(2):
                out[b, :, slot * 512 + lane : slot * 512 + lane + width] = total[
                    :, slot * width : (slot + 1) * width
                ]
        out[b, :, 1024:1152] = high
        out[b, :, 1152:1280] = low


def total_of(got):
    total = got[0].astype(F32)
    for k in range(1, got.shape[0]):
        total = total + got[k].astype(F32)
    high, low = split(total[:, 1024:1152] + total[:, 1152:1280])
    return total[:, :1024].astype(BF16), high, low


def deal_kernel(got, out):
    total, high, low = total_of(got)
    for z in range(8):
        rows = slice(z * 8, (z + 1) * 8)
        out[z, :, :1024] = total[rows]
        out[z, :, 1024:1152] = high[rows]
        out[z, :, 1152:1280] = low[rows]


def add_kernel(got, out):
    total, high, low = total_of(got)
    for y in range(8):
        out[y, :, :1024] = total
        out[y, :, 1024:1152] = high
        out[y, :, 1152:1280] = low


def place_kernel(got, out):
    def at(place, slot):
        lanes = slice(slot * 512, (slot + 1) * 512)
        return got[place, :, lanes].astype(F32) + got[place + QUAD, :, lanes].astype(F32)

    columns = (at(0, 0) + at(1, 0), at(1, 1) + at(2, 1), at(2, 0), at(3, 0))
    columns = [c.astype(BF16) for c in columns]
    extra = jnp.zeros((8, 128), F32)
    for y in range(8):
        extra = extra + got[y, :, 1024:1152].astype(F32) + got[y, :, 1152:1280].astype(F32)
    high, low = split(extra)
    for z in range(8):
        for s in range(4):
            for g in range(GROUPS):
                out[z, :, g * 512 + s * ROWS : g * 512 + (s + 1) * ROWS] = columns[s][
                    :, g * ROWS : (g + 1) * ROWS
                ]
        out[z, :, 2048:2176] = high
        out[z, :, 2176:2304] = low


def final_kernel(got, grad_mix, grad_bias, grad_gain, grad_shift):
    for z in range(8):
        rows = slice(z * 8, (z + 1) * 8)
        for g in range(GROUPS):
            grad_mix[rows, g, :] = got[z, :, g * 512 : (g + 1) * 512].astype(F32)
        small = got[z, :, 2048:2176].astype(F32) + got[z, :, 2176:2304].astype(F32)
        if z < 2:
            for i in range(8):
                g, p = 2 * z + i // QUAD, i % QUAD
                grad_bias[g : g + 1, p * ROWS : (p + 1) * ROWS] = small[i : i + 1]
        elif z < 5:
            grad_gain[(z - 2) * 8 : (z - 1) * 8] = small
        else:
            grad_shift[(z - 5) * 8 : (z - 4) * 8] = small


def post_kernel(place, values, upstream, stats, gain, *refs):
    n = len(CHUNKS)
    outs_u, outs_v, got, grad_u, grad_v = refs[:n], refs[n : 2 * n], refs[2 * n : 3 * n], refs[3 * n], refs[3 * n + 1]
    low = place[0] < 2
    step = 16

    def block(i, carry):
        rows = pl.ds(pl.multiple_of(i * step, step), step)
        mean = stats[0, rows, :1]
        inv = stats[1, rows, :1]
        first = jnp.zeros((step, 1), F32)
        second = jnp.zeros((step, 1), F32)
        for g in range(GROUPS):
            cols = slice(g * WIDTH, (g + 1) * WIDTH)
            c, lanes = lanes_of(g)
            long_side = outs_u[c][rows, lanes] + got[c][rows, lanes].astype(F32)
            short_side = outs_v[c][rows, lanes]
            mixed = jnp.where(low, short_side, long_side) + stats[2, rows, g : g + 1]
            mixed = mixed.astype(BF16).astype(F32)
            grad_u[0, rows, cols] = (upstream[0, rows, cols].astype(F32) * mixed).astype(BF16)
            back = jnp.where(low, long_side, short_side).astype(BF16).astype(F32)
            scaled = back * gain[:, cols]
            unit = (values[0, rows, cols].astype(F32) - mean) * inv
            first = first + jnp.sum(scaled, axis=1, keepdims=True)
            second = second + jnp.sum(scaled * unit, axis=1, keepdims=True)
        first = first * (1.0 / HALF)
        second = second * (1.0 / HALF)
        for g in range(GROUPS):
            cols = slice(g * WIDTH, (g + 1) * WIDTH)
            c, lanes = lanes_of(g)
            long_side = outs_u[c][rows, lanes] + got[c][rows, lanes].astype(F32)
            back = jnp.where(low, long_side, outs_v[c][rows, lanes]).astype(BF16).astype(F32)
            scaled = back * gain[:, cols]
            unit = (values[0, rows, cols].astype(F32) - mean) * inv
            grad_v[0, rows, cols] = (inv * (scaled - first - unit * second)).astype(BF16)
        return carry

    lax.fori_loop(0, ROWS // step, block, 0)


def exchanged(x, axis):
    return lax.all_to_all(x, axis, split_axis=0, concat_axis=0, tiled=True)


def compute(gated, values_in, upstream, gain, shift, mix_w, mix_bias):
    spot = lax.axis_index(Y) % QUAD
    place = jnp.stack([spot, lax.axis_index(X), lax.axis_index(CORE)]).astype(jnp.int32)
    gain_row, shift_row = gain.reshape(1, HALF), shift.reshape(1, HALF)
    n = len(CHUNKS)
    halves = [shape((ROWS, k * WIDTH), BF16) for k in CHUNKS]
    fulls = [shape((ROWS, k * WIDTH), F32) for k in CHUNKS]

    pre = call(
        pre_kernel,
        halves * 2 + [shape((3, ROWS, 128), F32), shape((16, 128), F32)],
        (place, values_in, gated, upstream, gain_row, shift_row, mix_bias),
    )
    us, vs, stats, bias_term = pre[:n], pre[n : 2 * n], pre[2 * n], pre[2 * n + 1]

    near, far, swap = [], [], []
    for i in range(n):
        near.append(lax.ppermute(vs[i], Y, NEAR))
        far.append(lax.ppermute(vs[i], Y, FAR))
        swap.append(lax.ppermute(vs[i], Y, SWAP))

    first = jnp.where(spot == 3, ROWS, 0)
    own_rows = lax.dynamic_slice_in_dim(jnp.swapaxes(mix_w, 0, 1), first, 3 * ROWS, 2)
    all_rows = exchanged(jnp.broadcast_to(own_rows, (8, *own_rows.shape)), DP)
    weights = call(weight_kernel, shape((GROUPS, 2 * ROWS, 3 * ROWS), BF16), (place, all_rows))

    outs_u, outs_v, got, keeps, sends = [], [], [], [], []
    for i in range(n):
        operands = (us[i], vs[i], near[i], far[i], swap[i])
        part, out_u, out_v = call(
            functools.partial(product_kernel, i),
            [halves[i], fulls[i], fulls[i]],
            (*operands, weights),
            0,
        )
        got.append(lax.ppermute(part, Y, OUT))
        outs_u.append(out_u)
        outs_v.append(out_v)
        dims = (4, SEG, 2 * CHUNKS[i] * ROWS)
        keep, send = call(
            functools.partial(mix_grad_kernel, CHUNKS[i]),
            [shape(dims, F32), shape(dims, BF16)],
            (place, *operands),
        )
        keeps.append(keep)
        sends.append(send)

    small, last = call(
        sums_kernel,
        [shape((64, 128), F32), shape((5, SEG, 2 * ROWS), BF16)],
        (place, values_in, stats, bias_term, sends[1], *outs_u, *outs_v, *got),
    )
    folded = [lax.ppermute(sends[0], CORE, PARTNER), lax.ppermute(last, CORE, PARTNER)]
    chip = call(chip_kernel, shape((4, SEG, 1280), BF16), (*keeps, small, *folded), 0)
    dealt = call(deal_kernel, shape((8, 8, 1280), BF16), (exchanged(chip, X),), 0)
    added = call(add_kernel, shape((8, 8, 1280), BF16), (exchanged(dealt, Z),), 0)
    placed = call(place_kernel, shape((8, 8, 2304), BF16), (exchanged(added, Y),), 0)
    grad_mix, grad_bias, grad_gain, grad_shift = call(
        final_kernel,
        [shape((SEG, GROUPS, 512), F32), shape((GROUPS, 512), F32)] + [shape((24, 128), F32)] * 2,
        (exchanged(placed, Z),),
        0,
    )

    grad_u, grad_v = call(
        post_kernel,
        [shape((1, ROWS, HALF), BF16)] * 2,
        (place, values_in, upstream, stats, gain_row, *outs_u, *outs_v, *got),
    )
    return (grad_u, grad_v, grad_mix, grad_bias, grad_gain.reshape(HALF), grad_shift.reshape(HALF))


def solution(mesh):
    torus = Mesh(mesh.devices.reshape(8, 8, 4, 2), ("sp_0", "sp_1", "dp_0", "dp_1"))
    return jax.shard_map(
        compute,
        mesh=torus,
        in_specs=(
            P(DP, SP, None),
            P(DP, SP, None),
            P(DP, SP, None),
            P(),
            P(),
            P(DP, None, None),
            P(),
        ),
        out_specs=(P(DP, SP, None), P(DP, SP, None), P(DP, None, None), P(), P(), P()),
        check_vma=False,
    )
```

time: 185 us -> 149 us (0.81)
  the two profiles are of different devices: /device:TPU:64 before, /device:TPU:2 now
where the time goes in v1:
time: 149 us; the launch traced here: 147 us
  blocking collectives  49.6 us (33%)
  starting transfers between devices  32.5 us (22%)
  waiting for transfers between devices  32.2 us (22%)
  Pallas kernels  17 us (11%)
  local copies, waits for them, and re-layouts  15.1 us (10%)
    all_to_all x3, blocking collectives, exchanged(): return lax.all_to_all(x, axis, split_axis=0, concat_axis=0, tiled=True)  49.6 us
    pallas_call x13, Pallas kernels, call(): pl.pallas_call(kernel, out_shape=out_shape, in_specs=[SMEM] * scalars + [...  17 us
    unnamed x58, local copies, waits for them, and re-layouts  13.6 us
    all_to_all x2, starting transfers between devices, exchanged(): return lax.all_to_all(x, axis, split_axis=0, concat_axis=0, tiled=True)  13.6 us
    ppermute x2, waiting for transfers between devices, compute(): far.append(lax.ppermute(vs[i], Y, FAR))  12.1 us
    all_to_all x2, waiting for transfers between devices, exchanged(): return lax.all_to_all(x, axis, split_axis=0, concat_axis=0, tiled=True)  8.87 us
    ppermute x2, waiting for transfers between devices, compute(): got.append(lax.ppermute(part, Y, OUT))  7.97 us
    ppermute x2, starting transfers between devices, compute(): near.append(lax.ppermute(vs[i], Y, NEAR))  5.9 us
  transfers between devices with their start and end apart: 12, of which 7 were waited for; matrix products, arithmetic and copies ran while one was open for 0% of the time, Pallas kernels for 8%

profile of v1, /device:TPU:2, one launch (start us, length us, event | category | flops | bytes accessed | tf_op | source)
XLA Modules:
  0.0 147.5 jit_solution(12514692837534856726)
XLA Ops:
  0.6 0.0 copy-start
  0.7 0.9 copy-done
  1.6 0.1 dynamic-slice_bitcast_fusion
  1.7 1.4 broadcast_in_dim.3
  3.1 0.0 copy-start.28
  3.1 9.5 %all-to-all-start = ((bf16[8,4,64,384]{3,2,1,0:T(8,128)(2,1)}), bf16[8,4,64,384]{3,2,1,0:T(8,128)(2,1)S(1)}, u32[]{:S(2)}, u32[]{:S(2)}) async-start(bf16[8,4,64,384]{3,2,1,0:T(8,128)(2,1)} %broadcast_in_dim.3), calls=%async_computation | async-start | bytes 3145728 | tf_op jit(solution)/shard_map/all_to_all | solution.py:345
  12.7 0.1 pad_add_fusion.place
  12.7 0.0 copy-done.2
  12.8 0.0 copy-start.25
  12.8 1.1 copy-done.25
  13.9 3.5 %shard_map.118 = (bf16[128,2304]{1,0:T(8,128)(2,1)S(1)}, bf16[128,768]{1,0:T(8,128)(2,1)S(1)}, bf16[128,2304]{1,0:T(8,128)(2,1)}, bf16[128,768]{1,0:T(8,128)(2,1...) custom-call(s32[3]{0:T(128)S(1)} %pad_add_fusion.place, bf16[1,128,3072]{2,1,0:T(8,128)(2,1)S(1)} %copy-done.1, ...), custom_call_target="tpu_custom_call" | custom-call | tf_op jit(solution)/shard_map/pallas_call | solution.py:43
  17.4 0.8 copy-done.6
  18.3 0.7 copy-done.16
  18.9 0.7 copy-done.19
  19.6 0.7 copy-done.21
  20.3 1.3 collective-permute-start
  21.6 2.1 %collective-permute-start.1 = (bf16[128,2304]{1,0:T(8,128)(2,1)}, bf16[128,2304]{1,0:T(8,128)(2,1)}, u32[]{:S(2)}, u32[]{:S(2)}) collective-permute-start(bf16[128,2304]{1,0:T(8,128)(2,1)} %get-tuple-element.32.v), channel_id=1, source_target_pairs={{0,16},{24,8},{32,48},{56,40},{1,17},{25,9},{33,49},{57,41},{2,18}... | collective-permute-start | bytes 1769480 | tf_op jit(solution)/shard_map/ppermute | solution.py:366
  23.7 1.5 %collective-permute-start.2 = (bf16[128,2304]{1,0:T(8,128)(2,1)}, bf16[128,2304]{1,0:T(8,128)(2,1)}, u32[]{:S(2)}, u32[]{:S(2)}) collective-permute-start(bf16[128,2304]{1,0:T(8,128)(2,1)} %get-tuple-element.32.v), channel_id=1, source_target_pairs={{8,16},{16,8},{40,48},{48,40},{9,17},{17,9},{41,49},{49,41},{10,18... | collective-permute-start | bytes 1769480 | tf_op jit(solution)/shard_map/ppermute | solution.py:367
  25.2 7.6 %all-to-all-done.held = bf16[8,4,64,384]{3,2,1,0:T(8,128)(2,1)S(1)} async-done(((bf16[8,4,64,384]{3,2,1,0:T(8,128)(2,1)}), bf16[8,4,64,384]{3,2,1,0:T(8,128)(2,1)S(1)}, u32[]{:S(2)}, u32[]{:S(2)}) %all-to-all-start) | async-done | bytes 1572896 | tf_op jit(solution)/shard_map/all_to_all | solution.py:345
  32.8 0.8 shard_map.119.weights
  33.6 2.0 %collective-permute-done.near = bf16[128,2304]{1,0:T(8,128)(2,1)S(1)} collective-permute-done((bf16[128,2304]{1,0:T(8,128)(2,1)}, bf16[128,2304]{1,0:T(8,128)(2,1)S(1)}, u32[]{:S(2)}, u32[]{:S(2)}) %collective-permute-start) | collective-permute-done | bytes 589856 | tf_op jit(solution)/shard_map/ppermute | solution.py:365
  35.6 0.8 copy-done.8
  36.4 11.3 %collective-permute-done.1.far = bf16[128,2304]{1,0:T(8,128)(2,1)} collective-permute-done((bf16[128,2304]{1,0:T(8,128)(2,1)}, bf16[128,2304]{1,0:T(8,128)(2,1)}, u32[]{:S(2)}, u32[]{:S(2)}) %collective-permute-start.1) | collective-permute-done | bytes 589856 | tf_op jit(solution)/shard_map/ppermute | solution.py:366
  47.7 0.0 collective-permute-done.2.swap
  47.7 1.1 copy-done.9
  48.8 2.4 %shard_map.120 = (bf16[128,2304]{1,0:T(8,128)(2,1)S(1)}, f32[128,2304]{1,0:T(8,128)S(1)}, f32[128,2304]{1,0:T(8,128)S(1)}) custom-call(bf16[128,2304]{1,0:T(8,128)(2,1)S(1)} %copy-done.7, bf16[128,2304]{1,0:T(8,128)(2,1)} %get-tuple-element.32.v, bf16[128,2304]{1,0:T(8,128)(2,1)S(1)} %copy-done.9, bf16[128,2304]{1,0:T(8,128)(2,1)} %collective-permute-done.1.far, ...), custom_call_target="tpu_custom_call" | custom-call | tf_op jit(solution)/shard_map/pallas_call | solution.py:43
  51.2 0.0 copy-start.20
  51.2 1.4 collective-permute-start.6
  52.6 4.6 %collective-permute-start.3 = (bf16[128,768]{1,0:T(8,128)(2,1)S(1)}, bf16[128,768]{1,0:T(8,128)(2,1)S(1)}, u32[]{:S(2)}, u32[]{:S(2)}) collective-permute-start(bf16[128,768]{1,0:T(8,128)(2,1)S(1)} %copy-done.22), channel_id=1, source_target_pairs={{0,8},{24,16},{32,40},{56,48},{1,9},{25,17},{33,41},{57,49},{2,10}... | collective-permute-start | bytes 589832 | tf_op jit(solution)/shard_map/ppermute | solution.py:365
  57.2 2.1 %collective-permute-start.4 = (bf16[128,768]{1,0:T(8,128)(2,1)S(1)}, bf16[128,768]{1,0:T(8,128)(2,1)S(1)}, u32[]{:S(2)}, u32[]{:S(2)}) collective-permute-start(bf16[128,768]{1,0:T(8,128)(2,1)S(1)} %copy-done.22), channel_id=1, source_target_pairs={{0,16},{24,8},{32,48},{56,40},{1,17},{25,9},{33,49},{57,41},{2,18}... | collective-permute-start | bytes 589832 | tf_op jit(solution)/shard_map/ppermute | solution.py:366
  59.3 0.7 collective-permute-start.5
  60.0 2.1 %shard_map.123 = (f32[4,64,768]{2,1,0:T(8,128)S(1)}, bf16[4,64,768]{2,1,0:T(8,128)(2,1)S(1)}) custom-call(s32[3]{0:T(128)S(1)} %pad_add_fusion.place, bf16[128,2304]{1,0:T(8,128)(2,1)S(1)} %copy-done.7, bf16[128,2304]{1,0:T(8,128)(2,1)} %get-tuple-element.32.v, bf16[128,2304]{1,0:T(8,128)(2,1)S(1)} %copy-done.10, ...), custom_call_target="tpu_custom_call" | custom-call | tf_op jit(solution)/shard_map/pallas_call | solution.py:43
  62.2 2.1 %collective-permute-start.8 = (bf16[4,64,768]{2,1,0:T(8,128)(2,1)S(1)}, bf16[4,64,768]{2,1,0:T(8,128)(2,1)S(1)}, u32[]{:S(2)}, u32[]{:S(2)}) collective-permute-start(bf16[4,64,768]{2,1,0:T(8,128)(2,1)S(1)} %get-tuple-element.48), channel_id=1, source_target_pairs={{0,1},{1,0},{2,3},{3,2},{4,5},{5,4},{6,7},{7,6},{8,9},{9,8},{10,11... | collective-permute-start | bytes 1179656 | tf_op jit(solution)/shard_map/ppermute | solution.py:400
  64.2 0.0 collective-permute-done.3.near
  64.3 0.8 collective-permute-done.4.far
  65.1 0.0 collective-permute-done.5.swap
  65.1 0.4 shard_map.121
  65.5 0.0 copy-start.11
  65.5 0.0 copy-start.13
  65.5 1.3 collective-permute-start.7
  66.8 0.8 shard_map.124
  67.6 8.0 %collective-permute-done.7.refs_5_ = bf16[128,768]{1,0:T(8,128)(2,1)S(1)} collective-permute-done((bf16[128,768]{1,0:T(8,128)(2,1)S(1)}, bf16[128,768]{1,0:T(8,128)(2,1)S(1)}, u32[]{:S(2)}, u32[]{:S(2)}) %collective-permute-start.7) | collective-permute-done | bytes 196640 | tf_op jit(solution)/shard_map/ppermute | solution.py:383
  75.6 0.0 collective-permute-done.6.refs_4_
  75.6 1.2 shard_map.125
  76.8 1.9 %collective-permute-start.9 = (bf16[5,64,256]{2,1,0:T(8,128)(2,1)S(1)}, bf16[5,64,256]{2,1,0:T(8,128)(2,1)S(1)}, u32[]{:S(2)}, u32[]{:S(2)}) collective-permute-start(bf16[5,64,256]{2,1,0:T(8,128)(2,1)S(1)} %get-tuple-element.49), channel_id=1, source_target_pairs={{0,1},{1,0},{2,3},{3,2},{4,5},{5,4},{6,7},{7,6},{8,9},{9,8},{10,11... | collective-permute-start | bytes 491528 | tf_op jit(solution)/shard_map/ppermute | solution.py:400
  78.7 0.0 collective-permute-done.8.got0
  78.8 1.4 collective-permute-done.9.got1
  80.1 0.1 shard_map.126
  80.2 14.3 %all_to_all.25.got = bf16[4,64,1280]{2,1,0:T(8,128)(2,1)S(1)} all-to-all(bf16[4,64,1280]{2,1,0:T(8,128)(2,1)S(1)} %shard_map.126), channel_id=1, replica_groups=mesh['sp_0'=8,'sp_1'=8,'dp_0'=4,'dp_1'=2] {'dp_0'}, dimensions={0} | all-to-all | bytes 1310720 | tf_op jit(solution)/shard_map/all_to_all | solution.py:345
  94.5 0.1 shard_map.127
  94.6 19.4 %all_to_all.26.got = bf16[8,8,1280]{2,1,0:T(8,128)(2,1)S(1)} all-to-all(bf16[8,8,1280]{2,1,0:T(8,128)(2,1)S(1)} %shard_map.127), channel_id=1, replica_groups=mesh['sp_0'=8,'sp_1'=8,'dp_0'=4,'dp_1'=2] {'sp_0'}, dimensions={0} | all-to-all | bytes 327680 | tf_op jit(solution)/shard_map/all_to_all | solution.py:345
  114.1 15.9 %all_to_all.27.got = bf16[8,8,1280]{2,1,0:T(8,128)(2,1)S(1)} all-to-all(bf16[8,8,1280]{2,1,0:T(8,128)(2,1)S(1)} %shard_map.128), channel_id=1, replica_groups=mesh['sp_0'=8,'sp_1'=8,'dp_0'=4,'dp_1'=2] {'sp_1'}, dimensions={0} | all-to-all | bytes 327680 | tf_op jit(solution)/shard_map/all_to_all | solution.py:345
  130.0 0.7 copy-done.15
  130.7 4.1 %all-to-all-start.4 = ((bf16[8,8,2304]{2,1,0:T(8,128)(2,1)}), bf16[8,8,2304]{2,1,0:T(8,128)(2,1)}, u32[]{:S(2)}, u32[]{:S(2)}) async-start(bf16[8,8,2304]{2,1,0:T(8,128)(2,1)} %copy-done.15), calls=%async_computation.4 | async-start | bytes 589824 | tf_op jit(solution)/shard_map/all_to_all | solution.py:345
  134.8 0.0 copy-start.3
  134.8 1.1 copy-done.3
  135.9 1.1 copy-done.5
  137.0 1.0 copy-done.12
  138.0 1.0 copy-done.14
  139.0 0.9 copy-done.18
  139.9 0.9 copy-done.24
  140.8 3.5 %shard_map.122 = (bf16[1,128,3072]{2,1,0:T(8,128)(2,1)}, bf16[1,128,3072]{2,1,0:T(8,128)(2,1)}) custom-call(s32[3]{0:T(128)S(1)} %pad_add_fusion.place, bf16[1,128,3072]{2,1,0:T(8,128)(2,1)S(1)} %copy-done.1, bf16[1,128,3072]{2,1,0:T(8,128)(2,1)S(1)} %copy-done.3, f32[3,128,128]{2,1,0:T(8,128)S(1)} %copy-done.18, f32[1,3072]{1,0:T(1,128)S(1)} %bitcast.10, ...), custom_call_target="tpu_custom_call" | custom-call | tf_op jit(solution)/shard_map/pallas_call | solution.py:43
  144.3 1.3 all-to-all-done.4.got
  145.6 1.9 %shard_map.130 = (f32[64,4,512]{2,1,0:T(4,128)}, f32[4,512]{1,0:T(4,128)}, f32[24,128]{1,0:T(8,128)}, f32[24,128]{1,0:T(8,128)}) custom-call(bf16[8,8,2304]{2,1,0:T(8,128)(2,1)} %all-to-all-done.4.got), custom_call_target="tpu_custom_call" | custom-call | tf_op jit(solution)/shard_map/pallas_call | solution.py:43
  (38 shorter events, 0.2 us)
Async XLA Ops:
  0.6 1.0 copy-start
  3.1 9.6 %copy-start.1 = (bf16[1,128,3072]{2,1,0:T(8,128)(2,1)S(1)}, bf16[1,128,3072]{2,1,0:T(8,128)(2,1)}, u32[]{:S(2)}) copy-start(bf16[1,128,3072]{2,1,0:T(8,128)(2,1)} %values.5) | copy-start | bytes 2359300
  3.1 9.6 %copy-start.2 = (bf16[1,128,3072]{2,1,0:T(8,128)(2,1)S(1)}, bf16[1,128,3072]{2,1,0:T(8,128)(2,1)}, u32[]{:S(2)}) copy-start(bf16[1,128,3072]{2,1,0:T(8,128)(2,1)} %upstream.3) | copy-start | bytes 2359300
  3.1 9.6 %copy-start.26 = (f32[3072]{0:T(1024)S(1)}, f32[3072]{0:T(1024)}, u32[]{:S(2)}) copy-start(f32[3072]{0:T(1024)} %param.10) | copy-start | bytes 36868
  3.1 9.6 %copy-start.27 = (f32[3072]{0:T(1024)S(1)}, f32[3072]{0:T(1024)}, u32[]{:S(2)}) copy-start(f32[3072]{0:T(1024)} %param.11) | copy-start | bytes 36868
  3.1 9.6 %copy-start.28 = (f32[4,512]{1,0:T(4,128)S(1)}, f32[4,512]{1,0:T(4,128)}, u32[]{:S(2)}) copy-start(f32[4,512]{1,0:T(4,128)} %mix_bias.1) | copy-start | bytes 24580
  3.1 29.6 %all-to-all-start = ((bf16[8,4,64,384]{3,2,1,0:T(8,128)(2,1)}), bf16[8,4,64,384]{3,2,1,0:T(8,128)(2,1)S(1)}, u32[]{:S(2)}, u32[]{:S(2)}) async-start(bf16[8,4,64,384]{3,2,1,0:T(8,128)(2,1)} %broadcast_in_dim.3), calls=%async_computation | async-start | bytes 3145728 | tf_op jit(solution)/shard_map/all_to_all | solution.py:345
  12.8 1.1 copy-start.25
  17.4 0.8 copy-start.6
  18.3 0.7 copy-start.16
  18.9 0.7 copy-start.19
  19.6 0.7 copy-start.21
  20.3 15.3 %collective-permute-start = (bf16[128,2304]{1,0:T(8,128)(2,1)}, bf16[128,2304]{1,0:T(8,128)(2,1)S(1)}, u32[]{:S(2)}, u32[]{:S(2)}) collective-permute-start(bf16[128,2304]{1,0:T(8,128)(2,1)} %get-tuple-element.32.v), channel_id=1, source_target_pairs={{0,8},{24,16},{32,40},{56,48},{1,9},{25,17},{33,41},{57,49},{2,10}... | collective-permute-start | bytes 1769480 | tf_op jit(solution)/shard_map/ppermute | solution.py:365
  21.6 26.1 %collective-permute-start.1 = (bf16[128,2304]{1,0:T(8,128)(2,1)}, bf16[128,2304]{1,0:T(8,128)(2,1)}, u32[]{:S(2)}, u32[]{:S(2)}) collective-permute-start(bf16[128,2304]{1,0:T(8,128)(2,1)} %get-tuple-element.32.v), channel_id=1, source_target_pairs={{0,16},{24,8},{32,48},{56,40},{1,17},{25,9},{33,49},{57,41},{2,18}... | collective-permute-start | bytes 1769480 | tf_op jit(solution)/shard_map/ppermute | solution.py:366
  23.7 24.0 %collective-permute-start.2 = (bf16[128,2304]{1,0:T(8,128)(2,1)}, bf16[128,2304]{1,0:T(8,128)(2,1)}, u32[]{:S(2)}, u32[]{:S(2)}) collective-permute-start(bf16[128,2304]{1,0:T(8,128)(2,1)} %get-tuple-element.32.v), channel_id=1, source_target_pairs={{8,16},{16,8},{40,48},{48,40},{9,17},{17,9},{41,49},{49,41},{10,18... | collective-permute-start | bytes 1769480 | tf_op jit(solution)/shard_map/ppermute | solution.py:367
  32.8 14.9 %copy-start.7 = (bf16[128,2304]{1,0:T(8,128)(2,1)S(1)}, bf16[128,2304]{1,0:T(8,128)(2,1)}, u32[]{:S(2)}) copy-start(bf16[128,2304]{1,0:T(8,128)(2,1)} %copy-done.6) | copy-start | bytes 1769476
  35.6 0.8 copy-start.8
  47.7 1.1 copy-start.9
  48.8 3.9 %copy-start.22 = (bf16[128,768]{1,0:T(8,128)(2,1)S(1)}, bf16[128,768]{1,0:T(8,128)(2,1)}, u32[]{:S(2)}) copy-start(bf16[128,768]{1,0:T(8,128)(2,1)} %copy-done.21) | copy-start | bytes 589828
  48.8 11.3 %copy-start.10 = (bf16[128,2304]{1,0:T(8,128)(2,1)S(1)}, bf16[128,2304]{1,0:T(8,128)(2,1)}, u32[]{:S(2)}) copy-start(bf16[128,2304]{1,0:T(8,128)(2,1)} %copy-done.8) | copy-start | bytes 1769476
  51.2 13.9 %copy-start.20 = (bf16[128,768]{1,0:T(8,128)(2,1)S(1)}, bf16[128,768]{1,0:T(8,128)(2,1)}, u32[]{:S(2)}) copy-start(bf16[128,768]{1,0:T(8,128)(2,1)} %copy-done.19) | copy-start | bytes 589828
  51.2 24.4 %collective-permute-start.6 = (bf16[128,2304]{1,0:T(8,128)(2,1)S(1)}, bf16[128,2304]{1,0:T(8,128)(2,1)S(1)}, u32[]{:S(2)}, u32[]{:S(2)}) collective-permute-start(bf16[128,2304]{1,0:T(8,128)(2,1)S(1)} %get-tuple-element.39), channel_id=1, source_target_pairs={{8,0},{16,24},{40,32},{48,56},{9,1},{17,25},{41,33},{49,57},{10,2}... | collective-permute-start | bytes 1769480 | tf_op jit(solution)/shard_map/ppermute | solution.py:383
  52.6 11.6 %collective-permute-start.3 = (bf16[128,768]{1,0:T(8,128)(2,1)S(1)}, bf16[128,768]{1,0:T(8,128)(2,1)S(1)}, u32[]{:S(2)}, u32[]{:S(2)}) collective-permute-start(bf16[128,768]{1,0:T(8,128)(2,1)S(1)} %copy-done.22), channel_id=1, source_target_pairs={{0,8},{24,16},{32,40},{56,48},{1,9},{25,17},{33,41},{57,49},{2,10}... | collective-permute-start | bytes 589832 | tf_op jit(solution)/shard_map/ppermute | solution.py:365
  57.2 7.8 %collective-permute-start.4 = (bf16[128,768]{1,0:T(8,128)(2,1)S(1)}, bf16[128,768]{1,0:T(8,128)(2,1)S(1)}, u32[]{:S(2)}, u32[]{:S(2)}) collective-permute-start(bf16[128,768]{1,0:T(8,128)(2,1)S(1)} %copy-done.22), channel_id=1, source_target_pairs={{0,16},{24,8},{32,48},{56,40},{1,17},{25,9},{33,49},{57,41},{2,18}... | collective-permute-start | bytes 589832 | tf_op jit(solution)/shard_map/ppermute | solution.py:366
  59.3 5.7 %collective-permute-start.5 = (bf16[128,768]{1,0:T(8,128)(2,1)S(1)}, bf16[128,768]{1,0:T(8,128)(2,1)S(1)}, u32[]{:S(2)}, u32[]{:S(2)}) collective-permute-start(bf16[128,768]{1,0:T(8,128)(2,1)S(1)} %copy-done.22), channel_id=1, source_target_pairs={{8,16},{16,8},{40,48},{48,40},{9,17},{17,9},{41,49},{49,41},{10,18... | collective-permute-start | bytes 589832 | tf_op jit(solution)/shard_map/ppermute | solution.py:367
  62.2 13.4 %copy-start.17 = (f32[3,128,128]{2,1,0:T(8,128)S(1)}, f32[3,128,128]{2,1,0:T(8,128)}, u32[]{:S(2)}) copy-start(f32[3,128,128]{2,1,0:T(8,128)} %copy-done.16) | copy-start | bytes 589828
  62.2 16.6 %collective-permute-start.8 = (bf16[4,64,768]{2,1,0:T(8,128)(2,1)S(1)}, bf16[4,64,768]{2,1,0:T(8,128)(2,1)S(1)}, u32[]{:S(2)}, u32[]{:S(2)}) collective-permute-start(bf16[4,64,768]{2,1,0:T(8,128)(2,1)S(1)} %get-tuple-element.48), channel_id=1, source_target_pairs={{0,1},{1,0},{2,3},{3,2},{4,5},{5,4},{6,7},{7,6},{8,9},{9,8},{10,11... | collective-permute-start | bytes 1179656 | tf_op jit(solution)/shard_map/ppermute | solution.py:400
  65.5 11.3 %copy-start.11 = (f32[128,768]{1,0:T(8,128)}, f32[128,768]{1,0:T(8,128)S(1)}, u32[]{:S(2)}) copy-start(f32[128,768]{1,0:T(8,128)S(1)} %get-tuple-element.36.refs_1_) | copy-start | bytes 1179652
  65.5 11.3 %copy-start.13 = (f32[128,768]{1,0:T(8,128)}, f32[128,768]{1,0:T(8,128)S(1)}, u32[]{:S(2)}) copy-start(f32[128,768]{1,0:T(8,128)S(1)} %get-tuple-element.38.refs_3_) | copy-start | bytes 1179652
  65.5 10.1 %collective-permute-start.7 = (bf16[128,768]{1,0:T(8,128)(2,1)S(1)}, bf16[128,768]{1,0:T(8,128)(2,1)S(1)}, u32[]{:S(2)}, u32[]{:S(2)}) collective-permute-start(bf16[128,768]{1,0:T(8,128)(2,1)S(1)} %get-tuple-element.40), channel_id=1, source_target_pairs={{8,0},{16,24},{40,32},{48,56},{9,1},{17,25},{41,33},{49,57},{10,2}... | collective-permute-start | bytes 589832 | tf_op jit(solution)/shard_map/ppermute | solution.py:383
  75.6 1.2 copy-start.23
  75.6 1.2 copy-start.4
  76.8 3.3 %collective-permute-start.9 = (bf16[5,64,256]{2,1,0:T(8,128)(2,1)S(1)}, bf16[5,64,256]{2,1,0:T(8,128)(2,1)S(1)}, u32[]{:S(2)}, u32[]{:S(2)}) collective-permute-start(bf16[5,64,256]{2,1,0:T(8,128)(2,1)S(1)} %get-tuple-element.49), channel_id=1, source_target_pairs={{0,1},{1,0},{2,3},{3,2},{4,5},{5,4},{6,7},{7,6},{8,9},{9,8},{10,11... | collective-permute-start | bytes 491528 | tf_op jit(solution)/shard_map/ppermute | solution.py:400
  130.0 0.7 copy-start.15
  130.7 14.9 %all-to-all-start.4 = ((bf16[8,8,2304]{2,1,0:T(8,128)(2,1)}), bf16[8,8,2304]{2,1,0:T(8,128)(2,1)}, u32[]{:S(2)}, u32[]{:S(2)}) async-start(bf16[8,8,2304]{2,1,0:T(8,128)(2,1)} %copy-done.15), calls=%async_computation.4 | async-start | bytes 589824 | tf_op jit(solution)/shard_map/all_to_all | solution.py:345
  134.8 1.1 copy-start.3
  135.9 1.1 copy-start.5
  137.0 1.0 copy-start.12
  138.0 1.0 copy-start.14
  139.0 0.9 copy-start.18
  139.9 0.9 copy-start.24

commit v2 on v1

--- a/solution.py
+++ b/solution.py
@@ -28,6 +28,7 @@
 SWAP = [(1, 2), (2, 1), (5, 6), (6, 5)]
 OUT = [(1, 0), (2, 3), (5, 4), (6, 7)]
 PARTNER = [(0, 1), (1, 0)]
+CHIPS = [[(i, (i + k) % 4) for i in range(4)] for k in range(4)]
 
 CHUNKS = (3, 1)
 PLACES = [(i, k * WIDTH) for i, n in enumerate(CHUNKS) for k in range(n)]
@@ -35,15 +36,20 @@
 
 VMEM = pl.BlockSpec(memory_space=pltpu.VMEM)
 SMEM = pl.BlockSpec(memory_space=pltpu.SMEM)
+HBM = pl.BlockSpec(memory_space=pltpu.HBM)
 F32 = jnp.float32
 BF16 = jnp.bfloat16
 
 
-def call(kernel, out_shape, inputs, scalars=1, scratch=(), vmem=16):
+def far_memory(x):
+    return pltpu.with_memory_space_constraint(x, pltpu.HBM)
+
+
+def call(kernel, out_shape, inputs, scalars=1, scratch=(), vmem=16, remote=()):
     return pl.pallas_call(
         kernel,
         out_shape=out_shape,
-        in_specs=[SMEM] * scalars + [VMEM] * (len(inputs) - scalars),
+        in_specs=[SMEM] * scalars + [HBM if i in remote else VMEM for i in range(scalars, len(inputs))],
         out_specs=jax.tree.map(lambda _: VMEM, out_shape),
         scratch_shapes=list(scratch),
         compiler_params=pltpu.CompilerParams(vmem_limit_bytes=vmem << 20),
@@ -72,12 +78,34 @@
     return chunk, slice(start, start + width)
 
 
-def pre_kernel(place, values, gated, upstream, gain, shift, mix_bias, *outs):
+def pre_kernel(place, values_in, gated_in, upstream_in, gain_in, shift_in, bias_in, *outs):
     n = len(CHUNKS)
     us, vs, stats, bias = outs[:n], outs[n : 2 * n], outs[2 * n], outs[2 * n + 1]
+    values, gated, upstream, gain, shift, mix_bias, sems, few = outs[2 * n + 2 :]
     p = place[0]
     low = p < 2
     step = 16
+    part = ROWS // 4
+    pairs = ((values_in, values), (gated_in, gated), (upstream_in, upstream))
+
+    def copy(k, i):
+        rows = slice(i * part, (i + 1) * part)
+        return pltpu.make_async_copy(pairs[k][0].at[0, rows], pairs[k][1].at[0, rows], sems.at[k, i])
+
+    singles = [
+        pltpu.make_async_copy(source, target, few.at[k])
+        for k, (source, target) in enumerate(((gain_in, gain), (shift_in, shift), (bias_in, mix_bias)))
+    ]
+    copy(0, 0).start()
+    for single in singles:
+        single.start()
+    copy(1, 0).start()
+    copy(2, 0).start()
+    for i in range(1, 4):
+        for k in range(3):
+            copy(k, i).start()
+    for single in singles:
+        single.wait()
 
     def block(i, carry):
         rows = pl.ds(pl.multiple_of(i * step, step), step)
@@ -98,7 +126,10 @@
             vs[i][rows, lanes] = jnp.where(low, normed, grad)
         return carry
 
-    lax.fori_loop(0, ROWS // step, block, 0)
+    for i in range(4):
+        for k in range(3):
+            copy(k, i).wait()
+        lax.fori_loop(i * part // step, (i + 1) * part // step, block, 0)
     own_bias = mix_bias[:, pl.ds(pl.multiple_of(p * ROWS, ROWS), ROWS)]
     stats[2] = jnp.concatenate([own_bias, jnp.zeros((ROWS - GROUPS, ROWS), F32)], axis=0).T
     bias[...] = jnp.zeros_like(bias)
@@ -109,16 +140,37 @@
         bias[pl.ds(g * QUAD + p, 1), :] = nt(ones, grad)[:1]
 
 
-def weight_kernel(place, held, out):
+def slab_kernel(place, rows, out):
     p = place[0]
+
+    @pl.when(p < 3)
+    def _():
+        for g in range(GROUPS):
+            out[g] = rows[:, g, : 3 * ROWS]
+
+    @pl.when(p == 3)
+    def _():
+        for g in range(GROUPS):
+            out[g] = rows[:, g, ROWS:]
+
+
+def join_kernel(place, *refs):
+    for k in range(4):
+        refs[4][(place[1] + 4 - k) % 4] = refs[k][...]
+
+
+def weight_kernel(place, mine, theirs, out):
+    p, core = place[0], place[2]
     low = p < 2
+    first = core == 0
     start = jnp.where(p == 3, 1, 0)
     r = lax.broadcasted_iota(jnp.int32, (ROWS, ROWS), 0) // SEG
     c = lax.broadcasted_iota(jnp.int32, (ROWS, ROWS), 1) // SEG
 
     def piece(t, g, s):
         cols = pl.ds(pl.multiple_of((s - start) * ROWS, ROWS), ROWS)
-        return jnp.concatenate([held[2 * t, g, :, cols], held[2 * t + 1, g, :, cols]], axis=0)
+        ours, others = mine[t, g, :, cols], theirs[t, g, :, cols]
+        return jnp.concatenate([jnp.where(first, ours, others), jnp.where(first, others, ours)], axis=0)
 
     @pl.when(low)
     def _():
@@ -199,65 +251,78 @@
     return high, (x - high.astype(F32)).astype(BF16)
 
 
-def sums_kernel(place, values, stats, bias, last, *refs):
-    n = len(CHUNKS)
-    outs_u, outs_v, got, small, send = refs[:n], refs[n : 2 * n], refs[2 * n : 3 * n], refs[3 * n], refs[3 * n + 1]
+def sums_kernel(chunk, place, values, stats, before, out_u, out_v, got, small):
     low = place[0] < 2
-    small[:16] = bias[...]
+    small[...] = before[...]
     mean = stats[0, :, :1]
     inv = stats[1, :, :1]
     for g in range(GROUPS):
         i, lanes = lanes_of(g)
+        if i != chunk:
+            continue
         for k in range(WIDTH // 128):
             own = slice(lanes.start + k * 128, lanes.start + (k + 1) * 128)
             cols = slice(g * WIDTH + k * 128, g * WIDTH + (k + 1) * 128)
-            back = jnp.where(low, outs_u[i][:, own] + got[i][:, own].astype(F32), outs_v[i][:, own])
+            back = jnp.where(low, out_u[:, own] + got[:, own].astype(F32), out_v[:, own])
             back = back.astype(BF16).astype(F32)
             unit = (values[0, :, cols].astype(F32) - mean) * inv
             row = 16 + g * 6 + k
             small[row : row + 1] = jnp.sum(back * unit, axis=0, keepdims=True)
             small[row + 24 : row + 25] = jnp.sum(back, axis=0, keepdims=True)
+
+
+def last_sums_kernel(place, values, stats, before, out_u, out_v, got, last, small, send):
+    sums_kernel(1, place, values, stats, before, out_u, out_v, got, small)
     send[:4] = last[...]
-    high, low_part = split(small[...])
+    high, low = split(small[...])
     send[4, :, :128] = high
-    send[4, :, 128:] = low_part
-
-
-def chip_kernel(keep0, keep1, small, got0, got1, out):
-    extra = small[...] + (got1[4, :, :128].astype(F32) + got1[4, :, 128:].astype(F32))
+    send[4, :, 128:] = low
+
+
+def chip_kernel(place, keep, got, *outs):
+    for k in range(4):
+        b = (place[1] + k) % 4
+        outs[k][...] = (keep[b] + got[b].astype(F32)).astype(BF16)
+
+
+def last_chip_kernel(keep, small, got, out):
+    extra = small[...] + (got[4, :, :128].astype(F32) + got[4, :, 128:].astype(F32))
     high, low = split(extra)
     for b in range(4):
-        for i, (keep, got) in enumerate(((keep0, got0), (keep1, got1))):
-            total = (keep[b] + got[b].astype(F32)).astype(BF16)
-            width = CHUNKS[i] * ROWS
-            lane = sum(CHUNKS[:i]) * ROWS
-            for slot in range(2):
-                out[b, :, slot * 512 + lane : slot * 512 + lane + width] = total[
-                    :, slot * width : (slot + 1) * width
-                ]
-        out[b, :, 1024:1152] = high
-        out[b, :, 1152:1280] = low
-
-
-def total_of(got):
+        out[b, :, :256] = (keep[b] + got[b].astype(F32)).astype(BF16)
+        out[b, :, 256:384] = high
+        out[b, :, 384:512] = low
+
+
+def deal_kernel(own, one, two, three, got1, out):
+    got0 = (own, one, two, three)
+
+    def total_of(parts, lanes):
+        total = parts[0][:, lanes].astype(F32)
+        for k in range(1, 4):
+            total = total + parts[k][:, lanes].astype(F32)
+        return total
+
+    got1 = [got1.at[k] for k in range(4)]
+
+    def put(lane, block):
+        for z in range(8):
+            out[z, :, lane : lane + block.shape[1]] = block[z * 8 : (z + 1) * 8]
+
+    for slot in range(2):
+        put(slot * 512, total_of(got0, slice(slot * 384, (slot + 1) * 384)).astype(BF16))
+        put(slot * 512 + 384, total_of(got1, slice(slot * 128, (slot + 1) * 128)).astype(BF16))
+    high, low = split(total_of(got1, slice(256, 384)) + total_of(got1, slice(384, 512)))
+    put(1024, high)
+    put(1152, low)
+
+
+def add_kernel(got, out):
     total = got[0].astype(F32)
-    for k in range(1, got.shape[0]):
-        total = total + got[k].astype(F32)
+    for z in range(1, 8):
+        total = total + got[z].astype(F32)
     high, low = split(total[:, 1024:1152] + total[:, 1152:1280])
-    return total[:, :1024].astype(BF16), high, low
-
-
-def deal_kernel(got, out):
-    total, high, low = total_of(got)
-    for z in range(8):
-        rows = slice(z * 8, (z + 1) * 8)
-        out[z, :, :1024] = total[rows]
-        out[z, :, 1024:1152] = high[rows]
-        out[z, :, 1152:1280] = low[rows]
-
-
-def add_kernel(got, out):
-    total, high, low = total_of(got)
+    total = total[:, :1024].astype(BF16)
     for y in range(8):
         out[y, :, :1024] = total
         out[y, :, 1024:1152] = high
@@ -355,8 +420,12 @@
 
     pre = call(
         pre_kernel,
-        halves * 2 + [shape((3, ROWS, 128), F32), shape((16, 128), F32)],
-        (place, values_in, gated, upstream, gain_row, shift_row, mix_bias),
+        halves * 2 + [shape((3, ROWS, 128), F32), shape((64, 128), F32)],
+        (place, *map(far_memory, (values_in, gated, upstream, gain_row, shift_row, mix_bias))),
+        scratch=[pltpu.VMEM((1, ROWS, HALF), BF16)] * 3
+        + [pltpu.VMEM((1, HALF), F32)] * 2
+        + [pltpu.VMEM((GROUPS, 512), F32), pltpu.SemaphoreType.DMA((3, 4)), pltpu.SemaphoreType.DMA((3,))],
+        remote=range(1, 7),
     )
     us, vs, stats, bias_term = pre[:n], pre[n : 2 * n], pre[2 * n], pre[2 * n + 1]
 
@@ -366,10 +435,11 @@
         far.append(lax.ppermute(vs[i], Y, FAR))
         swap.append(lax.ppermute(vs[i], Y, SWAP))
 
-    first = jnp.where(spot == 3, ROWS, 0)
-    own_rows = lax.dynamic_slice_in_dim(jnp.swapaxes(mix_w, 0, 1), first, 3 * ROWS, 2)
-    all_rows = exchanged(jnp.broadcast_to(own_rows, (8, *own_rows.shape)), DP)
-    weights = call(weight_kernel, shape((GROUPS, 2 * ROWS, 3 * ROWS), BF16), (place, all_rows))
+    slab = call(slab_kernel, shape((GROUPS, SEG, 3 * ROWS), BF16), (place, mix_w))
+    slabs = [slab] + [lax.ppermute(slab, X, CHIPS[k]) for k in range(1, 4)]
+    mine = call(join_kernel, shape((4, GROUPS, SEG, 3 * ROWS), BF16), (place, *slabs))
+    theirs = lax.ppermute(mine, CORE, PARTNER)
+    weights = call(weight_kernel, shape((GROUPS, 2 * ROWS, 3 * ROWS), BF16), (place, mine, theirs))
 
     outs_u, outs_v, got, keeps, sends = [], [], [], [], []
     for i in range(n):
@@ -392,14 +462,26 @@
         keeps.append(keep)
         sends.append(send)
 
+    folded = lax.ppermute(sends[0], CORE, PARTNER)
+    chip = call(chip_kernel, [shape((SEG, 768), BF16)] * 4, (place, keeps[0], folded))
+    chip = [chip[0]] + [lax.ppermute(chip[k], X, CHIPS[k]) for k in range(1, 4)]
+    sums = call(
+        functools.partial(sums_kernel, 0),
+        shape((64, 128), F32),
+        (place, values_in, stats, bias_term, outs_u[0], outs_v[0], got[0]),
+    )
     small, last = call(
-        sums_kernel,
+        last_sums_kernel,
         [shape((64, 128), F32), shape((5, SEG, 2 * ROWS), BF16)],
-        (place, values_in, stats, bias_term, sends[1], *outs_u, *outs_v, *got),
-    )
-    folded = [lax.ppermute(sends[0], CORE, PARTNER), lax.ppermute(last, CORE, PARTNER)]
-    chip = call(chip_kernel, shape((4, SEG, 1280), BF16), (*keeps, small, *folded), 0)
-    dealt = call(deal_kernel, shape((8, 8, 1280), BF16), (exchanged(chip, X),), 0)
+        (place, values_in, stats, sums, outs_u[1], outs_v[1], got[1], sends[1]),
+    )
+    last = call(
+        last_chip_kernel,
+        shape((4, SEG, 512), BF16),
+        (keeps[1], small, lax.ppermute(last, CORE, PARTNER)),
+        0,
+    )
+    dealt = call(deal_kernel, shape((8, 8, 1280), BF16), (*chip, exchanged(last, X)), 0)
     added = call(add_kernel, shape((8, 8, 1280), BF16), (exchanged(dealt, Z),), 0)
     placed = call(place_kernel, shape((8, 8, 2304), BF16), (exchanged(added, Y),), 0)
     grad_mix, grad_bias, grad_gain, grad_shift = call(

time: 149 us -> 171 us (1.15)
  the two profiles are of different devices: /device:TPU:2 before, /device:TPU:6 now
where the time goes in v2:
time: 171 us; the launch traced here: 170 us
  starting transfers between devices  51.8 us (30%)
  waiting for transfers between devices  46.1 us (27%)
  blocking collectives  36.4 us (21%)
  Pallas kernels  20.4 us (12%)
  local copies, waits for them, and re-layouts  13.8 us (8%)
    all_to_all x2, blocking collectives, exchanged(): return lax.all_to_all(x, axis, split_axis=0, concat_axis=0, tiled=True)  36.4 us
    pallas_call x17, Pallas kernels, call(): pl.pallas_call(kernel, out_shape=out_shape, in_specs=[SMEM] * scalars + [...  20.4 us
    ppermute x2, waiting for transfers between devices, compute(): far.append(lax.ppermute(vs[i], Y, FAR))  15.4 us
    unnamed x44, local copies, waits for them, and re-layouts  13.8 us
    ppermute x3, starting transfers between devices, compute(): slabs = [slab] + [lax.ppermute(slab, X, CHIPS[k]) for k in range(1, 4)]  12.4 us
    ppermute x2, waiting for transfers between devices, compute(): near.append(lax.ppermute(vs[i], Y, NEAR))  12.4 us
    all_to_all x2, starting transfers between devices, exchanged(): return lax.all_to_all(x, axis, split_axis=0, concat_axis=0, tiled=True)  8.92 us
    ppermute x3, starting transfers between devices, compute(): chip = [chip[0]] + [lax.ppermute(chip[k], X, CHIPS[k]) for k in range(1, 4)]  8.73 us
  transfers between devices with their start and end apart: 19, of which 12 were waited for; matrix products, arithmetic and copies ran while one was open for 0% of the time, Pallas kernels for 9%

profile of v2, /device:TPU:6, one launch (start us, length us, event | category | flops | bytes accessed | tf_op | source)
XLA Modules:
  0.0 169.7 jit_solution(6275722685814278196)
XLA Ops:
  0.6 0.1 pad_add_fusion.place
  0.7 0.9 copy-done.12
  1.7 1.0 shard_map.119.refs_0_
  2.6 7.7 %collective-permute-start.3 = (bf16[4,64,384]{2,1,0:T(8,128)(2,1)S(1)}, bf16[4,64,384]{2,1,0:T(8,128)(2,1)S(1)}, u32[]{:S(2)}, u32[]{:S(2)}) collective-permute-start(bf16[4,64,384]{2,1,0:T(8,128)(2,1)S(1)} %shard_map.119.refs_0_), channel_id=1, source_target_pairs={{0,2},{2,4},{4,6},{6,0},{1,3},{3,5},{5,7},{7,1},{8,10},{10,12},{12... | collective-permute-start | bytes 589832 | tf_op jit(solution)/shard_map/ppermute | solution.py:439
  10.4 1.9 %collective-permute-start.4 = (bf16[4,64,384]{2,1,0:T(8,128)(2,1)S(1)}, bf16[4,64,384]{2,1,0:T(8,128)(2,1)S(1)}, u32[]{:S(2)}, u32[]{:S(2)}) collective-permute-start(bf16[4,64,384]{2,1,0:T(8,128)(2,1)S(1)} %shard_map.119.refs_0_), channel_id=1, source_target_pairs={{0,4},{2,6},{4,0},{6,2},{1,5},{3,7},{5,1},{7,3},{8,12},{10,14},{12... | collective-permute-start | bytes 589832 | tf_op jit(solution)/shard_map/ppermute | solution.py:439
  12.3 2.8 %collective-permute-start.5 = (bf16[4,64,384]{2,1,0:T(8,128)(2,1)S(1)}, bf16[4,64,384]{2,1,0:T(8,128)(2,1)S(1)}, u32[]{:S(2)}, u32[]{:S(2)}) collective-permute-start(bf16[4,64,384]{2,1,0:T(8,128)(2,1)S(1)} %shard_map.119.refs_0_), channel_id=1, source_target_pairs={{0,6},{2,0},{4,2},{6,4},{1,7},{3,1},{5,3},{7,5},{8,14},{10,8},{12,... | collective-permute-start | bytes 589832 | tf_op jit(solution)/shard_map/ppermute | solution.py:439
  15.1 1.4 collective-permute-done.3.refs_1_
  16.5 3.0 %collective-permute-done.4.refs_2_ = bf16[4,64,384]{2,1,0:T(8,128)(2,1)S(1)} collective-permute-done((bf16[4,64,384]{2,1,0:T(8,128)(2,1)S(1)}, bf16[4,64,384]{2,1,0:T(8,128)(2,1)S(1)}, u32[]{:S(2)}, u32[]{:S(2)}) %collective-permute-start.4) | collective-permute-done | bytes 196640 | tf_op jit(solution)/shard_map/ppermute | solution.py:439
  19.5 2.1 %collective-permute-done.5.refs_3_ = bf16[4,64,384]{2,1,0:T(8,128)(2,1)S(1)} collective-permute-done((bf16[4,64,384]{2,1,0:T(8,128)(2,1)S(1)}, bf16[4,64,384]{2,1,0:T(8,128)(2,1)S(1)}, u32[]{:S(2)}, u32[]{:S(2)}) %collective-permute-start.5) | collective-permute-done | bytes 196640 | tf_op jit(solution)/shard_map/ppermute | solution.py:439
  21.5 0.6 shard_map.120.mine
  22.2 1.9 %collective-permute-start.6 = (bf16[4,4,64,384]{3,2,1,0:T(8,128)(2,1)S(1)}, bf16[4,4,64,384]{3,2,1,0:T(8,128)(2,1)S(1)}, u32[]{:S(2)}, u32[]{:S(2)}) collective-permute-start(bf16[4,4,64,384]{3,2,1,0:T(8,128)(2,1)S(1)} %shard_map.120.mine), channel_id=1, source_target_pairs={{0,1},{1,0},{2,3},{3,2},{4,5},{5,4},{6,7},{7,6},{8,9},{9,8},{10,11... | collective-permute-start | bytes 2359304 | tf_op jit(solution)/shard_map/ppermute | solution.py:441
  24.1 4.5 %shard_map.118 = (bf16[128,2304]{1,0:T(8,128)(2,1)S(1)}, bf16[128,768]{1,0:T(8,128)(2,1)S(1)}, bf16[128,2304]{1,0:T(8,128)(2,1)S(1)}, bf16[128,768]{1,0:T(8,128)...) custom-call(s32[3]{0:T(128)S(1)} %pad_add_fusion.place, bf16[1,128,3072]{2,1,0:T(8,128)(2,1)} %values.5, ...), custom_call_target="tpu_custom_call" | custom-call | tf_op jit(solution)/shard_map/pallas_call | solution.py:49
  28.6 1.3 collective-permute-start
  29.9 1.9 %collective-permute-start.1 = (bf16[128,2304]{1,0:T(8,128)(2,1)S(1)}, bf16[128,2304]{1,0:T(8,128)(2,1)S(1)}, u32[]{:S(2)}, u32[]{:S(2)}) collective-permute-start(bf16[128,2304]{1,0:T(8,128)(2,1)S(1)} %get-tuple-element.36.v), channel_id=1, source_target_pairs={{0,16},{24,8},{32,48},{56,40},{1,17},{25,9},{33,49},{57,41},{2,18}... | collective-permute-start | bytes 1769480 | tf_op jit(solution)/shard_map/ppermute | solution.py:435
  31.9 0.7 collective-permute-start.2
  32.6 0.9 shard_map.121.weights
  33.5 10.1 %collective-permute-done.near = bf16[128,2304]{1,0:T(8,128)(2,1)S(1)} collective-permute-done((bf16[128,2304]{1,0:T(8,128)(2,1)S(1)}, bf16[128,2304]{1,0:T(8,128)(2,1)S(1)}, u32[]{:S(2)}, u32[]{:S(2)}) %collective-permute-start) | collective-permute-done | bytes 589856 | tf_op jit(solution)/shard_map/ppermute | solution.py:434
  43.6 12.5 %collective-permute-done.1.far = bf16[128,2304]{1,0:T(8,128)(2,1)S(1)} collective-permute-done((bf16[128,2304]{1,0:T(8,128)(2,1)S(1)}, bf16[128,2304]{1,0:T(8,128)(2,1)S(1)}, u32[]{:S(2)}, u32[]{:S(2)}) %collective-permute-start.1) | collective-permute-done | bytes 589856 | tf_op jit(solution)/shard_map/ppermute | solution.py:435
  56.1 0.9 shard_map.122
  57.0 1.3 collective-permute-start.10
  58.3 6.3 %collective-permute-start.7 = (bf16[128,768]{1,0:T(8,128)(2,1)S(1)}, bf16[128,768]{1,0:T(8,128)(2,1)S(1)}, u32[]{:S(2)}, u32[]{:S(2)}) collective-permute-start(bf16[128,768]{1,0:T(8,128)(2,1)S(1)} %get-tuple-element.39.v), channel_id=1, source_target_pairs={{0,8},{24,16},{32,40},{56,48},{1,9},{25,17},{33,41},{57,49},{2,10}... | collective-permute-start | bytes 589832 | tf_op jit(solution)/shard_map/ppermute | solution.py:434
  64.7 2.3 %collective-permute-start.8 = (bf16[128,768]{1,0:T(8,128)(2,1)S(1)}, bf16[128,768]{1,0:T(8,128)(2,1)S(1)}, u32[]{:S(2)}, u32[]{:S(2)}) collective-permute-start(bf16[128,768]{1,0:T(8,128)(2,1)S(1)} %get-tuple-element.39.v), channel_id=1, source_target_pairs={{0,16},{24,8},{32,48},{56,40},{1,17},{25,9},{33,49},{57,41},{2,18}... | collective-permute-start | bytes 589832 | tf_op jit(solution)/shard_map/ppermute | solution.py:435
  67.0 0.7 collective-permute-start.9
  67.7 2.3 %collective-permute-done.7.near = bf16[128,768]{1,0:T(8,128)(2,1)S(1)} collective-permute-done((bf16[128,768]{1,0:T(8,128)(2,1)S(1)}, bf16[128,768]{1,0:T(8,128)(2,1)S(1)}, u32[]{:S(2)}, u32[]{:S(2)}) %collective-permute-start.7) | collective-permute-done | bytes 196640 | tf_op jit(solution)/shard_map/ppermute | solution.py:434
  69.9 2.9 %collective-permute-done.8.far = bf16[128,768]{1,0:T(8,128)(2,1)S(1)} collective-permute-done((bf16[128,768]{1,0:T(8,128)(2,1)S(1)}, bf16[128,768]{1,0:T(8,128)(2,1)S(1)}, u32[]{:S(2)}, u32[]{:S(2)}) %collective-permute-start.8) | collective-permute-done | bytes 196640 | tf_op jit(solution)/shard_map/ppermute | solution.py:435
  72.9 0.4 shard_map.123
  73.3 1.3 collective-permute-start.11
  74.6 2.0 %shard_map.125 = (f32[4,64,768]{2,1,0:T(8,128)S(1)}, bf16[4,64,768]{2,1,0:T(8,128)(2,1)}) custom-call(s32[3]{0:T(128)S(1)} %pad_add_fusion.place, bf16[128,2304]{1,0:T(8,128)(2,1)S(1)} %get-tuple-element.35.u, bf16[128,2304]{1,0:T(8,128)(2,1)S(1)} %get-tuple-element.36.v, bf16[128,2304]{1,0:T(8,128)(2,1)S(1)} %collective-permute-done.near, ...), custom_call_target="tpu_custom_call" | custom-call | tf_op jit(solution)/shard_map/pallas_call | solution.py:49
  76.6 2.0 %collective-permute-start.12 = (bf16[4,64,768]{2,1,0:T(8,128)(2,1)}, bf16[4,64,768]{2,1,0:T(8,128)(2,1)}, u32[]{:S(2)}, u32[]{:S(2)}) collective-permute-start(bf16[4,64,768]{2,1,0:T(8,128)(2,1)} %get-tuple-element.48), channel_id=1, source_target_pairs={{0,1},{1,0},{2,3},{3,2},{4,5},{5,4},{6,7},{7,6},{8,9},{9,8},{10,11... | collective-permute-start | bytes 1179656 | tf_op jit(solution)/shard_map/ppermute | solution.py:465
  78.7 0.8 shard_map.127
  79.5 1.0 shard_map.128.before
  80.6 2.9 %collective-permute-done.11.refs_5_.got = bf16[128,768]{1,0:T(8,128)(2,1)S(1)} collective-permute-done((bf16[128,768]{1,0:T(8,128)(2,1)S(1)}, bf16[128,768]{1,0:T(8,128)(2,1)S(1)}, u32[]{:S(2)}, u32[]{:S(2)}) %collective-permute-start.11) | collective-permute-done | bytes 196640 | tf_op jit(solution)/shard_map/ppermute | solution.py:453
  83.5 0.7 shard_map.129
  84.2 1.9 %collective-permute-start.16 = (bf16[5,64,256]{2,1,0:T(8,128)(2,1)S(1)}, bf16[5,64,256]{2,1,0:T(8,128)(2,1)S(1)}, u32[]{:S(2)}, u32[]{:S(2)}) collective-permute-start(bf16[5,64,256]{2,1,0:T(8,128)(2,1)S(1)} %get-tuple-element.57), channel_id=1, source_target_pairs={{0,1},{1,0},{2,3},{3,2},{4,5},{5,4},{6,7},{7,6},{8,9},{9,8},{10,11... | collective-permute-start | bytes 491528 | tf_op jit(solution)/shard_map/ppermute | solution.py:481
  86.1 1.4 collective-permute-done.16.got
  87.6 0.7 copy-done.9
  88.2 4.9 %all-to-all-start = ((bf16[4,64,512]{2,1,0:T(8,128)(2,1)}), bf16[4,64,512]{2,1,0:T(8,128)(2,1)}, u32[]{:S(2)}, u32[]{:S(2)}) async-start(bf16[4,64,512]{2,1,0:T(8,128)(2,1)} %copy-done.9), calls=%async_computation | async-start | bytes 524288 | tf_op jit(solution)/shard_map/all_to_all | solution.py:410
  93.1 1.1 copy-done.11
  94.2 1.1 shard_map.126
  95.3 0.6 copy-done.13
  96.0 1.9 %collective-permute-start.13 = (bf16[64,768]{1,0:T(8,128)(2,1)S(1)}, bf16[64,768]{1,0:T(8,128)(2,1)S(1)}, u32[]{:S(2)}, u32[]{:S(2)}) collective-permute-start(bf16[64,768]{1,0:T(8,128)(2,1)S(1)} %get-tuple-element.50), channel_id=1, source_target_pairs={{0,2},{2,4},{4,6},{6,0},{1,3},{3,5},{5,7},{7,1},{8,10},{10,12},{12... | collective-permute-start | bytes 294920 | tf_op jit(solution)/shard_map/ppermute | solution.py:467
  97.9 4.8 %collective-permute-start.14 = (bf16[64,768]{1,0:T(8,128)(2,1)S(1)}, bf16[64,768]{1,0:T(8,128)(2,1)S(1)}, u32[]{:S(2)}, u32[]{:S(2)}) collective-permute-start(bf16[64,768]{1,0:T(8,128)(2,1)S(1)} %get-tuple-element.51), channel_id=1, source_target_pairs={{0,4},{2,6},{4,0},{6,2},{1,5},{3,7},{5,1},{7,3},{8,12},{10,14},{12... | collective-permute-start | bytes 294920 | tf_op jit(solution)/shard_map/ppermute | solution.py:467
  102.7 2.0 %collective-permute-start.15 = (bf16[64,768]{1,0:T(8,128)(2,1)S(1)}, bf16[64,768]{1,0:T(8,128)(2,1)S(1)}, u32[]{:S(2)}, u32[]{:S(2)}) collective-permute-start(bf16[64,768]{1,0:T(8,128)(2,1)S(1)} %get-tuple-element.52), channel_id=1, source_target_pairs={{0,6},{2,0},{4,2},{6,4},{1,7},{3,1},{5,3},{7,5},{8,14},{10,8},{12,... | collective-permute-start | bytes 294920 | tf_op jit(solution)/shard_map/ppermute | solution.py:467
  104.8 0.6 copy-done.15
  105.4 0.5 collective-permute-done.14.two
  105.9 0.6 copy-done.17
  106.5 3.9 %collective-permute-done.15.three = bf16[64,768]{1,0:T(8,128)(2,1)S(1)} collective-permute-done((bf16[64,768]{1,0:T(8,128)(2,1)S(1)}, bf16[64,768]{1,0:T(8,128)(2,1)S(1)}, u32[]{:S(2)}, u32[]{:S(2)}) %collective-permute-start.15) | collective-permute-done | bytes 98336 | tf_op jit(solution)/shard_map/ppermute | solution.py:467
  110.4 0.6 copy-done.19
  111.1 0.9 copy-done.14
  112.0 0.9 copy-done.16
  112.9 0.9 copy-done.18
  113.8 0.9 copy-done.20
  114.7 1.0 shard_map.131
  115.7 19.5 %all_to_all.20.got = bf16[8,8,1280]{2,1,0:T(8,128)(2,1)S(1)} all-to-all(bf16[8,8,1280]{2,1,0:T(8,128)(2,1)S(1)} %shard_map.131), channel_id=1, replica_groups=mesh['sp_0'=8,'sp_1'=8,'dp_0'=4,'dp_1'=2] {'sp_0'}, dimensions={0} | all-to-all | bytes 327680 | tf_op jit(solution)/shard_map/all_to_all | solution.py:410
  135.3 16.9 %all_to_all.21.got = bf16[8,8,1280]{2,1,0:T(8,128)(2,1)S(1)} all-to-all(bf16[8,8,1280]{2,1,0:T(8,128)(2,1)S(1)} %shard_map.132), channel_id=1, replica_groups=mesh['sp_0'=8,'sp_1'=8,'dp_0'=4,'dp_1'=2] {'sp_1'}, dimensions={0} | all-to-all | bytes 327680 | tf_op jit(solution)/shard_map/all_to_all | solution.py:410
  152.2 0.7 copy-done.8
  152.9 4.1 %all-to-all-start.3 = ((bf16[8,8,2304]{2,1,0:T(8,128)(2,1)}), bf16[8,8,2304]{2,1,0:T(8,128)(2,1)}, u32[]{:S(2)}, u32[]{:S(2)}) async-start(bf16[8,8,2304]{2,1,0:T(8,128)(2,1)} %copy-done.8), calls=%async_computation.3 | async-start | bytes 589824 | tf_op jit(solution)/shard_map/all_to_all | solution.py:410
  157.0 1.1 copy-done.1
  158.1 1.1 copy-done.3
  159.2 1.0 copy-done.5
  160.2 1.0 copy-done.7
  161.2 3.5 %shard_map.124 = (bf16[1,128,3072]{2,1,0:T(8,128)(2,1)}, bf16[1,128,3072]{2,1,0:T(8,128)(2,1)}) custom-call(s32[3]{0:T(128)S(1)} %pad_add_fusion.place, bf16[1,128,3072]{2,1,0:T(8,128)(2,1)S(1)} %copy-done, bf16[1,128,3072]{2,1,0:T(8,128)(2,1)S(1)} %copy-done.1, f32[3,128,128]{2,1,0:T(8,128)S(1)} %get-tuple-element.34.stats, f32[1,3072]{1,0:T(1,128)S(1)} %bitcast.8, ...), custom_call_target="tpu_custom_call" | custom-call | tf_op jit(solution)/shard_map/pallas_call | solution.py:49
  164.7 3.1 %all-to-all-done.3.got = bf16[8,8,2304]{2,1,0:T(8,128)(2,1)} async-done(((bf16[8,8,2304]{2,1,0:T(8,128)(2,1)}), bf16[8,8,2304]{2,1,0:T(8,128)(2,1)}, u32[]{:S(2)}, u32[]{:S(2)}) %all-to-all-start.3) | async-done | bytes 294944 | tf_op jit(solution)/shard_map/all_to_all | solution.py:410
  167.8 1.9 %shard_map.134 = (f32[64,4,512]{2,1,0:T(4,128)}, f32[4,512]{1,0:T(4,128)}, f32[24,128]{1,0:T(8,128)}, f32[24,128]{1,0:T(8,128)}) custom-call(bf16[8,8,2304]{2,1,0:T(8,128)(2,1)} %all-to-all-done.3.got), custom_call_target="tpu_custom_call" | custom-call | tf_op jit(solution)/shard_map/pallas_call | solution.py:49
  (38 shorter events, 0.2 us)
Async XLA Ops:
  0.7 1.0 copy-start.12
  2.6 13.9 %collective-permute-start.3 = (bf16[4,64,384]{2,1,0:T(8,128)(2,1)S(1)}, bf16[4,64,384]{2,1,0:T(8,128)(2,1)S(1)}, u32[]{:S(2)}, u32[]{:S(2)}) collective-permute-start(bf16[4,64,384]{2,1,0:T(8,128)(2,1)S(1)} %shard_map.119.refs_0_), channel_id=1, source_target_pairs={{0,2},{2,4},{4,6},{6,0},{1,3},{3,5},{5,7},{7,1},{8,10},{10,12},{12... | collective-permute-start | bytes 589832 | tf_op jit(solution)/shard_map/ppermute | solution.py:439
  10.4 9.1 %collective-permute-start.4 = (bf16[4,64,384]{2,1,0:T(8,128)(2,1)S(1)}, bf16[4,64,384]{2,1,0:T(8,128)(2,1)S(1)}, u32[]{:S(2)}, u32[]{:S(2)}) collective-permute-start(bf16[4,64,384]{2,1,0:T(8,128)(2,1)S(1)} %shard_map.119.refs_0_), channel_id=1, source_target_pairs={{0,4},{2,6},{4,0},{6,2},{1,5},{3,7},{5,1},{7,3},{8,12},{10,14},{12... | collective-permute-start | bytes 589832 | tf_op jit(solution)/shard_map/ppermute | solution.py:439
  12.3 9.2 %collective-permute-start.5 = (bf16[4,64,384]{2,1,0:T(8,128)(2,1)S(1)}, bf16[4,64,384]{2,1,0:T(8,128)(2,1)S(1)}, u32[]{:S(2)}, u32[]{:S(2)}) collective-permute-start(bf16[4,64,384]{2,1,0:T(8,128)(2,1)S(1)} %shard_map.119.refs_0_), channel_id=1, source_target_pairs={{0,6},{2,0},{4,2},{6,4},{1,7},{3,1},{5,3},{7,5},{8,14},{10,8},{12,... | collective-permute-start | bytes 589832 | tf_op jit(solution)/shard_map/ppermute | solution.py:439
  22.2 10.4 %collective-permute-start.6 = (bf16[4,4,64,384]{3,2,1,0:T(8,128)(2,1)S(1)}, bf16[4,4,64,384]{3,2,1,0:T(8,128)(2,1)S(1)}, u32[]{:S(2)}, u32[]{:S(2)}) collective-permute-start(bf16[4,4,64,384]{3,2,1,0:T(8,128)(2,1)S(1)} %shard_map.120.mine), channel_id=1, source_target_pairs={{0,1},{1,0},{2,3},{3,2},{4,5},{5,4},{6,7},{7,6},{8,9},{9,8},{10,11... | collective-permute-start | bytes 2359304 | tf_op jit(solution)/shard_map/ppermute | solution.py:441
  28.6 15.0 %collective-permute-start = (bf16[128,2304]{1,0:T(8,128)(2,1)S(1)}, bf16[128,2304]{1,0:T(8,128)(2,1)S(1)}, u32[]{:S(2)}, u32[]{:S(2)}) collective-permute-start(bf16[128,2304]{1,0:T(8,128)(2,1)S(1)} %get-tuple-element.36.v), channel_id=1, source_target_pairs={{0,8},{24,16},{32,40},{56,48},{1,9},{25,17},{33,41},{57,49},{2,10}... | collective-permute-start | bytes 1769480 | tf_op jit(solution)/shard_map/ppermute | solution.py:434
  29.9 26.2 %collective-permute-start.1 = (bf16[128,2304]{1,0:T(8,128)(2,1)S(1)}, bf16[128,2304]{1,0:T(8,128)(2,1)S(1)}, u32[]{:S(2)}, u32[]{:S(2)}) collective-permute-start(bf16[128,2304]{1,0:T(8,128)(2,1)S(1)} %get-tuple-element.36.v), channel_id=1, source_target_pairs={{0,16},{24,8},{32,48},{56,40},{1,17},{25,9},{33,49},{57,41},{2,18}... | collective-permute-start | bytes 1769480 | tf_op jit(solution)/shard_map/ppermute | solution.py:435
  31.9 24.2 %collective-permute-start.2 = (bf16[128,2304]{1,0:T(8,128)(2,1)S(1)}, bf16[128,2304]{1,0:T(8,128)(2,1)S(1)}, u32[]{:S(2)}, u32[]{:S(2)}) collective-permute-start(bf16[128,2304]{1,0:T(8,128)(2,1)S(1)} %get-tuple-element.36.v), channel_id=1, source_target_pairs={{8,16},{16,8},{40,48},{48,40},{9,17},{17,9},{41,49},{49,41},{10,18... | collective-permute-start | bytes 1769480 | tf_op jit(solution)/shard_map/ppermute | solution.py:436
  57.0 22.5 %collective-permute-start.10 = (bf16[128,2304]{1,0:T(8,128)(2,1)S(1)}, bf16[128,2304]{1,0:T(8,128)(2,1)S(1)}, u32[]{:S(2)}, u32[]{:S(2)}) collective-permute-start(bf16[128,2304]{1,0:T(8,128)(2,1)S(1)} %get-tuple-element.43), channel_id=1, source_target_pairs={{8,0},{16,24},{40,32},{48,56},{9,1},{17,25},{41,33},{49,57},{10,2}... | collective-permute-start | bytes 1769480 | tf_op jit(solution)/shard_map/ppermute | solution.py:453
  58.3 11.6 %collective-permute-start.7 = (bf16[128,768]{1,0:T(8,128)(2,1)S(1)}, bf16[128,768]{1,0:T(8,128)(2,1)S(1)}, u32[]{:S(2)}, u32[]{:S(2)}) collective-permute-start(bf16[128,768]{1,0:T(8,128)(2,1)S(1)} %get-tuple-element.39.v), channel_id=1, source_target_pairs={{0,8},{24,16},{32,40},{56,48},{1,9},{25,17},{33,41},{57,49},{2,10}... | collective-permute-start | bytes 589832 | tf_op jit(solution)/shard_map/ppermute | solution.py:434
  64.7 8.2 %collective-permute-start.8 = (bf16[128,768]{1,0:T(8,128)(2,1)S(1)}, bf16[128,768]{1,0:T(8,128)(2,1)S(1)}, u32[]{:S(2)}, u32[]{:S(2)}) collective-permute-start(bf16[128,768]{1,0:T(8,128)(2,1)S(1)} %get-tuple-element.39.v), channel_id=1, source_target_pairs={{0,16},{24,8},{32,48},{56,40},{1,17},{25,9},{33,49},{57,41},{2,18}... | collective-permute-start | bytes 589832 | tf_op jit(solution)/shard_map/ppermute | solution.py:435
  67.0 5.9 %collective-permute-start.9 = (bf16[128,768]{1,0:T(8,128)(2,1)S(1)}, bf16[128,768]{1,0:T(8,128)(2,1)S(1)}, u32[]{:S(2)}, u32[]{:S(2)}) collective-permute-start(bf16[128,768]{1,0:T(8,128)(2,1)S(1)} %get-tuple-element.39.v), channel_id=1, source_target_pairs={{8,16},{16,8},{40,48},{48,40},{9,17},{17,9},{41,49},{49,41},{10,18... | collective-permute-start | bytes 589832 | tf_op jit(solution)/shard_map/ppermute | solution.py:436
  73.3 10.2 %copy-start.4 = (f32[128,768]{1,0:T(8,128)}, f32[128,768]{1,0:T(8,128)S(1)}, u32[]{:S(2)}) copy-start(f32[128,768]{1,0:T(8,128)S(1)} %get-tuple-element.40.refs_1_.out_u) | copy-start | bytes 1179652
  73.3 10.2 %copy-start.6 = (f32[128,768]{1,0:T(8,128)}, f32[128,768]{1,0:T(8,128)S(1)}, u32[]{:S(2)}) copy-start(f32[128,768]{1,0:T(8,128)S(1)} %get-tuple-element.42.refs_3_.out_v) | copy-start | bytes 1179652
  73.3 10.2 %collective-permute-start.11 = (bf16[128,768]{1,0:T(8,128)(2,1)S(1)}, bf16[128,768]{1,0:T(8,128)(2,1)S(1)}, u32[]{:S(2)}, u32[]{:S(2)}) collective-permute-start(bf16[128,768]{1,0:T(8,128)(2,1)S(1)} %get-tuple-element.44), channel_id=1, source_target_pairs={{8,0},{16,24},{40,32},{48,56},{9,1},{17,25},{41,33},{49,57},{10,2}... | collective-permute-start | bytes 589832 | tf_op jit(solution)/shard_map/ppermute | solution.py:453
  76.6 3.9 %copy-start.10 = (f32[4,64,768]{2,1,0:T(8,128)}, f32[4,64,768]{2,1,0:T(8,128)S(1)}, u32[]{:S(2)}) copy-start(f32[4,64,768]{2,1,0:T(8,128)S(1)} %get-tuple-element.47.keep) | copy-start | bytes 2359300
  76.6 2.9 %copy-start = (bf16[1,128,3072]{2,1,0:T(8,128)(2,1)S(1)}, bf16[1,128,3072]{2,1,0:T(8,128)(2,1)}, u32[]{:S(2)}) copy-start(bf16[1,128,3072]{2,1,0:T(8,128)(2,1)} %values.5) | copy-start | bytes 2359300
  76.6 16.5 %collective-permute-start.12 = (bf16[4,64,768]{2,1,0:T(8,128)(2,1)}, bf16[4,64,768]{2,1,0:T(8,128)(2,1)}, u32[]{:S(2)}, u32[]{:S(2)}) collective-permute-start(bf16[4,64,768]{2,1,0:T(8,128)(2,1)} %get-tuple-element.48), channel_id=1, source_target_pairs={{0,1},{1,0},{2,3},{3,2},{4,5},{5,4},{6,7},{7,6},{8,9},{9,8},{10,11... | collective-permute-start | bytes 1179656 | tf_op jit(solution)/shard_map/ppermute | solution.py:465
  79.5 1.1 copy-start.2
  84.2 3.3 %collective-permute-start.16 = (bf16[5,64,256]{2,1,0:T(8,128)(2,1)S(1)}, bf16[5,64,256]{2,1,0:T(8,128)(2,1)S(1)}, u32[]{:S(2)}, u32[]{:S(2)}) collective-permute-start(bf16[5,64,256]{2,1,0:T(8,128)(2,1)S(1)} %get-tuple-element.57), channel_id=1, source_target_pairs={{0,1},{1,0},{2,3},{3,2},{4,5},{5,4},{6,7},{7,6},{8,9},{9,8},{10,11... | collective-permute-start | bytes 491528 | tf_op jit(solution)/shard_map/ppermute | solution.py:481
  87.5 0.7 copy-start.9
  88.2 22.8 %all-to-all-start = ((bf16[4,64,512]{2,1,0:T(8,128)(2,1)}), bf16[4,64,512]{2,1,0:T(8,128)(2,1)}, u32[]{:S(2)}, u32[]{:S(2)}) async-start(bf16[4,64,512]{2,1,0:T(8,128)(2,1)} %copy-done.9), calls=%async_computation | async-start | bytes 524288 | tf_op jit(solution)/shard_map/all_to_all | solution.py:410
  93.1 1.1 copy-start.11
  95.3 0.6 copy-start.13
  96.0 8.8 %collective-permute-start.13 = (bf16[64,768]{1,0:T(8,128)(2,1)S(1)}, bf16[64,768]{1,0:T(8,128)(2,1)S(1)}, u32[]{:S(2)}, u32[]{:S(2)}) collective-permute-start(bf16[64,768]{1,0:T(8,128)(2,1)S(1)} %get-tuple-element.50), channel_id=1, source_target_pairs={{0,2},{2,4},{4,6},{6,0},{1,3},{3,5},{5,7},{7,1},{8,10},{10,12},{12... | collective-permute-start | bytes 294920 | tf_op jit(solution)/shard_map/ppermute | solution.py:467
  97.9 8.0 %collective-permute-start.14 = (bf16[64,768]{1,0:T(8,128)(2,1)S(1)}, bf16[64,768]{1,0:T(8,128)(2,1)S(1)}, u32[]{:S(2)}, u32[]{:S(2)}) collective-permute-start(bf16[64,768]{1,0:T(8,128)(2,1)S(1)} %get-tuple-element.51), channel_id=1, source_target_pairs={{0,4},{2,6},{4,0},{6,2},{1,5},{3,7},{5,1},{7,3},{8,12},{10,14},{12... | collective-permute-start | bytes 294920 | tf_op jit(solution)/shard_map/ppermute | solution.py:467
  102.7 7.7 %collective-permute-start.15 = (bf16[64,768]{1,0:T(8,128)(2,1)S(1)}, bf16[64,768]{1,0:T(8,128)(2,1)S(1)}, u32[]{:S(2)}, u32[]{:S(2)}) collective-permute-start(bf16[64,768]{1,0:T(8,128)(2,1)S(1)} %get-tuple-element.52), channel_id=1, source_target_pairs={{0,6},{2,0},{4,2},{6,4},{1,7},{3,1},{5,3},{7,5},{8,14},{10,8},{12,... | collective-permute-start | bytes 294920 | tf_op jit(solution)/shard_map/ppermute | solution.py:467
  104.7 0.6 copy-start.15
  105.9 0.6 copy-start.17
  110.4 0.6 copy-start.19
  111.1 0.9 copy-start.14
  112.0 0.9 copy-start.16
  112.9 0.9 copy-start.18
  113.8 0.9 copy-start.20
  115.7 41.3 %copy-start.21 = (f32[3072]{0:T(1024)S(1)}, f32[3072]{0:T(1024)}, u32[]{:S(2)}) copy-start(f32[3072]{0:T(1024)} %param.10) | copy-start | bytes 36868
  152.2 0.7 copy-start.8
  152.9 14.9 %all-to-all-start.3 = ((bf16[8,8,2304]{2,1,0:T(8,128)(2,1)}), bf16[8,8,2304]{2,1,0:T(8,128)(2,1)}, u32[]{:S(2)}, u32[]{:S(2)}) async-start(bf16[8,8,2304]{2,1,0:T(8,128)(2,1)} %copy-done.8), calls=%async_computation.3 | async-start | bytes 589824 | tf_op jit(solution)/shard_map/all_to_all | solution.py:410
  157.0 1.1 copy-start.1
  158.1 1.1 copy-start.3
  159.2 1.0 copy-start.5
  160.2 1.0 copy-start.7

commit v3 on v2

--- a/solution.py
+++ b/solution.py
@@ -28,7 +28,8 @@
 SWAP = [(1, 2), (2, 1), (5, 6), (6, 5)]
 OUT = [(1, 0), (2, 3), (5, 4), (6, 7)]
 PARTNER = [(0, 1), (1, 0)]
-CHIPS = [[(i, (i + k) % 4) for i in range(4)] for k in range(4)]
+ACROSS = [(0, 3), (3, 0), (1, 2), (2, 1)]
+WITHIN = [(0, 1), (1, 0), (2, 3), (3, 2)]
 
 CHUNKS = (3, 1)
 PLACES = [(i, k * WIDTH) for i, n in enumerate(CHUNKS) for k in range(n)]
@@ -78,12 +79,11 @@
     return chunk, slice(start, start + width)
 
 
-def pre_kernel(place, values_in, gated_in, upstream_in, gain_in, shift_in, bias_in, *outs):
+def pre_kernel(place, values_in, gated_in, upstream_in, gain_in, shift_in, *outs):
     n = len(CHUNKS)
-    us, vs, stats, bias = outs[:n], outs[n : 2 * n], outs[2 * n], outs[2 * n + 1]
-    values, gated, upstream, gain, shift, mix_bias, sems, few = outs[2 * n + 2 :]
-    p = place[0]
-    low = p < 2
+    us, vs, stats = outs[:n], outs[n : 2 * n], outs[2 * n]
+    values, gated, upstream, gain, shift, sems, few = outs[2 * n + 1 :]
+    low = place[0] < 2
     step = 16
     part = ROWS // 4
     pairs = ((values_in, values), (gated_in, gated), (upstream_in, upstream))
@@ -94,7 +94,7 @@
 
     singles = [
         pltpu.make_async_copy(source, target, few.at[k])
-        for k, (source, target) in enumerate(((gain_in, gain), (shift_in, shift), (bias_in, mix_bias)))
+        for k, (source, target) in enumerate(((gain_in, gain), (shift_in, shift)))
     ]
     copy(0, 0).start()
     for single in singles:
@@ -129,11 +129,17 @@
     for i in range(4):
         for k in range(3):
             copy(k, i).wait()
-        lax.fori_loop(i * part // step, (i + 1) * part // step, block, 0)
+        lax.fori_loop(i * part // step, (i + 1) * part // step, block, 0, unroll=True)
+
+
+def side_kernel(place, u, v, u1, v1, mix_bias, columns, bias):
+    p = place[0]
+    low = p < 2
     own_bias = mix_bias[:, pl.ds(pl.multiple_of(p * ROWS, ROWS), ROWS)]
-    stats[2] = jnp.concatenate([own_bias, jnp.zeros((ROWS - GROUPS, ROWS), F32)], axis=0).T
+    columns[...] = jnp.concatenate([own_bias, jnp.zeros((ROWS - GROUPS, ROWS), F32)], axis=0).T
     bias[...] = jnp.zeros_like(bias)
     ones = jnp.ones((8, WIDTH), BF16)
+    us, vs = (u, u1), (v, v1)
     for g in range(GROUPS):
         i, lanes = lanes_of(g)
         grad = jnp.where(low, us[i][:, lanes], vs[i][:, lanes])
@@ -143,20 +149,19 @@
 def slab_kernel(place, rows, out):
     p = place[0]
 
+    def fill(start):
+        for g in range(GROUPS):
+            got = rows[:, g, start : start + 3 * ROWS]
+            for x in range(4):
+                out[x, g] = got
+
     @pl.when(p < 3)
     def _():
-        for g in range(GROUPS):
-            out[g] = rows[:, g, : 3 * ROWS]
+        fill(0)
 
     @pl.when(p == 3)
     def _():
-        for g in range(GROUPS):
-            out[g] = rows[:, g, ROWS:]
-
-
-def join_kernel(place, *refs):
-    for k in range(4):
-        refs[4][(place[1] + 4 - k) % 4] = refs[k][...]
+        fill(ROWS)
 
 
 def weight_kernel(place, mine, theirs, out):
@@ -279,10 +284,18 @@
     send[4, :, 128:] = low
 
 
-def chip_kernel(place, keep, got, *outs):
-    for k in range(4):
-        b = (place[1] + k) % 4
-        outs[k][...] = (keep[b] + got[b].astype(F32)).astype(BF16)
+def chip_kernel(place, keep, got, own, send):
+    near = place[1] // 2 * 2
+    for k in range(2):
+        own[k] = keep[near + k] + got[near + k].astype(F32)
+        other = 2 - near + k
+        send[k] = (keep[other] + got[other].astype(F32)).astype(BF16)
+
+
+def chip_pair_kernel(place, keep, got, own, send):
+    b = place[1] % 2
+    own[...] = keep[b] + got[b].astype(F32)
+    send[...] = (keep[1 - b] + got[1 - b].astype(F32)).astype(BF16)
 
 
 def last_chip_kernel(keep, small, got, out):
@@ -294,15 +307,14 @@
         out[b, :, 384:512] = low
 
 
-def deal_kernel(own, one, two, three, got1, out):
-    got0 = (own, one, two, three)
-
+def deal_kernel(own, other, got1, out):
     def total_of(parts, lanes):
         total = parts[0][:, lanes].astype(F32)
-        for k in range(1, 4):
-            total = total + parts[k][:, lanes].astype(F32)
+        for part in parts[1:]:
+            total = total + part[:, lanes].astype(F32)
         return total
 
+    got0 = (own, other)
     got1 = [got1.at[k] for k in range(4)]
 
     def put(lane, block):
@@ -366,7 +378,7 @@
             grad_shift[(z - 5) * 8 : (z - 4) * 8] = small
 
 
-def post_kernel(place, values, upstream, stats, gain, *refs):
+def post_kernel(place, values, upstream, stats, columns, gain, *refs):
     n = len(CHUNKS)
     outs_u, outs_v, got, grad_u, grad_v = refs[:n], refs[n : 2 * n], refs[2 * n : 3 * n], refs[3 * n], refs[3 * n + 1]
     low = place[0] < 2
@@ -383,7 +395,7 @@
             c, lanes = lanes_of(g)
             long_side = outs_u[c][rows, lanes] + got[c][rows, lanes].astype(F32)
             short_side = outs_v[c][rows, lanes]
-            mixed = jnp.where(low, short_side, long_side) + stats[2, rows, g : g + 1]
+            mixed = jnp.where(low, short_side, long_side) + columns[rows, g : g + 1]
             mixed = mixed.astype(BF16).astype(F32)
             grad_u[0, rows, cols] = (upstream[0, rows, cols].astype(F32) * mixed).astype(BF16)
             back = jnp.where(low, long_side, short_side).astype(BF16).astype(F32)
@@ -403,7 +415,7 @@
             grad_v[0, rows, cols] = (inv * (scaled - first - unit * second)).astype(BF16)
         return carry
 
-    lax.fori_loop(0, ROWS // step, block, 0)
+    lax.fori_loop(0, ROWS // step, block, 0, unroll=2)
 
 
 def exchanged(x, axis):
@@ -420,14 +432,14 @@
 
     pre = call(
         pre_kernel,
-        halves * 2 + [shape((3, ROWS, 128), F32), shape((64, 128), F32)],
-        (place, *map(far_memory, (values_in, gated, upstream, gain_row, shift_row, mix_bias))),
+        halves * 2 + [shape((2, ROWS, 128), F32)],
+        (place, *map(far_memory, (values_in, gated, upstream, gain_row, shift_row))),
         scratch=[pltpu.VMEM((1, ROWS, HALF), BF16)] * 3
         + [pltpu.VMEM((1, HALF), F32)] * 2
-        + [pltpu.VMEM((GROUPS, 512), F32), pltpu.SemaphoreType.DMA((3, 4)), pltpu.SemaphoreType.DMA((3,))],
-        remote=range(1, 7),
-    )
-    us, vs, stats, bias_term = pre[:n], pre[n : 2 * n], pre[2 * n], pre[2 * n + 1]
+        + [pltpu.SemaphoreType.DMA((3, 4)), pltpu.SemaphoreType.DMA((2,))],
+        remote=range(1, 6),
+    )
+    us, vs, stats = pre[:n], pre[n : 2 * n], pre[2 * n]
 
     near, far, swap = [], [], []
     for i in range(n):
@@ -435,10 +447,14 @@
         far.append(lax.ppermute(vs[i], Y, FAR))
         swap.append(lax.ppermute(vs[i], Y, SWAP))
 
-    slab = call(slab_kernel, shape((GROUPS, SEG, 3 * ROWS), BF16), (place, mix_w))
-    slabs = [slab] + [lax.ppermute(slab, X, CHIPS[k]) for k in range(1, 4)]
-    mine = call(join_kernel, shape((4, GROUPS, SEG, 3 * ROWS), BF16), (place, *slabs))
+    slab = call(slab_kernel, shape((4, GROUPS, SEG, 3 * ROWS), BF16), (place, mix_w))
+    mine = exchanged(slab, X)
     theirs = lax.ppermute(mine, CORE, PARTNER)
+    columns, bias_term = call(
+        side_kernel,
+        [shape((ROWS, ROWS), F32), shape((64, 128), F32)],
+        (place, us[0], vs[0], us[1], vs[1], mix_bias),
+    )
     weights = call(weight_kernel, shape((GROUPS, 2 * ROWS, 3 * ROWS), BF16), (place, mine, theirs))
 
     outs_u, outs_v, got, keeps, sends = [], [], [], [], []
@@ -463,8 +479,17 @@
         sends.append(send)
 
     folded = lax.ppermute(sends[0], CORE, PARTNER)
-    chip = call(chip_kernel, [shape((SEG, 768), BF16)] * 4, (place, keeps[0], folded))
-    chip = [chip[0]] + [lax.ppermute(chip[k], X, CHIPS[k]) for k in range(1, 4)]
+    keep, send = call(
+        chip_kernel,
+        [shape((2, SEG, 768), F32), shape((2, SEG, 768), BF16)],
+        (place, keeps[0], folded),
+    )
+    own, send = call(
+        chip_pair_kernel,
+        [shape((SEG, 768), F32), shape((SEG, 768), BF16)],
+        (place, keep, lax.ppermute(send, X, ACROSS)),
+    )
+    chip = (own, lax.ppermute(send, X, WITHIN))
     sums = call(
         functools.partial(sums_kernel, 0),
         shape((64, 128), F32),
@@ -494,7 +519,7 @@
     grad_u, grad_v = call(
         post_kernel,
         [shape((1, ROWS, HALF), BF16)] * 2,
-        (place, values_in, upstream, stats, gain_row, *outs_u, *outs_v, *got),
+        (place, values_in, upstream, stats, columns, gain_row, *outs_u, *outs_v, *got),
     )
     return (grad_u, grad_v, grad_mix, grad_bias, grad_gain.reshape(HALF), grad_shift.reshape(HALF))
 

time: 171 us -> 163 us (0.953)
  the two profiles are of different devices: /device:TPU:6 before, /device:TPU:8 now
where the time goes in v3:
time: 163 us; the launch traced here: 162 us
  blocking collectives  52.8 us (32%)
  waiting for transfers between devices  40.4 us (25%)
  starting transfers between devices  33.7 us (21%)
  Pallas kernels  20.7 us (13%)
  local copies, waits for them, and re-layouts  13.1 us (8%)
    all_to_all x3, blocking collectives, exchanged(): return lax.all_to_all(x, axis, split_axis=0, concat_axis=0, tiled=True)  52.8 us
    pallas_call x18, Pallas kernels, call(): pl.pallas_call(kernel, out_shape=out_shape, in_specs=[SMEM] * scalars + [...  20.7 us
    ppermute x2, waiting for transfers between devices, compute(): far.append(lax.ppermute(vs[i], Y, FAR))  17.1 us
    unnamed x46, local copies, waits for them, and re-layouts  13.1 us
    ppermute x2, waiting for transfers between devices, compute(): near.append(lax.ppermute(vs[i], Y, NEAR))  11.1 us
    all_to_all x2, starting transfers between devices, exchanged(): return lax.all_to_all(x, axis, split_axis=0, concat_axis=0, tiled=True)  8.12 us
    ppermute x2, starting transfers between devices, compute(): swap.append(lax.ppermute(vs[i], Y, SWAP))  6.97 us
    ppermute x1, waiting for transfers between devices, compute(): chip = (own, lax.ppermute(send, X, WITHIN))  4.58 us
  transfers between devices with their start and end apart: 15, of which 9 were waited for; matrix products, arithmetic and copies ran while one was open for 0% of the time, Pallas kernels for 10%

profile of v3, /device:TPU:8, one launch (start us, length us, event | category | flops | bytes accessed | tf_op | source)
XLA Modules:
  0.0 162.0 jit_solution(17377375047128629740)
XLA Ops:
  0.6 0.1 pad_add_fusion.place
  0.7 0.9 copy-done.14
  1.7 1.0 shard_map.120
  2.6 16.4 %all_to_all.25.mine = bf16[4,4,64,384]{3,2,1,0:T(8,128)(2,1)S(1)} all-to-all(bf16[4,4,64,384]{3,2,1,0:T(8,128)(2,1)S(1)} %shard_map.120), channel_id=1, replica_groups=mesh['sp_0'=8,'sp_1'=8,'dp_0'=4,'dp_1'=2] {'dp_0'}, dimensions={0} | all-to-all | bytes 1572864 | tf_op jit(solution)/shard_map/all_to_all | solution.py:422
  19.0 1.9 %collective-permute-start.3 = (bf16[4,4,64,384]{3,2,1,0:T(8,128)(2,1)S(1)}, bf16[4,4,64,384]{3,2,1,0:T(8,128)(2,1)S(1)}, u32[]{:S(2)}, u32[]{:S(2)}) collective-permute-start(bf16[4,4,64,384]{3,2,1,0:T(8,128)(2,1)S(1)} %all_to_all.25.mine), channel_id=1, source_target_pairs={{0,1},{1,0},{2,3},{3,2},{4,5},{5,4},{6,7},{7,6},{8,9},{9,8},{10,11... | collective-permute-start | bytes 2359304 | tf_op jit(solution)/shard_map/ppermute | solution.py:452
  20.9 3.4 %shard_map.118 = (bf16[128,2304]{1,0:T(8,128)(2,1)S(1)}, bf16[128,768]{1,0:T(8,128)(2,1)S(1)}, bf16[128,2304]{1,0:T(8,128)(2,1)S(1)}, bf16[128,768]{1,0:T(8,128)(2,1)S(1)}, f32[2,128,128]{2,1,0:T(8,128)S(1)}) custom-call(s32[3]{0:T(128)S(1)} %pad_add_fusion.place, bf16[1,128,3072]{2,1,0:T(8,128)(2,1)} %values.5, bf16[1,128,3072]{2,1,0:T(8,128)(2,1)} %gated_in.1, ...), custom_call_target="tpu_custom_call" | custom-call | tf_op jit(solution)/shard_map/pallas_call | solution.py:50
  24.4 1.3 collective-permute-start
  25.7 1.3 collective-permute-start.1
  27.0 3.5 %collective-permute-start.2 = (bf16[128,2304]{1,0:T(8,128)(2,1)S(1)}, bf16[128,2304]{1,0:T(8,128)(2,1)S(1)}, u32[]{:S(2)}, u32[]{:S(2)}) collective-permute-start(bf16[128,2304]{1,0:T(8,128)(2,1)S(1)} %get-tuple-element.37.v), channel_id=1, source_target_pairs={{8,16},{16,8},{40,48},{48,40},{9,17},{17,9},{41,49},{49,41},{10,18... | collective-permute-start | bytes 1769480 | tf_op jit(solution)/shard_map/ppermute | solution.py:448
  30.5 0.9 shard_map.121.weights
  31.4 11.1 %collective-permute-done.near = bf16[128,2304]{1,0:T(8,128)(2,1)S(1)} collective-permute-done((bf16[128,2304]{1,0:T(8,128)(2,1)S(1)}, bf16[128,2304]{1,0:T(8,128)(2,1)S(1)}, u32[]{:S(2)}, u32[]{:S(2)}) %collective-permute-start) | collective-permute-done | bytes 589856 | tf_op jit(solution)/shard_map/ppermute | solution.py:446
  42.5 13.3 %collective-permute-done.1.far = bf16[128,2304]{1,0:T(8,128)(2,1)S(1)} collective-permute-done((bf16[128,2304]{1,0:T(8,128)(2,1)S(1)}, bf16[128,2304]{1,0:T(8,128)(2,1)S(1)}, u32[]{:S(2)}, u32[]{:S(2)}) %collective-permute-start.1) | collective-permute-done | bytes 589856 | tf_op jit(solution)/shard_map/ppermute | solution.py:447
  55.8 1.5 collective-permute-done.2.swap
  57.2 0.9 shard_map.122
  58.2 1.3 collective-permute-start.7
  59.5 1.3 collective-permute-start.4
  60.8 1.3 collective-permute-start.5
  62.1 3.5 %collective-permute-start.6 = (bf16[128,768]{1,0:T(8,128)(2,1)S(1)}, bf16[128,768]{1,0:T(8,128)(2,1)S(1)}, u32[]{:S(2)}, u32[]{:S(2)}) collective-permute-start(bf16[128,768]{1,0:T(8,128)(2,1)S(1)} %get-tuple-element.39.v1.v), channel_id=1, source_target_pairs={{8,16},{16,8},{40,48},{48,40},{9,17},{17,9},{41,49},{49,41},{10,18... | collective-permute-start | bytes 589832 | tf_op jit(solution)/shard_map/ppermute | solution.py:448
  65.6 1.7 %shard_map.125 = (f32[4,64,768]{2,1,0:T(8,128)S(1)}, bf16[4,64,768]{2,1,0:T(8,128)(2,1)S(1)}) custom-call(s32[3]{0:T(128)S(1)} %pad_add_fusion.place, bf16[128,2304]{1,0:T(8,128)(2,1)S(1)} %get-tuple-element.36.u, bf16[128,2304]{1,0:T(8,128)(2,1)S(1)} %get-tuple-element.37.v, bf16[128,2304]{1,0:T(8,128)(2,1)S(1)} %collective-permute-done.near, ...), custom_call_target="tpu_custom_call" | custom-call | tf_op jit(solution)/shard_map/pallas_call | solution.py:50
  67.4 0.0 copy-start.22
  67.4 1.9 %collective-permute-start.9 = (bf16[4,64,768]{2,1,0:T(8,128)(2,1)S(1)}, bf16[4,64,768]{2,1,0:T(8,128)(2,1)S(1)}, u32[]{:S(2)}, u32[]{:S(2)}) collective-permute-start(bf16[4,64,768]{2,1,0:T(8,128)(2,1)S(1)} %get-tuple-element.50), channel_id=1, source_target_pairs={{0,1},{1,0},{2,3},{3,2},{4,5},{5,4},{6,7},{7,6},{8,9},{9,8},{10,11... | collective-permute-start | bytes 1179656 | tf_op jit(solution)/shard_map/ppermute | solution.py:481
  69.3 3.9 %collective-permute-done.5.far = bf16[128,768]{1,0:T(8,128)(2,1)S(1)} collective-permute-done((bf16[128,768]{1,0:T(8,128)(2,1)S(1)}, bf16[128,768]{1,0:T(8,128)(2,1)S(1)}, u32[]{:S(2)}, u32[]{:S(2)}) %collective-permute-start.5) | collective-permute-done | bytes 196640 | tf_op jit(solution)/shard_map/ppermute | solution.py:447
  73.2 1.5 collective-permute-done.6.swap
  74.7 0.4 shard_map.123
  75.1 0.0 copy-start.4
  75.1 0.0 copy-start
  75.1 1.4 collective-permute-start.8
  76.6 0.9 shard_map.119
  77.4 1.0 shard_map.128
  78.4 0.0 copy-start.2
  78.4 1.0 shard_map.129.before
  79.5 0.5 collective-permute-done.8.refs_5_.got
  79.9 0.7 shard_map.130
  80.7 1.9 %collective-permute-start.12 = (bf16[5,64,256]{2,1,0:T(8,128)(2,1)S(1)}, bf16[5,64,256]{2,1,0:T(8,128)(2,1)S(1)}, u32[]{:S(2)}, u32[]{:S(2)}) collective-permute-start(bf16[5,64,256]{2,1,0:T(8,128)(2,1)S(1)} %get-tuple-element.59), channel_id=1, source_target_pairs={{0,1},{1,0},{2,3},{3,2},{4,5},{5,4},{6,7},{7,6},{8,9},{9,8},{10,11... | collective-permute-start | bytes 491528 | tf_op jit(solution)/shard_map/ppermute | solution.py:506
  82.6 1.3 shard_map.126
  83.9 0.7 copy-done.12
  84.6 3.1 %collective-permute-start.10 = (bf16[2,64,768]{2,1,0:T(8,128)(2,1)}, bf16[2,64,768]{2,1,0:T(8,128)(2,1)}, u32[]{:S(2)}, u32[]{:S(2)}) collective-permute-start(bf16[2,64,768]{2,1,0:T(8,128)(2,1)} %get-tuple-element.52), channel_id=1, source_target_pairs={{0,6},{6,0},{2,4},{4,2},{1,7},{7,1},{3,5},{5,3},{8,14},{14,8},{10,... | collective-permute-start | bytes 589832 | tf_op jit(solution)/shard_map/ppermute | solution.py:490
  87.7 0.7 copy-done.9
  88.4 4.1 %all-to-all-start.1 = ((bf16[4,64,512]{2,1,0:T(8,128)(2,1)}), bf16[4,64,512]{2,1,0:T(8,128)(2,1)}, u32[]{:S(2)}, u32[]{:S(2)}) async-start(bf16[4,64,512]{2,1,0:T(8,128)(2,1)} %copy-done.9), calls=%async_computation.1 | async-start | bytes 524288 | tf_op jit(solution)/shard_map/all_to_all | solution.py:422
  92.5 2.8 %collective-permute-done.10.got = bf16[2,64,768]{2,1,0:T(8,128)(2,1)} collective-permute-done((bf16[2,64,768]{2,1,0:T(8,128)(2,1)}, bf16[2,64,768]{2,1,0:T(8,128)(2,1)}, u32[]{:S(2)}, u32[]{:S(2)}) %collective-permute-start.10) | collective-permute-done | bytes 196640 | tf_op jit(solution)/shard_map/ppermute | solution.py:490
  95.3 1.0 copy-done.13
  96.3 1.0 shard_map.127
  97.3 0.0 copy-start.15
  97.3 0.7 copy-done.15
  98.0 1.9 %collective-permute-start.11 = (bf16[64,768]{1,0:T(8,128)(2,1)S(1)}, bf16[64,768]{1,0:T(8,128)(2,1)S(1)}, u32[]{:S(2)}, u32[]{:S(2)}) collective-permute-start(bf16[64,768]{1,0:T(8,128)(2,1)S(1)} %get-tuple-element.54), channel_id=1, source_target_pairs={{0,2},{2,0},{4,6},{6,4},{1,3},{3,1},{5,7},{7,5},{8,10},{10,8},{12,... | collective-permute-start | bytes 294920 | tf_op jit(solution)/shard_map/ppermute | solution.py:492
  99.9 4.6 %collective-permute-done.11.other = bf16[64,768]{1,0:T(8,128)(2,1)S(1)} collective-permute-done((bf16[64,768]{1,0:T(8,128)(2,1)S(1)}, bf16[64,768]{1,0:T(8,128)(2,1)S(1)}, u32[]{:S(2)}, u32[]{:S(2)}) %collective-permute-start.11) | collective-permute-done | bytes 98336 | tf_op jit(solution)/shard_map/ppermute | solution.py:492
  104.5 0.7 copy-done.17
  105.1 0.9 copy-done.16
  106.1 0.9 copy-done.18
  107.0 1.0 shard_map.132
  108.0 0.0 copy-start.21
  108.0 19.5 %all_to_all.26.got = bf16[8,8,1280]{2,1,0:T(8,128)(2,1)S(1)} all-to-all(bf16[8,8,1280]{2,1,0:T(8,128)(2,1)S(1)} %shard_map.132), channel_id=1, replica_groups=mesh['sp_0'=8,'sp_1'=8,'dp_0'=4,'dp_1'=2] {'sp_0'}, dimensions={0} | all-to-all | bytes 327680 | tf_op jit(solution)/shard_map/all_to_all | solution.py:422
  127.6 16.9 %all_to_all.27.got = bf16[8,8,1280]{2,1,0:T(8,128)(2,1)S(1)} all-to-all(bf16[8,8,1280]{2,1,0:T(8,128)(2,1)S(1)} %shard_map.133), channel_id=1, replica_groups=mesh['sp_0'=8,'sp_1'=8,'dp_0'=4,'dp_1'=2] {'sp_1'}, dimensions={0} | all-to-all | bytes 327680 | tf_op jit(solution)/shard_map/all_to_all | solution.py:422
  144.5 0.7 copy-done.8
  145.2 4.1 %all-to-all-start.4 = ((bf16[8,8,2304]{2,1,0:T(8,128)(2,1)}), bf16[8,8,2304]{2,1,0:T(8,128)(2,1)}, u32[]{:S(2)}, u32[]{:S(2)}) async-start(bf16[8,8,2304]{2,1,0:T(8,128)(2,1)} %copy-done.8), calls=%async_computation.4 | async-start | bytes 589824 | tf_op jit(solution)/shard_map/all_to_all | solution.py:422
  149.3 1.1 copy-done.1
  150.4 1.1 copy-done.3
  151.5 1.0 copy-done.5
  152.5 0.9 copy-done.7
  153.4 0.9 copy-done.11
  154.3 0.8 copy-done.20
  155.2 3.6 %shard_map.124 = (bf16[1,128,3072]{2,1,0:T(8,128)(2,1)}, bf16[1,128,3072]{2,1,0:T(8,128)(2,1)}) custom-call(s32[3]{0:T(128)S(1)} %pad_add_fusion.place, bf16[1,128,3072]{2,1,0:T(8,128)(2,1)S(1)} %copy-done, bf16[1,128,3072]{2,1,0:T(8,128)(2,1)S(1)} %copy-done.1, f32[2,128,128]{2,1,0:T(8,128)S(1)} %copy-done.7, f32[128,128]{1,0:T(8,128)S(1)} %copy-done.20, ...), custom_call_target="tpu_custom_call" | custom-call | tf_op jit(solution)/shard_map/pallas_call | solution.py:50
  158.8 1.3 all-to-all-done.4.got
  160.1 1.9 %shard_map.135 = (f32[64,4,512]{2,1,0:T(4,128)}, f32[4,512]{1,0:T(4,128)}, f32[24,128]{1,0:T(8,128)}, f32[24,128]{1,0:T(8,128)}) custom-call(bf16[8,8,2304]{2,1,0:T(8,128)(2,1)} %all-to-all-done.4.got), custom_call_target="tpu_custom_call" | custom-call | tf_op jit(solution)/shard_map/pallas_call | solution.py:50
  (34 shorter events, 0.2 us)
Async XLA Ops:
  0.7 1.0 copy-start.14
  19.0 11.5 %collective-permute-start.3 = (bf16[4,4,64,384]{3,2,1,0:T(8,128)(2,1)S(1)}, bf16[4,4,64,384]{3,2,1,0:T(8,128)(2,1)S(1)}, u32[]{:S(2)}, u32[]{:S(2)}) collective-permute-start(bf16[4,4,64,384]{3,2,1,0:T(8,128)(2,1)S(1)} %all_to_all.25.mine), channel_id=1, source_target_pairs={{0,1},{1,0},{2,3},{3,2},{4,5},{5,4},{6,7},{7,6},{8,9},{9,8},{10,11... | collective-permute-start | bytes 2359304 | tf_op jit(solution)/shard_map/ppermute | solution.py:452
  24.4 55.6 %copy-start.6 = (f32[2,128,128]{2,1,0:T(8,128)}, f32[2,128,128]{2,1,0:T(8,128)S(1)}, u32[]{:S(2)}) copy-start(f32[2,128,128]{2,1,0:T(8,128)S(1)} %get-tuple-element.35.stats) | copy-start | bytes 393220
  24.4 18.1 %collective-permute-start = (bf16[128,2304]{1,0:T(8,128)(2,1)S(1)}, bf16[128,2304]{1,0:T(8,128)(2,1)S(1)}, u32[]{:S(2)}, u32[]{:S(2)}) collective-permute-start(bf16[128,2304]{1,0:T(8,128)(2,1)S(1)} %get-tuple-element.37.v), channel_id=1, source_target_pairs={{0,8},{24,16},{32,40},{56,48},{1,9},{25,17},{33,41},{57,49},{2,10}... | collective-permute-start | bytes 1769480 | tf_op jit(solution)/shard_map/ppermute | solution.py:446
  25.7 30.1 %collective-permute-start.1 = (bf16[128,2304]{1,0:T(8,128)(2,1)S(1)}, bf16[128,2304]{1,0:T(8,128)(2,1)S(1)}, u32[]{:S(2)}, u32[]{:S(2)}) collective-permute-start(bf16[128,2304]{1,0:T(8,128)(2,1)S(1)} %get-tuple-element.37.v), channel_id=1, source_target_pairs={{0,16},{24,8},{32,48},{56,40},{1,17},{25,9},{33,49},{57,41},{2,18}... | collective-permute-start | bytes 1769480 | tf_op jit(solution)/shard_map/ppermute | solution.py:447
  27.0 30.3 %collective-permute-start.2 = (bf16[128,2304]{1,0:T(8,128)(2,1)S(1)}, bf16[128,2304]{1,0:T(8,128)(2,1)S(1)}, u32[]{:S(2)}, u32[]{:S(2)}) collective-permute-start(bf16[128,2304]{1,0:T(8,128)(2,1)S(1)} %get-tuple-element.37.v), channel_id=1, source_target_pairs={{8,16},{16,8},{40,48},{48,40},{9,17},{17,9},{41,49},{49,41},{10,18... | collective-permute-start | bytes 1769480 | tf_op jit(solution)/shard_map/ppermute | solution.py:448
  58.2 20.2 %collective-permute-start.7 = (bf16[128,2304]{1,0:T(8,128)(2,1)S(1)}, bf16[128,2304]{1,0:T(8,128)(2,1)S(1)}, u32[]{:S(2)}, u32[]{:S(2)}) collective-permute-start(bf16[128,2304]{1,0:T(8,128)(2,1)S(1)} %get-tuple-element.45), channel_id=1, source_target_pairs={{8,0},{16,24},{40,32},{48,56},{9,1},{17,25},{41,33},{49,57},{10,2}... | collective-permute-start | bytes 1769480 | tf_op jit(solution)/shard_map/ppermute | solution.py:469
  59.5 9.8 %collective-permute-start.4 = (bf16[128,768]{1,0:T(8,128)(2,1)S(1)}, bf16[128,768]{1,0:T(8,128)(2,1)S(1)}, u32[]{:S(2)}, u32[]{:S(2)}) collective-permute-start(bf16[128,768]{1,0:T(8,128)(2,1)S(1)} %get-tuple-element.39.v1.v), channel_id=1, source_target_pairs={{0,8},{24,16},{32,40},{56,48},{1,9},{25,17},{33,41},{57,49},{2,10}... | collective-permute-start | bytes 589832 | tf_op jit(solution)/shard_map/ppermute | solution.py:446
  60.8 12.4 %collective-permute-start.5 = (bf16[128,768]{1,0:T(8,128)(2,1)S(1)}, bf16[128,768]{1,0:T(8,128)(2,1)S(1)}, u32[]{:S(2)}, u32[]{:S(2)}) collective-permute-start(bf16[128,768]{1,0:T(8,128)(2,1)S(1)} %get-tuple-element.39.v1.v), channel_id=1, source_target_pairs={{0,16},{24,8},{32,48},{56,40},{1,17},{25,9},{33,49},{57,41},{2,18}... | collective-permute-start | bytes 589832 | tf_op jit(solution)/shard_map/ppermute | solution.py:447
  62.1 12.6 %collective-permute-start.6 = (bf16[128,768]{1,0:T(8,128)(2,1)S(1)}, bf16[128,768]{1,0:T(8,128)(2,1)S(1)}, u32[]{:S(2)}, u32[]{:S(2)}) collective-permute-start(bf16[128,768]{1,0:T(8,128)(2,1)S(1)} %get-tuple-element.39.v1.v), channel_id=1, source_target_pairs={{8,16},{16,8},{40,48},{48,40},{9,17},{17,9},{41,49},{49,41},{10,18... | collective-permute-start | bytes 589832 | tf_op jit(solution)/shard_map/ppermute | solution.py:448
  67.4 9.2 %copy-start.22 = (f32[4,512]{1,0:T(4,128)S(1)}, f32[4,512]{1,0:T(4,128)}, u32[]{:S(2)}) copy-start(f32[4,512]{1,0:T(4,128)} %mix_bias.1) | copy-start | bytes 24580
  67.4 15.2 %collective-permute-start.9 = (bf16[4,64,768]{2,1,0:T(8,128)(2,1)S(1)}, bf16[4,64,768]{2,1,0:T(8,128)(2,1)S(1)}, u32[]{:S(2)}, u32[]{:S(2)}) collective-permute-start(bf16[4,64,768]{2,1,0:T(8,128)(2,1)S(1)} %get-tuple-element.50), channel_id=1, source_target_pairs={{0,1},{1,0},{2,3},{3,2},{4,5},{5,4},{6,7},{7,6},{8,9},{9,8},{10,11... | collective-permute-start | bytes 1179656 | tf_op jit(solution)/shard_map/ppermute | solution.py:481
  75.1 4.8 %copy-start.4 = (f32[128,768]{1,0:T(8,128)}, f32[128,768]{1,0:T(8,128)S(1)}, u32[]{:S(2)}) copy-start(f32[128,768]{1,0:T(8,128)S(1)} %get-tuple-element.44.refs_3_.out_v) | copy-start | bytes 1179652
  75.1 3.3 %copy-start = (bf16[1,128,3072]{2,1,0:T(8,128)(2,1)S(1)}, bf16[1,128,3072]{2,1,0:T(8,128)(2,1)}, u32[]{:S(2)}) copy-start(bf16[1,128,3072]{2,1,0:T(8,128)(2,1)} %values.5) | copy-start | bytes 2359300
  75.1 4.8 %collective-permute-start.8 = (bf16[128,768]{1,0:T(8,128)(2,1)S(1)}, bf16[128,768]{1,0:T(8,128)(2,1)S(1)}, u32[]{:S(2)}, u32[]{:S(2)}) collective-permute-start(bf16[128,768]{1,0:T(8,128)(2,1)S(1)} %get-tuple-element.46), channel_id=1, source_target_pairs={{8,0},{16,24},{40,32},{48,56},{9,1},{17,25},{41,33},{49,57},{10,2}... | collective-permute-start | bytes 589832 | tf_op jit(solution)/shard_map/ppermute | solution.py:469
  77.4 1.0 copy-start.19
  78.4 1.1 copy-start.2
  79.9 3.9 %copy-start.10 = (bf16[128,768]{1,0:T(8,128)(2,1)}, bf16[128,768]{1,0:T(8,128)(2,1)S(1)}, u32[]{:S(2)}) copy-start(bf16[128,768]{1,0:T(8,128)(2,1)S(1)} %collective-permute-done.8.refs_5_.got) | copy-start | bytes 589828
  80.7 7.0 %collective-permute-start.12 = (bf16[5,64,256]{2,1,0:T(8,128)(2,1)S(1)}, bf16[5,64,256]{2,1,0:T(8,128)(2,1)S(1)}, u32[]{:S(2)}, u32[]{:S(2)}) collective-permute-start(bf16[5,64,256]{2,1,0:T(8,128)(2,1)S(1)} %get-tuple-element.59), channel_id=1, source_target_pairs={{0,1},{1,0},{2,3},{3,2},{4,5},{5,4},{6,7},{7,6},{8,9},{9,8},{10,11... | collective-permute-start | bytes 491528 | tf_op jit(solution)/shard_map/ppermute | solution.py:506
  83.9 0.7 copy-start.12
  84.6 10.7 %collective-permute-start.10 = (bf16[2,64,768]{2,1,0:T(8,128)(2,1)}, bf16[2,64,768]{2,1,0:T(8,128)(2,1)}, u32[]{:S(2)}, u32[]{:S(2)}) collective-permute-start(bf16[2,64,768]{2,1,0:T(8,128)(2,1)} %get-tuple-element.52), channel_id=1, source_target_pairs={{0,6},{6,0},{2,4},{4,2},{1,7},{7,1},{3,5},{5,3},{8,14},{14,8},{10,... | collective-permute-start | bytes 589832 | tf_op jit(solution)/shard_map/ppermute | solution.py:490
  87.7 0.7 copy-start.9
  88.4 16.7 %all-to-all-start.1 = ((bf16[4,64,512]{2,1,0:T(8,128)(2,1)}), bf16[4,64,512]{2,1,0:T(8,128)(2,1)}, u32[]{:S(2)}, u32[]{:S(2)}) async-start(bf16[4,64,512]{2,1,0:T(8,128)(2,1)} %copy-done.9), calls=%async_computation.1 | async-start | bytes 524288 | tf_op jit(solution)/shard_map/all_to_all | solution.py:422
  95.3 1.0 copy-start.13
  97.3 0.7 copy-start.15
  98.0 6.5 %collective-permute-start.11 = (bf16[64,768]{1,0:T(8,128)(2,1)S(1)}, bf16[64,768]{1,0:T(8,128)(2,1)S(1)}, u32[]{:S(2)}, u32[]{:S(2)}) collective-permute-start(bf16[64,768]{1,0:T(8,128)(2,1)S(1)} %get-tuple-element.54), channel_id=1, source_target_pairs={{0,2},{2,0},{4,6},{6,4},{1,3},{3,1},{5,7},{7,5},{8,10},{10,8},{12,... | collective-permute-start | bytes 294920 | tf_op jit(solution)/shard_map/ppermute | solution.py:492
  104.5 0.7 copy-start.17
  105.1 0.9 copy-start.16
  106.1 0.9 copy-start.18
  108.0 41.3 %copy-start.21 = (f32[3072]{0:T(1024)S(1)}, f32[3072]{0:T(1024)}, u32[]{:S(2)}) copy-start(f32[3072]{0:T(1024)} %param.10) | copy-start | bytes 36868
  144.5 0.7 copy-start.8
  145.2 14.9 %all-to-all-start.4 = ((bf16[8,8,2304]{2,1,0:T(8,128)(2,1)}), bf16[8,8,2304]{2,1,0:T(8,128)(2,1)}, u32[]{:S(2)}, u32[]{:S(2)}) async-start(bf16[8,8,2304]{2,1,0:T(8,128)(2,1)} %copy-done.8), calls=%async_computation.4 | async-start | bytes 589824 | tf_op jit(solution)/shard_map/all_to_all | solution.py:422
  149.3 1.1 copy-start.1
  150.4 1.1 copy-start.3
  151.5 1.0 copy-start.5
  152.5 0.9 copy-start.7
  153.4 0.9 copy-start.11
  154.3 0.8 copy-start.20

commit v4 on v3

--- a/solution.py
+++ b/solution.py
@@ -28,6 +28,7 @@
 SWAP = [(1, 2), (2, 1), (5, 6), (6, 5)]
 OUT = [(1, 0), (2, 3), (5, 4), (6, 7)]
 PARTNER = [(0, 1), (1, 0)]
+CHIPS = [[(i, (i + k) % 4) for i in range(4)] for k in range(4)]
 ACROSS = [(0, 3), (3, 0), (1, 2), (2, 1)]
 WITHIN = [(0, 1), (1, 0), (2, 3), (3, 2)]
 
@@ -120,10 +121,11 @@
             cols = slice(g * WIDTH, (g + 1) * WIDTH)
             unit = (values[0, rows, cols].astype(F32) - mean) * inv
             normed = (unit * gain[:, cols] + shift[:, cols]).astype(BF16)
+            sent = unit.astype(BF16)
             grad = (upstream[0, rows, cols].astype(F32) * gated[0, rows, cols].astype(F32)).astype(BF16)
             i, lanes = lanes_of(g)
             us[i][rows, lanes] = jnp.where(low, grad, normed)
-            vs[i][rows, lanes] = jnp.where(low, normed, grad)
+            vs[i][rows, lanes] = jnp.where(low, sent, grad)
         return carry
 
     for i in range(4):
@@ -149,19 +151,20 @@
 def slab_kernel(place, rows, out):
     p = place[0]
 
-    def fill(start):
-        for g in range(GROUPS):
-            got = rows[:, g, start : start + 3 * ROWS]
-            for x in range(4):
-                out[x, g] = got
-
     @pl.when(p < 3)
     def _():
-        fill(0)
+        for g in range(GROUPS):
+            out[g] = rows[:, g, : 3 * ROWS]
 
     @pl.when(p == 3)
     def _():
-        fill(ROWS)
+        for g in range(GROUPS):
+            out[g] = rows[:, g, ROWS:]
+
+
+def join_kernel(place, *refs):
+    for k in range(4):
+        refs[4][(place[1] + 4 - k) % 4] = refs[k][...]
 
 
 def weight_kernel(place, mine, theirs, out):
@@ -198,21 +201,43 @@
                     out[g, i * ROWS : (i + 1) * ROWS, j * ROWS : (j + 1) * ROWS] = got
 
 
-def product_kernel(chunk, u, v, near, far, swap, weights, part, out_u, out_v):
+def product_kernel(chunk, place, u, v, near, far, swap, weights, gain, shift, part, out_u, out_v, *normed):
+    p = place[0]
     for g in range(GROUPS):
         i, lanes = lanes_of(g)
         if i != chunk:
             continue
+        cols = slice(g * WIDTH, (g + 1) * WIDTH)
         own, other = weights[g, :ROWS, :], weights[g, ROWS:, :]
-        long_side = jnp.concatenate([u[:, lanes], swap[:, lanes], far[:, lanes]], axis=0)
-        part[:, lanes] = nn(other, long_side).astype(BF16)
-        out_u[:, lanes] = nn(own, long_side)
-        short_side = jnp.concatenate([v[:, lanes], near[:, lanes]], axis=0)
         both = jnp.concatenate([own[:, :ROWS], other[:, :ROWS]], axis=0)
-        out_v[:, lanes] = tn(both, short_side)
-
-
-def mix_grad_kernel(n, place, u, v, near, far, swap, keep, send):
+
+        def put(slot, ref, here):
+            got = ref[:, lanes].astype(F32) * gain[:, cols] + shift[:, cols]
+            if here is not None:
+                got = jnp.where(here, got, 0.0)
+            normed[slot][:, lanes] = got.astype(BF16)
+
+        def products(long_side, short_side):
+            long_side = jnp.concatenate([ref[:, lanes] for ref in long_side], axis=0)
+            short_side = jnp.concatenate([ref[:, lanes] for ref in short_side], axis=0)
+            part[:, lanes] = nn(other, long_side).astype(BF16)
+            out_u[:, lanes] = nn(own, long_side)
+            out_v[:, lanes] = tn(both, short_side)
+
+        @pl.when(p < 2)
+        def _():
+            put(0, v, None)
+            put(1, near, p == 1)
+            products((u, swap, far), normed)
+
+        @pl.when(p >= 2)
+        def _():
+            put(0, swap, p == 2)
+            put(1, far, p == 2)
+            products((u, *normed), (v, near))
+
+
+def mix_grad_kernel(n, place, u, v, near, far, swap, one, two, keep, send):
     p, core = place[0], place[2]
     first = core == 0
     r = lax.broadcasted_iota(jnp.int32, (ROWS, ROWS), 0) // SEG
@@ -230,21 +255,21 @@
 
         @pl.when(p == 0)
         def _():
-            put(0, 0, k, jnp.where(r >= c, nt(u[:, at], v[:, at]), 0.0))
+            put(0, 0, k, jnp.where(r >= c, nt(u[:, at], one[:, at]), 0.0))
 
         @pl.when(p == 1)
         def _():
-            put(1, 0, k, nt(u[:, at], near[:, at]))
-            put(1, 1, k, jnp.where(r >= c, nt(u[:, at], v[:, at]), 0.0))
-            put(2, 0, k, nt(swap[:, at], near[:, at]))
-            put(3, 0, k, nt(far[:, at], near[:, at]))
+            put(1, 0, k, nt(u[:, at], two[:, at]))
+            put(1, 1, k, jnp.where(r >= c, nt(u[:, at], one[:, at]), 0.0))
+            put(2, 0, k, nt(swap[:, at], two[:, at]))
+            put(3, 0, k, nt(far[:, at], two[:, at]))
 
         @pl.when(p == 2)
         def _():
             put(2, 0, k, jnp.where(r >= c, nt(v[:, at], u[:, at]), 0.0))
-            put(2, 1, k, nt(v[:, at], swap[:, at]))
+            put(2, 1, k, nt(v[:, at], one[:, at]))
             put(3, 0, k, nt(near[:, at], u[:, at]))
-            put(3, 1, k, nt(near[:, at], swap[:, at]))
+            put(3, 1, k, nt(near[:, at], one[:, at]))
 
         @pl.when(p == 3)
         def _():
@@ -256,8 +281,8 @@
     return high, (x - high.astype(F32)).astype(BF16)
 
 
-def sums_kernel(chunk, place, values, stats, before, out_u, out_v, got, small):
-    low = place[0] < 2
+def sums_kernel(chunk, place, values, stats, before, out_u, out_v, part, near, small):
+    p = place[0]
     small[...] = before[...]
     mean = stats[0, :, :1]
     inv = stats[1, :, :1]
@@ -268,16 +293,17 @@
         for k in range(WIDTH // 128):
             own = slice(lanes.start + k * 128, lanes.start + (k + 1) * 128)
             cols = slice(g * WIDTH + k * 128, g * WIDTH + (k + 1) * 128)
-            back = jnp.where(low, out_u[:, own] + got[:, own].astype(F32), out_v[:, own])
-            back = back.astype(BF16).astype(F32)
+            back = jnp.where(p < 2, out_u[:, own], out_v[:, own])
             unit = (values[0, :, cols].astype(F32) - mean) * inv
+            sent = jnp.where(p == 1, part[:, own].astype(F32), 0.0)
             row = 16 + g * 6 + k
-            small[row : row + 1] = jnp.sum(back * unit, axis=0, keepdims=True)
-            small[row + 24 : row + 25] = jnp.sum(back, axis=0, keepdims=True)
-
-
-def last_sums_kernel(place, values, stats, before, out_u, out_v, got, last, small, send):
-    sums_kernel(1, place, values, stats, before, out_u, out_v, got, small)
+            gain_rows = back * unit + sent * near[:, own].astype(F32)
+            small[row : row + 1] = jnp.sum(gain_rows, axis=0, keepdims=True)
+            small[row + 24 : row + 25] = jnp.sum(back + sent, axis=0, keepdims=True)
+
+
+def last_sums_kernel(place, values, stats, before, out_u, out_v, part, near, last, small, send):
+    sums_kernel(1, place, values, stats, before, out_u, out_v, part, near, small)
     send[:4] = last[...]
     high, low = split(small[...])
     send[4, :, :128] = high
@@ -447,8 +473,9 @@
         far.append(lax.ppermute(vs[i], Y, FAR))
         swap.append(lax.ppermute(vs[i], Y, SWAP))
 
-    slab = call(slab_kernel, shape((4, GROUPS, SEG, 3 * ROWS), BF16), (place, mix_w))
-    mine = exchanged(slab, X)
+    slab = call(slab_kernel, shape((GROUPS, SEG, 3 * ROWS), BF16), (place, mix_w))
+    slabs = [slab] + [lax.ppermute(slab, X, CHIPS[k]) for k in range(1, 4)]
+    mine = call(join_kernel, shape((4, GROUPS, SEG, 3 * ROWS), BF16), (place, *slabs))
     theirs = lax.ppermute(mine, CORE, PARTNER)
     columns, bias_term = call(
         side_kernel,
@@ -457,15 +484,15 @@
     )
     weights = call(weight_kernel, shape((GROUPS, 2 * ROWS, 3 * ROWS), BF16), (place, mine, theirs))
 
-    outs_u, outs_v, got, keeps, sends = [], [], [], [], []
+    outs_u, outs_v, got, keeps, sends, parts = [], [], [], [], [], []
     for i in range(n):
         operands = (us[i], vs[i], near[i], far[i], swap[i])
-        part, out_u, out_v = call(
+        part, out_u, out_v, one, two = call(
             functools.partial(product_kernel, i),
-            [halves[i], fulls[i], fulls[i]],
-            (*operands, weights),
-            0,
+            [halves[i], fulls[i], fulls[i], halves[i], halves[i]],
+            (place, *operands, weights, gain_row, shift_row),
         )
+        parts.append(part)
         got.append(lax.ppermute(part, Y, OUT))
         outs_u.append(out_u)
         outs_v.append(out_v)
@@ -473,7 +500,7 @@
         keep, send = call(
             functools.partial(mix_grad_kernel, CHUNKS[i]),
             [shape(dims, F32), shape(dims, BF16)],
-            (place, *operands),
+            (place, *operands, one, two),
         )
         keeps.append(keep)
         sends.append(send)
@@ -493,12 +520,12 @@
     sums = call(
         functools.partial(sums_kernel, 0),
         shape((64, 128), F32),
-        (place, values_in, stats, bias_term, outs_u[0], outs_v[0], got[0]),
+        (place, values_in, stats, bias_term, outs_u[0], outs_v[0], parts[0], near[0]),
     )
     small, last = call(
         last_sums_kernel,
         [shape((64, 128), F32), shape((5, SEG, 2 * ROWS), BF16)],
-        (place, values_in, stats, sums, outs_u[1], outs_v[1], got[1], sends[1]),
+        (place, values_in, stats, sums, outs_u[1], outs_v[1], parts[1], near[1], sends[1]),
     )
     last = call(
         last_chip_kernel,

time: 163 us -> 174 us (1.067)
  the two profiles are of different devices: /device:TPU:8 before, /device:TPU:64 now
where the time goes in v4:
time: 174 us; the launch traced here: 173 us
  waiting for transfers between devices  61.1 us (35%)
  starting transfers between devices  57.9 us (33%)
  Pallas kernels  24.6 us (14%)
  blocking collectives  17.7 us (10%)
  local copies, waits for them, and re-layouts  10.3 us (6%)
    pallas_call x19, Pallas kernels, call(): pl.pallas_call(kernel, out_shape=out_shape, in_specs=[SMEM] * scalars + [...  24.6 us
    all_to_all x1, blocking collectives, exchanged(): return lax.all_to_all(x, axis, split_axis=0, concat_axis=0, tiled=True)  17.7 us
    all_to_all x3, starting transfers between devices, exchanged(): return lax.all_to_all(x, axis, split_axis=0, concat_axis=0, tiled=True)  16.8 us
    ppermute x2, waiting for transfers between devices, compute(): near.append(lax.ppermute(vs[i], Y, NEAR))  15.3 us
    ppermute x2, waiting for transfers between devices, compute(): far.append(lax.ppermute(vs[i], Y, FAR))  14.3 us
    ppermute x2, starting transfers between devices, compute(): far.append(lax.ppermute(vs[i], Y, FAR))  13.8 us
    unnamed x42, local copies, waits for them, and re-layouts  10.3 us
    ppermute x3, starting transfers between devices, compute(): slabs = [slab] + [lax.ppermute(slab, X, CHIPS[k]) for k in range(1, 4)]  10.2 us
  transfers between devices with their start and end apart: 19, of which 11 were waited for; matrix products, arithmetic and copies ran while one was open for 0% of the time, Pallas kernels for 10%

profile of v4, /device:TPU:64, one launch (start us, length us, event | category | flops | bytes accessed | tf_op | source)
XLA Modules:
  0.0 172.7 jit_solution(4869031874883134654)
XLA Ops:
  0.6 0.1 pad_add_fusion.place
  0.7 0.9 copy-done.12
  1.7 1.0 shard_map.120.refs_0_
  2.6 4.7 %collective-permute-start.5 = (bf16[4,64,384]{2,1,0:T(8,128)(2,1)S(1)}, bf16[4,64,384]{2,1,0:T(8,128)(2,1)S(1)}, u32[]{:S(2)}, u32[]{:S(2)}) collective-permute-start(bf16[4,64,384]{2,1,0:T(8,128)(2,1)S(1)} %shard_map.120.refs_0_), channel_id=1, source_target_pairs={{0,6},{2,0},{4,2},{6,4},{1,7},{3,1},{5,3},{7,5},{8,14},{10,8},{12,... | collective-permute-start | bytes 589832 | tf_op jit(solution)/shard_map/ppermute | solution.py:477
  7.3 2.7 %collective-permute-start.4 = (bf16[4,64,384]{2,1,0:T(8,128)(2,1)S(1)}, bf16[4,64,384]{2,1,0:T(8,128)(2,1)S(1)}, u32[]{:S(2)}, u32[]{:S(2)}) collective-permute-start(bf16[4,64,384]{2,1,0:T(8,128)(2,1)S(1)} %shard_map.120.refs_0_), channel_id=1, source_target_pairs={{0,4},{2,6},{4,0},{6,2},{1,5},{3,7},{5,1},{7,3},{8,12},{10,14},{12... | collective-permute-start | bytes 589832 | tf_op jit(solution)/shard_map/ppermute | solution.py:477
  10.0 2.8 %collective-permute-start.3 = (bf16[4,64,384]{2,1,0:T(8,128)(2,1)S(1)}, bf16[4,64,384]{2,1,0:T(8,128)(2,1)S(1)}, u32[]{:S(2)}, u32[]{:S(2)}) collective-permute-start(bf16[4,64,384]{2,1,0:T(8,128)(2,1)S(1)} %shard_map.120.refs_0_), channel_id=1, source_target_pairs={{0,2},{2,4},{4,6},{6,0},{1,3},{3,5},{5,7},{7,1},{8,10},{10,12},{12... | collective-permute-start | bytes 589832 | tf_op jit(solution)/shard_map/ppermute | solution.py:477
  12.8 2.9 %collective-permute-done.5.refs_3_ = bf16[4,64,384]{2,1,0:T(8,128)(2,1)S(1)} collective-permute-done((bf16[4,64,384]{2,1,0:T(8,128)(2,1)S(1)}, bf16[4,64,384]{2,1,0:T(8,128)(2,1)S(1)}, u32[]{:S(2)}, u32[]{:S(2)}) %collective-permute-start.5) | collective-permute-done | bytes 196640 | tf_op jit(solution)/shard_map/ppermute | solution.py:477
  15.7 2.8 %collective-permute-done.4.refs_2_ = bf16[4,64,384]{2,1,0:T(8,128)(2,1)S(1)} collective-permute-done((bf16[4,64,384]{2,1,0:T(8,128)(2,1)S(1)}, bf16[4,64,384]{2,1,0:T(8,128)(2,1)S(1)}, u32[]{:S(2)}, u32[]{:S(2)}) %collective-permute-start.4) | collective-permute-done | bytes 196640 | tf_op jit(solution)/shard_map/ppermute | solution.py:477
  18.5 2.8 %collective-permute-done.3.refs_1_ = bf16[4,64,384]{2,1,0:T(8,128)(2,1)S(1)} collective-permute-done((bf16[4,64,384]{2,1,0:T(8,128)(2,1)S(1)}, bf16[4,64,384]{2,1,0:T(8,128)(2,1)S(1)}, u32[]{:S(2)}, u32[]{:S(2)}) %collective-permute-start.3) | collective-permute-done | bytes 196640 | tf_op jit(solution)/shard_map/ppermute | solution.py:477
  21.3 0.6 shard_map.121.mine
  21.9 1.9 %collective-permute-start.6 = (bf16[4,4,64,384]{3,2,1,0:T(8,128)(2,1)S(1)}, bf16[4,4,64,384]{3,2,1,0:T(8,128)(2,1)S(1)}, u32[]{:S(2)}, u32[]{:S(2)}) collective-permute-start(bf16[4,4,64,384]{3,2,1,0:T(8,128)(2,1)S(1)} %shard_map.121.mine), channel_id=1, source_target_pairs={{0,1},{1,0},{2,3},{3,2},{4,5},{5,4},{6,7},{7,6},{8,9},{9,8},{10,11... | collective-permute-start | bytes 2359304 | tf_op jit(solution)/shard_map/ppermute | solution.py:479
  23.8 3.5 %shard_map.118 = (bf16[128,2304]{1,0:T(8,128)(2,1)S(1)}, bf16[128,768]{1,0:T(8,128)(2,1)S(1)}, bf16[128,2304]{1,0:T(8,128)(2,1)S(1)}, bf16[128,768]{1,0:T(8,128)(2,1)S(1)}, f32[2,128,128]{2,1,0:T(8,128)S(1)}) custom-call(s32[3]{0:T(128)S(1)} %pad_add_fusion.place, bf16[1,128,3072]{2,1,0:T(8,128)(2,1)} %values.5, bf16[1,128,3072]{2,1,0:T(8,128)(2,1)} %gated_in.1, ...), custom_call_target="tpu_custom_call" | custom-call | tf_op jit(solution)/shard_map/pallas_call | solution.py:51
  27.3 0.0 copy-start.16
  27.4 0.8 collective-permute-start.2
  28.2 6.2 %collective-permute-start.1 = (bf16[128,2304]{1,0:T(8,128)(2,1)S(1)}, bf16[128,2304]{1,0:T(8,128)(2,1)S(1)}, u32[]{:S(2)}, u32[]{:S(2)}) collective-permute-start(bf16[128,2304]{1,0:T(8,128)(2,1)S(1)} %get-tuple-element.41.v), channel_id=1, source_target_pairs={{0,16},{24,8},{32,48},{56,40},{1,17},{25,9},{33,49},{57,41},{2,18}... | collective-permute-start | bytes 1769480 | tf_op jit(solution)/shard_map/ppermute | solution.py:473
  34.4 1.4 collective-permute-start
  35.8 0.9 shard_map.122.weights
  36.7 11.4 %collective-permute-done.1.far = bf16[128,2304]{1,0:T(8,128)(2,1)S(1)} collective-permute-done((bf16[128,2304]{1,0:T(8,128)(2,1)S(1)}, bf16[128,2304]{1,0:T(8,128)(2,1)S(1)}, u32[]{:S(2)}, u32[]{:S(2)}) %collective-permute-start.1) | collective-permute-done | bytes 589856 | tf_op jit(solution)/shard_map/ppermute | solution.py:473
  48.1 11.9 %collective-permute-done.near = bf16[128,2304]{1,0:T(8,128)(2,1)S(1)} collective-permute-done((bf16[128,2304]{1,0:T(8,128)(2,1)S(1)}, bf16[128,2304]{1,0:T(8,128)(2,1)S(1)}, u32[]{:S(2)}, u32[]{:S(2)}) %collective-permute-start) | collective-permute-done | bytes 589856 | tf_op jit(solution)/shard_map/ppermute | solution.py:472
  60.0 1.9 %shard_map.123 = (bf16[128,2304]{1,0:T(8,128)(2,1)S(1)}, f32[128,2304]{1,0:T(8,128)S(1)}, f32[128,2304]{1,0:T(8,128)S(1)}, bf16[128,2304]{1,0:T(8,128)(2,1)S(1)}, bf16[128,2304]{1,0:T(8,128)(2,1)S(1)}) custom-call(s32[3]{0:T(128)S(1)} %pad_add_fusion.place, bf16[128,2304]{1,0:T(8,128)(2,1)S(1)} %get-tuple-element.40.u, ...), custom_call_target="tpu_custom_call" | custom-call | tf_op jit(solution)/shard_map/pallas_call | solution.py:51
  61.9 0.0 copy-start.9
  61.9 1.3 shard_map.126
  63.2 1.9 %collective-permute-start.12 = (bf16[4,64,768]{2,1,0:T(8,128)(2,1)S(1)}, bf16[4,64,768]{2,1,0:T(8,128)(2,1)S(1)}, u32[]{:S(2)}, u32[]{:S(2)}) collective-permute-start(bf16[4,64,768]{2,1,0:T(8,128)(2,1)S(1)} %get-tuple-element.56), channel_id=1, source_target_pairs={{0,1},{1,0},{2,3},{3,2},{4,5},{5,4},{6,7},{7,6},{8,9},{9,8},{10,11... | collective-permute-start | bytes 1179656 | tf_op jit(solution)/shard_map/ppermute | solution.py:508
  65.1 0.7 collective-permute-start.9
  65.8 7.6 %collective-permute-start.8 = (bf16[128,768]{1,0:T(8,128)(2,1)S(1)}, bf16[128,768]{1,0:T(8,128)(2,1)S(1)}, u32[]{:S(2)}, u32[]{:S(2)}) collective-permute-start(bf16[128,768]{1,0:T(8,128)(2,1)S(1)} %get-tuple-element.43.v1.v), channel_id=1, source_target_pairs={{0,16},{24,8},{32,48},{56,40},{1,17},{25,9},{33,49},{57,41},{2,18}... | collective-permute-start | bytes 589832 | tf_op jit(solution)/shard_map/ppermute | solution.py:473
  73.4 1.5 collective-permute-start.7
  74.9 0.9 shard_map.119
  75.8 0.0 collective-permute-done.9.swap
  75.8 2.9 %collective-permute-done.8.far = bf16[128,768]{1,0:T(8,128)(2,1)S(1)} collective-permute-done((bf16[128,768]{1,0:T(8,128)(2,1)S(1)}, bf16[128,768]{1,0:T(8,128)(2,1)S(1)}, u32[]{:S(2)}, u32[]{:S(2)}) %collective-permute-start.8) | collective-permute-done | bytes 196640 | tf_op jit(solution)/shard_map/ppermute | solution.py:473
  78.7 3.5 %collective-permute-done.7.near = bf16[128,768]{1,0:T(8,128)(2,1)S(1)} collective-permute-done((bf16[128,768]{1,0:T(8,128)(2,1)S(1)}, bf16[128,768]{1,0:T(8,128)(2,1)S(1)}, u32[]{:S(2)}, u32[]{:S(2)}) %collective-permute-start.7) | collective-permute-done | bytes 196640 | tf_op jit(solution)/shard_map/ppermute | solution.py:472
  82.2 1.0 shard_map.124
  83.2 0.8 shard_map.129
  84.0 1.2 shard_map.130.before
  85.2 0.8 shard_map.131
  86.0 1.9 %collective-permute-start.15 = (bf16[5,64,256]{2,1,0:T(8,128)(2,1)S(1)}, bf16[5,64,256]{2,1,0:T(8,128)(2,1)S(1)}, u32[]{:S(2)}, u32[]{:S(2)}) collective-permute-start(bf16[5,64,256]{2,1,0:T(8,128)(2,1)S(1)} %get-tuple-element.67), channel_id=1, source_target_pairs={{0,1},{1,0},{2,3},{3,2},{4,5},{5,4},{6,7},{7,6},{8,9},{9,8},{10,11... | collective-permute-start | bytes 491528 | tf_op jit(solution)/shard_map/ppermute | solution.py:533
  87.9 1.3 shard_map.127
  89.2 0.7 copy-done.10
  89.9 2.5 %collective-permute-start.13 = (bf16[2,64,768]{2,1,0:T(8,128)(2,1)}, bf16[2,64,768]{2,1,0:T(8,128)(2,1)}, u32[]{:S(2)}, u32[]{:S(2)}) collective-permute-start(bf16[2,64,768]{2,1,0:T(8,128)(2,1)} %get-tuple-element.58), channel_id=1, source_target_pairs={{0,6},{6,0},{2,4},{4,2},{1,7},{7,1},{3,5},{5,3},{8,14},{14,8},{10,... | collective-permute-start | bytes 589832 | tf_op jit(solution)/shard_map/ppermute | solution.py:517
  92.5 0.7 copy-done.7
  93.2 4.0 %all-to-all-start = ((bf16[4,64,512]{2,1,0:T(8,128)(2,1)}), bf16[4,64,512]{2,1,0:T(8,128)(2,1)}, u32[]{:S(2)}, u32[]{:S(2)}) async-start(bf16[4,64,512]{2,1,0:T(8,128)(2,1)} %copy-done.7), calls=%async_computation | async-start | bytes 524288 | tf_op jit(solution)/shard_map/all_to_all | solution.py:448
  97.2 3.5 %collective-permute-done.13.got = bf16[2,64,768]{2,1,0:T(8,128)(2,1)} collective-permute-done((bf16[2,64,768]{2,1,0:T(8,128)(2,1)}, bf16[2,64,768]{2,1,0:T(8,128)(2,1)}, u32[]{:S(2)}, u32[]{:S(2)}) %collective-permute-start.13) | collective-permute-done | bytes 196640 | tf_op jit(solution)/shard_map/ppermute | solution.py:517
  100.7 1.0 copy-done.11
  101.7 1.6 shard_map.128
  103.3 0.7 copy-done.14
  103.9 1.9 %collective-permute-start.14 = (bf16[64,768]{1,0:T(8,128)(2,1)}, bf16[64,768]{1,0:T(8,128)(2,1)}, u32[]{:S(2)}, u32[]{:S(2)}) collective-permute-start(bf16[64,768]{1,0:T(8,128)(2,1)} %get-tuple-element.60), channel_id=1, source_target_pairs={{0,2},{2,0},{4,6},{6,4},{1,3},{3,1},{5,7},{7,5},{8,10},{10,8},{12,... | collective-permute-start | bytes 294920 | tf_op jit(solution)/shard_map/ppermute | solution.py:519
  105.9 4.9 %collective-permute-done.14.other = bf16[64,768]{1,0:T(8,128)(2,1)} collective-permute-done((bf16[64,768]{1,0:T(8,128)(2,1)}, bf16[64,768]{1,0:T(8,128)(2,1)}, u32[]{:S(2)}, u32[]{:S(2)}) %collective-permute-start.14) | collective-permute-done | bytes 98336 | tf_op jit(solution)/shard_map/ppermute | solution.py:519
  110.8 0.9 copy-done.15
  111.7 1.1 shard_map.133
  112.7 17.7 %all_to_all.20.got = bf16[8,8,1280]{2,1,0:T(8,128)(2,1)S(1)} all-to-all(bf16[8,8,1280]{2,1,0:T(8,128)(2,1)S(1)} %shard_map.133), channel_id=1, replica_groups=mesh['sp_0'=8,'sp_1'=8,'dp_0'=4,'dp_1'=2] {'sp_0'}, dimensions={0} | all-to-all | bytes 327680 | tf_op jit(solution)/shard_map/all_to_all | solution.py:448
  130.5 0.7 copy-done.8
  131.2 7.4 %all-to-all-start.2 = ((bf16[8,8,1280]{2,1,0:T(8,128)(2,1)}), bf16[8,8,1280]{2,1,0:T(8,128)(2,1)}, u32[]{:S(2)}, u32[]{:S(2)}) async-start(bf16[8,8,1280]{2,1,0:T(8,128)(2,1)} %copy-done.8), calls=%async_computation.2 | async-start | bytes 327680 | tf_op jit(solution)/shard_map/all_to_all | solution.py:448
  138.6 1.3 collective-permute-start.10
  139.9 8.1 %all-to-all-done.2.got = bf16[8,8,1280]{2,1,0:T(8,128)(2,1)} async-done(((bf16[8,8,1280]{2,1,0:T(8,128)(2,1)}), bf16[8,8,1280]{2,1,0:T(8,128)(2,1)}, u32[]{:S(2)}, u32[]{:S(2)}) %all-to-all-start.2) | async-done | bytes 163872 | tf_op jit(solution)/shard_map/all_to_all | solution.py:448
  148.0 1.0 shard_map.135
  149.0 0.7 copy-done.6
  149.7 5.4 %all-to-all-start.3 = ((bf16[8,8,2304]{2,1,0:T(8,128)(2,1)}), bf16[8,8,2304]{2,1,0:T(8,128)(2,1)}, u32[]{:S(2)}, u32[]{:S(2)}) async-start(bf16[8,8,2304]{2,1,0:T(8,128)(2,1)} %copy-done.6), calls=%async_computation.3 | async-start | bytes 589824 | tf_op jit(solution)/shard_map/all_to_all | solution.py:448
  155.1 1.3 collective-permute-start.11
  156.3 6.5 %collective-permute-done.11.refs_5_ = bf16[128,768]{1,0:T(8,128)(2,1)S(1)} collective-permute-done((bf16[128,768]{1,0:T(8,128)(2,1)}, bf16[128,768]{1,0:T(8,128)(2,1)S(1)}, u32[]{:S(2)}, u32[]{:S(2)}) %collective-permute-start.11) | collective-permute-done | bytes 196640 | tf_op jit(solution)/shard_map/ppermute | solution.py:496
  162.8 1.1 copy-done.1
  164.0 1.0 copy-done.3
  165.0 0.9 copy-done.5
  165.9 0.8 copy-done.19
  166.7 4.1 %shard_map.125 = (bf16[1,128,3072]{2,1,0:T(8,128)(2,1)}, bf16[1,128,3072]{2,1,0:T(8,128)(2,1)}) custom-call(s32[3]{0:T(128)S(1)} %pad_add_fusion.place, bf16[1,128,3072]{2,1,0:T(8,128)(2,1)S(1)} %copy-done, bf16[1,128,3072]{2,1,0:T(8,128)(2,1)S(1)} %copy-done.1, f32[2,128,128]{2,1,0:T(8,128)S(1)} %copy-done.5, f32[128,128]{1,0:T(8,128)S(1)} %copy-done.19, ...), custom_call_target="tpu_custom_call" | custom-call | tf_op jit(solution)/shard_map/pallas_call | solution.py:51
  170.8 1.9 %shard_map.136 = (f32[64,4,512]{2,1,0:T(4,128)}, f32[4,512]{1,0:T(4,128)}, f32[24,128]{1,0:T(8,128)}, f32[24,128]{1,0:T(8,128)}) custom-call(bf16[8,8,2304]{2,1,0:T(8,128)(2,1)} %all-to-all-done.3.got), custom_call_target="tpu_custom_call" | custom-call | tf_op jit(solution)/shard_map/pallas_call | solution.py:51
  (37 shorter events, 0.1 us)
Async XLA Ops:
  0.7 1.0 copy-start.12
  2.6 13.1 %collective-permute-start.5 = (bf16[4,64,384]{2,1,0:T(8,128)(2,1)S(1)}, bf16[4,64,384]{2,1,0:T(8,128)(2,1)S(1)}, u32[]{:S(2)}, u32[]{:S(2)}) collective-permute-start(bf16[4,64,384]{2,1,0:T(8,128)(2,1)S(1)} %shard_map.120.refs_0_), channel_id=1, source_target_pairs={{0,6},{2,0},{4,2},{6,4},{1,7},{3,1},{5,3},{7,5},{8,14},{10,8},{12,... | collective-permute-start | bytes 589832 | tf_op jit(solution)/shard_map/ppermute | solution.py:477
  7.3 11.2 %collective-permute-start.4 = (bf16[4,64,384]{2,1,0:T(8,128)(2,1)S(1)}, bf16[4,64,384]{2,1,0:T(8,128)(2,1)S(1)}, u32[]{:S(2)}, u32[]{:S(2)}) collective-permute-start(bf16[4,64,384]{2,1,0:T(8,128)(2,1)S(1)} %shard_map.120.refs_0_), channel_id=1, source_target_pairs={{0,4},{2,6},{4,0},{6,2},{1,5},{3,7},{5,1},{7,3},{8,12},{10,14},{12... | collective-permute-start | bytes 589832 | tf_op jit(solution)/shard_map/ppermute | solution.py:477
  10.0 11.3 %collective-permute-start.3 = (bf16[4,64,384]{2,1,0:T(8,128)(2,1)S(1)}, bf16[4,64,384]{2,1,0:T(8,128)(2,1)S(1)}, u32[]{:S(2)}, u32[]{:S(2)}) collective-permute-start(bf16[4,64,384]{2,1,0:T(8,128)(2,1)S(1)} %shard_map.120.refs_0_), channel_id=1, source_target_pairs={{0,2},{2,4},{4,6},{6,0},{1,3},{3,5},{5,7},{7,1},{8,10},{10,12},{12... | collective-permute-start | bytes 589832 | tf_op jit(solution)/shard_map/ppermute | solution.py:477
  21.9 13.9 %collective-permute-start.6 = (bf16[4,4,64,384]{3,2,1,0:T(8,128)(2,1)S(1)}, bf16[4,4,64,384]{3,2,1,0:T(8,128)(2,1)S(1)}, u32[]{:S(2)}, u32[]{:S(2)}) collective-permute-start(bf16[4,4,64,384]{3,2,1,0:T(8,128)(2,1)S(1)} %shard_map.121.mine), channel_id=1, source_target_pairs={{0,1},{1,0},{2,3},{3,2},{4,5},{5,4},{6,7},{7,6},{8,9},{9,8},{10,11... | collective-permute-start | bytes 2359304 | tf_op jit(solution)/shard_map/ppermute | solution.py:479
  27.3 57.9 %copy-start.4 = (f32[2,128,128]{2,1,0:T(8,128)}, f32[2,128,128]{2,1,0:T(8,128)S(1)}, u32[]{:S(2)}) copy-start(f32[2,128,128]{2,1,0:T(8,128)S(1)} %get-tuple-element.39.stats) | copy-start | bytes 393220
  27.3 32.7 %copy-start.16 = (f32[3072]{0:T(1024)S(1)}, f32[3072]{0:T(1024)}, u32[]{:S(2)}) copy-start(f32[3072]{0:T(1024)} %param.10) | copy-start | bytes 36868
  27.3 32.7 %copy-start.17 = (f32[3072]{0:T(1024)S(1)}, f32[3072]{0:T(1024)}, u32[]{:S(2)}) copy-start(f32[3072]{0:T(1024)} %param.11) | copy-start | bytes 36868
  27.4 9.3 %collective-permute-start.2 = (bf16[128,2304]{1,0:T(8,128)(2,1)S(1)}, bf16[128,2304]{1,0:T(8,128)(2,1)S(1)}, u32[]{:S(2)}, u32[]{:S(2)}) collective-permute-start(bf16[128,2304]{1,0:T(8,128)(2,1)S(1)} %get-tuple-element.41.v), channel_id=1, source_target_pairs={{8,16},{16,8},{40,48},{48,40},{9,17},{17,9},{41,49},{49,41},{10,18... | collective-permute-start | bytes 1769480 | tf_op jit(solution)/shard_map/ppermute | solution.py:474
  28.2 19.9 %collective-permute-start.1 = (bf16[128,2304]{1,0:T(8,128)(2,1)S(1)}, bf16[128,2304]{1,0:T(8,128)(2,1)S(1)}, u32[]{:S(2)}, u32[]{:S(2)}) collective-permute-start(bf16[128,2304]{1,0:T(8,128)(2,1)S(1)} %get-tuple-element.41.v), channel_id=1, source_target_pairs={{0,16},{24,8},{32,48},{56,40},{1,17},{25,9},{33,49},{57,41},{2,18}... | collective-permute-start | bytes 1769480 | tf_op jit(solution)/shard_map/ppermute | solution.py:473
  34.4 25.6 %collective-permute-start = (bf16[128,2304]{1,0:T(8,128)(2,1)S(1)}, bf16[128,2304]{1,0:T(8,128)(2,1)S(1)}, u32[]{:S(2)}, u32[]{:S(2)}) collective-permute-start(bf16[128,2304]{1,0:T(8,128)(2,1)S(1)} %get-tuple-element.41.v), channel_id=1, source_target_pairs={{0,8},{24,16},{32,40},{56,48},{1,9},{25,17},{33,41},{57,49},{2,10}... | collective-permute-start | bytes 1769480 | tf_op jit(solution)/shard_map/ppermute | solution.py:472
  61.9 22.1 %copy-start.9 = (bf16[128,2304]{1,0:T(8,128)(2,1)}, bf16[128,2304]{1,0:T(8,128)(2,1)S(1)}, u32[]{:S(2)}) copy-start(bf16[128,2304]{1,0:T(8,128)(2,1)S(1)} %get-tuple-element.49.part) | copy-start | bytes 1769476
  61.9 13.0 %copy-start.20 = (f32[4,512]{1,0:T(4,128)S(1)}, f32[4,512]{1,0:T(4,128)}, u32[]{:S(2)}) copy-start(f32[4,512]{1,0:T(4,128)} %mix_bias.1) | copy-start | bytes 24580
  63.2 24.7 %collective-permute-start.12 = (bf16[4,64,768]{2,1,0:T(8,128)(2,1)S(1)}, bf16[4,64,768]{2,1,0:T(8,128)(2,1)S(1)}, u32[]{:S(2)}, u32[]{:S(2)}) collective-permute-start(bf16[4,64,768]{2,1,0:T(8,128)(2,1)S(1)} %get-tuple-element.56), channel_id=1, source_target_pairs={{0,1},{1,0},{2,3},{3,2},{4,5},{5,4},{6,7},{7,6},{8,9},{9,8},{10,11... | collective-permute-start | bytes 1179656 | tf_op jit(solution)/shard_map/ppermute | solution.py:508
  65.1 10.7 %collective-permute-start.9 = (bf16[128,768]{1,0:T(8,128)(2,1)S(1)}, bf16[128,768]{1,0:T(8,128)(2,1)S(1)}, u32[]{:S(2)}, u32[]{:S(2)}) collective-permute-start(bf16[128,768]{1,0:T(8,128)(2,1)S(1)} %get-tuple-element.43.v1.v), channel_id=1, source_target_pairs={{8,16},{16,8},{40,48},{48,40},{9,17},{17,9},{41,49},{49,41},{10,18... | collective-permute-start | bytes 589832 | tf_op jit(solution)/shard_map/ppermute | solution.py:474
  65.8 12.9 %collective-permute-start.8 = (bf16[128,768]{1,0:T(8,128)(2,1)S(1)}, bf16[128,768]{1,0:T(8,128)(2,1)S(1)}, u32[]{:S(2)}, u32[]{:S(2)}) collective-permute-start(bf16[128,768]{1,0:T(8,128)(2,1)S(1)} %get-tuple-element.43.v1.v), channel_id=1, source_target_pairs={{0,16},{24,8},{32,48},{56,40},{1,17},{25,9},{33,49},{57,41},{2,18}... | collective-permute-start | bytes 589832 | tf_op jit(solution)/shard_map/ppermute | solution.py:473
  73.4 8.8 %collective-permute-start.7 = (bf16[128,768]{1,0:T(8,128)(2,1)S(1)}, bf16[128,768]{1,0:T(8,128)(2,1)S(1)}, u32[]{:S(2)}, u32[]{:S(2)}) collective-permute-start(bf16[128,768]{1,0:T(8,128)(2,1)S(1)} %get-tuple-element.43.v1.v), channel_id=1, source_target_pairs={{0,8},{24,16},{32,40},{56,48},{1,9},{25,17},{33,41},{57,49},{2,10}... | collective-permute-start | bytes 589832 | tf_op jit(solution)/shard_map/ppermute | solution.py:472
  75.8 8.2 %copy-start.18 = (f32[128,128]{1,0:T(8,128)}, f32[128,128]{1,0:T(8,128)S(1)}, u32[]{:S(2)}) copy-start(f32[128,128]{1,0:T(8,128)S(1)} %get-tuple-element.44.columns) | copy-start | bytes 196612
  75.8 8.2 %copy-start = (bf16[1,128,3072]{2,1,0:T(8,128)(2,1)S(1)}, bf16[1,128,3072]{2,1,0:T(8,128)(2,1)}, u32[]{:S(2)}) copy-start(bf16[1,128,3072]{2,1,0:T(8,128)(2,1)} %values.5) | copy-start | bytes 2359300
  83.2 2.0 %copy-start.2 = (f32[128,768]{1,0:T(8,128)}, f32[128,768]{1,0:T(8,128)S(1)}, u32[]{:S(2)}) copy-start(f32[128,768]{1,0:T(8,128)S(1)} %get-tuple-element.48.refs_3_.out_v) | copy-start | bytes 1179652
  83.2 2.0 %copy-start.13 = (bf16[128,768]{1,0:T(8,128)(2,1)}, bf16[128,768]{1,0:T(8,128)(2,1)S(1)}, u32[]{:S(2)}) copy-start(bf16[128,768]{1,0:T(8,128)(2,1)S(1)} %get-tuple-element.50.part) | copy-start | bytes 589828
  86.0 6.4 %collective-permute-start.15 = (bf16[5,64,256]{2,1,0:T(8,128)(2,1)S(1)}, bf16[5,64,256]{2,1,0:T(8,128)(2,1)S(1)}, u32[]{:S(2)}, u32[]{:S(2)}) collective-permute-start(bf16[5,64,256]{2,1,0:T(8,128)(2,1)S(1)} %get-tuple-element.67), channel_id=1, source_target_pairs={{0,1},{1,0},{2,3},{3,2},{4,5},{5,4},{6,7},{7,6},{8,9},{9,8},{10,11... | collective-permute-start | bytes 491528 | tf_op jit(solution)/shard_map/ppermute | solution.py:533
  89.2 0.7 copy-start.10
  89.9 10.7 %collective-permute-start.13 = (bf16[2,64,768]{2,1,0:T(8,128)(2,1)}, bf16[2,64,768]{2,1,0:T(8,128)(2,1)}, u32[]{:S(2)}, u32[]{:S(2)}) collective-permute-start(bf16[2,64,768]{2,1,0:T(8,128)(2,1)} %get-tuple-element.58), channel_id=1, source_target_pairs={{0,6},{6,0},{2,4},{4,2},{1,7},{7,1},{3,5},{5,3},{8,14},{14,8},{10,... | collective-permute-start | bytes 589832 | tf_op jit(solution)/shard_map/ppermute | solution.py:517
  92.5 0.7 copy-start.7
  93.2 12.7 %all-to-all-start = ((bf16[4,64,512]{2,1,0:T(8,128)(2,1)}), bf16[4,64,512]{2,1,0:T(8,128)(2,1)}, u32[]{:S(2)}, u32[]{:S(2)}) async-start(bf16[4,64,512]{2,1,0:T(8,128)(2,1)} %copy-done.7), calls=%async_computation | async-start | bytes 524288 | tf_op jit(solution)/shard_map/all_to_all | solution.py:448
  100.7 1.0 copy-start.11
  103.3 0.7 copy-start.14
  103.9 6.8 %collective-permute-start.14 = (bf16[64,768]{1,0:T(8,128)(2,1)}, bf16[64,768]{1,0:T(8,128)(2,1)}, u32[]{:S(2)}, u32[]{:S(2)}) collective-permute-start(bf16[64,768]{1,0:T(8,128)(2,1)} %get-tuple-element.60), channel_id=1, source_target_pairs={{0,2},{2,0},{4,6},{6,4},{1,3},{3,1},{5,7},{7,5},{8,10},{10,8},{12,... | collective-permute-start | bytes 294920 | tf_op jit(solution)/shard_map/ppermute | solution.py:519
  110.8 0.9 copy-start.15
  130.5 0.7 copy-start.8
  131.2 16.8 %all-to-all-start.2 = ((bf16[8,8,1280]{2,1,0:T(8,128)(2,1)}), bf16[8,8,1280]{2,1,0:T(8,128)(2,1)}, u32[]{:S(2)}, u32[]{:S(2)}) async-start(bf16[8,8,1280]{2,1,0:T(8,128)(2,1)} %copy-done.8), calls=%async_computation.2 | async-start | bytes 327680 | tf_op jit(solution)/shard_map/all_to_all | solution.py:448
  138.6 24.3 %collective-permute-start.10 = (bf16[128,2304]{1,0:T(8,128)(2,1)}, bf16[128,2304]{1,0:T(8,128)(2,1)}, u32[]{:S(2)}, u32[]{:S(2)}) collective-permute-start(bf16[128,2304]{1,0:T(8,128)(2,1)} %copy-done.9), channel_id=1, source_target_pairs={{8,0},{16,24},{40,32},{48,56},{9,1},{17,25},{41,33},{49,57},{10,2}... | collective-permute-start | bytes 1769480 | tf_op jit(solution)/shard_map/ppermute | solution.py:496
  148.9 0.7 copy-start.6
  149.7 21.1 %all-to-all-start.3 = ((bf16[8,8,2304]{2,1,0:T(8,128)(2,1)}), bf16[8,8,2304]{2,1,0:T(8,128)(2,1)}, u32[]{:S(2)}, u32[]{:S(2)}) async-start(bf16[8,8,2304]{2,1,0:T(8,128)(2,1)} %copy-done.6), calls=%async_computation.3 | async-start | bytes 589824 | tf_op jit(solution)/shard_map/all_to_all | solution.py:448
  155.1 7.8 %collective-permute-start.11 = (bf16[128,768]{1,0:T(8,128)(2,1)}, bf16[128,768]{1,0:T(8,128)(2,1)S(1)}, u32[]{:S(2)}, u32[]{:S(2)}) collective-permute-start(bf16[128,768]{1,0:T(8,128)(2,1)} %copy-done.13), channel_id=1, source_target_pairs={{8,0},{16,24},{40,32},{48,56},{9,1},{17,25},{41,33},{49,57},{10,2}... | collective-permute-start | bytes 589832 | tf_op jit(solution)/shard_map/ppermute | solution.py:496
  162.8 1.1 copy-start.1
  164.0 1.0 copy-start.3
  165.0 0.9 copy-start.5
  165.9 0.8 copy-start.19

commit v5 on v4

--- a/solution.py
+++ b/solution.py
@@ -324,33 +324,41 @@
     send[...] = (keep[1 - b] + got[1 - b].astype(F32)).astype(BF16)
 
 
-def last_chip_kernel(keep, small, got, out):
+def last_chip_kernel(place, keep, small, got, own, total, send):
     extra = small[...] + (got[4, :, :128].astype(F32) + got[4, :, 128:].astype(F32))
     high, low = split(extra)
-    for b in range(4):
-        out[b, :, :256] = (keep[b] + got[b].astype(F32)).astype(BF16)
-        out[b, :, 256:384] = high
-        out[b, :, 384:512] = low
-
-
-def deal_kernel(own, other, got1, out):
-    def total_of(parts, lanes):
-        total = parts[0][:, lanes].astype(F32)
-        for part in parts[1:]:
-            total = total + part[:, lanes].astype(F32)
-        return total
-
-    got0 = (own, other)
-    got1 = [got1.at[k] for k in range(4)]
-
+    total[...] = extra
+    send[2, :, :128] = high
+    send[2, :, 128:] = low
+    near = place[1] // 2 * 2
+    for k in range(2):
+        own[k] = keep[near + k] + got[near + k].astype(F32)
+        other = 2 - near + k
+        send[k] = (keep[other] + got[other].astype(F32)).astype(BF16)
+
+
+def last_pair_kernel(place, keep, small, got, own, total, send):
+    extra = small[...] + (got[2, :, :128].astype(F32) + got[2, :, 128:].astype(F32))
+    high, low = split(extra)
+    total[...] = extra
+    send[1, :, :128] = high
+    send[1, :, 128:] = low
+    b = place[1] % 2
+    own[...] = keep[b] + got[b].astype(F32)
+    send[0] = (keep[1 - b] + got[1 - b].astype(F32)).astype(BF16)
+
+
+def deal_kernel(own0, got0, own1, small, got1, out):
     def put(lane, block):
         for z in range(8):
             out[z, :, lane : lane + block.shape[1]] = block[z * 8 : (z + 1) * 8]
 
+    first = (own0[...] + got0[...].astype(F32)).astype(BF16)
+    last = (own1[...] + got1[0].astype(F32)).astype(BF16)
     for slot in range(2):
-        put(slot * 512, total_of(got0, slice(slot * 384, (slot + 1) * 384)).astype(BF16))
-        put(slot * 512 + 384, total_of(got1, slice(slot * 128, (slot + 1) * 128)).astype(BF16))
-    high, low = split(total_of(got1, slice(256, 384)) + total_of(got1, slice(384, 512)))
+        put(slot * 512, first[:, slot * 384 : (slot + 1) * 384])
+        put(slot * 512 + 384, last[:, slot * 128 : (slot + 1) * 128])
+    high, low = split(small[...] + (got1[1, :, :128].astype(F32) + got1[1, :, 128:].astype(F32)))
     put(1024, high)
     put(1152, low)
 
@@ -478,9 +486,7 @@
     mine = call(join_kernel, shape((4, GROUPS, SEG, 3 * ROWS), BF16), (place, *slabs))
     theirs = lax.ppermute(mine, CORE, PARTNER)
     columns, bias_term = call(
-        side_kernel,
-        [shape((ROWS, ROWS), F32), shape((64, 128), F32)],
-        (place, us[0], vs[0], us[1], vs[1], mix_bias),
+        side_kernel, [shape((ROWS, ROWS), F32), shape((64, 128), F32)], (place, us[0], vs[0], us[1], vs[1], mix_bias)
     )
     weights = call(weight_kernel, shape((GROUPS, 2 * ROWS, 3 * ROWS), BF16), (place, mine, theirs))
 
@@ -506,11 +512,7 @@
         sends.append(send)
 
     folded = lax.ppermute(sends[0], CORE, PARTNER)
-    keep, send = call(
-        chip_kernel,
-        [shape((2, SEG, 768), F32), shape((2, SEG, 768), BF16)],
-        (place, keeps[0], folded),
-    )
+    keep, send = call(chip_kernel, [shape((2, SEG, 768), F32), shape((2, SEG, 768), BF16)], (place, keeps[0], folded))
     own, send = call(
         chip_pair_kernel,
         [shape((SEG, 768), F32), shape((SEG, 768), BF16)],
@@ -527,13 +529,14 @@
         [shape((64, 128), F32), shape((5, SEG, 2 * ROWS), BF16)],
         (place, values_in, stats, sums, outs_u[1], outs_v[1], parts[1], near[1], sends[1]),
     )
-    last = call(
-        last_chip_kernel,
-        shape((4, SEG, 512), BF16),
-        (keeps[1], small, lax.ppermute(last, CORE, PARTNER)),
-        0,
-    )
-    dealt = call(deal_kernel, shape((8, 8, 1280), BF16), (*chip, exchanged(last, X)), 0)
+    half_terms = [shape((2, SEG, 256), F32), shape((64, 128), F32), shape((3, SEG, 256), BF16)]
+    own, small, send = call(last_chip_kernel, half_terms, (place, keeps[1], small, lax.ppermute(last, CORE, PARTNER)))
+    own, small, send = call(
+        last_pair_kernel,
+        [shape((SEG, 256), F32), shape((64, 128), F32), shape((2, SEG, 256), BF16)],
+        (place, own, small, lax.ppermute(send, X, ACROSS)),
+    )
+    dealt = call(deal_kernel, shape((8, 8, 1280), BF16), (*chip, own, small, lax.ppermute(send, X, WITHIN)), 0)
     added = call(add_kernel, shape((8, 8, 1280), BF16), (exchanged(dealt, Z),), 0)
     placed = call(place_kernel, shape((8, 8, 2304), BF16), (exchanged(added, Y),), 0)
     grad_mix, grad_bias, grad_gain, grad_shift = call(

time: 174 us -> 171 us (0.983)
  the two profiles are of different devices: /device:TPU:64 before, /device:TPU:2 now
where the time goes in v5:
time: 171 us; the launch traced here: 170 us
  starting transfers between devices  63.8 us (37%)
  waiting for transfers between devices  55.3 us (32%)
  Pallas kernels  22.9 us (13%)
  blocking collectives  19.5 us (11%)
  local copies, waits for them, and re-layouts  6.88 us (4%)
    pallas_call x20, Pallas kernels, call(): pl.pallas_call(kernel, out_shape=out_shape, in_specs=[SMEM] * scalars + [...  22.9 us
    all_to_all x1, blocking collectives, exchanged(): return lax.all_to_all(x, axis, split_axis=0, concat_axis=0, tiled=True)  19.5 us
    ppermute x2, waiting for transfers between devices, compute(): near.append(lax.ppermute(vs[i], Y, NEAR))  15.3 us
    ppermute x2, waiting for transfers between devices, compute(): far.append(lax.ppermute(vs[i], Y, FAR))  13.7 us
    ppermute x3, starting transfers between devices, compute(): slabs = [slab] + [lax.ppermute(slab, X, CHIPS[k]) for k in range(1, 4)]  13.1 us
    ppermute x2, starting transfers between devices, compute(): far.append(lax.ppermute(vs[i], Y, FAR))  12.9 us
    all_to_all x2, starting transfers between devices, exchanged(): return lax.all_to_all(x, axis, split_axis=0, concat_axis=0, tiled=True)  11.4 us
    all_to_all x2, waiting for transfers between devices, exchanged(): return lax.all_to_all(x, axis, split_axis=0, concat_axis=0, tiled=True)  8.13 us
  transfers between devices with their start and end apart: 20, of which 10 were waited for; matrix products, arithmetic and copies ran while one was open for 0% of the time, Pallas kernels for 10%

profile of v5, /device:TPU:2, one launch (start us, length us, event | category | flops | bytes accessed | tf_op | source)
XLA Modules:
  0.0 169.6 jit_solution(8123163790398707892)
XLA Ops:
  0.6 0.1 pad_add_fusion.place
  0.7 0.9 copy-done.9
  1.7 1.0 shard_map.120.refs_0_
  2.6 7.8 %collective-permute-start.5 = (bf16[4,64,384]{2,1,0:T(8,128)(2,1)S(1)}, bf16[4,64,384]{2,1,0:T(8,128)(2,1)S(1)}, u32[]{:S(2)}, u32[]{:S(2)}) collective-permute-start(bf16[4,64,384]{2,1,0:T(8,128)(2,1)S(1)} %shard_map.120.refs_0_), channel_id=1, source_target_pairs={{0,6},{2,0},{4,2},{6,4},{1,7},{3,1},{5,3},{7,5},{8,14},{10,8},{12,... | collective-permute-start | bytes 589832 | tf_op jit(solution)/shard_map/ppermute | solution.py:485
  10.4 1.9 %collective-permute-start.4 = (bf16[4,64,384]{2,1,0:T(8,128)(2,1)S(1)}, bf16[4,64,384]{2,1,0:T(8,128)(2,1)S(1)}, u32[]{:S(2)}, u32[]{:S(2)}) collective-permute-start(bf16[4,64,384]{2,1,0:T(8,128)(2,1)S(1)} %shard_map.120.refs_0_), channel_id=1, source_target_pairs={{0,4},{2,6},{4,0},{6,2},{1,5},{3,7},{5,1},{7,3},{8,12},{10,14},{12... | collective-permute-start | bytes 589832 | tf_op jit(solution)/shard_map/ppermute | solution.py:485
  12.4 3.4 %collective-permute-start.3 = (bf16[4,64,384]{2,1,0:T(8,128)(2,1)S(1)}, bf16[4,64,384]{2,1,0:T(8,128)(2,1)S(1)}, u32[]{:S(2)}, u32[]{:S(2)}) collective-permute-start(bf16[4,64,384]{2,1,0:T(8,128)(2,1)S(1)} %shard_map.120.refs_0_), channel_id=1, source_target_pairs={{0,2},{2,4},{4,6},{6,0},{1,3},{3,5},{5,7},{7,1},{8,10},{10,12},{12... | collective-permute-start | bytes 589832 | tf_op jit(solution)/shard_map/ppermute | solution.py:485
  15.7 3.8 %collective-permute-done.4.refs_2_ = bf16[4,64,384]{2,1,0:T(8,128)(2,1)S(1)} collective-permute-done((bf16[4,64,384]{2,1,0:T(8,128)(2,1)S(1)}, bf16[4,64,384]{2,1,0:T(8,128)(2,1)S(1)}, u32[]{:S(2)}, u32[]{:S(2)}) %collective-permute-start.4) | collective-permute-done | bytes 196640 | tf_op jit(solution)/shard_map/ppermute | solution.py:485
  19.5 0.4 collective-permute-done.3.refs_1_
  19.9 0.6 shard_map.121.mine
  20.5 1.9 %collective-permute-start.6 = (bf16[4,4,64,384]{3,2,1,0:T(8,128)(2,1)S(1)}, bf16[4,4,64,384]{3,2,1,0:T(8,128)(2,1)S(1)}, u32[]{:S(2)}, u32[]{:S(2)}) collective-permute-start(bf16[4,4,64,384]{3,2,1,0:T(8,128)(2,1)S(1)} %shard_map.121.mine), channel_id=1, source_target_pairs={{0,1},{1,0},{2,3},{3,2},{4,5},{5,4},{6,7},{7,6},{8,9},{9,8},{10,11... | collective-permute-start | bytes 2359304 | tf_op jit(solution)/shard_map/ppermute | solution.py:487
  22.5 3.5 %shard_map.118 = (bf16[128,2304]{1,0:T(8,128)(2,1)S(1)}, bf16[128,768]{1,0:T(8,128)(2,1)S(1)}, bf16[128,2304]{1,0:T(8,128)(2,1)S(1)}, bf16[128,768]{1,0:T(8,128)(2,1)S(1)}, f32[2,128,128]{2,1,0:T(8,128)S(1)}) custom-call(s32[3]{0:T(128)S(1)} %pad_add_fusion.place, bf16[1,128,3072]{2,1,0:T(8,128)(2,1)} %values.5, bf16[1,128,3072]{2,1,0:T(8,128)(2,1)} %gated_in.1, ...), custom_call_target="tpu_custom_call" | custom-call | tf_op jit(solution)/shard_map/pallas_call | solution.py:51
  26.0 0.0 copy-start.11
  26.0 0.0 copy-start.12
  26.0 0.8 collective-permute-start.2
  26.8 5.4 %collective-permute-start.1 = (bf16[128,2304]{1,0:T(8,128)(2,1)S(1)}, bf16[128,2304]{1,0:T(8,128)(2,1)S(1)}, u32[]{:S(2)}, u32[]{:S(2)}) collective-permute-start(bf16[128,2304]{1,0:T(8,128)(2,1)S(1)} %get-tuple-element.47.v), channel_id=1, source_target_pairs={{0,16},{24,8},{32,48},{56,40},{1,17},{25,9},{33,49},{57,41},{2,18}... | collective-permute-start | bytes 1769480 | tf_op jit(solution)/shard_map/ppermute | solution.py:481
  32.2 1.4 collective-permute-start
  33.6 0.9 shard_map.122.weights
  34.5 11.4 %collective-permute-done.1.far = bf16[128,2304]{1,0:T(8,128)(2,1)S(1)} collective-permute-done((bf16[128,2304]{1,0:T(8,128)(2,1)S(1)}, bf16[128,2304]{1,0:T(8,128)(2,1)S(1)}, u32[]{:S(2)}, u32[]{:S(2)}) %collective-permute-start.1) | collective-permute-done | bytes 589856 | tf_op jit(solution)/shard_map/ppermute | solution.py:481
  45.9 11.9 %collective-permute-done.near = bf16[128,2304]{1,0:T(8,128)(2,1)S(1)} collective-permute-done((bf16[128,2304]{1,0:T(8,128)(2,1)S(1)}, bf16[128,2304]{1,0:T(8,128)(2,1)S(1)}, u32[]{:S(2)}, u32[]{:S(2)}) %collective-permute-start) | collective-permute-done | bytes 589856 | tf_op jit(solution)/shard_map/ppermute | solution.py:480
  57.8 1.9 %shard_map.123 = (bf16[128,2304]{1,0:T(8,128)(2,1)S(1)}, f32[128,2304]{1,0:T(8,128)S(1)}, f32[128,2304]{1,0:T(8,128)S(1)}, bf16[128,2304]{1,0:T(8,128)(2,1)S(1)}, bf16[128,2304]{1,0:T(8,128)(2,1)S(1)}) custom-call(s32[3]{0:T(128)S(1)} %pad_add_fusion.place, bf16[128,2304]{1,0:T(8,128)(2,1)S(1)} %get-tuple-element.46.u, ...), custom_call_target="tpu_custom_call" | custom-call | tf_op jit(solution)/shard_map/pallas_call | solution.py:51
  59.7 0.0 copy-start.8
  59.7 0.0 copy-start.15
  59.7 1.3 shard_map.126
  61.0 1.9 %collective-permute-start.12 = (bf16[4,64,768]{2,1,0:T(8,128)(2,1)S(1)}, bf16[4,64,768]{2,1,0:T(8,128)(2,1)S(1)}, u32[]{:S(2)}, u32[]{:S(2)}) collective-permute-start(bf16[4,64,768]{2,1,0:T(8,128)(2,1)S(1)} %get-tuple-element.62), channel_id=1, source_target_pairs={{0,1},{1,0},{2,3},{3,2},{4,5},{5,4},{6,7},{7,6},{8,9},{9,8},{10,11... | collective-permute-start | bytes 1179656 | tf_op jit(solution)/shard_map/ppermute | solution.py:514
  62.9 0.7 collective-permute-start.9
  63.6 7.6 %collective-permute-start.8 = (bf16[128,768]{1,0:T(8,128)(2,1)S(1)}, bf16[128,768]{1,0:T(8,128)(2,1)S(1)}, u32[]{:S(2)}, u32[]{:S(2)}) collective-permute-start(bf16[128,768]{1,0:T(8,128)(2,1)S(1)} %get-tuple-element.49.v1.v), channel_id=1, source_target_pairs={{0,16},{24,8},{32,48},{56,40},{1,17},{25,9},{33,49},{57,41},{2,18}... | collective-permute-start | bytes 589832 | tf_op jit(solution)/shard_map/ppermute | solution.py:481
  71.2 1.5 collective-permute-start.7
  72.7 0.9 shard_map.119
  73.5 0.6 copy-done.13
  74.2 2.3 %collective-permute-done.8.far = bf16[128,768]{1,0:T(8,128)(2,1)S(1)} collective-permute-done((bf16[128,768]{1,0:T(8,128)(2,1)S(1)}, bf16[128,768]{1,0:T(8,128)(2,1)S(1)}, u32[]{:S(2)}, u32[]{:S(2)}) %collective-permute-start.8) | collective-permute-done | bytes 196640 | tf_op jit(solution)/shard_map/ppermute | solution.py:481
  76.5 3.5 %collective-permute-done.7.near = bf16[128,768]{1,0:T(8,128)(2,1)S(1)} collective-permute-done((bf16[128,768]{1,0:T(8,128)(2,1)S(1)}, bf16[128,768]{1,0:T(8,128)(2,1)S(1)}, u32[]{:S(2)}, u32[]{:S(2)}) %collective-permute-start.7) | collective-permute-done | bytes 196640 | tf_op jit(solution)/shard_map/ppermute | solution.py:480
  79.9 1.0 shard_map.124
  80.9 0.0 copy-start.2
  80.9 0.0 copy-start.10
  81.0 0.8 shard_map.129
  81.8 1.1 shard_map.130.before
  83.0 0.7 shard_map.131
  83.7 1.9 %collective-permute-start.15 = (bf16[5,64,256]{2,1,0:T(8,128)(2,1)S(1)}, bf16[5,64,256]{2,1,0:T(8,128)(2,1)S(1)}, u32[]{:S(2)}, u32[]{:S(2)}) collective-permute-start(bf16[5,64,256]{2,1,0:T(8,128)(2,1)S(1)} %get-tuple-element.73), channel_id=1, source_target_pairs={{0,1},{1,0},{2,3},{3,2},{4,5},{5,4},{6,7},{7,6},{8,9},{9,8},{10,11... | collective-permute-start | bytes 491528 | tf_op jit(solution)/shard_map/ppermute | solution.py:533
  85.6 0.6 shard_map.127
  86.3 3.4 %collective-permute-start.13 = (bf16[2,64,768]{2,1,0:T(8,128)(2,1)S(1)}, bf16[2,64,768]{2,1,0:T(8,128)(2,1)S(1)}, u32[]{:S(2)}, u32[]{:S(2)}) collective-permute-start(bf16[2,64,768]{2,1,0:T(8,128)(2,1)S(1)} %get-tuple-element.64), channel_id=1, source_target_pairs={{0,6},{6,0},{2,4},{4,2},{1,7},{7,1},{3,5},{5,3},{8,14},{14,8},{10,... | collective-permute-start | bytes 589832 | tf_op jit(solution)/shard_map/ppermute | solution.py:519
  89.7 0.6 shard_map.132
  90.3 2.4 %collective-permute-start.16 = (bf16[3,64,256]{2,1,0:T(8,128)(2,1)S(1)}, bf16[3,64,256]{2,1,0:T(8,128)(2,1)S(1)}, u32[]{:S(2)}, u32[]{:S(2)}) collective-permute-start(bf16[3,64,256]{2,1,0:T(8,128)(2,1)S(1)} %get-tuple-element.76), channel_id=1, source_target_pairs={{0,6},{6,0},{2,4},{4,2},{1,7},{7,1},{3,5},{5,3},{8,14},{14,8},{10,... | collective-permute-start | bytes 294920 | tf_op jit(solution)/shard_map/ppermute | solution.py:537
  92.7 3.2 %collective-permute-done.13.got = bf16[2,64,768]{2,1,0:T(8,128)(2,1)S(1)} collective-permute-done((bf16[2,64,768]{2,1,0:T(8,128)(2,1)S(1)}, bf16[2,64,768]{2,1,0:T(8,128)(2,1)S(1)}, u32[]{:S(2)}, u32[]{:S(2)}) %collective-permute-start.13) | collective-permute-done | bytes 196640 | tf_op jit(solution)/shard_map/ppermute | solution.py:519
  95.9 0.6 shard_map.128
  96.5 5.8 %collective-permute-start.14 = (bf16[64,768]{1,0:T(8,128)(2,1)S(1)}, bf16[64,768]{1,0:T(8,128)(2,1)S(1)}, u32[]{:S(2)}, u32[]{:S(2)}) collective-permute-start(bf16[64,768]{1,0:T(8,128)(2,1)S(1)} %get-tuple-element.66), channel_id=1, source_target_pairs={{0,2},{2,0},{4,6},{6,4},{1,3},{3,1},{5,7},{7,5},{8,10},{10,8},{12,... | collective-permute-start | bytes 294920 | tf_op jit(solution)/shard_map/ppermute | solution.py:521
  102.4 0.6 shard_map.133
  103.0 1.9 %collective-permute-start.17 = (bf16[2,64,256]{2,1,0:T(8,128)(2,1)S(1)}, bf16[2,64,256]{2,1,0:T(8,128)(2,1)S(1)}, u32[]{:S(2)}, u32[]{:S(2)}) collective-permute-start(bf16[2,64,256]{2,1,0:T(8,128)(2,1)S(1)} %get-tuple-element.79), channel_id=1, source_target_pairs={{0,2},{2,0},{4,6},{6,4},{1,3},{3,1},{5,7},{7,5},{8,10},{10,8},{12,... | collective-permute-start | bytes 196616 | tf_op jit(solution)/shard_map/ppermute | solution.py:539
  104.9 4.2 %collective-permute-done.17.got1 = bf16[2,64,256]{2,1,0:T(8,128)(2,1)S(1)} collective-permute-done((bf16[2,64,256]{2,1,0:T(8,128)(2,1)S(1)}, bf16[2,64,256]{2,1,0:T(8,128)(2,1)S(1)}, u32[]{:S(2)}, u32[]{:S(2)}) %collective-permute-start.17) | collective-permute-done | bytes 65568 | tf_op jit(solution)/shard_map/ppermute | solution.py:539
  109.2 19.5 %all_to_all.15.got = bf16[8,8,1280]{2,1,0:T(8,128)(2,1)S(1)} all-to-all(bf16[8,8,1280]{2,1,0:T(8,128)(2,1)S(1)} %shard_map.134), channel_id=1, replica_groups=mesh['sp_0'=8,'sp_1'=8,'dp_0'=4,'dp_1'=2] {'sp_0'}, dimensions={0} | all-to-all | bytes 327680 | tf_op jit(solution)/shard_map/all_to_all | solution.py:456
  128.7 0.7 copy-done.7
  129.4 7.4 %all-to-all-start.1 = ((bf16[8,8,1280]{2,1,0:T(8,128)(2,1)}), bf16[8,8,1280]{2,1,0:T(8,128)(2,1)}, u32[]{:S(2)}, u32[]{:S(2)}) async-start(bf16[8,8,1280]{2,1,0:T(8,128)(2,1)} %copy-done.7), calls=%async_computation.1 | async-start | bytes 327680 | tf_op jit(solution)/shard_map/all_to_all | solution.py:456
  136.8 1.3 collective-permute-start.10
  138.1 8.1 %all-to-all-done.1.got = bf16[8,8,1280]{2,1,0:T(8,128)(2,1)} async-done(((bf16[8,8,1280]{2,1,0:T(8,128)(2,1)}), bf16[8,8,1280]{2,1,0:T(8,128)(2,1)}, u32[]{:S(2)}, u32[]{:S(2)}) %all-to-all-start.1) | async-done | bytes 163872 | tf_op jit(solution)/shard_map/all_to_all | solution.py:456
  146.2 1.0 shard_map.136
  147.2 0.7 copy-done.6
  147.9 4.1 %all-to-all-start.2 = ((bf16[8,8,2304]{2,1,0:T(8,128)(2,1)}), bf16[8,8,2304]{2,1,0:T(8,128)(2,1)}, u32[]{:S(2)}, u32[]{:S(2)}) async-start(bf16[8,8,2304]{2,1,0:T(8,128)(2,1)} %copy-done.6), calls=%async_computation.2 | async-start | bytes 589824 | tf_op jit(solution)/shard_map/all_to_all | solution.py:456
  151.9 1.3 collective-permute-start.11
  153.2 6.5 %collective-permute-done.11.refs_5_ = bf16[128,768]{1,0:T(8,128)(2,1)S(1)} collective-permute-done((bf16[128,768]{1,0:T(8,128)(2,1)}, bf16[128,768]{1,0:T(8,128)(2,1)S(1)}, u32[]{:S(2)}, u32[]{:S(2)}) %collective-permute-start.11) | collective-permute-done | bytes 196640 | tf_op jit(solution)/shard_map/ppermute | solution.py:502
  159.7 1.1 copy-done.1
  160.9 1.0 copy-done.3
  161.9 0.9 copy-done.5
  162.8 0.8 copy-done.14
  163.6 4.1 %shard_map.125 = (bf16[1,128,3072]{2,1,0:T(8,128)(2,1)}, bf16[1,128,3072]{2,1,0:T(8,128)(2,1)}) custom-call(s32[3]{0:T(128)S(1)} %pad_add_fusion.place, bf16[1,128,3072]{2,1,0:T(8,128)(2,1)S(1)} %copy-done, bf16[1,128,3072]{2,1,0:T(8,128)(2,1)S(1)} %copy-done.1, f32[2,128,128]{2,1,0:T(8,128)S(1)} %copy-done.5, f32[128,128]{1,0:T(8,128)S(1)} %copy-done.14, ...), custom_call_target="tpu_custom_call" | custom-call | tf_op jit(solution)/shard_map/pallas_call | solution.py:51
  167.7 1.9 %shard_map.137 = (f32[64,4,512]{2,1,0:T(4,128)}, f32[4,512]{1,0:T(4,128)}, f32[24,128]{1,0:T(8,128)}, f32[24,128]{1,0:T(8,128)}) custom-call(bf16[8,8,2304]{2,1,0:T(8,128)(2,1)} %all-to-all-done.2.got), custom_call_target="tpu_custom_call" | custom-call | tf_op jit(solution)/shard_map/pallas_call | solution.py:51
  (30 shorter events, 0.1 us)
Async XLA Ops:
  0.7 1.0 copy-start.9
  2.6 13.1 %collective-permute-start.5 = (bf16[4,64,384]{2,1,0:T(8,128)(2,1)S(1)}, bf16[4,64,384]{2,1,0:T(8,128)(2,1)S(1)}, u32[]{:S(2)}, u32[]{:S(2)}) collective-permute-start(bf16[4,64,384]{2,1,0:T(8,128)(2,1)S(1)} %shard_map.120.refs_0_), channel_id=1, source_target_pairs={{0,6},{2,0},{4,2},{6,4},{1,7},{3,1},{5,3},{7,5},{8,14},{10,8},{12,... | collective-permute-start | bytes 589832 | tf_op jit(solution)/shard_map/ppermute | solution.py:485
  10.4 9.1 %collective-permute-start.4 = (bf16[4,64,384]{2,1,0:T(8,128)(2,1)S(1)}, bf16[4,64,384]{2,1,0:T(8,128)(2,1)S(1)}, u32[]{:S(2)}, u32[]{:S(2)}) collective-permute-start(bf16[4,64,384]{2,1,0:T(8,128)(2,1)S(1)} %shard_map.120.refs_0_), channel_id=1, source_target_pairs={{0,4},{2,6},{4,0},{6,2},{1,5},{3,7},{5,1},{7,3},{8,12},{10,14},{12... | collective-permute-start | bytes 589832 | tf_op jit(solution)/shard_map/ppermute | solution.py:485
  12.4 7.6 %collective-permute-start.3 = (bf16[4,64,384]{2,1,0:T(8,128)(2,1)S(1)}, bf16[4,64,384]{2,1,0:T(8,128)(2,1)S(1)}, u32[]{:S(2)}, u32[]{:S(2)}) collective-permute-start(bf16[4,64,384]{2,1,0:T(8,128)(2,1)S(1)} %shard_map.120.refs_0_), channel_id=1, source_target_pairs={{0,2},{2,4},{4,6},{6,0},{1,3},{3,5},{5,7},{7,1},{8,10},{10,12},{12... | collective-permute-start | bytes 589832 | tf_op jit(solution)/shard_map/ppermute | solution.py:485
  20.5 13.1 %collective-permute-start.6 = (bf16[4,4,64,384]{3,2,1,0:T(8,128)(2,1)S(1)}, bf16[4,4,64,384]{3,2,1,0:T(8,128)(2,1)S(1)}, u32[]{:S(2)}, u32[]{:S(2)}) collective-permute-start(bf16[4,4,64,384]{3,2,1,0:T(8,128)(2,1)S(1)} %shard_map.121.mine), channel_id=1, source_target_pairs={{0,1},{1,0},{2,3},{3,2},{4,5},{5,4},{6,7},{7,6},{8,9},{9,8},{10,11... | collective-permute-start | bytes 2359304 | tf_op jit(solution)/shard_map/ppermute | solution.py:487
  26.0 57.0 %copy-start.4 = (f32[2,128,128]{2,1,0:T(8,128)}, f32[2,128,128]{2,1,0:T(8,128)S(1)}, u32[]{:S(2)}) copy-start(f32[2,128,128]{2,1,0:T(8,128)S(1)} %get-tuple-element.45.stats) | copy-start | bytes 393220
  26.0 31.8 %copy-start.11 = (f32[3072]{0:T(1024)S(1)}, f32[3072]{0:T(1024)}, u32[]{:S(2)}) copy-start(f32[3072]{0:T(1024)} %param.10) | copy-start | bytes 36868
  26.0 31.8 %copy-start.12 = (f32[3072]{0:T(1024)S(1)}, f32[3072]{0:T(1024)}, u32[]{:S(2)}) copy-start(f32[3072]{0:T(1024)} %param.11) | copy-start | bytes 36868
  26.0 8.5 %collective-permute-start.2 = (bf16[128,2304]{1,0:T(8,128)(2,1)S(1)}, bf16[128,2304]{1,0:T(8,128)(2,1)S(1)}, u32[]{:S(2)}, u32[]{:S(2)}) collective-permute-start(bf16[128,2304]{1,0:T(8,128)(2,1)S(1)} %get-tuple-element.47.v), channel_id=1, source_target_pairs={{8,16},{16,8},{40,48},{48,40},{9,17},{17,9},{41,49},{49,41},{10,18... | collective-permute-start | bytes 1769480 | tf_op jit(solution)/shard_map/ppermute | solution.py:482
  26.8 19.1 %collective-permute-start.1 = (bf16[128,2304]{1,0:T(8,128)(2,1)S(1)}, bf16[128,2304]{1,0:T(8,128)(2,1)S(1)}, u32[]{:S(2)}, u32[]{:S(2)}) collective-permute-start(bf16[128,2304]{1,0:T(8,128)(2,1)S(1)} %get-tuple-element.47.v), channel_id=1, source_target_pairs={{0,16},{24,8},{32,48},{56,40},{1,17},{25,9},{33,49},{57,41},{2,18}... | collective-permute-start | bytes 1769480 | tf_op jit(solution)/shard_map/ppermute | solution.py:481
  32.2 25.6 %collective-permute-start = (bf16[128,2304]{1,0:T(8,128)(2,1)S(1)}, bf16[128,2304]{1,0:T(8,128)(2,1)S(1)}, u32[]{:S(2)}, u32[]{:S(2)}) collective-permute-start(bf16[128,2304]{1,0:T(8,128)(2,1)S(1)} %get-tuple-element.47.v), channel_id=1, source_target_pairs={{0,8},{24,16},{32,40},{56,48},{1,9},{25,17},{33,41},{57,49},{2,10}... | collective-permute-start | bytes 1769480 | tf_op jit(solution)/shard_map/ppermute | solution.py:480
  59.7 22.1 %copy-start.8 = (bf16[128,2304]{1,0:T(8,128)(2,1)}, bf16[128,2304]{1,0:T(8,128)(2,1)S(1)}, u32[]{:S(2)}) copy-start(bf16[128,2304]{1,0:T(8,128)(2,1)S(1)} %get-tuple-element.55.part) | copy-start | bytes 1769476
  59.7 13.0 %copy-start.15 = (f32[4,512]{1,0:T(4,128)S(1)}, f32[4,512]{1,0:T(4,128)}, u32[]{:S(2)}) copy-start(f32[4,512]{1,0:T(4,128)} %mix_bias.1) | copy-start | bytes 24580
  61.0 24.7 %collective-permute-start.12 = (bf16[4,64,768]{2,1,0:T(8,128)(2,1)S(1)}, bf16[4,64,768]{2,1,0:T(8,128)(2,1)S(1)}, u32[]{:S(2)}, u32[]{:S(2)}) collective-permute-start(bf16[4,64,768]{2,1,0:T(8,128)(2,1)S(1)} %get-tuple-element.62), channel_id=1, source_target_pairs={{0,1},{1,0},{2,3},{3,2},{4,5},{5,4},{6,7},{7,6},{8,9},{9,8},{10,11... | collective-permute-start | bytes 1179656 | tf_op jit(solution)/shard_map/ppermute | solution.py:514
  62.9 11.3 %collective-permute-start.9 = (bf16[128,768]{1,0:T(8,128)(2,1)S(1)}, bf16[128,768]{1,0:T(8,128)(2,1)S(1)}, u32[]{:S(2)}, u32[]{:S(2)}) collective-permute-start(bf16[128,768]{1,0:T(8,128)(2,1)S(1)} %get-tuple-element.49.v1.v), channel_id=1, source_target_pairs={{8,16},{16,8},{40,48},{48,40},{9,17},{17,9},{41,49},{49,41},{10,18... | collective-permute-start | bytes 589832 | tf_op jit(solution)/shard_map/ppermute | solution.py:482
  63.6 12.9 %collective-permute-start.8 = (bf16[128,768]{1,0:T(8,128)(2,1)S(1)}, bf16[128,768]{1,0:T(8,128)(2,1)S(1)}, u32[]{:S(2)}, u32[]{:S(2)}) collective-permute-start(bf16[128,768]{1,0:T(8,128)(2,1)S(1)} %get-tuple-element.49.v1.v), channel_id=1, source_target_pairs={{0,16},{24,8},{32,48},{56,40},{1,17},{25,9},{33,49},{57,41},{2,18}... | collective-permute-start | bytes 589832 | tf_op jit(solution)/shard_map/ppermute | solution.py:481
  71.2 8.8 %collective-permute-start.7 = (bf16[128,768]{1,0:T(8,128)(2,1)S(1)}, bf16[128,768]{1,0:T(8,128)(2,1)S(1)}, u32[]{:S(2)}, u32[]{:S(2)}) collective-permute-start(bf16[128,768]{1,0:T(8,128)(2,1)S(1)} %get-tuple-element.49.v1.v), channel_id=1, source_target_pairs={{0,8},{24,16},{32,40},{56,48},{1,9},{25,17},{33,41},{57,49},{2,10}... | collective-permute-start | bytes 589832 | tf_op jit(solution)/shard_map/ppermute | solution.py:480
  73.5 0.6 copy-start.13
  74.2 7.6 %copy-start = (bf16[1,128,3072]{2,1,0:T(8,128)(2,1)S(1)}, bf16[1,128,3072]{2,1,0:T(8,128)(2,1)}, u32[]{:S(2)}) copy-start(bf16[1,128,3072]{2,1,0:T(8,128)(2,1)} %values.5) | copy-start | bytes 2359300
  80.9 2.0 %copy-start.2 = (f32[128,768]{1,0:T(8,128)}, f32[128,768]{1,0:T(8,128)S(1)}, u32[]{:S(2)}) copy-start(f32[128,768]{1,0:T(8,128)S(1)} %get-tuple-element.54.refs_3_.out_v) | copy-start | bytes 1179652
  80.9 2.0 %copy-start.10 = (bf16[128,768]{1,0:T(8,128)(2,1)}, bf16[128,768]{1,0:T(8,128)(2,1)S(1)}, u32[]{:S(2)}) copy-start(bf16[128,768]{1,0:T(8,128)(2,1)S(1)} %get-tuple-element.56.part) | copy-start | bytes 589828
  83.7 6.0 %collective-permute-start.15 = (bf16[5,64,256]{2,1,0:T(8,128)(2,1)S(1)}, bf16[5,64,256]{2,1,0:T(8,128)(2,1)S(1)}, u32[]{:S(2)}, u32[]{:S(2)}) collective-permute-start(bf16[5,64,256]{2,1,0:T(8,128)(2,1)S(1)} %get-tuple-element.73), channel_id=1, source_target_pairs={{0,1},{1,0},{2,3},{3,2},{4,5},{5,4},{6,7},{7,6},{8,9},{9,8},{10,11... | collective-permute-start | bytes 491528 | tf_op jit(solution)/shard_map/ppermute | solution.py:533
  86.3 9.7 %collective-permute-start.13 = (bf16[2,64,768]{2,1,0:T(8,128)(2,1)S(1)}, bf16[2,64,768]{2,1,0:T(8,128)(2,1)S(1)}, u32[]{:S(2)}, u32[]{:S(2)}) collective-permute-start(bf16[2,64,768]{2,1,0:T(8,128)(2,1)S(1)} %get-tuple-element.64), channel_id=1, source_target_pairs={{0,6},{6,0},{2,4},{4,2},{1,7},{7,1},{3,5},{5,3},{8,14},{14,8},{10,... | collective-permute-start | bytes 589832 | tf_op jit(solution)/shard_map/ppermute | solution.py:519
  90.3 12.1 %collective-permute-start.16 = (bf16[3,64,256]{2,1,0:T(8,128)(2,1)S(1)}, bf16[3,64,256]{2,1,0:T(8,128)(2,1)S(1)}, u32[]{:S(2)}, u32[]{:S(2)}) collective-permute-start(bf16[3,64,256]{2,1,0:T(8,128)(2,1)S(1)} %get-tuple-element.76), channel_id=1, source_target_pairs={{0,6},{6,0},{2,4},{4,2},{1,7},{7,1},{3,5},{5,3},{8,14},{14,8},{10,... | collective-permute-start | bytes 294920 | tf_op jit(solution)/shard_map/ppermute | solution.py:537
  96.5 12.6 %collective-permute-start.14 = (bf16[64,768]{1,0:T(8,128)(2,1)S(1)}, bf16[64,768]{1,0:T(8,128)(2,1)S(1)}, u32[]{:S(2)}, u32[]{:S(2)}) collective-permute-start(bf16[64,768]{1,0:T(8,128)(2,1)S(1)} %get-tuple-element.66), channel_id=1, source_target_pairs={{0,2},{2,0},{4,6},{6,4},{1,3},{3,1},{5,7},{7,5},{8,10},{10,8},{12,... | collective-permute-start | bytes 294920 | tf_op jit(solution)/shard_map/ppermute | solution.py:521
  103.0 6.2 %collective-permute-start.17 = (bf16[2,64,256]{2,1,0:T(8,128)(2,1)S(1)}, bf16[2,64,256]{2,1,0:T(8,128)(2,1)S(1)}, u32[]{:S(2)}, u32[]{:S(2)}) collective-permute-start(bf16[2,64,256]{2,1,0:T(8,128)(2,1)S(1)} %get-tuple-element.79), channel_id=1, source_target_pairs={{0,2},{2,0},{4,6},{6,4},{1,3},{3,1},{5,7},{7,5},{8,10},{10,8},{12,... | collective-permute-start | bytes 196616 | tf_op jit(solution)/shard_map/ppermute | solution.py:539
  128.7 0.7 copy-start.7
  129.4 16.8 %all-to-all-start.1 = ((bf16[8,8,1280]{2,1,0:T(8,128)(2,1)}), bf16[8,8,1280]{2,1,0:T(8,128)(2,1)}, u32[]{:S(2)}, u32[]{:S(2)}) async-start(bf16[8,8,1280]{2,1,0:T(8,128)(2,1)} %copy-done.7), calls=%async_computation.1 | async-start | bytes 327680 | tf_op jit(solution)/shard_map/all_to_all | solution.py:456
  136.8 22.9 %collective-permute-start.10 = (bf16[128,2304]{1,0:T(8,128)(2,1)}, bf16[128,2304]{1,0:T(8,128)(2,1)}, u32[]{:S(2)}, u32[]{:S(2)}) collective-permute-start(bf16[128,2304]{1,0:T(8,128)(2,1)} %copy-done.8), channel_id=1, source_target_pairs={{8,0},{16,24},{40,32},{48,56},{9,1},{17,25},{41,33},{49,57},{10,2}... | collective-permute-start | bytes 1769480 | tf_op jit(solution)/shard_map/ppermute | solution.py:502
  147.2 0.7 copy-start.6
  147.9 19.8 %all-to-all-start.2 = ((bf16[8,8,2304]{2,1,0:T(8,128)(2,1)}), bf16[8,8,2304]{2,1,0:T(8,128)(2,1)}, u32[]{:S(2)}, u32[]{:S(2)}) async-start(bf16[8,8,2304]{2,1,0:T(8,128)(2,1)} %copy-done.6), calls=%async_computation.2 | async-start | bytes 589824 | tf_op jit(solution)/shard_map/all_to_all | solution.py:456
  151.9 7.8 %collective-permute-start.11 = (bf16[128,768]{1,0:T(8,128)(2,1)}, bf16[128,768]{1,0:T(8,128)(2,1)S(1)}, u32[]{:S(2)}, u32[]{:S(2)}) collective-permute-start(bf16[128,768]{1,0:T(8,128)(2,1)} %copy-done.10), channel_id=1, source_target_pairs={{8,0},{16,24},{40,32},{48,56},{9,1},{17,25},{41,33},{49,57},{10,2}... | collective-permute-start | bytes 589832 | tf_op jit(solution)/shard_map/ppermute | solution.py:502
  159.7 1.1 copy-start.1
  160.9 1.0 copy-start.3
  161.8 0.9 copy-start.5
  162.8 0.8 copy-start.14

commit v6 on v5

--- a/solution.py
+++ b/solution.py
@@ -47,12 +47,12 @@
     return pltpu.with_memory_space_constraint(x, pltpu.HBM)
 
 
-def call(kernel, out_shape, inputs, scalars=1, scratch=(), vmem=16, remote=()):
+def call(kernel, out_shape, inputs, scalars=1, scratch=(), vmem=16, remote=(), out=VMEM):
     return pl.pallas_call(
         kernel,
         out_shape=out_shape,
         in_specs=[SMEM] * scalars + [HBM if i in remote else VMEM for i in range(scalars, len(inputs))],
-        out_specs=jax.tree.map(lambda _: VMEM, out_shape),
+        out_specs=jax.tree.map(lambda _: out, out_shape),
         scratch_shapes=list(scratch),
         compiler_params=pltpu.CompilerParams(vmem_limit_bytes=vmem << 20),
     )(*inputs)
@@ -310,18 +310,19 @@
     send[4, :, 128:] = low
 
 
+def last_kernel(place, u, v, near, far, swap, weights, gain, shift, values, stats, before, *refs):
+    part, out_u, out_v, keep, small, send, one, two, terms = refs
+    product_kernel(1, place, u, v, near, far, swap, weights, gain, shift, part, out_u, out_v, one, two)
+    mix_grad_kernel(CHUNKS[1], place, u, v, near, far, swap, one, two, keep, terms)
+    last_sums_kernel(place, values, stats, before, out_u, out_v, part, near, terms, small, send)
+
+
 def chip_kernel(place, keep, got, own, send):
     near = place[1] // 2 * 2
     for k in range(2):
         own[k] = keep[near + k] + got[near + k].astype(F32)
         other = 2 - near + k
         send[k] = (keep[other] + got[other].astype(F32)).astype(BF16)
-
-
-def chip_pair_kernel(place, keep, got, own, send):
-    b = place[1] % 2
-    own[...] = keep[b] + got[b].astype(F32)
-    send[...] = (keep[1 - b] + got[1 - b].astype(F32)).astype(BF16)
 
 
 def last_chip_kernel(place, keep, small, got, own, total, send):
@@ -337,30 +338,30 @@
         send[k] = (keep[other] + got[other].astype(F32)).astype(BF16)
 
 
-def last_pair_kernel(place, keep, small, got, own, total, send):
-    extra = small[...] + (got[2, :, :128].astype(F32) + got[2, :, 128:].astype(F32))
+def last_pair_kernel(place, keep0, got0, keep1, small, got1, own, total, send):
+    extra = small[...] + (got1[2, :, :128].astype(F32) + got1[2, :, 128:].astype(F32))
     high, low = split(extra)
     total[...] = extra
-    send[1, :, :128] = high
-    send[1, :, 128:] = low
+    send[:, 1024:1152] = high
+    send[:, 1152:1280] = low
     b = place[1] % 2
-    own[...] = keep[b] + got[b].astype(F32)
-    send[0] = (keep[1 - b] + got[1 - b].astype(F32)).astype(BF16)
-
-
-def deal_kernel(own0, got0, own1, small, got1, out):
-    def put(lane, block):
-        for z in range(8):
-            out[z, :, lane : lane + block.shape[1]] = block[z * 8 : (z + 1) * 8]
-
-    first = (own0[...] + got0[...].astype(F32)).astype(BF16)
-    last = (own1[...] + got1[0].astype(F32)).astype(BF16)
-    for slot in range(2):
-        put(slot * 512, first[:, slot * 384 : (slot + 1) * 384])
-        put(slot * 512 + 384, last[:, slot * 128 : (slot + 1) * 128])
-    high, low = split(small[...] + (got1[1, :, :128].astype(F32) + got1[1, :, 128:].astype(F32)))
-    put(1024, high)
-    put(1152, low)
+    for keep, got, first, width in ((keep0, got0, 0, 384), (keep1, got1, 384, 128)):
+        mine = keep[b] + got[b].astype(F32)
+        theirs = (keep[1 - b] + got[1 - b].astype(F32)).astype(BF16)
+        for slot in range(2):
+            lanes = slice(slot * 512 + first, slot * 512 + first + width)
+            own[:, lanes] = mine[:, slot * width : (slot + 1) * width]
+            send[:, lanes] = theirs[:, slot * width : (slot + 1) * width]
+
+
+def deal_kernel(own, small, got, out):
+    total = (own[...] + got[:, :1024].astype(F32)).astype(BF16)
+    high, low = split(small[...] + (got[:, 1024:1152].astype(F32) + got[:, 1152:1280].astype(F32)))
+    for z in range(8):
+        rows = slice(z * 8, (z + 1) * 8)
+        out[z, :, :1024] = total[rows]
+        out[z, :, 1024:1152] = high[rows]
+        out[z, :, 1152:1280] = low[rows]
 
 
 def add_kernel(got, out):
@@ -414,9 +415,16 @@
 
 def post_kernel(place, values, upstream, stats, columns, gain, *refs):
     n = len(CHUNKS)
-    outs_u, outs_v, got, grad_u, grad_v = refs[:n], refs[n : 2 * n], refs[2 * n : 3 * n], refs[3 * n], refs[3 * n + 1]
+    outs_u, outs_v, got, to_u, to_v = refs[:n], refs[n : 2 * n], refs[2 * n : 3 * n], refs[3 * n], refs[3 * n + 1]
+    grad_u, grad_v, backs, sems = refs[3 * n + 2 :]
     low = place[0] < 2
     step = 16
+    part = ROWS // 4
+
+    def copy(k, i):
+        rows = slice(i * part, (i + 1) * part)
+        source, target = ((grad_u, to_u), (grad_v, to_v))[k]
+        return pltpu.make_async_copy(source.at[0, rows], target.at[0, rows], sems.at[k, i])
 
     def block(i, carry):
         rows = pl.ds(pl.multiple_of(i * step, step), step)
@@ -432,8 +440,9 @@
             mixed = jnp.where(low, short_side, long_side) + columns[rows, g : g + 1]
             mixed = mixed.astype(BF16).astype(F32)
             grad_u[0, rows, cols] = (upstream[0, rows, cols].astype(F32) * mixed).astype(BF16)
-            back = jnp.where(low, long_side, short_side).astype(BF16).astype(F32)
-            scaled = back * gain[:, cols]
+            back = jnp.where(low, long_side, short_side).astype(BF16)
+            backs[rows, cols] = back
+            scaled = back.astype(F32) * gain[:, cols]
             unit = (values[0, rows, cols].astype(F32) - mean) * inv
             first = first + jnp.sum(scaled, axis=1, keepdims=True)
             second = second + jnp.sum(scaled * unit, axis=1, keepdims=True)
@@ -441,15 +450,18 @@
         second = second * (1.0 / HALF)
         for g in range(GROUPS):
             cols = slice(g * WIDTH, (g + 1) * WIDTH)
-            c, lanes = lanes_of(g)
-            long_side = outs_u[c][rows, lanes] + got[c][rows, lanes].astype(F32)
-            back = jnp.where(low, long_side, outs_v[c][rows, lanes]).astype(BF16).astype(F32)
-            scaled = back * gain[:, cols]
+            scaled = backs[rows, cols].astype(F32) * gain[:, cols]
             unit = (values[0, rows, cols].astype(F32) - mean) * inv
             grad_v[0, rows, cols] = (inv * (scaled - first - unit * second)).astype(BF16)
         return carry
 
-    lax.fori_loop(0, ROWS // step, block, 0, unroll=2)
+    for i in range(4):
+        lax.fori_loop(i * part // step, (i + 1) * part // step, block, 0, unroll=True)
+        copy(0, i).start()
+        copy(1, i).start()
+    for i in range(4):
+        copy(0, i).wait()
+        copy(1, i).wait()
 
 
 def exchanged(x, axis):
@@ -490,53 +502,53 @@
     )
     weights = call(weight_kernel, shape((GROUPS, 2 * ROWS, 3 * ROWS), BF16), (place, mine, theirs))
 
-    outs_u, outs_v, got, keeps, sends, parts = [], [], [], [], [], []
-    for i in range(n):
-        operands = (us[i], vs[i], near[i], far[i], swap[i])
-        part, out_u, out_v, one, two = call(
-            functools.partial(product_kernel, i),
-            [halves[i], fulls[i], fulls[i], halves[i], halves[i]],
-            (place, *operands, weights, gain_row, shift_row),
-        )
-        parts.append(part)
-        got.append(lax.ppermute(part, Y, OUT))
-        outs_u.append(out_u)
-        outs_v.append(out_v)
-        dims = (4, SEG, 2 * CHUNKS[i] * ROWS)
-        keep, send = call(
-            functools.partial(mix_grad_kernel, CHUNKS[i]),
-            [shape(dims, F32), shape(dims, BF16)],
-            (place, *operands, one, two),
-        )
-        keeps.append(keep)
-        sends.append(send)
-
-    folded = lax.ppermute(sends[0], CORE, PARTNER)
-    keep, send = call(chip_kernel, [shape((2, SEG, 768), F32), shape((2, SEG, 768), BF16)], (place, keeps[0], folded))
-    own, send = call(
-        chip_pair_kernel,
-        [shape((SEG, 768), F32), shape((SEG, 768), BF16)],
-        (place, keep, lax.ppermute(send, X, ACROSS)),
-    )
-    chip = (own, lax.ppermute(send, X, WITHIN))
+    operands = [(us[i], vs[i], near[i], far[i], swap[i]) for i in range(n)]
+    part, out_u, out_v, one, two = call(
+        functools.partial(product_kernel, 0),
+        [halves[0], fulls[0], fulls[0], halves[0], halves[0]],
+        (place, *operands[0], weights, gain_row, shift_row),
+    )
+    first_got = lax.ppermute(part, Y, OUT)
+    dims = (4, SEG, 2 * CHUNKS[0] * ROWS)
+    keep, send = call(
+        functools.partial(mix_grad_kernel, CHUNKS[0]),
+        [shape(dims, F32), shape(dims, BF16)],
+        (place, *operands[0], one, two),
+    )
     sums = call(
         functools.partial(sums_kernel, 0),
         shape((64, 128), F32),
-        (place, values_in, stats, bias_term, outs_u[0], outs_v[0], parts[0], near[0]),
-    )
-    small, last = call(
-        last_sums_kernel,
-        [shape((64, 128), F32), shape((5, SEG, 2 * ROWS), BF16)],
-        (place, values_in, stats, sums, outs_u[1], outs_v[1], parts[1], near[1], sends[1]),
-    )
+        (place, values_in, stats, bias_term, out_u, out_v, part, near[0]),
+    )
+    keep, send = call(
+        chip_kernel,
+        [shape((2, SEG, 768), F32), shape((2, SEG, 768), BF16)],
+        (place, keep, lax.ppermute(send, CORE, PARTNER)),
+    )
+    chip = (keep, lax.ppermute(send, X, ACROSS))
+
+    part, last_u, last_v, keep, small, last = call(
+        last_kernel,
+        [
+            halves[1],
+            fulls[1],
+            fulls[1],
+            shape((4, SEG, 256), F32),
+            shape((64, 128), F32),
+            shape((5, SEG, 256), BF16),
+        ],
+        (place, *operands[1], weights, gain_row, shift_row, values_in, stats, sums),
+        scratch=[pltpu.VMEM((ROWS, WIDTH), BF16)] * 2 + [pltpu.VMEM((4, SEG, 256), BF16)],
+    )
+    outs_u, outs_v, got = (out_u, last_u), (out_v, last_v), (first_got, lax.ppermute(part, Y, OUT))
     half_terms = [shape((2, SEG, 256), F32), shape((64, 128), F32), shape((3, SEG, 256), BF16)]
-    own, small, send = call(last_chip_kernel, half_terms, (place, keeps[1], small, lax.ppermute(last, CORE, PARTNER)))
+    own, small, send = call(last_chip_kernel, half_terms, (place, keep, small, lax.ppermute(last, CORE, PARTNER)))
     own, small, send = call(
         last_pair_kernel,
-        [shape((SEG, 256), F32), shape((64, 128), F32), shape((2, SEG, 256), BF16)],
-        (place, own, small, lax.ppermute(send, X, ACROSS)),
-    )
-    dealt = call(deal_kernel, shape((8, 8, 1280), BF16), (*chip, own, small, lax.ppermute(send, X, WITHIN)), 0)
+        [shape((SEG, 1024), F32), shape((64, 128), F32), shape((SEG, 1280), BF16)],
+        (place, *chip, own, small, lax.ppermute(send, X, ACROSS)),
+    )
+    dealt = call(deal_kernel, shape((8, 8, 1280), BF16), (own, small, lax.ppermute(send, X, WITHIN)), 0)
     added = call(add_kernel, shape((8, 8, 1280), BF16), (exchanged(dealt, Z),), 0)
     placed = call(place_kernel, shape((8, 8, 2304), BF16), (exchanged(added, Y),), 0)
     grad_mix, grad_bias, grad_gain, grad_shift = call(
@@ -550,6 +562,9 @@
         post_kernel,
         [shape((1, ROWS, HALF), BF16)] * 2,
         (place, values_in, upstream, stats, columns, gain_row, *outs_u, *outs_v, *got),
+        scratch=[pltpu.VMEM((1, ROWS, HALF), BF16)] * 2
+        + [pltpu.VMEM((ROWS, HALF), BF16), pltpu.SemaphoreType.DMA((2, 4))],
+        out=HBM,
     )
     return (grad_u, grad_v, grad_mix, grad_bias, grad_gain.reshape(HALF), grad_shift.reshape(HALF))
 

time: 171 us -> 167 us (0.977)
  the two profiles are of different devices: /device:TPU:2 before, /device:TPU:1 now
where the time goes in v6:
time: 167 us; the launch traced here: 164 us
  starting transfers between devices  61.7 us (37%)
  waiting for transfers between devices  56.4 us (34%)
  Pallas kernels  20.2 us (12%)
  blocking collectives  18.1 us (11%)
  local copies, waits for them, and re-layouts  6.16 us (4%)
    pallas_call x17, Pallas kernels, call(): pl.pallas_call(kernel, out_shape=out_shape, in_specs=[SMEM] * scalars + [...  20.2 us
    all_to_all x1, blocking collectives, exchanged(): return lax.all_to_all(x, axis, split_axis=0, concat_axis=0, tiled=True)  18.1 us
    ppermute x2, waiting for transfers between devices, compute(): near.append(lax.ppermute(vs[i], Y, NEAR))  16.9 us
    ppermute x2, starting transfers between devices, compute(): far.append(lax.ppermute(vs[i], Y, FAR))  11.9 us
    all_to_all x2, starting transfers between devices, exchanged(): return lax.all_to_all(x, axis, split_axis=0, concat_axis=0, tiled=True)  11.2 us
    ppermute x2, waiting for transfers between devices, compute(): far.append(lax.ppermute(vs[i], Y, FAR))  10.5 us
    ppermute x3, starting transfers between devices, compute(): slabs = [slab] + [lax.ppermute(slab, X, CHIPS[k]) for k in range(1, 4)]  10.1 us
    all_to_all x2, waiting for transfers between devices, exchanged(): return lax.all_to_all(x, axis, split_axis=0, concat_axis=0, tiled=True)  7.09 us
  transfers between devices with their start and end apart: 19, of which 10 were waited for; matrix products, arithmetic and copies ran while one was open for 0% of the time, Pallas kernels for 8%

profile of v6, /device:TPU:1, one launch (start us, length us, event | category | flops | bytes accessed | tf_op | source)
XLA Modules:
  0.0 163.7 jit_solution(9481451298062460300)
XLA Ops:
  0.6 0.1 pad_add_fusion.place
  0.7 0.9 copy-done.9
  1.7 1.0 shard_map.120.refs_0_
  2.6 5.2 %collective-permute-start.5 = (bf16[4,64,384]{2,1,0:T(8,128)(2,1)S(1)}, bf16[4,64,384]{2,1,0:T(8,128)(2,1)S(1)}, u32[]{:S(2)}, u32[]{:S(2)}) collective-permute-start(bf16[4,64,384]{2,1,0:T(8,128)(2,1)S(1)} %shard_map.120.refs_0_), channel_id=1, source_target_pairs={{0,6},{2,0},{4,2},{6,4},{1,7},{3,1},{5,3},{7,5},{8,14},{10,8},{12,... | collective-permute-start | bytes 589832 | tf_op jit(solution)/shard_map/ppermute | solution.py:497
  7.8 2.4 %collective-permute-start.4 = (bf16[4,64,384]{2,1,0:T(8,128)(2,1)S(1)}, bf16[4,64,384]{2,1,0:T(8,128)(2,1)S(1)}, u32[]{:S(2)}, u32[]{:S(2)}) collective-permute-start(bf16[4,64,384]{2,1,0:T(8,128)(2,1)S(1)} %shard_map.120.refs_0_), channel_id=1, source_target_pairs={{0,4},{2,6},{4,0},{6,2},{1,5},{3,7},{5,1},{7,3},{8,12},{10,14},{12... | collective-permute-start | bytes 589832 | tf_op jit(solution)/shard_map/ppermute | solution.py:497
  10.3 2.5 %collective-permute-start.3 = (bf16[4,64,384]{2,1,0:T(8,128)(2,1)S(1)}, bf16[4,64,384]{2,1,0:T(8,128)(2,1)S(1)}, u32[]{:S(2)}, u32[]{:S(2)}) collective-permute-start(bf16[4,64,384]{2,1,0:T(8,128)(2,1)S(1)} %shard_map.120.refs_0_), channel_id=1, source_target_pairs={{0,2},{2,4},{4,6},{6,0},{1,3},{3,5},{5,7},{7,1},{8,10},{10,12},{12... | collective-permute-start | bytes 589832 | tf_op jit(solution)/shard_map/ppermute | solution.py:497
  12.8 0.0 collective-permute-done.5.refs_3_
  12.8 2.9 %collective-permute-done.4.refs_2_ = bf16[4,64,384]{2,1,0:T(8,128)(2,1)S(1)} collective-permute-done((bf16[4,64,384]{2,1,0:T(8,128)(2,1)S(1)}, bf16[4,64,384]{2,1,0:T(8,128)(2,1)S(1)}, u32[]{:S(2)}, u32[]{:S(2)}) %collective-permute-start.4) | collective-permute-done | bytes 196640 | tf_op jit(solution)/shard_map/ppermute | solution.py:497
  15.8 2.6 %collective-permute-done.3.refs_1_ = bf16[4,64,384]{2,1,0:T(8,128)(2,1)S(1)} collective-permute-done((bf16[4,64,384]{2,1,0:T(8,128)(2,1)S(1)}, bf16[4,64,384]{2,1,0:T(8,128)(2,1)S(1)}, u32[]{:S(2)}, u32[]{:S(2)}) %collective-permute-start.3) | collective-permute-done | bytes 196640 | tf_op jit(solution)/shard_map/ppermute | solution.py:497
  18.4 0.6 shard_map.121.mine
  19.0 7.1 %collective-permute-start.6 = (bf16[4,4,64,384]{3,2,1,0:T(8,128)(2,1)S(1)}, bf16[4,4,64,384]{3,2,1,0:T(8,128)(2,1)S(1)}, u32[]{:S(2)}, u32[]{:S(2)}) collective-permute-start(bf16[4,4,64,384]{3,2,1,0:T(8,128)(2,1)S(1)} %shard_map.121.mine), channel_id=1, source_target_pairs={{0,1},{1,0},{2,3},{3,2},{4,5},{5,4},{6,7},{7,6},{8,9},{9,8},{10,11... | collective-permute-start | bytes 2359304 | tf_op jit(solution)/shard_map/ppermute | solution.py:499
  26.1 3.5 %shard_map.118 = (bf16[128,2304]{1,0:T(8,128)(2,1)S(1)}, bf16[128,768]{1,0:T(8,128)(2,1)S(1)}, bf16[128,2304]{1,0:T(8,128)(2,1)S(1)}, bf16[128,768]{1,0:T(8,128)(2,1)S(1)}, f32[2,128,128]{2,1,0:T(8,128)S(1)}) custom-call(s32[3]{0:T(128)S(1)} %pad_add_fusion.place, bf16[1,128,3072]{2,1,0:T(8,128)(2,1)} %values.5, bf16[1,128,3072]{2,1,0:T(8,128)(2,1)} %gated_in.1, ...), custom_call_target="tpu_custom_call" | custom-call | tf_op jit(solution)/shard_map/pallas_call | solution.py:51
  29.6 0.0 copy-start.10
  29.6 0.0 copy-start.11
  29.6 0.7 collective-permute-start.2
  30.3 4.9 %collective-permute-start.1 = (bf16[128,2304]{1,0:T(8,128)(2,1)S(1)}, bf16[128,2304]{1,0:T(8,128)(2,1)S(1)}, u32[]{:S(2)}, u32[]{:S(2)}) collective-permute-start(bf16[128,2304]{1,0:T(8,128)(2,1)S(1)} %get-tuple-element.42.v), channel_id=1, source_target_pairs={{0,16},{24,8},{32,48},{56,40},{1,17},{25,9},{33,49},{57,41},{2,18}... | collective-permute-start | bytes 1769480 | tf_op jit(solution)/shard_map/ppermute | solution.py:493
  35.2 1.4 collective-permute-start
  36.6 0.0 collective-permute-done.6.theirs
  36.6 0.9 shard_map.122.weights
  37.5 0.0 collective-permute-done.2.swap
  37.5 10.1 %collective-permute-done.1.far = bf16[128,2304]{1,0:T(8,128)(2,1)S(1)} collective-permute-done((bf16[128,2304]{1,0:T(8,128)(2,1)S(1)}, bf16[128,2304]{1,0:T(8,128)(2,1)S(1)}, u32[]{:S(2)}, u32[]{:S(2)}) %collective-permute-start.1) | collective-permute-done | bytes 589856 | tf_op jit(solution)/shard_map/ppermute | solution.py:493
  47.6 12.6 %collective-permute-done.near = bf16[128,2304]{1,0:T(8,128)(2,1)S(1)} collective-permute-done((bf16[128,2304]{1,0:T(8,128)(2,1)S(1)}, bf16[128,2304]{1,0:T(8,128)(2,1)S(1)}, u32[]{:S(2)}, u32[]{:S(2)}) %collective-permute-start) | collective-permute-done | bytes 589856 | tf_op jit(solution)/shard_map/ppermute | solution.py:492
  60.2 1.9 %shard_map.123 = (bf16[128,2304]{1,0:T(8,128)(2,1)S(1)}, f32[128,2304]{1,0:T(8,128)S(1)}, f32[128,2304]{1,0:T(8,128)S(1)}, bf16[128,2304]{1,0:T(8,128)(2,1)S(1)}, bf16[128,2304]{1,0:T(8,128)(2,1)S(1)}) custom-call(s32[3]{0:T(128)S(1)} %pad_add_fusion.place, bf16[128,2304]{1,0:T(8,128)(2,1)S(1)} %get-tuple-element.41.u, ...), custom_call_target="tpu_custom_call" | custom-call | tf_op jit(solution)/shard_map/pallas_call | solution.py:51
  62.1 0.0 copy-start.4
  62.1 0.0 copy-start.12
  62.1 1.3 shard_map.127
  63.4 0.0 copy-start
  63.4 3.2 %collective-permute-start.12 = (bf16[4,64,768]{2,1,0:T(8,128)(2,1)S(1)}, bf16[4,64,768]{2,1,0:T(8,128)(2,1)S(1)}, u32[]{:S(2)}, u32[]{:S(2)}) collective-permute-start(bf16[4,64,768]{2,1,0:T(8,128)(2,1)S(1)} %get-tuple-element.58), channel_id=1, source_target_pairs={{0,1},{1,0},{2,3},{3,2},{4,5},{5,4},{6,7},{7,6},{8,9},{9,8},{10,11... | collective-permute-start | bytes 1179656 | tf_op jit(solution)/shard_map/ppermute | solution.py:526
  66.6 0.7 collective-permute-start.9
  67.3 7.0 %collective-permute-start.8 = (bf16[128,768]{1,0:T(8,128)(2,1)S(1)}, bf16[128,768]{1,0:T(8,128)(2,1)S(1)}, u32[]{:S(2)}, u32[]{:S(2)}) collective-permute-start(bf16[128,768]{1,0:T(8,128)(2,1)S(1)} %get-tuple-element.44.v1.v), channel_id=1, source_target_pairs={{0,16},{24,8},{32,48},{56,40},{1,17},{25,9},{33,49},{57,41},{2,18}... | collective-permute-start | bytes 589832 | tf_op jit(solution)/shard_map/ppermute | solution.py:493
  74.3 1.5 collective-permute-start.7
  75.9 0.9 shard_map.119
  76.7 1.2 shard_map.124.before
  77.9 0.0 collective-permute-done.9.swap
  77.9 0.4 collective-permute-done.8.far
  78.3 4.2 %collective-permute-done.7.near = bf16[128,768]{1,0:T(8,128)(2,1)S(1)} collective-permute-done((bf16[128,768]{1,0:T(8,128)(2,1)S(1)}, bf16[128,768]{1,0:T(8,128)(2,1)S(1)}, u32[]{:S(2)}, u32[]{:S(2)}) %collective-permute-start.7) | collective-permute-done | bytes 196640 | tf_op jit(solution)/shard_map/ppermute | solution.py:492
  82.5 1.4 shard_map.125
  84.0 0.7 copy-done.13
  84.6 3.0 %collective-permute-start.14 = (bf16[5,64,256]{2,1,0:T(8,128)(2,1)S(1)}, bf16[5,64,256]{2,1,0:T(8,128)(2,1)S(1)}, u32[]{:S(2)}, u32[]{:S(2)}) collective-permute-start(bf16[5,64,256]{2,1,0:T(8,128)(2,1)S(1)} %get-tuple-element.63), channel_id=1, source_target_pairs={{0,1},{1,0},{2,3},{3,2},{4,5},{5,4},{6,7},{7,6},{8,9},{9,8},{10,11... | collective-permute-start | bytes 491528 | tf_op jit(solution)/shard_map/ppermute | solution.py:545
  87.7 0.0 collective-permute-done.12.got
  87.7 0.6 shard_map.128
  88.3 2.2 %collective-permute-start.13 = (bf16[2,64,768]{2,1,0:T(8,128)(2,1)S(1)}, bf16[2,64,768]{2,1,0:T(8,128)(2,1)S(1)}, u32[]{:S(2)}, u32[]{:S(2)}) collective-permute-start(bf16[2,64,768]{2,1,0:T(8,128)(2,1)S(1)} %get-tuple-element.60), channel_id=1, source_target_pairs={{0,6},{6,0},{2,4},{4,2},{1,7},{7,1},{3,5},{5,3},{8,14},{14,8},{10,... | collective-permute-start | bytes 589832 | tf_op jit(solution)/shard_map/ppermute | solution.py:528
  90.6 0.6 shard_map.129
  91.1 4.3 %collective-permute-start.15 = (bf16[3,64,256]{2,1,0:T(8,128)(2,1)S(1)}, bf16[3,64,256]{2,1,0:T(8,128)(2,1)S(1)}, u32[]{:S(2)}, u32[]{:S(2)}) collective-permute-start(bf16[3,64,256]{2,1,0:T(8,128)(2,1)S(1)} %get-tuple-element.66), channel_id=1, source_target_pairs={{0,6},{6,0},{2,4},{4,2},{1,7},{7,1},{3,5},{5,3},{8,14},{14,8},{10,... | collective-permute-start | bytes 294920 | tf_op jit(solution)/shard_map/ppermute | solution.py:549
  95.4 4.6 %collective-permute-done.15.got1 = bf16[3,64,256]{2,1,0:T(8,128)(2,1)S(1)} collective-permute-done((bf16[3,64,256]{2,1,0:T(8,128)(2,1)S(1)}, bf16[3,64,256]{2,1,0:T(8,128)(2,1)S(1)}, u32[]{:S(2)}, u32[]{:S(2)}) %collective-permute-start.15) | collective-permute-done | bytes 98336 | tf_op jit(solution)/shard_map/ppermute | solution.py:549
  100.0 0.6 shard_map.130
  100.6 1.9 %collective-permute-start.16 = (bf16[64,1280]{1,0:T(8,128)(2,1)S(1)}, bf16[64,1280]{1,0:T(8,128)(2,1)S(1)}, u32[]{:S(2)}, u32[]{:S(2)}) collective-permute-start(bf16[64,1280]{1,0:T(8,128)(2,1)S(1)} %get-tuple-element.69), channel_id=1, source_target_pairs={{0,2},{2,0},{4,6},{6,4},{1,3},{3,1},{5,7},{7,5},{8,10},{10,8},{12,... | collective-permute-start | bytes 491528 | tf_op jit(solution)/shard_map/ppermute | solution.py:551
  102.5 4.9 %collective-permute-done.16.got = bf16[64,1280]{1,0:T(8,128)(2,1)S(1)} collective-permute-done((bf16[64,1280]{1,0:T(8,128)(2,1)S(1)}, bf16[64,1280]{1,0:T(8,128)(2,1)S(1)}, u32[]{:S(2)}, u32[]{:S(2)}) %collective-permute-start.16) | collective-permute-done | bytes 163872 | tf_op jit(solution)/shard_map/ppermute | solution.py:551
  107.4 18.1 %all_to_all.15.got = bf16[8,8,1280]{2,1,0:T(8,128)(2,1)S(1)} all-to-all(bf16[8,8,1280]{2,1,0:T(8,128)(2,1)S(1)} %shard_map.131), channel_id=1, replica_groups=mesh['sp_0'=8,'sp_1'=8,'dp_0'=4,'dp_1'=2] {'sp_0'}, dimensions={0} | all-to-all | bytes 327680 | tf_op jit(solution)/shard_map/all_to_all | solution.py:468
  125.6 0.7 copy-done.3
  126.3 7.1 %all-to-all-start.1 = ((bf16[8,8,1280]{2,1,0:T(8,128)(2,1)}), bf16[8,8,1280]{2,1,0:T(8,128)(2,1)S(1)}, u32[]{:S(2)}, u32[]{:S(2)}) async-start(bf16[8,8,1280]{2,1,0:T(8,128)(2,1)} %copy-done.3), calls=%async_computation.1 | async-start | bytes 327680 | tf_op jit(solution)/shard_map/all_to_all | solution.py:468
  133.4 1.3 collective-permute-start.10
  134.7 7.1 %all-to-all-done.1.got = bf16[8,8,1280]{2,1,0:T(8,128)(2,1)S(1)} async-done(((bf16[8,8,1280]{2,1,0:T(8,128)(2,1)}), bf16[8,8,1280]{2,1,0:T(8,128)(2,1)S(1)}, u32[]{:S(2)}, u32[]{:S(2)}) %all-to-all-start.1) | async-done | bytes 163872 | tf_op jit(solution)/shard_map/all_to_all | solution.py:468
  141.8 0.7 copy-done.2
  142.5 4.1 %all-to-all-start.2 = ((bf16[8,8,2304]{2,1,0:T(8,128)(2,1)}), bf16[8,8,2304]{2,1,0:T(8,128)(2,1)}, u32[]{:S(2)}, u32[]{:S(2)}) async-start(bf16[8,8,2304]{2,1,0:T(8,128)(2,1)} %copy-done.2), calls=%async_computation.2 | async-start | bytes 589824 | tf_op jit(solution)/shard_map/all_to_all | solution.py:468
  146.6 1.3 collective-permute-start.11
  147.9 7.0 %collective-permute-done.11.refs_5_ = bf16[128,768]{1,0:T(8,128)(2,1)S(1)} collective-permute-done((bf16[128,768]{1,0:T(8,128)(2,1)}, bf16[128,768]{1,0:T(8,128)(2,1)S(1)}, u32[]{:S(2)}, u32[]{:S(2)}) %collective-permute-start.11) | collective-permute-done | bytes 196640 | tf_op jit(solution)/shard_map/ppermute | solution.py:543
  154.8 0.0 collective-permute-done.10.refs_4_
  154.8 1.1 copy-done.1
  156.0 1.0 copy-done.6
  157.0 1.0 copy-done.8
  158.0 3.8 %shard_map.126 = (bf16[1,128,3072]{2,1,0:T(8,128)(2,1)}, bf16[1,128,3072]{2,1,0:T(8,128)(2,1)}) custom-call(s32[3]{0:T(128)S(1)} %pad_add_fusion.place, bf16[1,128,3072]{2,1,0:T(8,128)(2,1)S(1)} %copy-done, bf16[1,128,3072]{2,1,0:T(8,128)(2,1)S(1)} %copy-done.1, f32[2,128,128]{2,1,0:T(8,128)S(1)} %get-tuple-element.40.stats, ...), custom_call_target="tpu_custom_call" | custom-call | tf_op jit(solution)/shard_map/pallas_call | solution.py:51
  161.8 0.0 all-to-all-done.2.got
  161.8 1.9 %shard_map.134 = (f32[64,4,512]{2,1,0:T(4,128)}, f32[4,512]{1,0:T(4,128)}, f32[24,128]{1,0:T(8,128)}, f32[24,128]{1,0:T(8,128)}) custom-call(bf16[8,8,2304]{2,1,0:T(8,128)(2,1)} %all-to-all-done.2.got), custom_call_target="tpu_custom_call" | custom-call | tf_op jit(solution)/shard_map/pallas_call | solution.py:51
  (21 shorter events, 0.1 us)
Async XLA Ops:
  0.7 1.0 copy-start.9
  2.6 10.2 %collective-permute-start.5 = (bf16[4,64,384]{2,1,0:T(8,128)(2,1)S(1)}, bf16[4,64,384]{2,1,0:T(8,128)(2,1)S(1)}, u32[]{:S(2)}, u32[]{:S(2)}) collective-permute-start(bf16[4,64,384]{2,1,0:T(8,128)(2,1)S(1)} %shard_map.120.refs_0_), channel_id=1, source_target_pairs={{0,6},{2,0},{4,2},{6,4},{1,7},{3,1},{5,3},{7,5},{8,14},{10,8},{12,... | collective-permute-start | bytes 589832 | tf_op jit(solution)/shard_map/ppermute | solution.py:497
  7.8 7.9 %collective-permute-start.4 = (bf16[4,64,384]{2,1,0:T(8,128)(2,1)S(1)}, bf16[4,64,384]{2,1,0:T(8,128)(2,1)S(1)}, u32[]{:S(2)}, u32[]{:S(2)}) collective-permute-start(bf16[4,64,384]{2,1,0:T(8,128)(2,1)S(1)} %shard_map.120.refs_0_), channel_id=1, source_target_pairs={{0,4},{2,6},{4,0},{6,2},{1,5},{3,7},{5,1},{7,3},{8,12},{10,14},{12... | collective-permute-start | bytes 589832 | tf_op jit(solution)/shard_map/ppermute | solution.py:497
  10.3 8.1 %collective-permute-start.3 = (bf16[4,64,384]{2,1,0:T(8,128)(2,1)S(1)}, bf16[4,64,384]{2,1,0:T(8,128)(2,1)S(1)}, u32[]{:S(2)}, u32[]{:S(2)}) collective-permute-start(bf16[4,64,384]{2,1,0:T(8,128)(2,1)S(1)} %shard_map.120.refs_0_), channel_id=1, source_target_pairs={{0,2},{2,4},{4,6},{6,0},{1,3},{3,5},{5,7},{7,1},{8,10},{10,12},{12... | collective-permute-start | bytes 589832 | tf_op jit(solution)/shard_map/ppermute | solution.py:497
  19.0 17.5 %collective-permute-start.6 = (bf16[4,4,64,384]{3,2,1,0:T(8,128)(2,1)S(1)}, bf16[4,4,64,384]{3,2,1,0:T(8,128)(2,1)S(1)}, u32[]{:S(2)}, u32[]{:S(2)}) collective-permute-start(bf16[4,4,64,384]{3,2,1,0:T(8,128)(2,1)S(1)} %shard_map.121.mine), channel_id=1, source_target_pairs={{0,1},{1,0},{2,3},{3,2},{4,5},{5,4},{6,7},{7,6},{8,9},{9,8},{10,11... | collective-permute-start | bytes 2359304 | tf_op jit(solution)/shard_map/ppermute | solution.py:499
  29.6 30.6 %copy-start.10 = (f32[3072]{0:T(1024)S(1)}, f32[3072]{0:T(1024)}, u32[]{:S(2)}) copy-start(f32[3072]{0:T(1024)} %param.10) | copy-start | bytes 36868
  29.6 30.6 %copy-start.11 = (f32[3072]{0:T(1024)S(1)}, f32[3072]{0:T(1024)}, u32[]{:S(2)}) copy-start(f32[3072]{0:T(1024)} %param.11) | copy-start | bytes 36868
  29.6 7.9 %collective-permute-start.2 = (bf16[128,2304]{1,0:T(8,128)(2,1)S(1)}, bf16[128,2304]{1,0:T(8,128)(2,1)S(1)}, u32[]{:S(2)}, u32[]{:S(2)}) collective-permute-start(bf16[128,2304]{1,0:T(8,128)(2,1)S(1)} %get-tuple-element.42.v), channel_id=1, source_target_pairs={{8,16},{16,8},{40,48},{48,40},{9,17},{17,9},{41,49},{49,41},{10,18... | collective-permute-start | bytes 1769480 | tf_op jit(solution)/shard_map/ppermute | solution.py:494
  30.3 17.2 %collective-permute-start.1 = (bf16[128,2304]{1,0:T(8,128)(2,1)S(1)}, bf16[128,2304]{1,0:T(8,128)(2,1)S(1)}, u32[]{:S(2)}, u32[]{:S(2)}) collective-permute-start(bf16[128,2304]{1,0:T(8,128)(2,1)S(1)} %get-tuple-element.42.v), channel_id=1, source_target_pairs={{0,16},{24,8},{32,48},{56,40},{1,17},{25,9},{33,49},{57,41},{2,18}... | collective-permute-start | bytes 1769480 | tf_op jit(solution)/shard_map/ppermute | solution.py:493
  35.2 25.0 %collective-permute-start = (bf16[128,2304]{1,0:T(8,128)(2,1)S(1)}, bf16[128,2304]{1,0:T(8,128)(2,1)S(1)}, u32[]{:S(2)}, u32[]{:S(2)}) collective-permute-start(bf16[128,2304]{1,0:T(8,128)(2,1)S(1)} %get-tuple-element.42.v), channel_id=1, source_target_pairs={{0,8},{24,16},{32,40},{56,48},{1,9},{25,17},{33,41},{57,49},{2,10}... | collective-permute-start | bytes 1769480 | tf_op jit(solution)/shard_map/ppermute | solution.py:492
  62.1 14.6 %copy-start.4 = (bf16[128,2304]{1,0:T(8,128)(2,1)}, bf16[128,2304]{1,0:T(8,128)(2,1)S(1)}, u32[]{:S(2)}) copy-start(bf16[128,2304]{1,0:T(8,128)(2,1)S(1)} %get-tuple-element.49.part) | copy-start | bytes 1769476
  62.1 13.7 %copy-start.12 = (f32[4,512]{1,0:T(4,128)S(1)}, f32[4,512]{1,0:T(4,128)}, u32[]{:S(2)}) copy-start(f32[4,512]{1,0:T(4,128)} %mix_bias.1) | copy-start | bytes 24580
  63.4 13.3 %copy-start = (bf16[1,128,3072]{2,1,0:T(8,128)(2,1)S(1)}, bf16[1,128,3072]{2,1,0:T(8,128)(2,1)}, u32[]{:S(2)}) copy-start(bf16[1,128,3072]{2,1,0:T(8,128)(2,1)} %values.5) | copy-start | bytes 2359300
  63.4 24.3 %collective-permute-start.12 = (bf16[4,64,768]{2,1,0:T(8,128)(2,1)S(1)}, bf16[4,64,768]{2,1,0:T(8,128)(2,1)S(1)}, u32[]{:S(2)}, u32[]{:S(2)}) collective-permute-start(bf16[4,64,768]{2,1,0:T(8,128)(2,1)S(1)} %get-tuple-element.58), channel_id=1, source_target_pairs={{0,1},{1,0},{2,3},{3,2},{4,5},{5,4},{6,7},{7,6},{8,9},{9,8},{10,11... | collective-permute-start | bytes 1179656 | tf_op jit(solution)/shard_map/ppermute | solution.py:526
  66.6 11.3 %collective-permute-start.9 = (bf16[128,768]{1,0:T(8,128)(2,1)S(1)}, bf16[128,768]{1,0:T(8,128)(2,1)S(1)}, u32[]{:S(2)}, u32[]{:S(2)}) collective-permute-start(bf16[128,768]{1,0:T(8,128)(2,1)S(1)} %get-tuple-element.44.v1.v), channel_id=1, source_target_pairs={{8,16},{16,8},{40,48},{48,40},{9,17},{17,9},{41,49},{49,41},{10,18... | collective-permute-start | bytes 589832 | tf_op jit(solution)/shard_map/ppermute | solution.py:494
  67.3 11.0 %collective-permute-start.8 = (bf16[128,768]{1,0:T(8,128)(2,1)S(1)}, bf16[128,768]{1,0:T(8,128)(2,1)S(1)}, u32[]{:S(2)}, u32[]{:S(2)}) collective-permute-start(bf16[128,768]{1,0:T(8,128)(2,1)S(1)} %get-tuple-element.44.v1.v), channel_id=1, source_target_pairs={{0,16},{24,8},{32,48},{56,40},{1,17},{25,9},{33,49},{57,41},{2,18}... | collective-permute-start | bytes 589832 | tf_op jit(solution)/shard_map/ppermute | solution.py:493
  74.3 8.2 %collective-permute-start.7 = (bf16[128,768]{1,0:T(8,128)(2,1)S(1)}, bf16[128,768]{1,0:T(8,128)(2,1)S(1)}, u32[]{:S(2)}, u32[]{:S(2)}) collective-permute-start(bf16[128,768]{1,0:T(8,128)(2,1)S(1)} %get-tuple-element.44.v1.v), channel_id=1, source_target_pairs={{0,8},{24,16},{32,40},{56,48},{1,9},{25,17},{33,41},{57,49},{2,10}... | collective-permute-start | bytes 589832 | tf_op jit(solution)/shard_map/ppermute | solution.py:492
  84.0 0.7 copy-start.13
  84.6 3.7 %copy-start.5 = (f32[128,768]{1,0:T(8,128)}, f32[128,768]{1,0:T(8,128)S(1)}, u32[]{:S(2)}) copy-start(f32[128,768]{1,0:T(8,128)S(1)} %get-tuple-element.50.refs_1_) | copy-start | bytes 1179652
  84.6 16.0 %copy-start.7 = (f32[128,768]{1,0:T(8,128)}, f32[128,768]{1,0:T(8,128)S(1)}, u32[]{:S(2)}) copy-start(f32[128,768]{1,0:T(8,128)S(1)} %get-tuple-element.51.refs_3_) | copy-start | bytes 1179652
  84.6 5.9 %collective-permute-start.14 = (bf16[5,64,256]{2,1,0:T(8,128)(2,1)S(1)}, bf16[5,64,256]{2,1,0:T(8,128)(2,1)S(1)}, u32[]{:S(2)}, u32[]{:S(2)}) collective-permute-start(bf16[5,64,256]{2,1,0:T(8,128)(2,1)S(1)} %get-tuple-element.63), channel_id=1, source_target_pairs={{0,1},{1,0},{2,3},{3,2},{4,5},{5,4},{6,7},{7,6},{8,9},{9,8},{10,11... | collective-permute-start | bytes 491528 | tf_op jit(solution)/shard_map/ppermute | solution.py:545
  88.3 11.7 %collective-permute-start.13 = (bf16[2,64,768]{2,1,0:T(8,128)(2,1)S(1)}, bf16[2,64,768]{2,1,0:T(8,128)(2,1)S(1)}, u32[]{:S(2)}, u32[]{:S(2)}) collective-permute-start(bf16[2,64,768]{2,1,0:T(8,128)(2,1)S(1)} %get-tuple-element.60), channel_id=1, source_target_pairs={{0,6},{6,0},{2,4},{4,2},{1,7},{7,1},{3,5},{5,3},{8,14},{14,8},{10,... | collective-permute-start | bytes 589832 | tf_op jit(solution)/shard_map/ppermute | solution.py:528
  91.1 8.8 %collective-permute-start.15 = (bf16[3,64,256]{2,1,0:T(8,128)(2,1)S(1)}, bf16[3,64,256]{2,1,0:T(8,128)(2,1)S(1)}, u32[]{:S(2)}, u32[]{:S(2)}) collective-permute-start(bf16[3,64,256]{2,1,0:T(8,128)(2,1)S(1)} %get-tuple-element.66), channel_id=1, source_target_pairs={{0,6},{6,0},{2,4},{4,2},{1,7},{7,1},{3,5},{5,3},{8,14},{14,8},{10,... | collective-permute-start | bytes 294920 | tf_op jit(solution)/shard_map/ppermute | solution.py:549
  100.6 6.8 %collective-permute-start.16 = (bf16[64,1280]{1,0:T(8,128)(2,1)S(1)}, bf16[64,1280]{1,0:T(8,128)(2,1)S(1)}, u32[]{:S(2)}, u32[]{:S(2)}) collective-permute-start(bf16[64,1280]{1,0:T(8,128)(2,1)S(1)} %get-tuple-element.69), channel_id=1, source_target_pairs={{0,2},{2,0},{4,6},{6,4},{1,3},{3,1},{5,7},{7,5},{8,10},{10,8},{12,... | collective-permute-start | bytes 491528 | tf_op jit(solution)/shard_map/ppermute | solution.py:551
  125.6 0.7 copy-start.3
  126.3 15.5 %all-to-all-start.1 = ((bf16[8,8,1280]{2,1,0:T(8,128)(2,1)}), bf16[8,8,1280]{2,1,0:T(8,128)(2,1)S(1)}, u32[]{:S(2)}, u32[]{:S(2)}) async-start(bf16[8,8,1280]{2,1,0:T(8,128)(2,1)} %copy-done.3), calls=%async_computation.1 | async-start | bytes 327680 | tf_op jit(solution)/shard_map/all_to_all | solution.py:468
  133.4 21.5 %collective-permute-start.10 = (bf16[128,2304]{1,0:T(8,128)(2,1)}, bf16[128,2304]{1,0:T(8,128)(2,1)}, u32[]{:S(2)}, u32[]{:S(2)}) collective-permute-start(bf16[128,2304]{1,0:T(8,128)(2,1)} %copy-done.4), channel_id=1, source_target_pairs={{8,0},{16,24},{40,32},{48,56},{9,1},{17,25},{41,33},{49,57},{10,2}... | collective-permute-start | bytes 1769480 | tf_op jit(solution)/shard_map/ppermute | solution.py:511
  141.8 0.7 copy-start.2
  142.5 19.3 %all-to-all-start.2 = ((bf16[8,8,2304]{2,1,0:T(8,128)(2,1)}), bf16[8,8,2304]{2,1,0:T(8,128)(2,1)}, u32[]{:S(2)}, u32[]{:S(2)}) async-start(bf16[8,8,2304]{2,1,0:T(8,128)(2,1)} %copy-done.2), calls=%async_computation.2 | async-start | bytes 589824 | tf_op jit(solution)/shard_map/all_to_all | solution.py:468
  146.6 8.3 %collective-permute-start.11 = (bf16[128,768]{1,0:T(8,128)(2,1)}, bf16[128,768]{1,0:T(8,128)(2,1)S(1)}, u32[]{:S(2)}, u32[]{:S(2)}) collective-permute-start(bf16[128,768]{1,0:T(8,128)(2,1)} %copy-done.13), channel_id=1, source_target_pairs={{8,0},{16,24},{40,32},{48,56},{9,1},{17,25},{41,33},{49,57},{10,2}... | collective-permute-start | bytes 589832 | tf_op jit(solution)/shard_map/ppermute | solution.py:543
  154.8 1.1 copy-start.1
  156.0 1.0 copy-start.6
  157.0 1.0 copy-start.8

commit v7 on v6

--- a/solution.py
+++ b/solution.py
@@ -317,41 +317,32 @@
     last_sums_kernel(place, values, stats, before, out_u, out_v, part, near, terms, small, send)
 
 
-def chip_kernel(place, keep, got, own, send):
+def chip_kernel(place, keep0, got0, keep1, small, got1, own, total, send):
+    extra = small[...] + (got1[4, :, :128].astype(F32) + got1[4, :, 128:].astype(F32))
+    high, low = split(extra)
+    total[...] = extra
+    send[0, :, 1024:] = high
+    send[1, :, 1024:] = low
     near = place[1] // 2 * 2
     for k in range(2):
-        own[k] = keep[near + k] + got[near + k].astype(F32)
         other = 2 - near + k
-        send[k] = (keep[other] + got[other].astype(F32)).astype(BF16)
-
-
-def last_chip_kernel(place, keep, small, got, own, total, send):
-    extra = small[...] + (got[4, :, :128].astype(F32) + got[4, :, 128:].astype(F32))
-    high, low = split(extra)
-    total[...] = extra
-    send[2, :, :128] = high
-    send[2, :, 128:] = low
-    near = place[1] // 2 * 2
-    for k in range(2):
-        own[k] = keep[near + k] + got[near + k].astype(F32)
-        other = 2 - near + k
-        send[k] = (keep[other] + got[other].astype(F32)).astype(BF16)
-
-
-def last_pair_kernel(place, keep0, got0, keep1, small, got1, own, total, send):
-    extra = small[...] + (got1[2, :, :128].astype(F32) + got1[2, :, 128:].astype(F32))
+        for keep, got, first, width in ((keep0, got0, 0, 384), (keep1, got1, 384, 128)):
+            for slot in range(2):
+                at = slice(slot * width, (slot + 1) * width)
+                lanes = slice(slot * 512 + first, slot * 512 + first + width)
+                own[k, :, lanes] = keep[near + k, :, at] + got[near + k, :, at].astype(F32)
+                send[k, :, lanes] = (keep[other, :, at] + got[other, :, at].astype(F32)).astype(BF16)
+
+
+def pair_kernel(place, keep, small, got, own, total, send):
+    extra = small[...] + (got[0, :, 1024:].astype(F32) + got[1, :, 1024:].astype(F32))
     high, low = split(extra)
     total[...] = extra
     send[:, 1024:1152] = high
     send[:, 1152:1280] = low
     b = place[1] % 2
-    for keep, got, first, width in ((keep0, got0, 0, 384), (keep1, got1, 384, 128)):
-        mine = keep[b] + got[b].astype(F32)
-        theirs = (keep[1 - b] + got[1 - b].astype(F32)).astype(BF16)
-        for slot in range(2):
-            lanes = slice(slot * 512 + first, slot * 512 + first + width)
-            own[:, lanes] = mine[:, slot * width : (slot + 1) * width]
-            send[:, lanes] = theirs[:, slot * width : (slot + 1) * width]
+    own[...] = keep[b] + got[b, :, :1024].astype(F32)
+    send[:, :1024] = (keep[1 - b] + got[1 - b, :, :1024].astype(F32)).astype(BF16)
 
 
 def deal_kernel(own, small, got, out):
@@ -520,12 +511,7 @@
         shape((64, 128), F32),
         (place, values_in, stats, bias_term, out_u, out_v, part, near[0]),
     )
-    keep, send = call(
-        chip_kernel,
-        [shape((2, SEG, 768), F32), shape((2, SEG, 768), BF16)],
-        (place, keep, lax.ppermute(send, CORE, PARTNER)),
-    )
-    chip = (keep, lax.ppermute(send, X, ACROSS))
+    folded = (keep, lax.ppermute(send, CORE, PARTNER))
 
     part, last_u, last_v, keep, small, last = call(
         last_kernel,
@@ -541,12 +527,15 @@
         scratch=[pltpu.VMEM((ROWS, WIDTH), BF16)] * 2 + [pltpu.VMEM((4, SEG, 256), BF16)],
     )
     outs_u, outs_v, got = (out_u, last_u), (out_v, last_v), (first_got, lax.ppermute(part, Y, OUT))
-    half_terms = [shape((2, SEG, 256), F32), shape((64, 128), F32), shape((3, SEG, 256), BF16)]
-    own, small, send = call(last_chip_kernel, half_terms, (place, keep, small, lax.ppermute(last, CORE, PARTNER)))
     own, small, send = call(
-        last_pair_kernel,
+        chip_kernel,
+        [shape((2, SEG, 1024), F32), shape((64, 128), F32), shape((2, SEG, 1152), BF16)],
+        (place, *folded, keep, small, lax.ppermute(last, CORE, PARTNER)),
+    )
+    own, small, send = call(
+        pair_kernel,
         [shape((SEG, 1024), F32), shape((64, 128), F32), shape((SEG, 1280), BF16)],
-        (place, *chip, own, small, lax.ppermute(send, X, ACROSS)),
+        (place, own, small, lax.ppermute(send, X, ACROSS)),
     )
     dealt = call(deal_kernel, shape((8, 8, 1280), BF16), (own, small, lax.ppermute(send, X, WITHIN)), 0)
     added = call(add_kernel, shape((8, 8, 1280), BF16), (exchanged(dealt, Z),), 0)

time: 167 us -> 165 us (0.988)
  the two profiles are of different devices: /device:TPU:1 before, /device:TPU:6 now
where the time goes in v7:
time: 165 us; the launch traced here: 164 us
  waiting for transfers between devices  63.9 us (39%)
  starting transfers between devices  53.1 us (32%)
  Pallas kernels  19.6 us (12%)
  blocking collectives  19.5 us (12%)
  local copies, waits for them, and re-layouts  6.95 us (4%)
    pallas_call x16, Pallas kernels, call(): pl.pallas_call(kernel, out_shape=out_shape, in_specs=[SMEM] * scalars + [...  19.6 us
    all_to_all x1, blocking collectives, exchanged(): return lax.all_to_all(x, axis, split_axis=0, concat_axis=0, tiled=True)  19.5 us
    ppermute x2, waiting for transfers between devices, compute(): far.append(lax.ppermute(vs[i], Y, FAR))  16.3 us
    all_to_all x2, starting transfers between devices, exchanged(): return lax.all_to_all(x, axis, split_axis=0, concat_axis=0, tiled=True)  14 us
    ppermute x3, starting transfers between devices, compute(): slabs = [slab] + [lax.ppermute(slab, X, CHIPS[k]) for k in range(1, 4)]  12.4 us
    ppermute x2, waiting for transfers between devices, compute(): near.append(lax.ppermute(vs[i], Y, NEAR))  10.2 us
    ppermute x1, waiting for transfers between devices, compute(): lax.ppermute(send, X, ACROSS)  9.68 us
    ppermute x2, starting transfers between devices, compute(): near.append(lax.ppermute(vs[i], Y, NEAR))  8.12 us
  transfers between devices with their start and end apart: 18, of which 12 were waited for; matrix products, arithmetic and copies ran while one was open for 0% of the time, Pallas kernels for 7%

profile of v7, /device:TPU:6, one launch (start us, length us, event | category | flops | bytes accessed | tf_op | source)
XLA Modules:
  0.0 164.2 jit_solution(14044538601132441388)
XLA Ops:
  0.6 0.1 pad_add_fusion.place
  0.7 0.9 copy-done.9
  1.7 1.0 shard_map.120.refs_0_
  2.6 7.7 %collective-permute-start.3 = (bf16[4,64,384]{2,1,0:T(8,128)(2,1)S(1)}, bf16[4,64,384]{2,1,0:T(8,128)(2,1)S(1)}, u32[]{:S(2)}, u32[]{:S(2)}) collective-permute-start(bf16[4,64,384]{2,1,0:T(8,128)(2,1)S(1)} %shard_map.120.refs_0_), channel_id=1, source_target_pairs={{0,2},{2,4},{4,6},{6,0},{1,3},{3,5},{5,7},{7,1},{8,10},{10,12},{12... | collective-permute-start | bytes 589832 | tf_op jit(solution)/shard_map/ppermute | solution.py:488
  10.4 1.9 %collective-permute-start.4 = (bf16[4,64,384]{2,1,0:T(8,128)(2,1)S(1)}, bf16[4,64,384]{2,1,0:T(8,128)(2,1)S(1)}, u32[]{:S(2)}, u32[]{:S(2)}) collective-permute-start(bf16[4,64,384]{2,1,0:T(8,128)(2,1)S(1)} %shard_map.120.refs_0_), channel_id=1, source_target_pairs={{0,4},{2,6},{4,0},{6,2},{1,5},{3,7},{5,1},{7,3},{8,12},{10,14},{12... | collective-permute-start | bytes 589832 | tf_op jit(solution)/shard_map/ppermute | solution.py:488
  12.3 2.8 %collective-permute-start.5 = (bf16[4,64,384]{2,1,0:T(8,128)(2,1)S(1)}, bf16[4,64,384]{2,1,0:T(8,128)(2,1)S(1)}, u32[]{:S(2)}, u32[]{:S(2)}) collective-permute-start(bf16[4,64,384]{2,1,0:T(8,128)(2,1)S(1)} %shard_map.120.refs_0_), channel_id=1, source_target_pairs={{0,6},{2,0},{4,2},{6,4},{1,7},{3,1},{5,3},{7,5},{8,14},{10,8},{12,... | collective-permute-start | bytes 589832 | tf_op jit(solution)/shard_map/ppermute | solution.py:488
  15.1 1.4 collective-permute-done.3.refs_1_
  16.5 3.0 %collective-permute-done.4.refs_2_ = bf16[4,64,384]{2,1,0:T(8,128)(2,1)S(1)} collective-permute-done((bf16[4,64,384]{2,1,0:T(8,128)(2,1)S(1)}, bf16[4,64,384]{2,1,0:T(8,128)(2,1)S(1)}, u32[]{:S(2)}, u32[]{:S(2)}) %collective-permute-start.4) | collective-permute-done | bytes 196640 | tf_op jit(solution)/shard_map/ppermute | solution.py:488
  19.5 2.1 %collective-permute-done.5.refs_3_ = bf16[4,64,384]{2,1,0:T(8,128)(2,1)S(1)} collective-permute-done((bf16[4,64,384]{2,1,0:T(8,128)(2,1)S(1)}, bf16[4,64,384]{2,1,0:T(8,128)(2,1)S(1)}, u32[]{:S(2)}, u32[]{:S(2)}) %collective-permute-start.5) | collective-permute-done | bytes 196640 | tf_op jit(solution)/shard_map/ppermute | solution.py:488
  21.5 0.6 shard_map.121.mine
  22.2 1.9 %collective-permute-start.6 = (bf16[4,4,64,384]{3,2,1,0:T(8,128)(2,1)S(1)}, bf16[4,4,64,384]{3,2,1,0:T(8,128)(2,1)S(1)}, u32[]{:S(2)}, u32[]{:S(2)}) collective-permute-start(bf16[4,4,64,384]{3,2,1,0:T(8,128)(2,1)S(1)} %shard_map.121.mine), channel_id=1, source_target_pairs={{0,1},{1,0},{2,3},{3,2},{4,5},{5,4},{6,7},{7,6},{8,9},{9,8},{10,11... | collective-permute-start | bytes 2359304 | tf_op jit(solution)/shard_map/ppermute | solution.py:490
  24.1 3.5 %shard_map.118 = (bf16[128,2304]{1,0:T(8,128)(2,1)S(1)}, bf16[128,768]{1,0:T(8,128)(2,1)S(1)}, bf16[128,2304]{1,0:T(8,128)(2,1)S(1)}, bf16[128,768]{1,0:T(8,128)(2,1)S(1)}, f32[2,128,128]{2,1,0:T(8,128)S(1)}) custom-call(s32[3]{0:T(128)S(1)} %pad_add_fusion.place, bf16[1,128,3072]{2,1,0:T(8,128)(2,1)} %values.5, bf16[1,128,3072]{2,1,0:T(8,128)(2,1)} %gated_in.1, ...), custom_call_target="tpu_custom_call" | custom-call | tf_op jit(solution)/shard_map/pallas_call | solution.py:51
  27.6 0.0 copy-start.10
  27.6 0.0 copy-start.11
  27.6 1.3 collective-permute-start
  28.9 1.9 %collective-permute-start.1 = (bf16[128,2304]{1,0:T(8,128)(2,1)S(1)}, bf16[128,2304]{1,0:T(8,128)(2,1)S(1)}, u32[]{:S(2)}, u32[]{:S(2)}) collective-permute-start(bf16[128,2304]{1,0:T(8,128)(2,1)S(1)} %get-tuple-element.40.v), channel_id=1, source_target_pairs={{0,16},{24,8},{32,48},{56,40},{1,17},{25,9},{33,49},{57,41},{2,18}... | collective-permute-start | bytes 1769480 | tf_op jit(solution)/shard_map/ppermute | solution.py:484
  30.9 0.7 collective-permute-start.2
  31.6 0.0 collective-permute-done.6.theirs
  31.6 0.9 shard_map.122.weights
  32.5 10.1 %collective-permute-done.near = bf16[128,2304]{1,0:T(8,128)(2,1)S(1)} collective-permute-done((bf16[128,2304]{1,0:T(8,128)(2,1)S(1)}, bf16[128,2304]{1,0:T(8,128)(2,1)S(1)}, u32[]{:S(2)}, u32[]{:S(2)}) %collective-permute-start) | collective-permute-done | bytes 589856 | tf_op jit(solution)/shard_map/ppermute | solution.py:483
  42.6 12.5 %collective-permute-done.1.far = bf16[128,2304]{1,0:T(8,128)(2,1)S(1)} collective-permute-done((bf16[128,2304]{1,0:T(8,128)(2,1)S(1)}, bf16[128,2304]{1,0:T(8,128)(2,1)S(1)}, u32[]{:S(2)}, u32[]{:S(2)}) %collective-permute-start.1) | collective-permute-done | bytes 589856 | tf_op jit(solution)/shard_map/ppermute | solution.py:484
  55.1 0.0 collective-permute-done.2.swap
  55.1 1.9 %shard_map.123 = (bf16[128,2304]{1,0:T(8,128)(2,1)S(1)}, f32[128,2304]{1,0:T(8,128)S(1)}, f32[128,2304]{1,0:T(8,128)S(1)}, bf16[128,2304]{1,0:T(8,128)(2,1)S(1)}, bf16[128,2304]{1,0:T(8,128)(2,1)S(1)}) custom-call(s32[3]{0:T(128)S(1)} %pad_add_fusion.place, bf16[128,2304]{1,0:T(8,128)(2,1)S(1)} %get-tuple-element.39.u, ...), custom_call_target="tpu_custom_call" | custom-call | tf_op jit(solution)/shard_map/pallas_call | solution.py:51
  57.0 0.0 copy-start.4
  57.1 0.0 copy-start.12
  57.1 1.3 shard_map.127
  58.3 0.0 copy-start
  58.3 2.1 %collective-permute-start.12 = (bf16[4,64,768]{2,1,0:T(8,128)(2,1)S(1)}, bf16[4,64,768]{2,1,0:T(8,128)(2,1)S(1)}, u32[]{:S(2)}, u32[]{:S(2)}) collective-permute-start(bf16[4,64,768]{2,1,0:T(8,128)(2,1)S(1)} %get-tuple-element.56), channel_id=1, source_target_pairs={{0,1},{1,0},{2,3},{3,2},{4,5},{5,4},{6,7},{7,6},{8,9},{9,8},{10,11... | collective-permute-start | bytes 1179656 | tf_op jit(solution)/shard_map/ppermute | solution.py:514
  60.4 6.8 %collective-permute-start.7 = (bf16[128,768]{1,0:T(8,128)(2,1)S(1)}, bf16[128,768]{1,0:T(8,128)(2,1)S(1)}, u32[]{:S(2)}, u32[]{:S(2)}) collective-permute-start(bf16[128,768]{1,0:T(8,128)(2,1)S(1)} %get-tuple-element.42.v1.v), channel_id=1, source_target_pairs={{0,8},{24,16},{32,40},{56,48},{1,9},{25,17},{33,41},{57,49},{2,10}... | collective-permute-start | bytes 589832 | tf_op jit(solution)/shard_map/ppermute | solution.py:483
  67.2 2.4 %collective-permute-start.8 = (bf16[128,768]{1,0:T(8,128)(2,1)S(1)}, bf16[128,768]{1,0:T(8,128)(2,1)S(1)}, u32[]{:S(2)}, u32[]{:S(2)}) collective-permute-start(bf16[128,768]{1,0:T(8,128)(2,1)S(1)} %get-tuple-element.42.v1.v), channel_id=1, source_target_pairs={{0,16},{24,8},{32,48},{56,40},{1,17},{25,9},{33,49},{57,41},{2,18}... | collective-permute-start | bytes 589832 | tf_op jit(solution)/shard_map/ppermute | solution.py:484
  69.6 0.7 collective-permute-start.9
  70.3 0.9 shard_map.119
  71.2 1.2 shard_map.124.before
  72.4 0.1 collective-permute-done.7.near
  72.5 3.8 %collective-permute-done.8.far = bf16[128,768]{1,0:T(8,128)(2,1)S(1)} collective-permute-done((bf16[128,768]{1,0:T(8,128)(2,1)S(1)}, bf16[128,768]{1,0:T(8,128)(2,1)S(1)}, u32[]{:S(2)}, u32[]{:S(2)}) %collective-permute-start.8) | collective-permute-done | bytes 196640 | tf_op jit(solution)/shard_map/ppermute | solution.py:484
  76.3 0.0 collective-permute-done.9.swap
  76.3 1.4 shard_map.125
  77.7 0.0 copy-start.5
  77.7 0.7 copy-done.5
  78.5 0.7 copy-done.7
  79.2 1.9 %collective-permute-start.13 = (bf16[5,64,256]{2,1,0:T(8,128)(2,1)S(1)}, bf16[5,64,256]{2,1,0:T(8,128)(2,1)S(1)}, u32[]{:S(2)}, u32[]{:S(2)}) collective-permute-start(bf16[5,64,256]{2,1,0:T(8,128)(2,1)S(1)} %get-tuple-element.59), channel_id=1, source_target_pairs={{0,1},{1,0},{2,3},{3,2},{4,5},{5,4},{6,7},{7,6},{8,9},{9,8},{10,11... | collective-permute-start | bytes 491528 | tf_op jit(solution)/shard_map/ppermute | solution.py:533
  81.1 1.4 collective-permute-done.13.got1
  82.5 0.6 shard_map.128
  83.1 2.5 %collective-permute-start.14 = (bf16[2,64,1152]{2,1,0:T(8,128)(2,1)S(1)}, bf16[2,64,1152]{2,1,0:T(8,128)(2,1)S(1)}, u32[]{:S(2)}, u32[]{:S(2)}) collective-permute-start(bf16[2,64,1152]{2,1,0:T(8,128)(2,1)S(1)} %get-tuple-element.62), channel_id=1, source_target_pairs={{0,6},{6,0},{2,4},{4,2},{1,7},{7,1},{3,5},{5,3},{8,14},{14,8},{10,... | collective-permute-start | bytes 884744 | tf_op jit(solution)/shard_map/ppermute | solution.py:538
  85.6 9.7 %collective-permute-done.14.got = bf16[2,64,1152]{2,1,0:T(8,128)(2,1)S(1)} collective-permute-done((bf16[2,64,1152]{2,1,0:T(8,128)(2,1)S(1)}, bf16[2,64,1152]{2,1,0:T(8,128)(2,1)S(1)}, u32[]{:S(2)}, u32[]{:S(2)}) %collective-permute-start.14) | collective-permute-done | bytes 294944 | tf_op jit(solution)/shard_map/ppermute | solution.py:538
  95.3 0.6 shard_map.129
  95.9 1.9 %collective-permute-start.15 = (bf16[64,1280]{1,0:T(8,128)(2,1)S(1)}, bf16[64,1280]{1,0:T(8,128)(2,1)S(1)}, u32[]{:S(2)}, u32[]{:S(2)}) collective-permute-start(bf16[64,1280]{1,0:T(8,128)(2,1)S(1)} %get-tuple-element.65), channel_id=1, source_target_pairs={{0,2},{2,0},{4,6},{6,4},{1,3},{3,1},{5,7},{7,5},{8,10},{10,8},{12,... | collective-permute-start | bytes 491528 | tf_op jit(solution)/shard_map/ppermute | solution.py:540
  97.8 5.4 %collective-permute-done.15.got = bf16[64,1280]{1,0:T(8,128)(2,1)S(1)} collective-permute-done((bf16[64,1280]{1,0:T(8,128)(2,1)S(1)}, bf16[64,1280]{1,0:T(8,128)(2,1)S(1)}, u32[]{:S(2)}, u32[]{:S(2)}) %collective-permute-start.15) | collective-permute-done | bytes 163872 | tf_op jit(solution)/shard_map/ppermute | solution.py:540
  103.2 19.5 %all_to_all.15.got = bf16[8,8,1280]{2,1,0:T(8,128)(2,1)S(1)} all-to-all(bf16[8,8,1280]{2,1,0:T(8,128)(2,1)S(1)} %shard_map.130), channel_id=1, replica_groups=mesh['sp_0'=8,'sp_1'=8,'dp_0'=4,'dp_1'=2] {'sp_0'}, dimensions={0} | all-to-all | bytes 327680 | tf_op jit(solution)/shard_map/all_to_all | solution.py:459
  122.8 0.7 copy-done.3
  123.5 9.9 %all-to-all-start.1 = ((bf16[8,8,1280]{2,1,0:T(8,128)(2,1)}), bf16[8,8,1280]{2,1,0:T(8,128)(2,1)S(1)}, u32[]{:S(2)}, u32[]{:S(2)}) async-start(bf16[8,8,1280]{2,1,0:T(8,128)(2,1)} %copy-done.3), calls=%async_computation.1 | async-start | bytes 327680 | tf_op jit(solution)/shard_map/all_to_all | solution.py:459
  133.4 1.3 collective-permute-start.10
  134.7 8.0 %all-to-all-done.1.got = bf16[8,8,1280]{2,1,0:T(8,128)(2,1)S(1)} async-done(((bf16[8,8,1280]{2,1,0:T(8,128)(2,1)}), bf16[8,8,1280]{2,1,0:T(8,128)(2,1)S(1)}, u32[]{:S(2)}, u32[]{:S(2)}) %all-to-all-start.1) | async-done | bytes 163872 | tf_op jit(solution)/shard_map/all_to_all | solution.py:459
  142.8 0.7 copy-done.2
  143.5 4.1 %all-to-all-start.2 = ((bf16[8,8,2304]{2,1,0:T(8,128)(2,1)}), bf16[8,8,2304]{2,1,0:T(8,128)(2,1)}, u32[]{:S(2)}, u32[]{:S(2)}) async-start(bf16[8,8,2304]{2,1,0:T(8,128)(2,1)} %copy-done.2), calls=%async_computation.2 | async-start | bytes 589824 | tf_op jit(solution)/shard_map/all_to_all | solution.py:459
  147.5 1.3 collective-permute-start.11
  148.8 6.5 %collective-permute-done.11.refs_5_ = bf16[128,768]{1,0:T(8,128)(2,1)S(1)} collective-permute-done((bf16[128,768]{1,0:T(8,128)(2,1)}, bf16[128,768]{1,0:T(8,128)(2,1)S(1)}, u32[]{:S(2)}, u32[]{:S(2)}) %collective-permute-start.11) | collective-permute-done | bytes 196640 | tf_op jit(solution)/shard_map/ppermute | solution.py:529
  155.3 0.0 collective-permute-done.10.refs_4_
  155.3 1.1 copy-done.1
  156.4 1.0 copy-done.6
  157.4 1.0 copy-done.8
  158.4 3.8 %shard_map.126 = (bf16[1,128,3072]{2,1,0:T(8,128)(2,1)}, bf16[1,128,3072]{2,1,0:T(8,128)(2,1)}) custom-call(s32[3]{0:T(128)S(1)} %pad_add_fusion.place, bf16[1,128,3072]{2,1,0:T(8,128)(2,1)S(1)} %copy-done, bf16[1,128,3072]{2,1,0:T(8,128)(2,1)S(1)} %copy-done.1, f32[2,128,128]{2,1,0:T(8,128)S(1)} %get-tuple-element.38.stats, ...), custom_call_target="tpu_custom_call" | custom-call | tf_op jit(solution)/shard_map/pallas_call | solution.py:51
  162.3 0.0 all-to-all-done.2.got
  162.3 1.9 %shard_map.133 = (f32[64,4,512]{2,1,0:T(4,128)}, f32[4,512]{1,0:T(4,128)}, f32[24,128]{1,0:T(8,128)}, f32[24,128]{1,0:T(8,128)}) custom-call(bf16[8,8,2304]{2,1,0:T(8,128)(2,1)} %all-to-all-done.2.got), custom_call_target="tpu_custom_call" | custom-call | tf_op jit(solution)/shard_map/pallas_call | solution.py:51
  (18 shorter events, 0.1 us)
Async XLA Ops:
  0.7 1.0 copy-start.9
  2.6 13.9 %collective-permute-start.3 = (bf16[4,64,384]{2,1,0:T(8,128)(2,1)S(1)}, bf16[4,64,384]{2,1,0:T(8,128)(2,1)S(1)}, u32[]{:S(2)}, u32[]{:S(2)}) collective-permute-start(bf16[4,64,384]{2,1,0:T(8,128)(2,1)S(1)} %shard_map.120.refs_0_), channel_id=1, source_target_pairs={{0,2},{2,4},{4,6},{6,0},{1,3},{3,5},{5,7},{7,1},{8,10},{10,12},{12... | collective-permute-start | bytes 589832 | tf_op jit(solution)/shard_map/ppermute | solution.py:488
  10.4 9.1 %collective-permute-start.4 = (bf16[4,64,384]{2,1,0:T(8,128)(2,1)S(1)}, bf16[4,64,384]{2,1,0:T(8,128)(2,1)S(1)}, u32[]{:S(2)}, u32[]{:S(2)}) collective-permute-start(bf16[4,64,384]{2,1,0:T(8,128)(2,1)S(1)} %shard_map.120.refs_0_), channel_id=1, source_target_pairs={{0,4},{2,6},{4,0},{6,2},{1,5},{3,7},{5,1},{7,3},{8,12},{10,14},{12... | collective-permute-start | bytes 589832 | tf_op jit(solution)/shard_map/ppermute | solution.py:488
  12.3 9.2 %collective-permute-start.5 = (bf16[4,64,384]{2,1,0:T(8,128)(2,1)S(1)}, bf16[4,64,384]{2,1,0:T(8,128)(2,1)S(1)}, u32[]{:S(2)}, u32[]{:S(2)}) collective-permute-start(bf16[4,64,384]{2,1,0:T(8,128)(2,1)S(1)} %shard_map.120.refs_0_), channel_id=1, source_target_pairs={{0,6},{2,0},{4,2},{6,4},{1,7},{3,1},{5,3},{7,5},{8,14},{10,8},{12,... | collective-permute-start | bytes 589832 | tf_op jit(solution)/shard_map/ppermute | solution.py:488
  22.2 9.4 %collective-permute-start.6 = (bf16[4,4,64,384]{3,2,1,0:T(8,128)(2,1)S(1)}, bf16[4,4,64,384]{3,2,1,0:T(8,128)(2,1)S(1)}, u32[]{:S(2)}, u32[]{:S(2)}) collective-permute-start(bf16[4,4,64,384]{3,2,1,0:T(8,128)(2,1)S(1)} %shard_map.121.mine), channel_id=1, source_target_pairs={{0,1},{1,0},{2,3},{3,2},{4,5},{5,4},{6,7},{7,6},{8,9},{9,8},{10,11... | collective-permute-start | bytes 2359304 | tf_op jit(solution)/shard_map/ppermute | solution.py:490
  27.6 27.5 %copy-start.10 = (f32[3072]{0:T(1024)S(1)}, f32[3072]{0:T(1024)}, u32[]{:S(2)}) copy-start(f32[3072]{0:T(1024)} %param.10) | copy-start | bytes 36868
  27.6 27.5 %copy-start.11 = (f32[3072]{0:T(1024)S(1)}, f32[3072]{0:T(1024)}, u32[]{:S(2)}) copy-start(f32[3072]{0:T(1024)} %param.11) | copy-start | bytes 36868
  27.6 15.0 %collective-permute-start = (bf16[128,2304]{1,0:T(8,128)(2,1)S(1)}, bf16[128,2304]{1,0:T(8,128)(2,1)S(1)}, u32[]{:S(2)}, u32[]{:S(2)}) collective-permute-start(bf16[128,2304]{1,0:T(8,128)(2,1)S(1)} %get-tuple-element.40.v), channel_id=1, source_target_pairs={{0,8},{24,16},{32,40},{56,48},{1,9},{25,17},{33,41},{57,49},{2,10}... | collective-permute-start | bytes 1769480 | tf_op jit(solution)/shard_map/ppermute | solution.py:483
  28.9 26.2 %collective-permute-start.1 = (bf16[128,2304]{1,0:T(8,128)(2,1)S(1)}, bf16[128,2304]{1,0:T(8,128)(2,1)S(1)}, u32[]{:S(2)}, u32[]{:S(2)}) collective-permute-start(bf16[128,2304]{1,0:T(8,128)(2,1)S(1)} %get-tuple-element.40.v), channel_id=1, source_target_pairs={{0,16},{24,8},{32,48},{56,40},{1,17},{25,9},{33,49},{57,41},{2,18}... | collective-permute-start | bytes 1769480 | tf_op jit(solution)/shard_map/ppermute | solution.py:484
  30.9 24.2 %collective-permute-start.2 = (bf16[128,2304]{1,0:T(8,128)(2,1)S(1)}, bf16[128,2304]{1,0:T(8,128)(2,1)S(1)}, u32[]{:S(2)}, u32[]{:S(2)}) collective-permute-start(bf16[128,2304]{1,0:T(8,128)(2,1)S(1)} %get-tuple-element.40.v), channel_id=1, source_target_pairs={{8,16},{16,8},{40,48},{48,40},{9,17},{17,9},{41,49},{49,41},{10,18... | collective-permute-start | bytes 1769480 | tf_op jit(solution)/shard_map/ppermute | solution.py:485
  57.0 14.1 %copy-start.4 = (bf16[128,2304]{1,0:T(8,128)(2,1)}, bf16[128,2304]{1,0:T(8,128)(2,1)S(1)}, u32[]{:S(2)}) copy-start(bf16[128,2304]{1,0:T(8,128)(2,1)S(1)} %get-tuple-element.47.part) | copy-start | bytes 1769476
  57.1 13.2 %copy-start.12 = (f32[4,512]{1,0:T(4,128)S(1)}, f32[4,512]{1,0:T(4,128)}, u32[]{:S(2)}) copy-start(f32[4,512]{1,0:T(4,128)} %mix_bias.1) | copy-start | bytes 24580
  58.3 12.8 %copy-start = (bf16[1,128,3072]{2,1,0:T(8,128)(2,1)S(1)}, bf16[1,128,3072]{2,1,0:T(8,128)(2,1)}, u32[]{:S(2)}) copy-start(bf16[1,128,3072]{2,1,0:T(8,128)(2,1)} %values.5) | copy-start | bytes 2359300
  58.3 24.1 %collective-permute-start.12 = (bf16[4,64,768]{2,1,0:T(8,128)(2,1)S(1)}, bf16[4,64,768]{2,1,0:T(8,128)(2,1)S(1)}, u32[]{:S(2)}, u32[]{:S(2)}) collective-permute-start(bf16[4,64,768]{2,1,0:T(8,128)(2,1)S(1)} %get-tuple-element.56), channel_id=1, source_target_pairs={{0,1},{1,0},{2,3},{3,2},{4,5},{5,4},{6,7},{7,6},{8,9},{9,8},{10,11... | collective-permute-start | bytes 1179656 | tf_op jit(solution)/shard_map/ppermute | solution.py:514
  60.4 12.1 %collective-permute-start.7 = (bf16[128,768]{1,0:T(8,128)(2,1)S(1)}, bf16[128,768]{1,0:T(8,128)(2,1)S(1)}, u32[]{:S(2)}, u32[]{:S(2)}) collective-permute-start(bf16[128,768]{1,0:T(8,128)(2,1)S(1)} %get-tuple-element.42.v1.v), channel_id=1, source_target_pairs={{0,8},{24,16},{32,40},{56,48},{1,9},{25,17},{33,41},{57,49},{2,10}... | collective-permute-start | bytes 589832 | tf_op jit(solution)/shard_map/ppermute | solution.py:483
  67.2 9.1 %collective-permute-start.8 = (bf16[128,768]{1,0:T(8,128)(2,1)S(1)}, bf16[128,768]{1,0:T(8,128)(2,1)S(1)}, u32[]{:S(2)}, u32[]{:S(2)}) collective-permute-start(bf16[128,768]{1,0:T(8,128)(2,1)S(1)} %get-tuple-element.42.v1.v), channel_id=1, source_target_pairs={{0,16},{24,8},{32,48},{56,40},{1,17},{25,9},{33,49},{57,41},{2,18}... | collective-permute-start | bytes 589832 | tf_op jit(solution)/shard_map/ppermute | solution.py:484
  69.6 6.7 %collective-permute-start.9 = (bf16[128,768]{1,0:T(8,128)(2,1)S(1)}, bf16[128,768]{1,0:T(8,128)(2,1)S(1)}, u32[]{:S(2)}, u32[]{:S(2)}) collective-permute-start(bf16[128,768]{1,0:T(8,128)(2,1)S(1)} %get-tuple-element.42.v1.v), channel_id=1, source_target_pairs={{8,16},{16,8},{40,48},{48,40},{9,17},{17,9},{41,49},{49,41},{10,18... | collective-permute-start | bytes 589832 | tf_op jit(solution)/shard_map/ppermute | solution.py:485
  77.7 0.7 copy-start.5
  78.4 0.7 copy-start.7
  79.2 16.7 %copy-start.13 = (bf16[128,768]{1,0:T(8,128)(2,1)}, bf16[128,768]{1,0:T(8,128)(2,1)S(1)}, u32[]{:S(2)}) copy-start(bf16[128,768]{1,0:T(8,128)(2,1)S(1)} %get-tuple-element.50) | copy-start | bytes 589828
  79.2 3.3 %collective-permute-start.13 = (bf16[5,64,256]{2,1,0:T(8,128)(2,1)S(1)}, bf16[5,64,256]{2,1,0:T(8,128)(2,1)S(1)}, u32[]{:S(2)}, u32[]{:S(2)}) collective-permute-start(bf16[5,64,256]{2,1,0:T(8,128)(2,1)S(1)} %get-tuple-element.59), channel_id=1, source_target_pairs={{0,1},{1,0},{2,3},{3,2},{4,5},{5,4},{6,7},{7,6},{8,9},{9,8},{10,11... | collective-permute-start | bytes 491528 | tf_op jit(solution)/shard_map/ppermute | solution.py:533
  83.1 12.2 %collective-permute-start.14 = (bf16[2,64,1152]{2,1,0:T(8,128)(2,1)S(1)}, bf16[2,64,1152]{2,1,0:T(8,128)(2,1)S(1)}, u32[]{:S(2)}, u32[]{:S(2)}) collective-permute-start(bf16[2,64,1152]{2,1,0:T(8,128)(2,1)S(1)} %get-tuple-element.62), channel_id=1, source_target_pairs={{0,6},{6,0},{2,4},{4,2},{1,7},{7,1},{3,5},{5,3},{8,14},{14,8},{10,... | collective-permute-start | bytes 884744 | tf_op jit(solution)/shard_map/ppermute | solution.py:538
  95.9 7.3 %collective-permute-start.15 = (bf16[64,1280]{1,0:T(8,128)(2,1)S(1)}, bf16[64,1280]{1,0:T(8,128)(2,1)S(1)}, u32[]{:S(2)}, u32[]{:S(2)}) collective-permute-start(bf16[64,1280]{1,0:T(8,128)(2,1)S(1)} %get-tuple-element.65), channel_id=1, source_target_pairs={{0,2},{2,0},{4,6},{6,4},{1,3},{3,1},{5,7},{7,5},{8,10},{10,8},{12,... | collective-permute-start | bytes 491528 | tf_op jit(solution)/shard_map/ppermute | solution.py:540
  122.8 0.7 copy-start.3
  123.5 19.3 %all-to-all-start.1 = ((bf16[8,8,1280]{2,1,0:T(8,128)(2,1)}), bf16[8,8,1280]{2,1,0:T(8,128)(2,1)S(1)}, u32[]{:S(2)}, u32[]{:S(2)}) async-start(bf16[8,8,1280]{2,1,0:T(8,128)(2,1)} %copy-done.3), calls=%async_computation.1 | async-start | bytes 327680 | tf_op jit(solution)/shard_map/all_to_all | solution.py:459
  133.4 21.9 %collective-permute-start.10 = (bf16[128,2304]{1,0:T(8,128)(2,1)}, bf16[128,2304]{1,0:T(8,128)(2,1)}, u32[]{:S(2)}, u32[]{:S(2)}) collective-permute-start(bf16[128,2304]{1,0:T(8,128)(2,1)} %copy-done.4), channel_id=1, source_target_pairs={{8,0},{16,24},{40,32},{48,56},{9,1},{17,25},{41,33},{49,57},{10,2}... | collective-permute-start | bytes 1769480 | tf_op jit(solution)/shard_map/ppermute | solution.py:502
  142.8 0.7 copy-start.2
  143.5 18.8 %all-to-all-start.2 = ((bf16[8,8,2304]{2,1,0:T(8,128)(2,1)}), bf16[8,8,2304]{2,1,0:T(8,128)(2,1)}, u32[]{:S(2)}, u32[]{:S(2)}) async-start(bf16[8,8,2304]{2,1,0:T(8,128)(2,1)} %copy-done.2), calls=%async_computation.2 | async-start | bytes 589824 | tf_op jit(solution)/shard_map/all_to_all | solution.py:459
  147.5 7.8 %collective-permute-start.11 = (bf16[128,768]{1,0:T(8,128)(2,1)}, bf16[128,768]{1,0:T(8,128)(2,1)S(1)}, u32[]{:S(2)}, u32[]{:S(2)}) collective-permute-start(bf16[128,768]{1,0:T(8,128)(2,1)} %copy-done.13), channel_id=1, source_target_pairs={{8,0},{16,24},{40,32},{48,56},{9,1},{17,25},{41,33},{49,57},{10,2}... | collective-permute-start | bytes 589832 | tf_op jit(solution)/shard_map/ppermute | solution.py:529
  155.3 1.1 copy-start.1
  156.4 1.0 copy-start.6
  157.4 1.0 copy-start.8

commit v8 on v7

--- a/solution.py
+++ b/solution.py
@@ -78,6 +78,27 @@
     chunk, start = PLACES[g]
     start = start // WIDTH * width
     return chunk, slice(start, start + width)
+
+
+TILES = [slice(k * 128, (k + 1) * 128) for k in range(HALF // 128)]
+
+
+def tile_of(k):
+    chunk, start = PLACES[k * 128 // WIDTH]
+    start += k * 128 % WIDTH
+    return chunk, slice(start, start + 128)
+
+
+def row_mean(terms):
+    totals = [None] * 4
+    for k, term in enumerate(terms):
+        totals[k % 4] = term if totals[k % 4] is None else totals[k % 4] + term
+    total = (totals[0] + totals[1]) + (totals[2] + totals[3])
+    return jnp.sum(total, axis=1, keepdims=True) * (1.0 / HALF)
+
+
+def add_term(totals, term):
+    return totals + [term] if len(totals) < 4 else totals[1:] + [totals[0] + term]
 
 
 def pre_kernel(place, values_in, gated_in, upstream_in, gain_in, shift_in, *outs):
@@ -108,30 +129,44 @@
     for single in singles:
         single.wait()
 
-    def block(i, carry):
+    def measure(i, carry):
         rows = pl.ds(pl.multiple_of(i * step, step), step)
-        raw = values[0, rows, :].astype(F32)
-        mean = jnp.sum(raw, axis=1, keepdims=True) * (1.0 / HALF)
-        centred = raw - mean
-        var = jnp.sum(centred * centred, axis=1, keepdims=True) * (1.0 / HALF)
-        inv = lax.rsqrt(var + EPS)
+        mean = row_mean(values[0, rows, at].astype(F32) for at in TILES)
+        centred = (values[0, rows, at].astype(F32) - mean for at in TILES)
+        inv = lax.rsqrt(row_mean(c * c for c in centred) + EPS)
         stats[0, rows, :] = jnp.broadcast_to(mean, (step, 128))
         stats[1, rows, :] = jnp.broadcast_to(inv, (step, 128))
-        for g in range(GROUPS):
-            cols = slice(g * WIDTH, (g + 1) * WIDTH)
-            unit = (values[0, rows, cols].astype(F32) - mean) * inv
-            normed = (unit * gain[:, cols] + shift[:, cols]).astype(BF16)
-            sent = unit.astype(BF16)
-            grad = (upstream[0, rows, cols].astype(F32) * gated[0, rows, cols].astype(F32)).astype(BF16)
-            i, lanes = lanes_of(g)
-            us[i][rows, lanes] = jnp.where(low, grad, normed)
-            vs[i][rows, lanes] = jnp.where(low, sent, grad)
         return carry
 
+    def block(low, i, carry):
+        rows = pl.ds(pl.multiple_of(i * step, step), step)
+        mean, inv = stats[0, rows, :], stats[1, rows, :]
+        for k, at in enumerate(TILES):
+            chunk, lanes = tile_of(k)
+            unit = (values[0, rows, at].astype(F32) - mean) * inv
+            grad = (upstream[0, rows, at].astype(F32) * gated[0, rows, at].astype(F32)).astype(BF16)
+            if low:
+                us[chunk][rows, lanes] = grad
+                vs[chunk][rows, lanes] = unit.astype(BF16)
+            else:
+                us[chunk][rows, lanes] = (unit * gain[:, at] + shift[:, at]).astype(BF16)
+                vs[chunk][rows, lanes] = grad
+        return carry
+
     for i in range(4):
-        for k in range(3):
+        copy(0, i).wait()
+        lax.fori_loop(i * part // step, (i + 1) * part // step, measure, 0, unroll=True)
+    for k in range(1, 3):
+        for i in range(4):
             copy(k, i).wait()
-        lax.fori_loop(i * part // step, (i + 1) * part // step, block, 0, unroll=True)
+
+    @pl.when(low)
+    def _():
+        lax.fori_loop(0, ROWS // step, functools.partial(block, True), 0, unroll=2)
+
+    @pl.when(jnp.logical_not(low))
+    def _():
+        lax.fori_loop(0, ROWS // step, functools.partial(block, False), 0, unroll=2)
 
 
 def side_kernel(place, u, v, u1, v1, mix_bias, columns, bias):
@@ -419,31 +454,26 @@
 
     def block(i, carry):
         rows = pl.ds(pl.multiple_of(i * step, step), step)
-        mean = stats[0, rows, :1]
-        inv = stats[1, rows, :1]
-        first = jnp.zeros((step, 1), F32)
-        second = jnp.zeros((step, 1), F32)
-        for g in range(GROUPS):
-            cols = slice(g * WIDTH, (g + 1) * WIDTH)
-            c, lanes = lanes_of(g)
-            long_side = outs_u[c][rows, lanes] + got[c][rows, lanes].astype(F32)
-            short_side = outs_v[c][rows, lanes]
+        mean, inv = stats[0, rows, :], stats[1, rows, :]
+        firsts, seconds = [], []
+        for k, at in enumerate(TILES):
+            chunk, lanes = tile_of(k)
+            g = k * 128 // WIDTH
+            long_side = outs_u[chunk][rows, lanes] + got[chunk][rows, lanes].astype(F32)
+            short_side = outs_v[chunk][rows, lanes]
             mixed = jnp.where(low, short_side, long_side) + columns[rows, g : g + 1]
             mixed = mixed.astype(BF16).astype(F32)
-            grad_u[0, rows, cols] = (upstream[0, rows, cols].astype(F32) * mixed).astype(BF16)
+            grad_u[0, rows, at] = (upstream[0, rows, at].astype(F32) * mixed).astype(BF16)
             back = jnp.where(low, long_side, short_side).astype(BF16)
-            backs[rows, cols] = back
-            scaled = back.astype(F32) * gain[:, cols]
-            unit = (values[0, rows, cols].astype(F32) - mean) * inv
-            first = first + jnp.sum(scaled, axis=1, keepdims=True)
-            second = second + jnp.sum(scaled * unit, axis=1, keepdims=True)
-        first = first * (1.0 / HALF)
-        second = second * (1.0 / HALF)
-        for g in range(GROUPS):
-            cols = slice(g * WIDTH, (g + 1) * WIDTH)
-            scaled = backs[rows, cols].astype(F32) * gain[:, cols]
-            unit = (values[0, rows, cols].astype(F32) - mean) * inv
-            grad_v[0, rows, cols] = (inv * (scaled - first - unit * second)).astype(BF16)
+            backs[rows, at] = back
+            scaled = back.astype(F32) * gain[:, at]
+            unit = (values[0, rows, at].astype(F32) - mean) * inv
+            firsts, seconds = add_term(firsts, scaled), add_term(seconds, scaled * unit)
+        first, second = row_mean(firsts), row_mean(seconds)
+        for at in TILES:
+            scaled = backs[rows, at].astype(F32) * gain[:, at]
+            unit = (values[0, rows, at].astype(F32) - mean) * inv
+            grad_v[0, rows, at] = (inv * (scaled - first - unit * second)).astype(BF16)
         return carry
 
     for i in range(4):

time: 165 us -> 165 us (level)
  transfers between devices with their start and end apart: 18 -> 18, of which waited for: 12 -> 11; matrix products, arithmetic and copies ran while one was open for 0% -> 0% of each run, Pallas kernels for 7% -> 7%
where the time goes in v8:
time: 165 us; the launch traced here: 164 us
  waiting for transfers between devices  63.7 us (39%)
  starting transfers between devices  53.3 us (32%)
  Pallas kernels  19.6 us (12%)
  blocking collectives  19.5 us (12%)
  local copies, waits for them, and re-layouts  6.95 us (4%)
    pallas_call x16, Pallas kernels, call(): pl.pallas_call(kernel, out_shape=out_shape, in_specs=[SMEM] * scalars + [...  19.6 us
    all_to_all x1, blocking collectives, exchanged(): return lax.all_to_all(x, axis, split_axis=0, concat_axis=0, tiled=True)  19.5 us
    ppermute x2, waiting for transfers between devices, compute(): far.append(lax.ppermute(vs[i], Y, FAR))  16.3 us
    all_to_all x2, starting transfers between devices, exchanged(): return lax.all_to_all(x, axis, split_axis=0, concat_axis=0, tiled=True)  14 us
    ppermute x3, starting transfers between devices, compute(): slabs = [slab] + [lax.ppermute(slab, X, CHIPS[k]) for k in range(1, 4)]  12.4 us
    ppermute x2, waiting for transfers between devices, compute(): near.append(lax.ppermute(vs[i], Y, NEAR))  10 us
    ppermute x1, waiting for transfers between devices, compute(): lax.ppermute(send, X, ACROSS)  9.68 us
    ppermute x2, starting transfers between devices, compute(): near.append(lax.ppermute(vs[i], Y, NEAR))  8.12 us
  transfers between devices with their start and end apart: 18, of which 11 were waited for; matrix products, arithmetic and copies ran while one was open for 0% of the time, Pallas kernels for 7%

profile of v8, /device:TPU:6, one launch (start us, length us, event | category | flops | bytes accessed | tf_op | source)
XLA Modules:
  0.0 164.1 jit_solution(11534591239636648640)
XLA Ops:
  0.6 0.1 pad_add_fusion.place
  0.7 0.9 copy-done.9
  1.7 1.0 shard_map.120.refs_0_
  2.6 7.7 %collective-permute-start.3 = (bf16[4,64,384]{2,1,0:T(8,128)(2,1)S(1)}, bf16[4,64,384]{2,1,0:T(8,128)(2,1)S(1)}, u32[]{:S(2)}, u32[]{:S(2)}) collective-permute-start(bf16[4,64,384]{2,1,0:T(8,128)(2,1)S(1)} %shard_map.120.refs_0_), channel_id=1, source_target_pairs={{0,2},{2,4},{4,6},{6,0},{1,3},{3,5},{5,7},{7,1},{8,10},{10,12},{12... | collective-permute-start | bytes 589832 | tf_op jit(solution)/shard_map/ppermute | solution.py:518
  10.4 1.9 %collective-permute-start.4 = (bf16[4,64,384]{2,1,0:T(8,128)(2,1)S(1)}, bf16[4,64,384]{2,1,0:T(8,128)(2,1)S(1)}, u32[]{:S(2)}, u32[]{:S(2)}) collective-permute-start(bf16[4,64,384]{2,1,0:T(8,128)(2,1)S(1)} %shard_map.120.refs_0_), channel_id=1, source_target_pairs={{0,4},{2,6},{4,0},{6,2},{1,5},{3,7},{5,1},{7,3},{8,12},{10,14},{12... | collective-permute-start | bytes 589832 | tf_op jit(solution)/shard_map/ppermute | solution.py:518
  12.3 2.8 %collective-permute-start.5 = (bf16[4,64,384]{2,1,0:T(8,128)(2,1)S(1)}, bf16[4,64,384]{2,1,0:T(8,128)(2,1)S(1)}, u32[]{:S(2)}, u32[]{:S(2)}) collective-permute-start(bf16[4,64,384]{2,1,0:T(8,128)(2,1)S(1)} %shard_map.120.refs_0_), channel_id=1, source_target_pairs={{0,6},{2,0},{4,2},{6,4},{1,7},{3,1},{5,3},{7,5},{8,14},{10,8},{12,... | collective-permute-start | bytes 589832 | tf_op jit(solution)/shard_map/ppermute | solution.py:518
  15.1 1.4 collective-permute-done.3.refs_1_
  16.5 3.0 %collective-permute-done.4.refs_2_ = bf16[4,64,384]{2,1,0:T(8,128)(2,1)S(1)} collective-permute-done((bf16[4,64,384]{2,1,0:T(8,128)(2,1)S(1)}, bf16[4,64,384]{2,1,0:T(8,128)(2,1)S(1)}, u32[]{:S(2)}, u32[]{:S(2)}) %collective-permute-start.4) | collective-permute-done | bytes 196640 | tf_op jit(solution)/shard_map/ppermute | solution.py:518
  19.5 2.1 %collective-permute-done.5.refs_3_ = bf16[4,64,384]{2,1,0:T(8,128)(2,1)S(1)} collective-permute-done((bf16[4,64,384]{2,1,0:T(8,128)(2,1)S(1)}, bf16[4,64,384]{2,1,0:T(8,128)(2,1)S(1)}, u32[]{:S(2)}, u32[]{:S(2)}) %collective-permute-start.5) | collective-permute-done | bytes 196640 | tf_op jit(solution)/shard_map/ppermute | solution.py:518
  21.5 0.6 shard_map.121.mine
  22.2 1.9 %collective-permute-start.6 = (bf16[4,4,64,384]{3,2,1,0:T(8,128)(2,1)S(1)}, bf16[4,4,64,384]{3,2,1,0:T(8,128)(2,1)S(1)}, u32[]{:S(2)}, u32[]{:S(2)}) collective-permute-start(bf16[4,4,64,384]{3,2,1,0:T(8,128)(2,1)S(1)} %shard_map.121.mine), channel_id=1, source_target_pairs={{0,1},{1,0},{2,3},{3,2},{4,5},{5,4},{6,7},{7,6},{8,9},{9,8},{10,11... | collective-permute-start | bytes 2359304 | tf_op jit(solution)/shard_map/ppermute | solution.py:520
  24.1 3.4 %shard_map.118 = (bf16[128,2304]{1,0:T(8,128)(2,1)S(1)}, bf16[128,768]{1,0:T(8,128)(2,1)S(1)}, bf16[128,2304]{1,0:T(8,128)(2,1)S(1)}, bf16[128,768]{1,0:T(8,128)(2,1)S(1)}, f32[2,128,128]{2,1,0:T(8,128)S(1)}) custom-call(s32[3]{0:T(128)S(1)} %pad_add_fusion.place, bf16[1,128,3072]{2,1,0:T(8,128)(2,1)} %values.5, bf16[1,128,3072]{2,1,0:T(8,128)(2,1)} %gated_in.1, ...), custom_call_target="tpu_custom_call" | custom-call | tf_op jit(solution)/shard_map/pallas_call | solution.py:51
  27.5 0.0 copy-start.10
  27.5 0.0 copy-start.11
  27.6 1.3 collective-permute-start
  28.9 2.1 %collective-permute-start.1 = (bf16[128,2304]{1,0:T(8,128)(2,1)S(1)}, bf16[128,2304]{1,0:T(8,128)(2,1)S(1)}, u32[]{:S(2)}, u32[]{:S(2)}) collective-permute-start(bf16[128,2304]{1,0:T(8,128)(2,1)S(1)} %get-tuple-element.40.v), channel_id=1, source_target_pairs={{0,16},{24,8},{32,48},{56,40},{1,17},{25,9},{33,49},{57,41},{2,18}... | collective-permute-start | bytes 1769480 | tf_op jit(solution)/shard_map/ppermute | solution.py:514
  31.0 0.7 collective-permute-start.2
  31.7 0.0 collective-permute-done.6.theirs
  31.7 0.9 shard_map.122.weights
  32.6 10.0 %collective-permute-done.near = bf16[128,2304]{1,0:T(8,128)(2,1)S(1)} collective-permute-done((bf16[128,2304]{1,0:T(8,128)(2,1)S(1)}, bf16[128,2304]{1,0:T(8,128)(2,1)S(1)}, u32[]{:S(2)}, u32[]{:S(2)}) %collective-permute-start) | collective-permute-done | bytes 589856 | tf_op jit(solution)/shard_map/ppermute | solution.py:513
  42.6 12.5 %collective-permute-done.1.far = bf16[128,2304]{1,0:T(8,128)(2,1)S(1)} collective-permute-done((bf16[128,2304]{1,0:T(8,128)(2,1)S(1)}, bf16[128,2304]{1,0:T(8,128)(2,1)S(1)}, u32[]{:S(2)}, u32[]{:S(2)}) %collective-permute-start.1) | collective-permute-done | bytes 589856 | tf_op jit(solution)/shard_map/ppermute | solution.py:514
  55.1 0.0 collective-permute-done.2.swap
  55.1 1.9 %shard_map.123 = (bf16[128,2304]{1,0:T(8,128)(2,1)S(1)}, f32[128,2304]{1,0:T(8,128)S(1)}, f32[128,2304]{1,0:T(8,128)S(1)}, bf16[128,2304]{1,0:T(8,128)(2,1)S(1)}, bf16[128,2304]{1,0:T(8,128)(2,1)S(1)}) custom-call(s32[3]{0:T(128)S(1)} %pad_add_fusion.place, bf16[128,2304]{1,0:T(8,128)(2,1)S(1)} %get-tuple-element.39.u, ...), custom_call_target="tpu_custom_call" | custom-call | tf_op jit(solution)/shard_map/pallas_call | solution.py:51
  57.0 0.0 copy-start.4
  57.0 0.0 copy-start.12
  57.0 1.3 shard_map.127
  58.3 0.0 copy-start
  58.3 2.1 %collective-permute-start.12 = (bf16[4,64,768]{2,1,0:T(8,128)(2,1)S(1)}, bf16[4,64,768]{2,1,0:T(8,128)(2,1)S(1)}, u32[]{:S(2)}, u32[]{:S(2)}) collective-permute-start(bf16[4,64,768]{2,1,0:T(8,128)(2,1)S(1)} %get-tuple-element.56), channel_id=1, source_target_pairs={{0,1},{1,0},{2,3},{3,2},{4,5},{5,4},{6,7},{7,6},{8,9},{9,8},{10,11... | collective-permute-start | bytes 1179656 | tf_op jit(solution)/shard_map/ppermute | solution.py:544
  60.4 6.8 %collective-permute-start.7 = (bf16[128,768]{1,0:T(8,128)(2,1)S(1)}, bf16[128,768]{1,0:T(8,128)(2,1)S(1)}, u32[]{:S(2)}, u32[]{:S(2)}) collective-permute-start(bf16[128,768]{1,0:T(8,128)(2,1)S(1)} %get-tuple-element.42.v1.v), channel_id=1, source_target_pairs={{0,8},{24,16},{32,40},{56,48},{1,9},{25,17},{33,41},{57,49},{2,10}... | collective-permute-start | bytes 589832 | tf_op jit(solution)/shard_map/ppermute | solution.py:513
  67.2 2.5 %collective-permute-start.8 = (bf16[128,768]{1,0:T(8,128)(2,1)S(1)}, bf16[128,768]{1,0:T(8,128)(2,1)S(1)}, u32[]{:S(2)}, u32[]{:S(2)}) collective-permute-start(bf16[128,768]{1,0:T(8,128)(2,1)S(1)} %get-tuple-element.42.v1.v), channel_id=1, source_target_pairs={{0,16},{24,8},{32,48},{56,40},{1,17},{25,9},{33,49},{57,41},{2,18}... | collective-permute-start | bytes 589832 | tf_op jit(solution)/shard_map/ppermute | solution.py:514
  69.7 0.7 collective-permute-start.9
  70.4 0.9 shard_map.119
  71.2 1.2 shard_map.124.before
  72.4 0.0 collective-permute-done.7.near
  72.4 3.8 %collective-permute-done.8.far = bf16[128,768]{1,0:T(8,128)(2,1)S(1)} collective-permute-done((bf16[128,768]{1,0:T(8,128)(2,1)S(1)}, bf16[128,768]{1,0:T(8,128)(2,1)S(1)}, u32[]{:S(2)}, u32[]{:S(2)}) %collective-permute-start.8) | collective-permute-done | bytes 196640 | tf_op jit(solution)/shard_map/ppermute | solution.py:514
  76.2 0.0 collective-permute-done.9.swap
  76.2 1.4 shard_map.125
  77.7 0.0 copy-start.5
  77.7 0.7 copy-done.5
  78.4 0.7 copy-done.7
  79.1 1.9 %collective-permute-start.13 = (bf16[5,64,256]{2,1,0:T(8,128)(2,1)S(1)}, bf16[5,64,256]{2,1,0:T(8,128)(2,1)S(1)}, u32[]{:S(2)}, u32[]{:S(2)}) collective-permute-start(bf16[5,64,256]{2,1,0:T(8,128)(2,1)S(1)} %get-tuple-element.59), channel_id=1, source_target_pairs={{0,1},{1,0},{2,3},{3,2},{4,5},{5,4},{6,7},{7,6},{8,9},{9,8},{10,11... | collective-permute-start | bytes 491528 | tf_op jit(solution)/shard_map/ppermute | solution.py:563
  81.1 1.4 collective-permute-done.13.got1
  82.4 0.0 collective-permute-done.12.got0
  82.4 0.6 shard_map.128
  83.1 2.5 %collective-permute-start.14 = (bf16[2,64,1152]{2,1,0:T(8,128)(2,1)S(1)}, bf16[2,64,1152]{2,1,0:T(8,128)(2,1)S(1)}, u32[]{:S(2)}, u32[]{:S(2)}) collective-permute-start(bf16[2,64,1152]{2,1,0:T(8,128)(2,1)S(1)} %get-tuple-element.62), channel_id=1, source_target_pairs={{0,6},{6,0},{2,4},{4,2},{1,7},{7,1},{3,5},{5,3},{8,14},{14,8},{10,... | collective-permute-start | bytes 884744 | tf_op jit(solution)/shard_map/ppermute | solution.py:568
  85.6 9.7 %collective-permute-done.14.got = bf16[2,64,1152]{2,1,0:T(8,128)(2,1)S(1)} collective-permute-done((bf16[2,64,1152]{2,1,0:T(8,128)(2,1)S(1)}, bf16[2,64,1152]{2,1,0:T(8,128)(2,1)S(1)}, u32[]{:S(2)}, u32[]{:S(2)}) %collective-permute-start.14) | collective-permute-done | bytes 294944 | tf_op jit(solution)/shard_map/ppermute | solution.py:568
  95.2 0.6 shard_map.129
  95.8 1.9 %collective-permute-start.15 = (bf16[64,1280]{1,0:T(8,128)(2,1)S(1)}, bf16[64,1280]{1,0:T(8,128)(2,1)S(1)}, u32[]{:S(2)}, u32[]{:S(2)}) collective-permute-start(bf16[64,1280]{1,0:T(8,128)(2,1)S(1)} %get-tuple-element.65), channel_id=1, source_target_pairs={{0,2},{2,0},{4,6},{6,4},{1,3},{3,1},{5,7},{7,5},{8,10},{10,8},{12,... | collective-permute-start | bytes 491528 | tf_op jit(solution)/shard_map/ppermute | solution.py:570
  97.8 5.4 %collective-permute-done.15.got = bf16[64,1280]{1,0:T(8,128)(2,1)S(1)} collective-permute-done((bf16[64,1280]{1,0:T(8,128)(2,1)S(1)}, bf16[64,1280]{1,0:T(8,128)(2,1)S(1)}, u32[]{:S(2)}, u32[]{:S(2)}) %collective-permute-start.15) | collective-permute-done | bytes 163872 | tf_op jit(solution)/shard_map/ppermute | solution.py:570
  103.2 19.5 %all_to_all.15.got = bf16[8,8,1280]{2,1,0:T(8,128)(2,1)S(1)} all-to-all(bf16[8,8,1280]{2,1,0:T(8,128)(2,1)S(1)} %shard_map.130), channel_id=1, replica_groups=mesh['sp_0'=8,'sp_1'=8,'dp_0'=4,'dp_1'=2] {'sp_0'}, dimensions={0} | all-to-all | bytes 327680 | tf_op jit(solution)/shard_map/all_to_all | solution.py:489
  122.8 0.7 copy-done.3
  123.4 9.9 %all-to-all-start.1 = ((bf16[8,8,1280]{2,1,0:T(8,128)(2,1)}), bf16[8,8,1280]{2,1,0:T(8,128)(2,1)S(1)}, u32[]{:S(2)}, u32[]{:S(2)}) async-start(bf16[8,8,1280]{2,1,0:T(8,128)(2,1)} %copy-done.3), calls=%async_computation.1 | async-start | bytes 327680 | tf_op jit(solution)/shard_map/all_to_all | solution.py:489
  133.4 1.3 collective-permute-start.10
  134.6 8.0 %all-to-all-done.1.got = bf16[8,8,1280]{2,1,0:T(8,128)(2,1)S(1)} async-done(((bf16[8,8,1280]{2,1,0:T(8,128)(2,1)}), bf16[8,8,1280]{2,1,0:T(8,128)(2,1)S(1)}, u32[]{:S(2)}, u32[]{:S(2)}) %all-to-all-start.1) | async-done | bytes 163872 | tf_op jit(solution)/shard_map/all_to_all | solution.py:489
  142.7 0.7 copy-done.2
  143.4 4.1 %all-to-all-start.2 = ((bf16[8,8,2304]{2,1,0:T(8,128)(2,1)}), bf16[8,8,2304]{2,1,0:T(8,128)(2,1)}, u32[]{:S(2)}, u32[]{:S(2)}) async-start(bf16[8,8,2304]{2,1,0:T(8,128)(2,1)} %copy-done.2), calls=%async_computation.2 | async-start | bytes 589824 | tf_op jit(solution)/shard_map/all_to_all | solution.py:489
  147.5 1.3 collective-permute-start.11
  148.8 6.5 %collective-permute-done.11.refs_5_ = bf16[128,768]{1,0:T(8,128)(2,1)S(1)} collective-permute-done((bf16[128,768]{1,0:T(8,128)(2,1)}, bf16[128,768]{1,0:T(8,128)(2,1)S(1)}, u32[]{:S(2)}, u32[]{:S(2)}) %collective-permute-start.11) | collective-permute-done | bytes 196640 | tf_op jit(solution)/shard_map/ppermute | solution.py:559
  155.2 0.0 collective-permute-done.10.refs_4_
  155.2 1.1 copy-done.1
  156.4 1.0 copy-done.6
  157.4 1.0 copy-done.8
  158.4 3.9 %shard_map.126 = (bf16[1,128,3072]{2,1,0:T(8,128)(2,1)}, bf16[1,128,3072]{2,1,0:T(8,128)(2,1)}) custom-call(s32[3]{0:T(128)S(1)} %pad_add_fusion.place, bf16[1,128,3072]{2,1,0:T(8,128)(2,1)S(1)} %copy-done, bf16[1,128,3072]{2,1,0:T(8,128)(2,1)S(1)} %copy-done.1, f32[2,128,128]{2,1,0:T(8,128)S(1)} %get-tuple-element.38.stats, ...), custom_call_target="tpu_custom_call" | custom-call | tf_op jit(solution)/shard_map/pallas_call | solution.py:51
  162.3 1.9 %shard_map.133 = (f32[64,4,512]{2,1,0:T(4,128)}, f32[4,512]{1,0:T(4,128)}, f32[24,128]{1,0:T(8,128)}, f32[24,128]{1,0:T(8,128)}) custom-call(bf16[8,8,2304]{2,1,0:T(8,128)(2,1)} %all-to-all-done.2.got), custom_call_target="tpu_custom_call" | custom-call | tf_op jit(solution)/shard_map/pallas_call | solution.py:51
  (18 shorter events, 0.1 us)
Async XLA Ops:
  0.7 1.0 copy-start.9
  2.6 13.9 %collective-permute-start.3 = (bf16[4,64,384]{2,1,0:T(8,128)(2,1)S(1)}, bf16[4,64,384]{2,1,0:T(8,128)(2,1)S(1)}, u32[]{:S(2)}, u32[]{:S(2)}) collective-permute-start(bf16[4,64,384]{2,1,0:T(8,128)(2,1)S(1)} %shard_map.120.refs_0_), channel_id=1, source_target_pairs={{0,2},{2,4},{4,6},{6,0},{1,3},{3,5},{5,7},{7,1},{8,10},{10,12},{12... | collective-permute-start | bytes 589832 | tf_op jit(solution)/shard_map/ppermute | solution.py:518
  10.4 9.1 %collective-permute-start.4 = (bf16[4,64,384]{2,1,0:T(8,128)(2,1)S(1)}, bf16[4,64,384]{2,1,0:T(8,128)(2,1)S(1)}, u32[]{:S(2)}, u32[]{:S(2)}) collective-permute-start(bf16[4,64,384]{2,1,0:T(8,128)(2,1)S(1)} %shard_map.120.refs_0_), channel_id=1, source_target_pairs={{0,4},{2,6},{4,0},{6,2},{1,5},{3,7},{5,1},{7,3},{8,12},{10,14},{12... | collective-permute-start | bytes 589832 | tf_op jit(solution)/shard_map/ppermute | solution.py:518
  12.3 9.2 %collective-permute-start.5 = (bf16[4,64,384]{2,1,0:T(8,128)(2,1)S(1)}, bf16[4,64,384]{2,1,0:T(8,128)(2,1)S(1)}, u32[]{:S(2)}, u32[]{:S(2)}) collective-permute-start(bf16[4,64,384]{2,1,0:T(8,128)(2,1)S(1)} %shard_map.120.refs_0_), channel_id=1, source_target_pairs={{0,6},{2,0},{4,2},{6,4},{1,7},{3,1},{5,3},{7,5},{8,14},{10,8},{12,... | collective-permute-start | bytes 589832 | tf_op jit(solution)/shard_map/ppermute | solution.py:518
  22.2 9.5 %collective-permute-start.6 = (bf16[4,4,64,384]{3,2,1,0:T(8,128)(2,1)S(1)}, bf16[4,4,64,384]{3,2,1,0:T(8,128)(2,1)S(1)}, u32[]{:S(2)}, u32[]{:S(2)}) collective-permute-start(bf16[4,4,64,384]{3,2,1,0:T(8,128)(2,1)S(1)} %shard_map.121.mine), channel_id=1, source_target_pairs={{0,1},{1,0},{2,3},{3,2},{4,5},{5,4},{6,7},{7,6},{8,9},{9,8},{10,11... | collective-permute-start | bytes 2359304 | tf_op jit(solution)/shard_map/ppermute | solution.py:520
  27.5 27.5 %copy-start.10 = (f32[3072]{0:T(1024)S(1)}, f32[3072]{0:T(1024)}, u32[]{:S(2)}) copy-start(f32[3072]{0:T(1024)} %param.10) | copy-start | bytes 36868
  27.5 27.5 %copy-start.11 = (f32[3072]{0:T(1024)S(1)}, f32[3072]{0:T(1024)}, u32[]{:S(2)}) copy-start(f32[3072]{0:T(1024)} %param.11) | copy-start | bytes 36868
  27.6 15.0 %collective-permute-start = (bf16[128,2304]{1,0:T(8,128)(2,1)S(1)}, bf16[128,2304]{1,0:T(8,128)(2,1)S(1)}, u32[]{:S(2)}, u32[]{:S(2)}) collective-permute-start(bf16[128,2304]{1,0:T(8,128)(2,1)S(1)} %get-tuple-element.40.v), channel_id=1, source_target_pairs={{0,8},{24,16},{32,40},{56,48},{1,9},{25,17},{33,41},{57,49},{2,10}... | collective-permute-start | bytes 1769480 | tf_op jit(solution)/shard_map/ppermute | solution.py:513
  28.9 26.2 %collective-permute-start.1 = (bf16[128,2304]{1,0:T(8,128)(2,1)S(1)}, bf16[128,2304]{1,0:T(8,128)(2,1)S(1)}, u32[]{:S(2)}, u32[]{:S(2)}) collective-permute-start(bf16[128,2304]{1,0:T(8,128)(2,1)S(1)} %get-tuple-element.40.v), channel_id=1, source_target_pairs={{0,16},{24,8},{32,48},{56,40},{1,17},{25,9},{33,49},{57,41},{2,18}... | collective-permute-start | bytes 1769480 | tf_op jit(solution)/shard_map/ppermute | solution.py:514
  31.0 24.1 %collective-permute-start.2 = (bf16[128,2304]{1,0:T(8,128)(2,1)S(1)}, bf16[128,2304]{1,0:T(8,128)(2,1)S(1)}, u32[]{:S(2)}, u32[]{:S(2)}) collective-permute-start(bf16[128,2304]{1,0:T(8,128)(2,1)S(1)} %get-tuple-element.40.v), channel_id=1, source_target_pairs={{8,16},{16,8},{40,48},{48,40},{9,17},{17,9},{41,49},{49,41},{10,18... | collective-permute-start | bytes 1769480 | tf_op jit(solution)/shard_map/ppermute | solution.py:515
  57.0 14.2 %copy-start.4 = (bf16[128,2304]{1,0:T(8,128)(2,1)}, bf16[128,2304]{1,0:T(8,128)(2,1)S(1)}, u32[]{:S(2)}) copy-start(bf16[128,2304]{1,0:T(8,128)(2,1)S(1)} %get-tuple-element.47.part) | copy-start | bytes 1769476
  57.0 13.4 %copy-start.12 = (f32[4,512]{1,0:T(4,128)S(1)}, f32[4,512]{1,0:T(4,128)}, u32[]{:S(2)}) copy-start(f32[4,512]{1,0:T(4,128)} %mix_bias.1) | copy-start | bytes 24580
  58.3 12.9 %copy-start = (bf16[1,128,3072]{2,1,0:T(8,128)(2,1)S(1)}, bf16[1,128,3072]{2,1,0:T(8,128)(2,1)}, u32[]{:S(2)}) copy-start(bf16[1,128,3072]{2,1,0:T(8,128)(2,1)} %values.5) | copy-start | bytes 2359300
  58.3 24.1 %collective-permute-start.12 = (bf16[4,64,768]{2,1,0:T(8,128)(2,1)S(1)}, bf16[4,64,768]{2,1,0:T(8,128)(2,1)S(1)}, u32[]{:S(2)}, u32[]{:S(2)}) collective-permute-start(bf16[4,64,768]{2,1,0:T(8,128)(2,1)S(1)} %get-tuple-element.56), channel_id=1, source_target_pairs={{0,1},{1,0},{2,3},{3,2},{4,5},{5,4},{6,7},{7,6},{8,9},{9,8},{10,11... | collective-permute-start | bytes 1179656 | tf_op jit(solution)/shard_map/ppermute | solution.py:544
  60.4 12.1 %collective-permute-start.7 = (bf16[128,768]{1,0:T(8,128)(2,1)S(1)}, bf16[128,768]{1,0:T(8,128)(2,1)S(1)}, u32[]{:S(2)}, u32[]{:S(2)}) collective-permute-start(bf16[128,768]{1,0:T(8,128)(2,1)S(1)} %get-tuple-element.42.v1.v), channel_id=1, source_target_pairs={{0,8},{24,16},{32,40},{56,48},{1,9},{25,17},{33,41},{57,49},{2,10}... | collective-permute-start | bytes 589832 | tf_op jit(solution)/shard_map/ppermute | solution.py:513
  67.2 9.1 %collective-permute-start.8 = (bf16[128,768]{1,0:T(8,128)(2,1)S(1)}, bf16[128,768]{1,0:T(8,128)(2,1)S(1)}, u32[]{:S(2)}, u32[]{:S(2)}) collective-permute-start(bf16[128,768]{1,0:T(8,128)(2,1)S(1)} %get-tuple-element.42.v1.v), channel_id=1, source_target_pairs={{0,16},{24,8},{32,48},{56,40},{1,17},{25,9},{33,49},{57,41},{2,18}... | collective-permute-start | bytes 589832 | tf_op jit(solution)/shard_map/ppermute | solution.py:514
  69.7 6.5 %collective-permute-start.9 = (bf16[128,768]{1,0:T(8,128)(2,1)S(1)}, bf16[128,768]{1,0:T(8,128)(2,1)S(1)}, u32[]{:S(2)}, u32[]{:S(2)}) collective-permute-start(bf16[128,768]{1,0:T(8,128)(2,1)S(1)} %get-tuple-element.42.v1.v), channel_id=1, source_target_pairs={{8,16},{16,8},{40,48},{48,40},{9,17},{17,9},{41,49},{49,41},{10,18... | collective-permute-start | bytes 589832 | tf_op jit(solution)/shard_map/ppermute | solution.py:515
  77.7 0.7 copy-start.5
  78.4 0.7 copy-start.7
  79.1 16.7 %copy-start.13 = (bf16[128,768]{1,0:T(8,128)(2,1)}, bf16[128,768]{1,0:T(8,128)(2,1)S(1)}, u32[]{:S(2)}) copy-start(bf16[128,768]{1,0:T(8,128)(2,1)S(1)} %get-tuple-element.50) | copy-start | bytes 589828
  79.1 3.3 %collective-permute-start.13 = (bf16[5,64,256]{2,1,0:T(8,128)(2,1)S(1)}, bf16[5,64,256]{2,1,0:T(8,128)(2,1)S(1)}, u32[]{:S(2)}, u32[]{:S(2)}) collective-permute-start(bf16[5,64,256]{2,1,0:T(8,128)(2,1)S(1)} %get-tuple-element.59), channel_id=1, source_target_pairs={{0,1},{1,0},{2,3},{3,2},{4,5},{5,4},{6,7},{7,6},{8,9},{9,8},{10,11... | collective-permute-start | bytes 491528 | tf_op jit(solution)/shard_map/ppermute | solution.py:563
  83.1 12.2 %collective-permute-start.14 = (bf16[2,64,1152]{2,1,0:T(8,128)(2,1)S(1)}, bf16[2,64,1152]{2,1,0:T(8,128)(2,1)S(1)}, u32[]{:S(2)}, u32[]{:S(2)}) collective-permute-start(bf16[2,64,1152]{2,1,0:T(8,128)(2,1)S(1)} %get-tuple-element.62), channel_id=1, source_target_pairs={{0,6},{6,0},{2,4},{4,2},{1,7},{7,1},{3,5},{5,3},{8,14},{14,8},{10,... | collective-permute-start | bytes 884744 | tf_op jit(solution)/shard_map/ppermute | solution.py:568
  95.8 7.3 %collective-permute-start.15 = (bf16[64,1280]{1,0:T(8,128)(2,1)S(1)}, bf16[64,1280]{1,0:T(8,128)(2,1)S(1)}, u32[]{:S(2)}, u32[]{:S(2)}) collective-permute-start(bf16[64,1280]{1,0:T(8,128)(2,1)S(1)} %get-tuple-element.65), channel_id=1, source_target_pairs={{0,2},{2,0},{4,6},{6,4},{1,3},{3,1},{5,7},{7,5},{8,10},{10,8},{12,... | collective-permute-start | bytes 491528 | tf_op jit(solution)/shard_map/ppermute | solution.py:570
  122.7 0.7 copy-start.3
  123.4 19.3 %all-to-all-start.1 = ((bf16[8,8,1280]{2,1,0:T(8,128)(2,1)}), bf16[8,8,1280]{2,1,0:T(8,128)(2,1)S(1)}, u32[]{:S(2)}, u32[]{:S(2)}) async-start(bf16[8,8,1280]{2,1,0:T(8,128)(2,1)} %copy-done.3), calls=%async_computation.1 | async-start | bytes 327680 | tf_op jit(solution)/shard_map/all_to_all | solution.py:489
  133.4 21.9 %collective-permute-start.10 = (bf16[128,2304]{1,0:T(8,128)(2,1)}, bf16[128,2304]{1,0:T(8,128)(2,1)}, u32[]{:S(2)}, u32[]{:S(2)}) collective-permute-start(bf16[128,2304]{1,0:T(8,128)(2,1)} %copy-done.4), channel_id=1, source_target_pairs={{8,0},{16,24},{40,32},{48,56},{9,1},{17,25},{41,33},{49,57},{10,2}... | collective-permute-start | bytes 1769480 | tf_op jit(solution)/shard_map/ppermute | solution.py:532
  142.7 0.7 copy-start.2
  143.4 18.8 %all-to-all-start.2 = ((bf16[8,8,2304]{2,1,0:T(8,128)(2,1)}), bf16[8,8,2304]{2,1,0:T(8,128)(2,1)}, u32[]{:S(2)}, u32[]{:S(2)}) async-start(bf16[8,8,2304]{2,1,0:T(8,128)(2,1)} %copy-done.2), calls=%async_computation.2 | async-start | bytes 589824 | tf_op jit(solution)/shard_map/all_to_all | solution.py:489
  147.5 7.8 %collective-permute-start.11 = (bf16[128,768]{1,0:T(8,128)(2,1)}, bf16[128,768]{1,0:T(8,128)(2,1)S(1)}, u32[]{:S(2)}, u32[]{:S(2)}) collective-permute-start(bf16[128,768]{1,0:T(8,128)(2,1)} %copy-done.13), channel_id=1, source_target_pairs={{8,0},{16,24},{40,32},{48,56},{9,1},{17,25},{41,33},{49,57},{10,2}... | collective-permute-start | bytes 589832 | tf_op jit(solution)/shard_map/ppermute | solution.py:559
  155.2 1.1 copy-start.1
  156.4 1.0 copy-start.6
  157.4 1.0 copy-start.8

commit v9 on v8

--- a/solution.py
+++ b/solution.py
@@ -519,7 +519,9 @@
     mine = call(join_kernel, shape((4, GROUPS, SEG, 3 * ROWS), BF16), (place, *slabs))
     theirs = lax.ppermute(mine, CORE, PARTNER)
     columns, bias_term = call(
-        side_kernel, [shape((ROWS, ROWS), F32), shape((64, 128), F32)], (place, us[0], vs[0], us[1], vs[1], mix_bias)
+        side_kernel,
+        [shape((ROWS, ROWS), F32), shape((64, 128), F32)],
+        (place, us[0], vs[0], us[1], vs[1], mix_bias),
     )
     weights = call(weight_kernel, shape((GROUPS, 2 * ROWS, 3 * ROWS), BF16), (place, mine, theirs))
 
@@ -567,7 +569,9 @@
         [shape((SEG, 1024), F32), shape((64, 128), F32), shape((SEG, 1280), BF16)],
         (place, own, small, lax.ppermute(send, X, ACROSS)),
     )
-    dealt = call(deal_kernel, shape((8, 8, 1280), BF16), (own, small, lax.ppermute(send, X, WITHIN)), 0)
+    dealt = call(
+        deal_kernel, shape((8, 8, 1280), BF16), (own, small, lax.ppermute(send, X, WITHIN)), 0
+    )
     added = call(add_kernel, shape((8, 8, 1280), BF16), (exchanged(dealt, Z),), 0)
     placed = call(place_kernel, shape((8, 8, 2304), BF16), (exchanged(added, Y),), 0)
     grad_mix, grad_bias, grad_gain, grad_shift = call(

time: 165 us -> 165 us (level)
  no operation moved by 1% of the time
where the time goes in v9:
time: 165 us; the launch traced here: 164 us
  waiting for transfers between devices  63.7 us (39%)
  starting transfers between devices  53.3 us (32%)
  Pallas kernels  19.6 us (12%)
  blocking collectives  19.5 us (12%)
  local copies, waits for them, and re-layouts  6.95 us (4%)
    pallas_call x16, Pallas kernels, call(): pl.pallas_call(kernel, out_shape=out_shape, in_specs=[SMEM] * scalars + [...  19.6 us
    all_to_all x1, blocking collectives, exchanged(): return lax.all_to_all(x, axis, split_axis=0, concat_axis=0, tiled=True)  19.5 us
    ppermute x2, waiting for transfers between devices, compute(): far.append(lax.ppermute(vs[i], Y, FAR))  16.3 us
    all_to_all x2, starting transfers between devices, exchanged(): return lax.all_to_all(x, axis, split_axis=0, concat_axis=0, tiled=True)  14 us
    ppermute x3, starting transfers between devices, compute(): slabs = [slab] + [lax.ppermute(slab, X, CHIPS[k]) for k in range(1, 4)]  12.4 us
    ppermute x2, waiting for transfers between devices, compute(): near.append(lax.ppermute(vs[i], Y, NEAR))  10 us
    ppermute x1, waiting for transfers between devices, compute(): lax.ppermute(send, X, ACROSS)  9.68 us
    ppermute x2, starting transfers between devices, compute(): near.append(lax.ppermute(vs[i], Y, NEAR))  8.12 us
  transfers between devices with their start and end apart: 18, of which 11 were waited for; matrix products, arithmetic and copies ran while one was open for 0% of the time, Pallas kernels for 7%

profile of v9, /device:TPU:6, one launch (start us, length us, event | category | flops | bytes accessed | tf_op | source)
XLA Modules:
  0.0 164.1 jit_solution(11534591239636648640)
XLA Ops:
  0.6 0.1 pad_add_fusion.place
  0.7 0.9 copy-done.9
  1.7 1.0 shard_map.120.refs_0_
  2.6 7.7 %collective-permute-start.3 = (bf16[4,64,384]{2,1,0:T(8,128)(2,1)S(1)}, bf16[4,64,384]{2,1,0:T(8,128)(2,1)S(1)}, u32[]{:S(2)}, u32[]{:S(2)}) collective-permute-start(bf16[4,64,384]{2,1,0:T(8,128)(2,1)S(1)} %shard_map.120.refs_0_), channel_id=1, source_target_pairs={{0,2},{2,4},{4,6},{6,0},{1,3},{3,5},{5,7},{7,1},{8,10},{10,12},{12... | collective-permute-start | bytes 589832 | tf_op jit(solution)/shard_map/ppermute | solution.py:518
  10.4 1.9 %collective-permute-start.4 = (bf16[4,64,384]{2,1,0:T(8,128)(2,1)S(1)}, bf16[4,64,384]{2,1,0:T(8,128)(2,1)S(1)}, u32[]{:S(2)}, u32[]{:S(2)}) collective-permute-start(bf16[4,64,384]{2,1,0:T(8,128)(2,1)S(1)} %shard_map.120.refs_0_), channel_id=1, source_target_pairs={{0,4},{2,6},{4,0},{6,2},{1,5},{3,7},{5,1},{7,3},{8,12},{10,14},{12... | collective-permute-start | bytes 589832 | tf_op jit(solution)/shard_map/ppermute | solution.py:518
  12.3 2.8 %collective-permute-start.5 = (bf16[4,64,384]{2,1,0:T(8,128)(2,1)S(1)}, bf16[4,64,384]{2,1,0:T(8,128)(2,1)S(1)}, u32[]{:S(2)}, u32[]{:S(2)}) collective-permute-start(bf16[4,64,384]{2,1,0:T(8,128)(2,1)S(1)} %shard_map.120.refs_0_), channel_id=1, source_target_pairs={{0,6},{2,0},{4,2},{6,4},{1,7},{3,1},{5,3},{7,5},{8,14},{10,8},{12,... | collective-permute-start | bytes 589832 | tf_op jit(solution)/shard_map/ppermute | solution.py:518
  15.1 1.4 collective-permute-done.3.refs_1_
  16.5 3.0 %collective-permute-done.4.refs_2_ = bf16[4,64,384]{2,1,0:T(8,128)(2,1)S(1)} collective-permute-done((bf16[4,64,384]{2,1,0:T(8,128)(2,1)S(1)}, bf16[4,64,384]{2,1,0:T(8,128)(2,1)S(1)}, u32[]{:S(2)}, u32[]{:S(2)}) %collective-permute-start.4) | collective-permute-done | bytes 196640 | tf_op jit(solution)/shard_map/ppermute | solution.py:518
  19.5 2.1 %collective-permute-done.5.refs_3_ = bf16[4,64,384]{2,1,0:T(8,128)(2,1)S(1)} collective-permute-done((bf16[4,64,384]{2,1,0:T(8,128)(2,1)S(1)}, bf16[4,64,384]{2,1,0:T(8,128)(2,1)S(1)}, u32[]{:S(2)}, u32[]{:S(2)}) %collective-permute-start.5) | collective-permute-done | bytes 196640 | tf_op jit(solution)/shard_map/ppermute | solution.py:518
  21.5 0.6 shard_map.121.mine
  22.2 1.9 %collective-permute-start.6 = (bf16[4,4,64,384]{3,2,1,0:T(8,128)(2,1)S(1)}, bf16[4,4,64,384]{3,2,1,0:T(8,128)(2,1)S(1)}, u32[]{:S(2)}, u32[]{:S(2)}) collective-permute-start(bf16[4,4,64,384]{3,2,1,0:T(8,128)(2,1)S(1)} %shard_map.121.mine), channel_id=1, source_target_pairs={{0,1},{1,0},{2,3},{3,2},{4,5},{5,4},{6,7},{7,6},{8,9},{9,8},{10,11... | collective-permute-start | bytes 2359304 | tf_op jit(solution)/shard_map/ppermute | solution.py:520
  24.1 3.4 %shard_map.118 = (bf16[128,2304]{1,0:T(8,128)(2,1)S(1)}, bf16[128,768]{1,0:T(8,128)(2,1)S(1)}, bf16[128,2304]{1,0:T(8,128)(2,1)S(1)}, bf16[128,768]{1,0:T(8,128)(2,1)S(1)}, f32[2,128,128]{2,1,0:T(8,128)S(1)}) custom-call(s32[3]{0:T(128)S(1)} %pad_add_fusion.place, bf16[1,128,3072]{2,1,0:T(8,128)(2,1)} %values.5, bf16[1,128,3072]{2,1,0:T(8,128)(2,1)} %gated_in.1, ...), custom_call_target="tpu_custom_call" | custom-call | tf_op jit(solution)/shard_map/pallas_call | solution.py:51
  27.5 0.0 copy-start.10
  27.5 0.0 copy-start.11
  27.6 1.3 collective-permute-start
  28.9 2.1 %collective-permute-start.1 = (bf16[128,2304]{1,0:T(8,128)(2,1)S(1)}, bf16[128,2304]{1,0:T(8,128)(2,1)S(1)}, u32[]{:S(2)}, u32[]{:S(2)}) collective-permute-start(bf16[128,2304]{1,0:T(8,128)(2,1)S(1)} %get-tuple-element.40.v), channel_id=1, source_target_pairs={{0,16},{24,8},{32,48},{56,40},{1,17},{25,9},{33,49},{57,41},{2,18}... | collective-permute-start | bytes 1769480 | tf_op jit(solution)/shard_map/ppermute | solution.py:514
  31.0 0.7 collective-permute-start.2
  31.7 0.0 collective-permute-done.6.theirs
  31.7 0.9 shard_map.122.weights
  32.6 10.0 %collective-permute-done.near = bf16[128,2304]{1,0:T(8,128)(2,1)S(1)} collective-permute-done((bf16[128,2304]{1,0:T(8,128)(2,1)S(1)}, bf16[128,2304]{1,0:T(8,128)(2,1)S(1)}, u32[]{:S(2)}, u32[]{:S(2)}) %collective-permute-start) | collective-permute-done | bytes 589856 | tf_op jit(solution)/shard_map/ppermute | solution.py:513
  42.6 12.5 %collective-permute-done.1.far = bf16[128,2304]{1,0:T(8,128)(2,1)S(1)} collective-permute-done((bf16[128,2304]{1,0:T(8,128)(2,1)S(1)}, bf16[128,2304]{1,0:T(8,128)(2,1)S(1)}, u32[]{:S(2)}, u32[]{:S(2)}) %collective-permute-start.1) | collective-permute-done | bytes 589856 | tf_op jit(solution)/shard_map/ppermute | solution.py:514
  55.1 0.0 collective-permute-done.2.swap
  55.1 1.9 %shard_map.123 = (bf16[128,2304]{1,0:T(8,128)(2,1)S(1)}, f32[128,2304]{1,0:T(8,128)S(1)}, f32[128,2304]{1,0:T(8,128)S(1)}, bf16[128,2304]{1,0:T(8,128)(2,1)S(1)}, bf16[128,2304]{1,0:T(8,128)(2,1)S(1)}) custom-call(s32[3]{0:T(128)S(1)} %pad_add_fusion.place, bf16[128,2304]{1,0:T(8,128)(2,1)S(1)} %get-tuple-element.39.u, ...), custom_call_target="tpu_custom_call" | custom-call | tf_op jit(solution)/shard_map/pallas_call | solution.py:51
  57.0 0.0 copy-start.4
  57.0 0.0 copy-start.12
  57.0 1.3 shard_map.127
  58.3 0.0 copy-start
  58.3 2.1 %collective-permute-start.12 = (bf16[4,64,768]{2,1,0:T(8,128)(2,1)S(1)}, bf16[4,64,768]{2,1,0:T(8,128)(2,1)S(1)}, u32[]{:S(2)}, u32[]{:S(2)}) collective-permute-start(bf16[4,64,768]{2,1,0:T(8,128)(2,1)S(1)} %get-tuple-element.56), channel_id=1, source_target_pairs={{0,1},{1,0},{2,3},{3,2},{4,5},{5,4},{6,7},{7,6},{8,9},{9,8},{10,11... | collective-permute-start | bytes 1179656 | tf_op jit(solution)/shard_map/ppermute | solution.py:546
  60.4 6.8 %collective-permute-start.7 = (bf16[128,768]{1,0:T(8,128)(2,1)S(1)}, bf16[128,768]{1,0:T(8,128)(2,1)S(1)}, u32[]{:S(2)}, u32[]{:S(2)}) collective-permute-start(bf16[128,768]{1,0:T(8,128)(2,1)S(1)} %get-tuple-element.42.v1.v), channel_id=1, source_target_pairs={{0,8},{24,16},{32,40},{56,48},{1,9},{25,17},{33,41},{57,49},{2,10}... | collective-permute-start | bytes 589832 | tf_op jit(solution)/shard_map/ppermute | solution.py:513
  67.2 2.5 %collective-permute-start.8 = (bf16[128,768]{1,0:T(8,128)(2,1)S(1)}, bf16[128,768]{1,0:T(8,128)(2,1)S(1)}, u32[]{:S(2)}, u32[]{:S(2)}) collective-permute-start(bf16[128,768]{1,0:T(8,128)(2,1)S(1)} %get-tuple-element.42.v1.v), channel_id=1, source_target_pairs={{0,16},{24,8},{32,48},{56,40},{1,17},{25,9},{33,49},{57,41},{2,18}... | collective-permute-start | bytes 589832 | tf_op jit(solution)/shard_map/ppermute | solution.py:514
  69.7 0.7 collective-permute-start.9
  70.4 0.9 shard_map.119
  71.2 1.2 shard_map.124.before
  72.4 0.0 collective-permute-done.7.near
  72.4 3.8 %collective-permute-done.8.far = bf16[128,768]{1,0:T(8,128)(2,1)S(1)} collective-permute-done((bf16[128,768]{1,0:T(8,128)(2,1)S(1)}, bf16[128,768]{1,0:T(8,128)(2,1)S(1)}, u32[]{:S(2)}, u32[]{:S(2)}) %collective-permute-start.8) | collective-permute-done | bytes 196640 | tf_op jit(solution)/shard_map/ppermute | solution.py:514
  76.2 0.0 collective-permute-done.9.swap
  76.2 1.4 shard_map.125
  77.7 0.0 copy-start.5
  77.7 0.7 copy-done.5
  78.4 0.7 copy-done.7
  79.1 1.9 %collective-permute-start.13 = (bf16[5,64,256]{2,1,0:T(8,128)(2,1)S(1)}, bf16[5,64,256]{2,1,0:T(8,128)(2,1)S(1)}, u32[]{:S(2)}, u32[]{:S(2)}) collective-permute-start(bf16[5,64,256]{2,1,0:T(8,128)(2,1)S(1)} %get-tuple-element.59), channel_id=1, source_target_pairs={{0,1},{1,0},{2,3},{3,2},{4,5},{5,4},{6,7},{7,6},{8,9},{9,8},{10,11... | collective-permute-start | bytes 491528 | tf_op jit(solution)/shard_map/ppermute | solution.py:565
  81.1 1.4 collective-permute-done.13.got1
  82.4 0.0 collective-permute-done.12.got0
  82.4 0.6 shard_map.128
  83.1 2.5 %collective-permute-start.14 = (bf16[2,64,1152]{2,1,0:T(8,128)(2,1)S(1)}, bf16[2,64,1152]{2,1,0:T(8,128)(2,1)S(1)}, u32[]{:S(2)}, u32[]{:S(2)}) collective-permute-start(bf16[2,64,1152]{2,1,0:T(8,128)(2,1)S(1)} %get-tuple-element.62), channel_id=1, source_target_pairs={{0,6},{6,0},{2,4},{4,2},{1,7},{7,1},{3,5},{5,3},{8,14},{14,8},{10,... | collective-permute-start | bytes 884744 | tf_op jit(solution)/shard_map/ppermute | solution.py:570
  85.6 9.7 %collective-permute-done.14.got = bf16[2,64,1152]{2,1,0:T(8,128)(2,1)S(1)} collective-permute-done((bf16[2,64,1152]{2,1,0:T(8,128)(2,1)S(1)}, bf16[2,64,1152]{2,1,0:T(8,128)(2,1)S(1)}, u32[]{:S(2)}, u32[]{:S(2)}) %collective-permute-start.14) | collective-permute-done | bytes 294944 | tf_op jit(solution)/shard_map/ppermute | solution.py:570
  95.2 0.6 shard_map.129
  95.8 1.9 %collective-permute-start.15 = (bf16[64,1280]{1,0:T(8,128)(2,1)S(1)}, bf16[64,1280]{1,0:T(8,128)(2,1)S(1)}, u32[]{:S(2)}, u32[]{:S(2)}) collective-permute-start(bf16[64,1280]{1,0:T(8,128)(2,1)S(1)} %get-tuple-element.65), channel_id=1, source_target_pairs={{0,2},{2,0},{4,6},{6,4},{1,3},{3,1},{5,7},{7,5},{8,10},{10,8},{12,... | collective-permute-start | bytes 491528 | tf_op jit(solution)/shard_map/ppermute | solution.py:573
  97.8 5.4 %collective-permute-done.15.got = bf16[64,1280]{1,0:T(8,128)(2,1)S(1)} collective-permute-done((bf16[64,1280]{1,0:T(8,128)(2,1)S(1)}, bf16[64,1280]{1,0:T(8,128)(2,1)S(1)}, u32[]{:S(2)}, u32[]{:S(2)}) %collective-permute-start.15) | collective-permute-done | bytes 163872 | tf_op jit(solution)/shard_map/ppermute | solution.py:573
  103.2 19.5 %all_to_all.15.got = bf16[8,8,1280]{2,1,0:T(8,128)(2,1)S(1)} all-to-all(bf16[8,8,1280]{2,1,0:T(8,128)(2,1)S(1)} %shard_map.130), channel_id=1, replica_groups=mesh['sp_0'=8,'sp_1'=8,'dp_0'=4,'dp_1'=2] {'sp_0'}, dimensions={0} | all-to-all | bytes 327680 | tf_op jit(solution)/shard_map/all_to_all | solution.py:489
  122.8 0.7 copy-done.3
  123.4 9.9 %all-to-all-start.1 = ((bf16[8,8,1280]{2,1,0:T(8,128)(2,1)}), bf16[8,8,1280]{2,1,0:T(8,128)(2,1)S(1)}, u32[]{:S(2)}, u32[]{:S(2)}) async-start(bf16[8,8,1280]{2,1,0:T(8,128)(2,1)} %copy-done.3), calls=%async_computation.1 | async-start | bytes 327680 | tf_op jit(solution)/shard_map/all_to_all | solution.py:489
  133.4 1.3 collective-permute-start.10
  134.6 8.0 %all-to-all-done.1.got = bf16[8,8,1280]{2,1,0:T(8,128)(2,1)S(1)} async-done(((bf16[8,8,1280]{2,1,0:T(8,128)(2,1)}), bf16[8,8,1280]{2,1,0:T(8,128)(2,1)S(1)}, u32[]{:S(2)}, u32[]{:S(2)}) %all-to-all-start.1) | async-done | bytes 163872 | tf_op jit(solution)/shard_map/all_to_all | solution.py:489
  142.7 0.7 copy-done.2
  143.4 4.1 %all-to-all-start.2 = ((bf16[8,8,2304]{2,1,0:T(8,128)(2,1)}), bf16[8,8,2304]{2,1,0:T(8,128)(2,1)}, u32[]{:S(2)}, u32[]{:S(2)}) async-start(bf16[8,8,2304]{2,1,0:T(8,128)(2,1)} %copy-done.2), calls=%async_computation.2 | async-start | bytes 589824 | tf_op jit(solution)/shard_map/all_to_all | solution.py:489
  147.5 1.3 collective-permute-start.11
  148.8 6.5 %collective-permute-done.11.refs_5_ = bf16[128,768]{1,0:T(8,128)(2,1)S(1)} collective-permute-done((bf16[128,768]{1,0:T(8,128)(2,1)}, bf16[128,768]{1,0:T(8,128)(2,1)S(1)}, u32[]{:S(2)}, u32[]{:S(2)}) %collective-permute-start.11) | collective-permute-done | bytes 196640 | tf_op jit(solution)/shard_map/ppermute | solution.py:561
  155.2 0.0 collective-permute-done.10.refs_4_
  155.2 1.1 copy-done.1
  156.4 1.0 copy-done.6
  157.4 1.0 copy-done.8
  158.4 3.9 %shard_map.126 = (bf16[1,128,3072]{2,1,0:T(8,128)(2,1)}, bf16[1,128,3072]{2,1,0:T(8,128)(2,1)}) custom-call(s32[3]{0:T(128)S(1)} %pad_add_fusion.place, bf16[1,128,3072]{2,1,0:T(8,128)(2,1)S(1)} %copy-done, bf16[1,128,3072]{2,1,0:T(8,128)(2,1)S(1)} %copy-done.1, f32[2,128,128]{2,1,0:T(8,128)S(1)} %get-tuple-element.38.stats, ...), custom_call_target="tpu_custom_call" | custom-call | tf_op jit(solution)/shard_map/pallas_call | solution.py:51
  162.3 1.9 %shard_map.133 = (f32[64,4,512]{2,1,0:T(4,128)}, f32[4,512]{1,0:T(4,128)}, f32[24,128]{1,0:T(8,128)}, f32[24,128]{1,0:T(8,128)}) custom-call(bf16[8,8,2304]{2,1,0:T(8,128)(2,1)} %all-to-all-done.2.got), custom_call_target="tpu_custom_call" | custom-call | tf_op jit(solution)/shard_map/pallas_call | solution.py:51
  (18 shorter events, 0.1 us)
Async XLA Ops:
  0.7 1.0 copy-start.9
  2.6 13.9 %collective-permute-start.3 = (bf16[4,64,384]{2,1,0:T(8,128)(2,1)S(1)}, bf16[4,64,384]{2,1,0:T(8,128)(2,1)S(1)}, u32[]{:S(2)}, u32[]{:S(2)}) collective-permute-start(bf16[4,64,384]{2,1,0:T(8,128)(2,1)S(1)} %shard_map.120.refs_0_), channel_id=1, source_target_pairs={{0,2},{2,4},{4,6},{6,0},{1,3},{3,5},{5,7},{7,1},{8,10},{10,12},{12... | collective-permute-start | bytes 589832 | tf_op jit(solution)/shard_map/ppermute | solution.py:518
  10.4 9.1 %collective-permute-start.4 = (bf16[4,64,384]{2,1,0:T(8,128)(2,1)S(1)}, bf16[4,64,384]{2,1,0:T(8,128)(2,1)S(1)}, u32[]{:S(2)}, u32[]{:S(2)}) collective-permute-start(bf16[4,64,384]{2,1,0:T(8,128)(2,1)S(1)} %shard_map.120.refs_0_), channel_id=1, source_target_pairs={{0,4},{2,6},{4,0},{6,2},{1,5},{3,7},{5,1},{7,3},{8,12},{10,14},{12... | collective-permute-start | bytes 589832 | tf_op jit(solution)/shard_map/ppermute | solution.py:518
  12.3 9.2 %collective-permute-start.5 = (bf16[4,64,384]{2,1,0:T(8,128)(2,1)S(1)}, bf16[4,64,384]{2,1,0:T(8,128)(2,1)S(1)}, u32[]{:S(2)}, u32[]{:S(2)}) collective-permute-start(bf16[4,64,384]{2,1,0:T(8,128)(2,1)S(1)} %shard_map.120.refs_0_), channel_id=1, source_target_pairs={{0,6},{2,0},{4,2},{6,4},{1,7},{3,1},{5,3},{7,5},{8,14},{10,8},{12,... | collective-permute-start | bytes 589832 | tf_op jit(solution)/shard_map/ppermute | solution.py:518
  22.2 9.5 %collective-permute-start.6 = (bf16[4,4,64,384]{3,2,1,0:T(8,128)(2,1)S(1)}, bf16[4,4,64,384]{3,2,1,0:T(8,128)(2,1)S(1)}, u32[]{:S(2)}, u32[]{:S(2)}) collective-permute-start(bf16[4,4,64,384]{3,2,1,0:T(8,128)(2,1)S(1)} %shard_map.121.mine), channel_id=1, source_target_pairs={{0,1},{1,0},{2,3},{3,2},{4,5},{5,4},{6,7},{7,6},{8,9},{9,8},{10,11... | collective-permute-start | bytes 2359304 | tf_op jit(solution)/shard_map/ppermute | solution.py:520
  27.5 27.5 %copy-start.10 = (f32[3072]{0:T(1024)S(1)}, f32[3072]{0:T(1024)}, u32[]{:S(2)}) copy-start(f32[3072]{0:T(1024)} %param.10) | copy-start | bytes 36868
  27.5 27.5 %copy-start.11 = (f32[3072]{0:T(1024)S(1)}, f32[3072]{0:T(1024)}, u32[]{:S(2)}) copy-start(f32[3072]{0:T(1024)} %param.11) | copy-start | bytes 36868
  27.6 15.0 %collective-permute-start = (bf16[128,2304]{1,0:T(8,128)(2,1)S(1)}, bf16[128,2304]{1,0:T(8,128)(2,1)S(1)}, u32[]{:S(2)}, u32[]{:S(2)}) collective-permute-start(bf16[128,2304]{1,0:T(8,128)(2,1)S(1)} %get-tuple-element.40.v), channel_id=1, source_target_pairs={{0,8},{24,16},{32,40},{56,48},{1,9},{25,17},{33,41},{57,49},{2,10}... | collective-permute-start | bytes 1769480 | tf_op jit(solution)/shard_map/ppermute | solution.py:513
  28.9 26.2 %collective-permute-start.1 = (bf16[128,2304]{1,0:T(8,128)(2,1)S(1)}, bf16[128,2304]{1,0:T(8,128)(2,1)S(1)}, u32[]{:S(2)}, u32[]{:S(2)}) collective-permute-start(bf16[128,2304]{1,0:T(8,128)(2,1)S(1)} %get-tuple-element.40.v), channel_id=1, source_target_pairs={{0,16},{24,8},{32,48},{56,40},{1,17},{25,9},{33,49},{57,41},{2,18}... | collective-permute-start | bytes 1769480 | tf_op jit(solution)/shard_map/ppermute | solution.py:514
  31.0 24.1 %collective-permute-start.2 = (bf16[128,2304]{1,0:T(8,128)(2,1)S(1)}, bf16[128,2304]{1,0:T(8,128)(2,1)S(1)}, u32[]{:S(2)}, u32[]{:S(2)}) collective-permute-start(bf16[128,2304]{1,0:T(8,128)(2,1)S(1)} %get-tuple-element.40.v), channel_id=1, source_target_pairs={{8,16},{16,8},{40,48},{48,40},{9,17},{17,9},{41,49},{49,41},{10,18... | collective-permute-start | bytes 1769480 | tf_op jit(solution)/shard_map/ppermute | solution.py:515
  57.0 14.2 %copy-start.4 = (bf16[128,2304]{1,0:T(8,128)(2,1)}, bf16[128,2304]{1,0:T(8,128)(2,1)S(1)}, u32[]{:S(2)}) copy-start(bf16[128,2304]{1,0:T(8,128)(2,1)S(1)} %get-tuple-element.47.part) | copy-start | bytes 1769476
  57.0 13.4 %copy-start.12 = (f32[4,512]{1,0:T(4,128)S(1)}, f32[4,512]{1,0:T(4,128)}, u32[]{:S(2)}) copy-start(f32[4,512]{1,0:T(4,128)} %mix_bias.1) | copy-start | bytes 24580
  58.3 12.9 %copy-start = (bf16[1,128,3072]{2,1,0:T(8,128)(2,1)S(1)}, bf16[1,128,3072]{2,1,0:T(8,128)(2,1)}, u32[]{:S(2)}) copy-start(bf16[1,128,3072]{2,1,0:T(8,128)(2,1)} %values.5) | copy-start | bytes 2359300
  58.3 24.1 %collective-permute-start.12 = (bf16[4,64,768]{2,1,0:T(8,128)(2,1)S(1)}, bf16[4,64,768]{2,1,0:T(8,128)(2,1)S(1)}, u32[]{:S(2)}, u32[]{:S(2)}) collective-permute-start(bf16[4,64,768]{2,1,0:T(8,128)(2,1)S(1)} %get-tuple-element.56), channel_id=1, source_target_pairs={{0,1},{1,0},{2,3},{3,2},{4,5},{5,4},{6,7},{7,6},{8,9},{9,8},{10,11... | collective-permute-start | bytes 1179656 | tf_op jit(solution)/shard_map/ppermute | solution.py:546
  60.4 12.1 %collective-permute-start.7 = (bf16[128,768]{1,0:T(8,128)(2,1)S(1)}, bf16[128,768]{1,0:T(8,128)(2,1)S(1)}, u32[]{:S(2)}, u32[]{:S(2)}) collective-permute-start(bf16[128,768]{1,0:T(8,128)(2,1)S(1)} %get-tuple-element.42.v1.v), channel_id=1, source_target_pairs={{0,8},{24,16},{32,40},{56,48},{1,9},{25,17},{33,41},{57,49},{2,10}... | collective-permute-start | bytes 589832 | tf_op jit(solution)/shard_map/ppermute | solution.py:513
  67.2 9.1 %collective-permute-start.8 = (bf16[128,768]{1,0:T(8,128)(2,1)S(1)}, bf16[128,768]{1,0:T(8,128)(2,1)S(1)}, u32[]{:S(2)}, u32[]{:S(2)}) collective-permute-start(bf16[128,768]{1,0:T(8,128)(2,1)S(1)} %get-tuple-element.42.v1.v), channel_id=1, source_target_pairs={{0,16},{24,8},{32,48},{56,40},{1,17},{25,9},{33,49},{57,41},{2,18}... | collective-permute-start | bytes 589832 | tf_op jit(solution)/shard_map/ppermute | solution.py:514
  69.7 6.5 %collective-permute-start.9 = (bf16[128,768]{1,0:T(8,128)(2,1)S(1)}, bf16[128,768]{1,0:T(8,128)(2,1)S(1)}, u32[]{:S(2)}, u32[]{:S(2)}) collective-permute-start(bf16[128,768]{1,0:T(8,128)(2,1)S(1)} %get-tuple-element.42.v1.v), channel_id=1, source_target_pairs={{8,16},{16,8},{40,48},{48,40},{9,17},{17,9},{41,49},{49,41},{10,18... | collective-permute-start | bytes 589832 | tf_op jit(solution)/shard_map/ppermute | solution.py:515
  77.7 0.7 copy-start.5
  78.4 0.7 copy-start.7
  79.1 16.7 %copy-start.13 = (bf16[128,768]{1,0:T(8,128)(2,1)}, bf16[128,768]{1,0:T(8,128)(2,1)S(1)}, u32[]{:S(2)}) copy-start(bf16[128,768]{1,0:T(8,128)(2,1)S(1)} %get-tuple-element.50) | copy-start | bytes 589828
  79.1 3.3 %collective-permute-start.13 = (bf16[5,64,256]{2,1,0:T(8,128)(2,1)S(1)}, bf16[5,64,256]{2,1,0:T(8,128)(2,1)S(1)}, u32[]{:S(2)}, u32[]{:S(2)}) collective-permute-start(bf16[5,64,256]{2,1,0:T(8,128)(2,1)S(1)} %get-tuple-element.59), channel_id=1, source_target_pairs={{0,1},{1,0},{2,3},{3,2},{4,5},{5,4},{6,7},{7,6},{8,9},{9,8},{10,11... | collective-permute-start | bytes 491528 | tf_op jit(solution)/shard_map/ppermute | solution.py:565
  83.1 12.2 %collective-permute-start.14 = (bf16[2,64,1152]{2,1,0:T(8,128)(2,1)S(1)}, bf16[2,64,1152]{2,1,0:T(8,128)(2,1)S(1)}, u32[]{:S(2)}, u32[]{:S(2)}) collective-permute-start(bf16[2,64,1152]{2,1,0:T(8,128)(2,1)S(1)} %get-tuple-element.62), channel_id=1, source_target_pairs={{0,6},{6,0},{2,4},{4,2},{1,7},{7,1},{3,5},{5,3},{8,14},{14,8},{10,... | collective-permute-start | bytes 884744 | tf_op jit(solution)/shard_map/ppermute | solution.py:570
  95.8 7.3 %collective-permute-start.15 = (bf16[64,1280]{1,0:T(8,128)(2,1)S(1)}, bf16[64,1280]{1,0:T(8,128)(2,1)S(1)}, u32[]{:S(2)}, u32[]{:S(2)}) collective-permute-start(bf16[64,1280]{1,0:T(8,128)(2,1)S(1)} %get-tuple-element.65), channel_id=1, source_target_pairs={{0,2},{2,0},{4,6},{6,4},{1,3},{3,1},{5,7},{7,5},{8,10},{10,8},{12,... | collective-permute-start | bytes 491528 | tf_op jit(solution)/shard_map/ppermute | solution.py:573
  122.7 0.7 copy-start.3
  123.4 19.3 %all-to-all-start.1 = ((bf16[8,8,1280]{2,1,0:T(8,128)(2,1)}), bf16[8,8,1280]{2,1,0:T(8,128)(2,1)S(1)}, u32[]{:S(2)}, u32[]{:S(2)}) async-start(bf16[8,8,1280]{2,1,0:T(8,128)(2,1)} %copy-done.3), calls=%async_computation.1 | async-start | bytes 327680 | tf_op jit(solution)/shard_map/all_to_all | solution.py:489
  133.4 21.9 %collective-permute-start.10 = (bf16[128,2304]{1,0:T(8,128)(2,1)}, bf16[128,2304]{1,0:T(8,128)(2,1)}, u32[]{:S(2)}, u32[]{:S(2)}) collective-permute-start(bf16[128,2304]{1,0:T(8,128)(2,1)} %copy-done.4), channel_id=1, source_target_pairs={{8,0},{16,24},{40,32},{48,56},{9,1},{17,25},{41,33},{49,57},{10,2}... | collective-permute-start | bytes 1769480 | tf_op jit(solution)/shard_map/ppermute | solution.py:534
  142.7 0.7 copy-start.2
  143.4 18.8 %all-to-all-start.2 = ((bf16[8,8,2304]{2,1,0:T(8,128)(2,1)}), bf16[8,8,2304]{2,1,0:T(8,128)(2,1)}, u32[]{:S(2)}, u32[]{:S(2)}) async-start(bf16[8,8,2304]{2,1,0:T(8,128)(2,1)} %copy-done.2), calls=%async_computation.2 | async-start | bytes 589824 | tf_op jit(solution)/shard_map/all_to_all | solution.py:489
  147.5 7.8 %collective-permute-start.11 = (bf16[128,768]{1,0:T(8,128)(2,1)}, bf16[128,768]{1,0:T(8,128)(2,1)S(1)}, u32[]{:S(2)}, u32[]{:S(2)}) collective-permute-start(bf16[128,768]{1,0:T(8,128)(2,1)} %copy-done.13), channel_id=1, source_target_pairs={{8,0},{16,24},{40,32},{48,56},{9,1},{17,25},{41,33},{49,57},{10,2}... | collective-permute-start | bytes 589832 | tf_op jit(solution)/shard_map/ppermute | solution.py:561
  155.2 1.1 copy-start.1
  156.4 1.0 copy-start.6
  157.4 1.0 copy-start.8

commit v10 on v9

--- a/solution.py
+++ b/solution.py
@@ -32,7 +32,8 @@
 ACROSS = [(0, 3), (3, 0), (1, 2), (2, 1)]
 WITHIN = [(0, 1), (1, 0), (2, 3), (3, 2)]
 
-CHUNKS = (3, 1)
+CHUNKS = (2, 2)
+WIDE = CHUNKS[0] * ROWS
 PLACES = [(i, k * WIDTH) for i, n in enumerate(CHUNKS) for k in range(n)]
 
 
@@ -340,9 +341,10 @@
 def last_sums_kernel(place, values, stats, before, out_u, out_v, part, near, last, small, send):
     sums_kernel(1, place, values, stats, before, out_u, out_v, part, near, small)
     send[:4] = last[...]
+    send[4] = jnp.zeros_like(send[4])
     high, low = split(small[...])
     send[4, :, :128] = high
-    send[4, :, 128:] = low
+    send[4, :, 128:256] = low
 
 
 def last_kernel(place, u, v, near, far, swap, weights, gain, shift, values, stats, before, *refs):
@@ -353,7 +355,7 @@
 
 
 def chip_kernel(place, keep0, got0, keep1, small, got1, own, total, send):
-    extra = small[...] + (got1[4, :, :128].astype(F32) + got1[4, :, 128:].astype(F32))
+    extra = small[...] + (got1[4, :, :128].astype(F32) + got1[4, :, 128:256].astype(F32))
     high, low = split(extra)
     total[...] = extra
     send[0, :, 1024:] = high
@@ -361,7 +363,7 @@
     near = place[1] // 2 * 2
     for k in range(2):
         other = 2 - near + k
-        for keep, got, first, width in ((keep0, got0, 0, 384), (keep1, got1, 384, 128)):
+        for keep, got, first, width in ((keep0, got0, 0, WIDE), (keep1, got1, WIDE, 512 - WIDE)):
             for slot in range(2):
                 at = slice(slot * width, (slot + 1) * width)
                 lanes = slice(slot * 512 + first, slot * 512 + first + width)
@@ -545,18 +547,19 @@
     )
     folded = (keep, lax.ppermute(send, CORE, PARTNER))
 
+    last_dims = (4, SEG, 2 * CHUNKS[1] * ROWS)
     part, last_u, last_v, keep, small, last = call(
         last_kernel,
         [
             halves[1],
             fulls[1],
             fulls[1],
-            shape((4, SEG, 256), F32),
+            shape(last_dims, F32),
             shape((64, 128), F32),
-            shape((5, SEG, 256), BF16),
+            shape((5, *last_dims[1:]), BF16),
         ],
         (place, *operands[1], weights, gain_row, shift_row, values_in, stats, sums),
-        scratch=[pltpu.VMEM((ROWS, WIDTH), BF16)] * 2 + [pltpu.VMEM((4, SEG, 256), BF16)],
+        scratch=[pltpu.VMEM(halves[1].shape, BF16)] * 2 + [pltpu.VMEM(last_dims, BF16)],
     )
     outs_u, outs_v, got = (out_u, last_u), (out_v, last_v), (first_got, lax.ppermute(part, Y, OUT))
     own, small, send = call(

time: 165 us -> 167 us (1.012)
  the two profiles are of different devices: /device:TPU:6 before, /device:TPU:64 now
where the time goes in v10:
time: 167 us; the launch traced here: 166 us
  starting transfers between devices  57 us (34%)
  waiting for transfers between devices  50.3 us (30%)
  blocking collectives  34.1 us (20%)
  Pallas kernels  19 us (11%)
  local copies, waits for them, and re-layouts  4.86 us (3%)
    all_to_all x2, blocking collectives, exchanged(): return lax.all_to_all(x, axis, split_axis=0, concat_axis=0, tiled=True)  34.1 us
    ppermute x2, starting transfers between devices, compute(): far.append(lax.ppermute(vs[i], Y, FAR))  24 us
    pallas_call x16, Pallas kernels, call(): pl.pallas_call(kernel, out_shape=out_shape, in_specs=[SMEM] * scalars + [...  19 us
    ppermute x1, waiting for transfers between devices, compute(): lax.ppermute(part, Y, OUT)  10.5 us
    ppermute x3, starting transfers between devices, compute(): slabs = [slab] + [lax.ppermute(slab, X, CHIPS[k]) for k in range(1, 4)]  10.2 us
    ppermute x1, waiting for transfers between devices, compute(): lax.ppermute(send, X, ACROSS)  9.91 us
    ppermute x3, waiting for transfers between devices, compute(): slabs = [slab] + [lax.ppermute(slab, X, CHIPS[k]) for k in range(1, 4)]  8.45 us
    ppermute x2, waiting for transfers between devices, compute(): near.append(lax.ppermute(vs[i], Y, NEAR))  6.67 us
  transfers between devices with their start and end apart: 17, of which 10 were waited for; matrix products, arithmetic and copies ran while one was open for 0% of the time, Pallas kernels for 7%

profile of v10, /device:TPU:64, one launch (start us, length us, event | category | flops | bytes accessed | tf_op | source)
XLA Modules:
  0.0 166.4 jit_solution(18140062568961267072)
XLA Ops:
  0.6 0.1 pad_add_fusion.place
  0.7 0.9 copy-done.8
  1.7 1.0 shard_map.120.refs_0_
  2.6 4.7 %collective-permute-start.5 = (bf16[4,64,384]{2,1,0:T(8,128)(2,1)S(1)}, bf16[4,64,384]{2,1,0:T(8,128)(2,1)S(1)}, u32[]{:S(2)}, u32[]{:S(2)}) collective-permute-start(bf16[4,64,384]{2,1,0:T(8,128)(2,1)S(1)} %shard_map.120.refs_0_), channel_id=1, source_target_pairs={{0,6},{2,0},{4,2},{6,4},{1,7},{3,1},{5,3},{7,5},{8,14},{10,8},{12,... | collective-permute-start | bytes 589832 | tf_op jit(solution)/shard_map/ppermute | solution.py:520
  7.3 2.7 %collective-permute-start.4 = (bf16[4,64,384]{2,1,0:T(8,128)(2,1)S(1)}, bf16[4,64,384]{2,1,0:T(8,128)(2,1)S(1)}, u32[]{:S(2)}, u32[]{:S(2)}) collective-permute-start(bf16[4,64,384]{2,1,0:T(8,128)(2,1)S(1)} %shard_map.120.refs_0_), channel_id=1, source_target_pairs={{0,4},{2,6},{4,0},{6,2},{1,5},{3,7},{5,1},{7,3},{8,12},{10,14},{12... | collective-permute-start | bytes 589832 | tf_op jit(solution)/shard_map/ppermute | solution.py:520
  10.0 2.8 %collective-permute-start.3 = (bf16[4,64,384]{2,1,0:T(8,128)(2,1)S(1)}, bf16[4,64,384]{2,1,0:T(8,128)(2,1)S(1)}, u32[]{:S(2)}, u32[]{:S(2)}) collective-permute-start(bf16[4,64,384]{2,1,0:T(8,128)(2,1)S(1)} %shard_map.120.refs_0_), channel_id=1, source_target_pairs={{0,2},{2,4},{4,6},{6,0},{1,3},{3,5},{5,7},{7,1},{8,10},{10,12},{12... | collective-permute-start | bytes 589832 | tf_op jit(solution)/shard_map/ppermute | solution.py:520
  12.8 2.9 %collective-permute-done.5.refs_3_ = bf16[4,64,384]{2,1,0:T(8,128)(2,1)S(1)} collective-permute-done((bf16[4,64,384]{2,1,0:T(8,128)(2,1)S(1)}, bf16[4,64,384]{2,1,0:T(8,128)(2,1)S(1)}, u32[]{:S(2)}, u32[]{:S(2)}) %collective-permute-start.5) | collective-permute-done | bytes 196640 | tf_op jit(solution)/shard_map/ppermute | solution.py:520
  15.7 2.8 %collective-permute-done.4.refs_2_ = bf16[4,64,384]{2,1,0:T(8,128)(2,1)S(1)} collective-permute-done((bf16[4,64,384]{2,1,0:T(8,128)(2,1)S(1)}, bf16[4,64,384]{2,1,0:T(8,128)(2,1)S(1)}, u32[]{:S(2)}, u32[]{:S(2)}) %collective-permute-start.4) | collective-permute-done | bytes 196640 | tf_op jit(solution)/shard_map/ppermute | solution.py:520
  18.5 2.8 %collective-permute-done.3.refs_1_ = bf16[4,64,384]{2,1,0:T(8,128)(2,1)S(1)} collective-permute-done((bf16[4,64,384]{2,1,0:T(8,128)(2,1)S(1)}, bf16[4,64,384]{2,1,0:T(8,128)(2,1)S(1)}, u32[]{:S(2)}, u32[]{:S(2)}) %collective-permute-start.3) | collective-permute-done | bytes 196640 | tf_op jit(solution)/shard_map/ppermute | solution.py:520
  21.3 0.6 shard_map.121.mine
  21.9 1.9 %collective-permute-start.6 = (bf16[4,4,64,384]{3,2,1,0:T(8,128)(2,1)S(1)}, bf16[4,4,64,384]{3,2,1,0:T(8,128)(2,1)S(1)}, u32[]{:S(2)}, u32[]{:S(2)}) collective-permute-start(bf16[4,4,64,384]{3,2,1,0:T(8,128)(2,1)S(1)} %shard_map.121.mine), channel_id=1, source_target_pairs={{0,1},{1,0},{2,3},{3,2},{4,5},{5,4},{6,7},{7,6},{8,9},{9,8},{10,11... | collective-permute-start | bytes 2359304 | tf_op jit(solution)/shard_map/ppermute | solution.py:522
  23.8 0.0 copy-start.11
  23.8 3.4 %shard_map.118 = (bf16[128,1536]{1,0:T(8,128)(2,1)S(1)}, bf16[128,1536]{1,0:T(8,128)(2,1)S(1)}, bf16[128,1536]{1,0:T(8,128)(2,1)S(1)}, bf16[128,1536]{1,0:T(8,128)(2,1)S(1)}, f32[2,128,128]{2,1,0:T(8,128)S(1)}) custom-call(s32[3]{0:T(128)S(1)} %pad_add_fusion.place, bf16[1,128,3072]{2,1,0:T(8,128)(2,1)} %values.5, bf16[1,128,3072]{2,1,0:T(8,128)(2,1)} %gated_in.1, ...), custom_call_target="tpu_custom_call" | custom-call | tf_op jit(solution)/shard_map/pallas_call | solution.py:52
  27.3 0.7 collective-permute-start.2
  28.0 6.2 %collective-permute-start.1 = (bf16[128,1536]{1,0:T(8,128)(2,1)S(1)}, bf16[128,1536]{1,0:T(8,128)(2,1)S(1)}, u32[]{:S(2)}, u32[]{:S(2)}) collective-permute-start(bf16[128,1536]{1,0:T(8,128)(2,1)S(1)} %get-tuple-element.40.v), channel_id=1, source_target_pairs={{0,16},{24,8},{32,48},{56,40},{1,17},{25,9},{33,49},{57,41},{2,18}... | collective-permute-start | bytes 1179656 | tf_op jit(solution)/shard_map/ppermute | solution.py:516
  34.2 1.5 collective-permute-start
  35.7 0.7 collective-permute-start.9
  36.4 0.0 collective-permute-done.2.swap
  36.4 17.8 %collective-permute-start.8 = (bf16[128,1536]{1,0:T(8,128)(2,1)S(1)}, bf16[128,1536]{1,0:T(8,128)(2,1)S(1)}, u32[]{:S(2)}, u32[]{:S(2)}) collective-permute-start(bf16[128,1536]{1,0:T(8,128)(2,1)S(1)} %get-tuple-element.42.v1.v), channel_id=1, source_target_pairs={{0,16},{24,8},{32,48},{56,40},{1,17},{25,9},{33,49},{57,41},{2,18}... | collective-permute-start | bytes 1179656 | tf_op jit(solution)/shard_map/ppermute | solution.py:516
  54.2 0.0 collective-permute-done.6.theirs
  54.2 1.3 collective-permute-start.7
  55.6 0.0 copy-done.11
  55.6 0.9 shard_map.119
  56.4 0.9 shard_map.122.weights
  57.3 0.0 copy-start
  57.3 0.0 collective-permute-done.1.far
  57.3 0.0 collective-permute-done.near
  57.4 0.0 copy-done.9
  57.4 0.0 copy-done.10
  57.4 1.5 shard_map.123
  58.8 0.0 copy-start.7
  58.9 0.0 copy-done
  58.9 0.9 shard_map.124.before
  59.8 0.0 copy-done.7
  59.8 0.0 collective-permute-done.9.swap
  59.8 3.9 %collective-permute-done.8.far = bf16[128,1536]{1,0:T(8,128)(2,1)S(1)} collective-permute-done((bf16[128,1536]{1,0:T(8,128)(2,1)S(1)}, bf16[128,1536]{1,0:T(8,128)(2,1)S(1)}, u32[]{:S(2)}, u32[]{:S(2)}) %collective-permute-start.8) | collective-permute-done | bytes 393248 | tf_op jit(solution)/shard_map/ppermute | solution.py:516
  63.7 6.7 %collective-permute-done.7.near = bf16[128,1536]{1,0:T(8,128)(2,1)S(1)} collective-permute-done((bf16[128,1536]{1,0:T(8,128)(2,1)S(1)}, bf16[128,1536]{1,0:T(8,128)(2,1)S(1)}, u32[]{:S(2)}, u32[]{:S(2)}) %collective-permute-start.7) | collective-permute-done | bytes 393248 | tf_op jit(solution)/shard_map/ppermute | solution.py:515
  70.4 2.3 %shard_map.125 = (bf16[128,1536]{1,0:T(8,128)(2,1)S(1)}, f32[128,1536]{1,0:T(8,128)S(1)}, f32[128,1536]{1,0:T(8,128)S(1)}, f32[4,64,512]{2,1,0:T(8,128)S(1)}, f3...) custom-call(s32[3]{0:T(128)S(1)} %pad_add_fusion.place, bf16[128,1536]{1,0:T(8,128)(2,1)S(1)} %get-tuple-element.41.u1.u, ...), custom_call_target="tpu_custom_call" | custom-call | tf_op jit(solution)/shard_map/pallas_call | solution.py:52
  72.7 0.9 copy-done.3
  73.6 1.9 %collective-permute-start.13 = (bf16[5,64,512]{2,1,0:T(8,128)(2,1)S(1)}, bf16[5,64,512]{2,1,0:T(8,128)(2,1)S(1)}, u32[]{:S(2)}, u32[]{:S(2)}) collective-permute-start(bf16[5,64,512]{2,1,0:T(8,128)(2,1)S(1)} %get-tuple-element.59), channel_id=1, source_target_pairs={{0,1},{1,0},{2,3},{3,2},{4,5},{5,4},{6,7},{7,6},{8,9},{9,8},{10,11... | collective-permute-start | bytes 983048 | tf_op jit(solution)/shard_map/ppermute | solution.py:568
  75.5 1.0 shard_map.127
  76.5 0.0 copy-done.5
  76.5 2.4 %collective-permute-start.12 = (bf16[4,64,512]{2,1,0:T(8,128)(2,1)S(1)}, bf16[4,64,512]{2,1,0:T(8,128)(2,1)S(1)}, u32[]{:S(2)}, u32[]{:S(2)}) collective-permute-start(bf16[4,64,512]{2,1,0:T(8,128)(2,1)S(1)} %get-tuple-element.56), channel_id=1, source_target_pairs={{0,1},{1,0},{2,3},{3,2},{4,5},{5,4},{6,7},{7,6},{8,9},{9,8},{10,11... | collective-permute-start | bytes 786440 | tf_op jit(solution)/shard_map/ppermute | solution.py:548
  78.9 1.1 collective-permute-done.12.got0
  80.1 0.0 collective-permute-done.13.got1
  80.1 0.6 shard_map.128
  80.7 2.5 %collective-permute-start.14 = (bf16[2,64,1152]{2,1,0:T(8,128)(2,1)S(1)}, bf16[2,64,1152]{2,1,0:T(8,128)(2,1)S(1)}, u32[]{:S(2)}, u32[]{:S(2)}) collective-permute-start(bf16[2,64,1152]{2,1,0:T(8,128)(2,1)S(1)} %get-tuple-element.62), channel_id=1, source_target_pairs={{0,6},{6,0},{2,4},{4,2},{1,7},{7,1},{3,5},{5,3},{8,14},{14,8},{10,... | collective-permute-start | bytes 884744 | tf_op jit(solution)/shard_map/ppermute | solution.py:573
  83.2 9.9 %collective-permute-done.14.got = bf16[2,64,1152]{2,1,0:T(8,128)(2,1)S(1)} collective-permute-done((bf16[2,64,1152]{2,1,0:T(8,128)(2,1)S(1)}, bf16[2,64,1152]{2,1,0:T(8,128)(2,1)S(1)}, u32[]{:S(2)}, u32[]{:S(2)}) %collective-permute-start.14) | collective-permute-done | bytes 294944 | tf_op jit(solution)/shard_map/ppermute | solution.py:573
  93.1 0.6 shard_map.129
  93.7 1.9 %collective-permute-start.15 = (bf16[64,1280]{1,0:T(8,128)(2,1)S(1)}, bf16[64,1280]{1,0:T(8,128)(2,1)S(1)}, u32[]{:S(2)}, u32[]{:S(2)}) collective-permute-start(bf16[64,1280]{1,0:T(8,128)(2,1)S(1)} %get-tuple-element.65), channel_id=1, source_target_pairs={{0,2},{2,0},{4,6},{6,4},{1,3},{3,1},{5,7},{7,5},{8,10},{10,8},{12,... | collective-permute-start | bytes 491528 | tf_op jit(solution)/shard_map/ppermute | solution.py:576
  95.7 5.6 %collective-permute-done.15.got = bf16[64,1280]{1,0:T(8,128)(2,1)S(1)} collective-permute-done((bf16[64,1280]{1,0:T(8,128)(2,1)S(1)}, bf16[64,1280]{1,0:T(8,128)(2,1)S(1)}, u32[]{:S(2)}, u32[]{:S(2)}) %collective-permute-start.15) | collective-permute-done | bytes 163872 | tf_op jit(solution)/shard_map/ppermute | solution.py:576
  101.3 17.7 %all_to_all.15.got = bf16[8,8,1280]{2,1,0:T(8,128)(2,1)S(1)} all-to-all(bf16[8,8,1280]{2,1,0:T(8,128)(2,1)S(1)} %shard_map.130), channel_id=1, replica_groups=mesh['sp_0'=8,'sp_1'=8,'dp_0'=4,'dp_1'=2] {'sp_0'}, dimensions={0} | all-to-all | bytes 327680 | tf_op jit(solution)/shard_map/all_to_all | solution.py:491
  119.0 16.4 %all_to_all.16.got = bf16[8,8,1280]{2,1,0:T(8,128)(2,1)S(1)} all-to-all(bf16[8,8,1280]{2,1,0:T(8,128)(2,1)S(1)} %shard_map.131), channel_id=1, replica_groups=mesh['sp_0'=8,'sp_1'=8,'dp_0'=4,'dp_1'=2] {'sp_1'}, dimensions={0} | all-to-all | bytes 327680 | tf_op jit(solution)/shard_map/all_to_all | solution.py:491
  135.4 0.7 copy-done.2
  136.2 5.4 %all-to-all-start.2 = ((bf16[8,8,2304]{2,1,0:T(8,128)(2,1)}), bf16[8,8,2304]{2,1,0:T(8,128)(2,1)}, u32[]{:S(2)}, u32[]{:S(2)}) async-start(bf16[8,8,2304]{2,1,0:T(8,128)(2,1)} %copy-done.2), calls=%async_computation.2 | async-start | bytes 589824 | tf_op jit(solution)/shard_map/all_to_all | solution.py:491
  141.6 1.3 collective-permute-start.11
  142.9 1.3 collective-permute-start.10
  144.2 10.5 %collective-permute-done.11.refs_5_ = bf16[128,1536]{1,0:T(8,128)(2,1)S(1)} collective-permute-done((bf16[128,1536]{1,0:T(8,128)(2,1)}, bf16[128,1536]{1,0:T(8,128)(2,1)S(1)}, u32[]{:S(2)}, u32[]{:S(2)}) %collective-permute-start.11) | collective-permute-done | bytes 393248 | tf_op jit(solution)/shard_map/ppermute | solution.py:564
  154.6 4.2 %collective-permute-done.10.refs_4_ = bf16[128,1536]{1,0:T(8,128)(2,1)S(1)} collective-permute-done((bf16[128,1536]{1,0:T(8,128)(2,1)}, bf16[128,1536]{1,0:T(8,128)(2,1)S(1)}, u32[]{:S(2)}, u32[]{:S(2)}) %collective-permute-start.10) | collective-permute-done | bytes 393248 | tf_op jit(solution)/shard_map/ppermute | solution.py:536
  158.8 1.1 copy-done.4
  160.0 1.1 copy-done.6
  161.1 3.4 %shard_map.126 = (bf16[1,128,3072]{2,1,0:T(8,128)(2,1)}, bf16[1,128,3072]{2,1,0:T(8,128)(2,1)}) custom-call(s32[3]{0:T(128)S(1)} %pad_add_fusion.place, bf16[1,128,3072]{2,1,0:T(8,128)(2,1)S(1)} %copy-done, bf16[1,128,3072]{2,1,0:T(8,128)(2,1)S(1)} %copy-done.1, f32[2,128,128]{2,1,0:T(8,128)S(1)} %get-tuple-element.38.stats, ...), custom_call_target="tpu_custom_call" | custom-call | tf_op jit(solution)/shard_map/pallas_call | solution.py:52
  164.5 0.0 all-to-all-done.2.got
  164.5 1.9 %shard_map.133 = (f32[64,4,512]{2,1,0:T(4,128)}, f32[4,512]{1,0:T(4,128)}, f32[24,128]{1,0:T(8,128)}, f32[24,128]{1,0:T(8,128)}) custom-call(bf16[8,8,2304]{2,1,0:T(8,128)(2,1)} %all-to-all-done.2.got), custom_call_target="tpu_custom_call" | custom-call | tf_op jit(solution)/shard_map/pallas_call | solution.py:52
  (15 shorter events, 0.1 us)
Async XLA Ops:
  0.7 1.0 copy-start.8
  2.6 13.1 %collective-permute-start.5 = (bf16[4,64,384]{2,1,0:T(8,128)(2,1)S(1)}, bf16[4,64,384]{2,1,0:T(8,128)(2,1)S(1)}, u32[]{:S(2)}, u32[]{:S(2)}) collective-permute-start(bf16[4,64,384]{2,1,0:T(8,128)(2,1)S(1)} %shard_map.120.refs_0_), channel_id=1, source_target_pairs={{0,6},{2,0},{4,2},{6,4},{1,7},{3,1},{5,3},{7,5},{8,14},{10,8},{12,... | collective-permute-start | bytes 589832 | tf_op jit(solution)/shard_map/ppermute | solution.py:520
  7.3 11.2 %collective-permute-start.4 = (bf16[4,64,384]{2,1,0:T(8,128)(2,1)S(1)}, bf16[4,64,384]{2,1,0:T(8,128)(2,1)S(1)}, u32[]{:S(2)}, u32[]{:S(2)}) collective-permute-start(bf16[4,64,384]{2,1,0:T(8,128)(2,1)S(1)} %shard_map.120.refs_0_), channel_id=1, source_target_pairs={{0,4},{2,6},{4,0},{6,2},{1,5},{3,7},{5,1},{7,3},{8,12},{10,14},{12... | collective-permute-start | bytes 589832 | tf_op jit(solution)/shard_map/ppermute | solution.py:520
  10.0 11.3 %collective-permute-start.3 = (bf16[4,64,384]{2,1,0:T(8,128)(2,1)S(1)}, bf16[4,64,384]{2,1,0:T(8,128)(2,1)S(1)}, u32[]{:S(2)}, u32[]{:S(2)}) collective-permute-start(bf16[4,64,384]{2,1,0:T(8,128)(2,1)S(1)} %shard_map.120.refs_0_), channel_id=1, source_target_pairs={{0,2},{2,4},{4,6},{6,0},{1,3},{3,5},{5,7},{7,1},{8,10},{10,12},{12... | collective-permute-start | bytes 589832 | tf_op jit(solution)/shard_map/ppermute | solution.py:520
  21.9 32.3 %collective-permute-start.6 = (bf16[4,4,64,384]{3,2,1,0:T(8,128)(2,1)S(1)}, bf16[4,4,64,384]{3,2,1,0:T(8,128)(2,1)S(1)}, u32[]{:S(2)}, u32[]{:S(2)}) collective-permute-start(bf16[4,4,64,384]{3,2,1,0:T(8,128)(2,1)S(1)} %shard_map.121.mine), channel_id=1, source_target_pairs={{0,1},{1,0},{2,3},{3,2},{4,5},{5,4},{6,7},{7,6},{8,9},{9,8},{10,11... | collective-permute-start | bytes 2359304 | tf_op jit(solution)/shard_map/ppermute | solution.py:522
  23.8 31.7 %copy-start.11 = (f32[4,512]{1,0:T(4,128)S(1)}, f32[4,512]{1,0:T(4,128)}, u32[]{:S(2)}) copy-start(f32[4,512]{1,0:T(4,128)} %mix_bias.1) | copy-start | bytes 24580
  27.3 9.1 %collective-permute-start.2 = (bf16[128,1536]{1,0:T(8,128)(2,1)S(1)}, bf16[128,1536]{1,0:T(8,128)(2,1)S(1)}, u32[]{:S(2)}, u32[]{:S(2)}) collective-permute-start(bf16[128,1536]{1,0:T(8,128)(2,1)S(1)} %get-tuple-element.40.v), channel_id=1, source_target_pairs={{8,16},{16,8},{40,48},{48,40},{9,17},{17,9},{41,49},{49,41},{10,18... | collective-permute-start | bytes 1179656 | tf_op jit(solution)/shard_map/ppermute | solution.py:517
  28.0 29.4 %collective-permute-start.1 = (bf16[128,1536]{1,0:T(8,128)(2,1)S(1)}, bf16[128,1536]{1,0:T(8,128)(2,1)S(1)}, u32[]{:S(2)}, u32[]{:S(2)}) collective-permute-start(bf16[128,1536]{1,0:T(8,128)(2,1)S(1)} %get-tuple-element.40.v), channel_id=1, source_target_pairs={{0,16},{24,8},{32,48},{56,40},{1,17},{25,9},{33,49},{57,41},{2,18}... | collective-permute-start | bytes 1179656 | tf_op jit(solution)/shard_map/ppermute | solution.py:516
  34.2 23.2 %collective-permute-start = (bf16[128,1536]{1,0:T(8,128)(2,1)S(1)}, bf16[128,1536]{1,0:T(8,128)(2,1)S(1)}, u32[]{:S(2)}, u32[]{:S(2)}) collective-permute-start(bf16[128,1536]{1,0:T(8,128)(2,1)S(1)} %get-tuple-element.40.v), channel_id=1, source_target_pairs={{0,8},{24,16},{32,40},{56,48},{1,9},{25,17},{33,41},{57,49},{2,10}... | collective-permute-start | bytes 1179656 | tf_op jit(solution)/shard_map/ppermute | solution.py:515
  35.7 24.1 %collective-permute-start.9 = (bf16[128,1536]{1,0:T(8,128)(2,1)S(1)}, bf16[128,1536]{1,0:T(8,128)(2,1)S(1)}, u32[]{:S(2)}, u32[]{:S(2)}) collective-permute-start(bf16[128,1536]{1,0:T(8,128)(2,1)S(1)} %get-tuple-element.42.v1.v), channel_id=1, source_target_pairs={{8,16},{16,8},{40,48},{48,40},{9,17},{17,9},{41,49},{49,41},{10,18... | collective-permute-start | bytes 1179656 | tf_op jit(solution)/shard_map/ppermute | solution.py:517
  36.4 27.3 %collective-permute-start.8 = (bf16[128,1536]{1,0:T(8,128)(2,1)S(1)}, bf16[128,1536]{1,0:T(8,128)(2,1)S(1)}, u32[]{:S(2)}, u32[]{:S(2)}) collective-permute-start(bf16[128,1536]{1,0:T(8,128)(2,1)S(1)} %get-tuple-element.42.v1.v), channel_id=1, source_target_pairs={{0,16},{24,8},{32,48},{56,40},{1,17},{25,9},{33,49},{57,41},{2,18}... | collective-permute-start | bytes 1179656 | tf_op jit(solution)/shard_map/ppermute | solution.py:516
  54.2 16.1 %collective-permute-start.7 = (bf16[128,1536]{1,0:T(8,128)(2,1)S(1)}, bf16[128,1536]{1,0:T(8,128)(2,1)S(1)}, u32[]{:S(2)}, u32[]{:S(2)}) collective-permute-start(bf16[128,1536]{1,0:T(8,128)(2,1)S(1)} %get-tuple-element.42.v1.v), channel_id=1, source_target_pairs={{0,8},{24,16},{32,40},{56,48},{1,9},{25,17},{33,41},{57,49},{2,10}... | collective-permute-start | bytes 1179656 | tf_op jit(solution)/shard_map/ppermute | solution.py:515
  56.4 0.9 copy-start.9
  56.4 0.9 copy-start.10
  57.3 1.5 copy-start
  58.8 1.0 copy-start.7
  72.7 0.9 copy-start.3
  73.6 2.9 %copy-start.5 = (f32[128,1536]{1,0:T(8,128)}, f32[128,1536]{1,0:T(8,128)S(1)}, u32[]{:S(2)}) copy-start(f32[128,1536]{1,0:T(8,128)S(1)} %get-tuple-element.49.refs_3_) | copy-start | bytes 2359300
  73.6 3.0 %copy-start.12 = (bf16[128,1536]{1,0:T(8,128)(2,1)}, bf16[128,1536]{1,0:T(8,128)(2,1)S(1)}, u32[]{:S(2)}) copy-start(bf16[128,1536]{1,0:T(8,128)(2,1)S(1)} %get-tuple-element.50) | copy-start | bytes 1179652
  73.6 6.5 %collective-permute-start.13 = (bf16[5,64,512]{2,1,0:T(8,128)(2,1)S(1)}, bf16[5,64,512]{2,1,0:T(8,128)(2,1)S(1)}, u32[]{:S(2)}, u32[]{:S(2)}) collective-permute-start(bf16[5,64,512]{2,1,0:T(8,128)(2,1)S(1)} %get-tuple-element.59), channel_id=1, source_target_pairs={{0,1},{1,0},{2,3},{3,2},{4,5},{5,4},{6,7},{7,6},{8,9},{9,8},{10,11... | collective-permute-start | bytes 983048 | tf_op jit(solution)/shard_map/ppermute | solution.py:568
  76.5 3.6 %collective-permute-start.12 = (bf16[4,64,512]{2,1,0:T(8,128)(2,1)S(1)}, bf16[4,64,512]{2,1,0:T(8,128)(2,1)S(1)}, u32[]{:S(2)}, u32[]{:S(2)}) collective-permute-start(bf16[4,64,512]{2,1,0:T(8,128)(2,1)S(1)} %get-tuple-element.56), channel_id=1, source_target_pairs={{0,1},{1,0},{2,3},{3,2},{4,5},{5,4},{6,7},{7,6},{8,9},{9,8},{10,11... | collective-permute-start | bytes 786440 | tf_op jit(solution)/shard_map/ppermute | solution.py:548
  80.7 12.4 %collective-permute-start.14 = (bf16[2,64,1152]{2,1,0:T(8,128)(2,1)S(1)}, bf16[2,64,1152]{2,1,0:T(8,128)(2,1)S(1)}, u32[]{:S(2)}, u32[]{:S(2)}) collective-permute-start(bf16[2,64,1152]{2,1,0:T(8,128)(2,1)S(1)} %get-tuple-element.62), channel_id=1, source_target_pairs={{0,6},{6,0},{2,4},{4,2},{1,7},{7,1},{3,5},{5,3},{8,14},{14,8},{10,... | collective-permute-start | bytes 884744 | tf_op jit(solution)/shard_map/ppermute | solution.py:573
  93.7 7.5 %collective-permute-start.15 = (bf16[64,1280]{1,0:T(8,128)(2,1)S(1)}, bf16[64,1280]{1,0:T(8,128)(2,1)S(1)}, u32[]{:S(2)}, u32[]{:S(2)}) collective-permute-start(bf16[64,1280]{1,0:T(8,128)(2,1)S(1)} %get-tuple-element.65), channel_id=1, source_target_pairs={{0,2},{2,0},{4,6},{6,4},{1,3},{3,1},{5,7},{7,5},{8,10},{10,8},{12,... | collective-permute-start | bytes 491528 | tf_op jit(solution)/shard_map/ppermute | solution.py:576
  119.0 39.8 %copy-start.1 = (bf16[1,128,3072]{2,1,0:T(8,128)(2,1)S(1)}, bf16[1,128,3072]{2,1,0:T(8,128)(2,1)}, u32[]{:S(2)}) copy-start(bf16[1,128,3072]{2,1,0:T(8,128)(2,1)} %upstream.1) | copy-start | bytes 2359300
  135.4 0.7 copy-start.2
  136.2 28.3 %all-to-all-start.2 = ((bf16[8,8,2304]{2,1,0:T(8,128)(2,1)}), bf16[8,8,2304]{2,1,0:T(8,128)(2,1)}, u32[]{:S(2)}, u32[]{:S(2)}) async-start(bf16[8,8,2304]{2,1,0:T(8,128)(2,1)} %copy-done.2), calls=%async_computation.2 | async-start | bytes 589824 | tf_op jit(solution)/shard_map/all_to_all | solution.py:491
  141.6 13.1 %collective-permute-start.11 = (bf16[128,1536]{1,0:T(8,128)(2,1)}, bf16[128,1536]{1,0:T(8,128)(2,1)S(1)}, u32[]{:S(2)}, u32[]{:S(2)}) collective-permute-start(bf16[128,1536]{1,0:T(8,128)(2,1)} %copy-done.12), channel_id=1, source_target_pairs={{8,0},{16,24},{40,32},{48,56},{9,1},{17,25},{41,33},{49,57},{10,2}... | collective-permute-start | bytes 1179656 | tf_op jit(solution)/shard_map/ppermute | solution.py:564
  142.9 16.0 %collective-permute-start.10 = (bf16[128,1536]{1,0:T(8,128)(2,1)}, bf16[128,1536]{1,0:T(8,128)(2,1)S(1)}, u32[]{:S(2)}, u32[]{:S(2)}) collective-permute-start(bf16[128,1536]{1,0:T(8,128)(2,1)} %copy-done.7), channel_id=1, source_target_pairs={{8,0},{16,24},{40,32},{48,56},{9,1},{17,25},{41,33},{49,57},{10,2}... | collective-permute-start | bytes 1179656 | tf_op jit(solution)/shard_map/ppermute | solution.py:536
  158.8 1.1 copy-start.4
  160.0 1.1 copy-start.6
